TPU v7x, 128 devices: a whole 4x4x4 slice. The times are simulated.
128 devices in a mesh: ep: 64 (over z, y, x), tp: 2 (over core).
Axes of the slice: x: 4, y: 4, z: 4, core: 2. Of those that a mesh axis runs over, the one named last changes fastest.
Arguments:
- tokens: bfloat16 [1536, 4096], P('ep'), may hold values from -6 to 6
- cotangent: bfloat16 [1536, 4096], P('ep'), may hold values from -6 to 6
- routes: int32 [1536, 2], P('ep'), may hold values from 0 to 7, all different within a row; in each aligned block of 24 rows (0 to 23, 24 to 47, ...) at most 12 rows name the same one
- route_weights: float32 [1536, 2], P('ep'), may hold values from 0.1 to 0.9
- gate_weight: bfloat16 [64, 4096, 688], P('ep', None, 'tp'), may hold values from -0.09375 to 0.09375
- up_weight: bfloat16 [64, 4096, 688], P('ep', None, 'tp'), may hold values from -0.09375 to 0.09375
- down_weight: bfloat16 [64, 688, 4096], P('ep', 'tp'), may hold values from -0.078125 to 0.078125
Outputs:
- token_grad: bfloat16 [1536, 4096], P('ep', 'tp')
- route_grad: float32 [1536, 2], P('ep')
- gate_grad: bfloat16 [64, 4096, 688], P('ep', None, 'tp')
- up_grad: bfloat16 [64, 4096, 688], P('ep', None, 'tp')
- down_grad: bfloat16 [64, 688, 4096], P('ep', 'tp')
Inputs may be any that keep to these rules, and one draw needn't show every extreme that they name: `routes`: each row names 2 different experts of 0 to 7; within the rows of one device (24 aligned rows) no expert is named more than 12 times, and in some blocks one is named exactly 12 times.
All inputs are finite; a program needn't handle non-finite values.
Results may differ from a plain program's by a relative error of at most 0.01.
Values may be sent and summed in bfloat16 or wider, within the bound.
No kernel may reach another device: no remote copies, remote signals or barrier semaphores. Data moves between devices by JAX's collectives and lax.ppermute only.
A program may use at most 192 MiB of HBM per device.

v0:
```python
import functools

import jax
import jax.numpy as jnp
from jax import lax
from jax.experimental import pallas as pl
from jax.experimental.pallas import tpu as pltpu
from jax.sharding import Mesh
from jax.sharding import PartitionSpec as P


EXPERTS = 8
TOP = 2
CAP = 12
ROOM = 16
LANES = 128
BF = jnp.bfloat16
F32 = jnp.float32
MIB = 1 << 20


VMEM = pl.BlockSpec(memory_space=pltpu.VMEM)
SMEM = pl.BlockSpec(memory_space=pltpu.SMEM)


def along_x(value, step):
    return lax.ppermute(value, "x", [(i, (i + step) % 4) for i in range(4)])


def pair_y(value):
    return lax.ppermute(value, "yl", [(0, 1), (1, 0)])


def pair_core(value):
    return lax.ppermute(value, "core", [(0, 1), (1, 0)])


def to_expert(value, dz, dy, sign):
    perm = []
    for z in range(4):
        for y in range(4):
            there = (z + sign * dz) % 4 * 4 + (3 - y if dy else y)
            perm.append((z * 4 + y, there))
    return lax.ppermute(value, ("z", "yh", "yl"), perm)


def dot_f32(a, b, left, right):
    return lax.dot_general(a, b, (((left,), (right,)), ((), ())), preferred_element_type=F32)


def slots_kernel(half, place_ref, tok_ref, cot_ref, routes_ref, weights_ref, *outs):
    core, z, yh = place_ref[0], place_ref[1], place_ref[2]
    first_ref, second_ref = outs[EXPERTS:]
    rows = tok_ref.shape[0]
    slot = lax.broadcasted_iota(jnp.int32, (rows, EXPERTS * ROOM), 1)
    index = slot // ROOM
    expert = 2 * ((z + index // 2) % 4) + (yh + index % 2) % 2
    is_first = routes_ref[:, 0:1] == expert
    is_second = routes_ref[:, 1:2] == expert
    hot = jnp.where(is_first | is_second, 1.0, 0.0).astype(BF)
    below = lax.broadcasted_iota(jnp.int32, (rows, rows), 1) < lax.broadcasted_iota(
        jnp.int32, (rows, rows), 0
    )
    position = dot_f32(jnp.where(below, 1.0, 0.0).astype(BF), hot, 1, 0)
    fits = position == (slot % ROOM).astype(F32)
    first = jnp.where(is_first & fits, 1.0, 0.0).astype(BF)
    second = jnp.where(is_second & fits, 1.0, 0.0).astype(BF)
    first_ref[...] = first
    second_ref[...] = second
    here = pl.ds(pl.multiple_of(core * half, half), half)
    slot_tok = dot_f32(first + second, tok_ref[:, here], 0, 0).astype(BF)
    cot = cot_ref[:, here].astype(F32)
    scaled = dot_f32(first, (cot * weights_ref[:, 0:1]).astype(BF), 0, 0)
    scaled = scaled + dot_f32(second, (cot * weights_ref[:, 1:2]).astype(BF), 0, 0)
    scaled = scaled.astype(BF)
    for k in range(EXPERTS):
        outs[k][:, :half] = slot_tok[k * ROOM : (k + 1) * ROOM]
        outs[k][:, half:] = scaled[k * ROOM : (k + 1) * ROOM]


def make_slots(place, tokens, cotangent, routes, weights):
    rows, width = tokens.shape
    shapes = [jax.ShapeDtypeStruct((ROOM, width), BF)] * EXPERTS
    shapes += [jax.ShapeDtypeStruct((rows, EXPERTS * ROOM), BF)] * 2
    return pl.pallas_call(
        functools.partial(slots_kernel, width // 2),
        out_shape=shapes,
        in_specs=[SMEM] + [VMEM] * 4,
        out_specs=[VMEM] * len(shapes),
        compiler_params=pltpu.CompilerParams(vmem_limit_bytes=8 * MIB),
        cost_estimate=pl.CostEstimate(
            flops=2 * 128 * 24 * width * 2, bytes_accessed=3 * MIB, transcendentals=0
        ),
        name="slots",
    )(place, tokens, cotangent, routes, weights)


def padded(n):
    return -(-n // LANES) * LANES


def group_kernel(count, half, place_ref, *refs):
    core = place_ref[0]
    ours, theirs = refs[:count], refs[count : 2 * count]
    gate_ref, up_ref, down_ref = refs[2 * count : 2 * count + 3]
    keep_ref, send_ref, gate_out, up_out, hidden_out = refs[2 * count + 3 :]
    here = pl.ds(pl.multiple_of(core * half, half), half)
    there = pl.ds(pl.multiple_of((1 - core) * half, half), half)
    tok = [jnp.concatenate([r[:, :half] for r in side], axis=0) for side in (ours, theirs)]
    gate = dot_f32(tok[0], gate_ref[:, here], 1, 1) + dot_f32(tok[1], gate_ref[:, there], 1, 1)
    up = dot_f32(tok[0], up_ref[:, here], 1, 1) + dot_f32(tok[1], up_ref[:, there], 1, 1)
    cot = [jnp.concatenate([r[:, half:] for r in side], axis=0) for side in (ours, theirs)]
    grad = dot_f32(cot[0], down_ref[:, here], 1, 1) + dot_f32(cot[1], down_ref[:, there], 1, 1)
    sigma = 1.0 / (1.0 + jnp.exp(-gate))
    active = gate * sigma
    hidden = (active * up).astype(BF)
    gate_side = (grad * up * (sigma * (1.0 + gate * (1.0 - sigma)))).astype(BF)
    up_side = (grad * active).astype(BF)
    hid = hidden.shape[1]
    for out, value in ((hidden_out, hidden), (gate_out, gate_side), (up_out, up_side)):
        out[:, :hid] = value
        out[:, hid:] = jnp.zeros((out.shape[0], out.shape[1] - hid), BF)
    share = jnp.sum(hidden.astype(F32) * grad, axis=1, keepdims=True).astype(BF)
    share = jnp.broadcast_to(share, (share.shape[0], LANES))
    tile = 512
    for base, out in ((core * half, keep_ref), ((1 - core) * half, send_ref)):
        out[:, half:] = share

        @pl.loop(0, half // tile)
        def _(j):
            where = pl.ds(pl.multiple_of(base + j * tile, tile), tile)
            term = dot_f32(gate_out[:, :hid], gate_ref[:, where], 1, 0)
            term = term + dot_f32(up_out[:, :hid], up_ref[:, where], 1, 0)
            out[:, pl.ds(pl.multiple_of(j * tile, tile), tile)] = term.astype(BF)


def run_group(place, ours, theirs, gate, up, down):
    rows = sum(r.shape[0] for r in ours)
    hid, width = gate.shape
    half = width // 2
    shapes = [jax.ShapeDtypeStruct((rows, half + LANES), BF)] * 2
    shapes += [jax.ShapeDtypeStruct((rows, padded(hid)), BF)] * 3
    return pl.pallas_call(
        functools.partial(group_kernel, len(ours), half),
        out_shape=shapes,
        in_specs=[SMEM] + [VMEM] * (2 * len(ours) + 3),
        out_specs=[VMEM] * len(shapes),
        compiler_params=pltpu.CompilerParams(vmem_limit_bytes=40 * MIB),
        cost_estimate=pl.CostEstimate(
            flops=10 * rows * hid * width, bytes_accessed=16 * MIB, transcendentals=rows * hid
        ),
        name="group",
    )(place, *ours, *theirs, gate, up, down)


def weight_kernel(sizes, half, hid, tile, place_ref, *refs):
    count = len(sizes)
    ours, theirs = refs[:count], refs[count : 2 * count]
    sides = refs[2 * count : 2 * count + 6]
    outs = refs[2 * count + 6 : 2 * count + 9]
    rows_ref, pair_t, hidden_t, stage, in_sem, out_sem = refs[2 * count + 9 :]
    core = place_ref[0]
    loads = []
    for s, group in enumerate((ours, theirs)):
        at = 0
        copies = []
        for i, size in enumerate(sizes):
            copies.append(
                pltpu.make_async_copy(
                    group[i], rows_ref.at[s, pl.ds(at, size), :], in_sem.at[s, i]
                )
            )
            at += size
        loads.append(copies)
    for copies in loads:
        for c in copies:
            c.start()
    wide = sides[0].shape[1]
    depth = sides[0].shape[0]
    for i in range(2):
        columns = slice(depth * i, depth * (i + 1))
        pair_t[:wide, columns] = sides[i][...].T
        pair_t[wide:, columns] = sides[2 + i][...].T
        hidden_t[:, columns] = sides[4 + i][...].T
    stores = []
    for s in range(2):
        for c in loads[s]:
            c.wait()
        base = (core if s == 0 else 1 - core) * half

        @pl.loop(0, half // tile)
        def _(j):
            to = pl.ds(pl.multiple_of(base + j * tile, tile), tile)
            block = rows_ref[s, :, pl.ds(pl.multiple_of(j * tile, tile), tile)]
            pair = dot_f32(pair_t[...], block, 1, 0).astype(BF)
            stage[0, :, to] = pair[:hid]
            stage[1, :, to] = pair[wide : wide + hid]
            block = rows_ref[s, :, pl.ds(pl.multiple_of(half + j * tile, tile), tile)]
            stage[2, :, to] = dot_f32(hidden_t[...], block, 1, 0).astype(BF)[:hid]

        whole = pl.ds(pl.multiple_of(base, half), half)
        for t in range(3):
            copy = pltpu.make_async_copy(
                stage.at[t, :, whole], outs[t].at[:, whole], out_sem.at[s, t]
            )
            copy.start()
            stores.append(copy)
    for copy in stores:
        copy.wait()


def weight_grads(place, ours, theirs, sides, hid):
    sizes = [r.shape[0] for r in ours]
    rows = sum(sizes)
    width = ours[0].shape[1]
    wide = sides[0].shape[1]
    anywhere = pl.BlockSpec(memory_space=pl.ANY)
    return pl.pallas_call(
        functools.partial(weight_kernel, sizes, width // 2, hid, 512),
        out_shape=[jax.ShapeDtypeStruct((hid, width), BF)] * 3,
        in_specs=[SMEM] + [anywhere] * (2 * len(sizes)) + [VMEM] * 6,
        out_specs=[anywhere] * 3,
        scratch_shapes=[
            pltpu.VMEM((2, rows, width), BF),
            pltpu.VMEM((2 * wide, rows), BF),
            pltpu.VMEM((wide, rows), BF),
            pltpu.VMEM((3, hid, width), BF),
            pltpu.SemaphoreType.DMA((2, len(sizes))),
            pltpu.SemaphoreType.DMA((2, 3)),
        ],
        compiler_params=pltpu.CompilerParams(vmem_limit_bytes=36 * MIB),
        cost_estimate=pl.CostEstimate(
            flops=6 * rows * hid * width, bytes_accessed=22 * MIB, transcendentals=0
        ),
        name="weight_grads",
    )(place, *ours, *theirs, *sides)


def final_kernel(half, weights_ref, first_ref, second_ref, *refs):
    backs = refs[:EXPERTS]
    token_ref, route_ref = refs[EXPERTS:]
    back = jnp.concatenate([b[...] for b in backs], axis=0)
    first, second = first_ref[...], second_ref[...]
    token_ref[...] = dot_f32(first + second, back[:, :half], 1, 0).astype(BF)
    share = back[:, half:]
    route_ref[:, 0:1] = dot_f32(first, share, 1, 0)[:, 0:1] / weights_ref[:, 0:1]
    route_ref[:, 1:2] = dot_f32(second, share, 1, 0)[:, 0:1] / weights_ref[:, 1:2]


def combine(weights, first, second, backs):
    rows = weights.shape[0]
    half = backs[0].shape[1] - LANES
    return pl.pallas_call(
        functools.partial(final_kernel, half),
        out_shape=[
            jax.ShapeDtypeStruct((rows, half), BF),
            jax.ShapeDtypeStruct((rows, TOP), F32),
        ],
        in_specs=[VMEM] * (3 + EXPERTS),
        out_specs=[VMEM] * 2,
        compiler_params=pltpu.CompilerParams(vmem_limit_bytes=8 * MIB),
        cost_estimate=pl.CostEstimate(
            flops=2 * 128 * 24 * half, bytes_accessed=MIB, transcendentals=0
        ),
        name="combine",
    )(weights, first, second, *backs)


def per_device(tokens, cotangent, routes, route_weights, gate_weight, up_weight, down_weight):
    place = jnp.stack([lax.axis_index("core"), lax.axis_index("z"), lax.axis_index("yh")])
    place = place.astype(jnp.int32)
    packed = EXPERTS * CAP
    third = packed // 3

    made = make_slots(place, tokens, cotangent, routes, route_weights)
    first, second = made[EXPERTS:]
    part = packed // 2
    row_of = jnp.arange(part)
    pack = (
        (row_of // CAP * ROOM + row_of % CAP)[:, None] == jnp.arange(EXPERTS * ROOM // 2)[None, :]
    ).astype(BF)

    def packing(sent, dy):
        got = list(sent)
        for dz in (2, 1, 3, 0):
            if dz or dy:
                got[dz] = to_expert(sent[dz], dz, dy, 1)
        return dot_f32(pack, jnp.concatenate(got, axis=0), 1, 0).astype(BF)

    own, left, right, partner, far_left, far_right, across = ([] for _ in range(7))
    own = [packing(made[h:EXPERTS:2], h) for h in range(2)]
    for h in range(2):
        left.append(along_x(own[h], 1))
        right.append(along_x(own[h], -1))
        partner.append(pair_y(own[h]))
    for h in range(2):
        far_left.append(along_x(partner[h], 1))
        far_right.append(pair_y(right[h]))
        across.append(along_x(right[h], -1))

    gate_t = gate_weight[0].T
    up_t = up_weight[0].T
    down_t = down_weight[0]
    near = own + left + right + partner
    near_other = [pair_core(v) for v in near]
    near_out = run_group(place, near, near_other, gate_t, up_t, down_t)
    far = far_left + far_right + across
    tied = lax.optimization_barrier((*far, *near_out))
    far = list(tied[: len(far)])
    near_out = tied[len(far) :]
    middle = jnp.concatenate([far[2][third:], far[3][: 2 * third - part]], axis=0)
    last = [along_x(far[0][:third], 1), along_x(middle, -1), pair_y(far[5][2 * third - part :])]
    far = far + last
    far_other = [pair_core(v) for v in far]
    far_out = run_group(place, far, far_other, gate_t, up_t, down_t)

    def add(a, *more):
        total = a.astype(F32)
        for m in more:
            total = total + m.astype(F32)
        return total.astype(BF)

    near_got = pair_core(near_out[1])
    far_got = pair_core(far_out[1])

    def chunk(out, got, i, a=0, b=packed):
        return add(out[0][packed * i + a : packed * i + b], got[packed * i + a : packed * i + b])

    t_last = [chunk(far_out, far_got, 3, third * i, third * (i + 1)) for i in range(3)]
    a_left = along_x(t_last[0], -1)
    a_right = along_x(t_last[1], 1)
    a_pair = pair_y(t_last[2])
    pads = [[(third * i, packed - third * (i + 1)), (0, 0)] for i in range(3)]
    t_far_left = add(chunk(far_out, far_got, 0), jnp.pad(a_left, pads[0]))
    t_far_right = add(chunk(far_out, far_got, 1), jnp.pad(a_right, pads[1]))
    t_across = add(chunk(far_out, far_got, 2), jnp.pad(a_pair, pads[2]))
    b_partner = along_x(t_far_left, -1)
    b_right_pair = pair_y(t_far_right)
    b_right = along_x(t_across, 1)
    hid = gate_t.shape[0]
    sides = [g for t in (2, 3, 4) for g in (near_out[t], far_out[t])]
    grads = weight_grads(place, near + far, near_other + far_other, sides, hid)
    tied = lax.optimization_barrier((b_partner, b_right_pair, b_right, *grads))
    b_partner, b_right_pair, b_right, gate_grad, up_grad, down_grad = tied
    c_left = along_x(chunk(near_out, near_got, 1), -1)
    c_right = along_x(add(chunk(near_out, near_got, 2), b_right_pair, b_right), 1)
    c_pair = pair_y(add(chunk(near_out, near_got, 3), b_partner))
    home = add(chunk(near_out, near_got, 0), c_left, c_right, c_pair)

    backs = [None] * EXPERTS
    for dy in range(2):
        spread = dot_f32(pack, home[part * dy : part * (dy + 1)], 0, 0).astype(BF)
        for dz in (2, 1, 3, 0):
            k = 2 * dz + dy
            piece = spread[ROOM * dz : ROOM * (dz + 1)]
            if k:
                piece = to_expert(piece, dz, dy, -1)
            backs[k] = piece
    token_grad, route_grad = combine(route_weights, first, second, backs)

    return token_grad, route_grad, gate_grad.T[None], up_grad.T[None], down_grad[None]


def solution(mesh):
    names = ("z", "yh", "yl", "x", "core")
    fine = Mesh(mesh.devices.reshape(4, 2, 2, 4, 2), names)
    ep = names[:4]
    return jax.shard_map(
        per_device,
        mesh=fine,
        in_specs=(
            P(ep, None),
            P(ep, None),
            P(ep, None),
            P(ep, None),
            P(ep, None, "core"),
            P(ep, None, "core"),
            P(ep, "core", None),
        ),
        out_specs=(
            P(ep, "core"),
            P(ep, None),
            P(ep, None, "core"),
            P(ep, None, "core"),
            P(ep, "core", None),
        ),
        check_vma=False,
    )
```

profile of v0, /device:TPU:2, one launch (start us, length us, event | category | flops | bytes accessed | tf_op | source)
XLA Modules:
  0.0 182.5 jit_solution(14271984520323007210)
XLA Ops:
  0.6 0.8 copy.14.weights_ref
  1.4 0.8 copy.12.routes_ref
  2.2 0.9 copy-done
  3.2 0.9 copy-done.1
  4.1 1.3 slots.1
  5.4 4.1 %collective-permute-start.2 = (bf16[16,4096]{1,0:T(8,128)(2,1)S(1)}, bf16[16,4096]{1,0:T(8,128)(2,1)S(1)}, u32[]{:S(2)}, u32[]{:S(2)}) collective-permute-start(bf16[16,4096]{1,0:T(8,128)(2,1)S(1)} %get-tuple-element.52), channel_id=1, source_target_pairs={{0,96},{8,104},{16,112},{24,120},{32,0},{40,8},{48,16},{56,24},{64... | collective-permute-start | bytes 393224 | tf_op jit(solution)/shard_map/ppermute | solution.py:44
  9.5 1.3 collective-permute-start
  10.8 4.4 %collective-permute-start.8 = (bf16[16,4096]{1,0:T(8,128)(2,1)S(1)}, bf16[16,4096]{1,0:T(8,128)(2,1)S(1)}, u32[]{:S(2)}, u32[]{:S(2)}) collective-permute-start(bf16[16,4096]{1,0:T(8,128)(2,1)S(1)} %get-tuple-element.56), channel_id=1, source_target_pairs={{0,120},{8,112},{16,104},{24,96},{32,24},{40,16},{48,8},{56,0},{64... | collective-permute-start | bytes 393224 | tf_op jit(solution)/shard_map/ppermute | solution.py:44
  15.2 2.0 %collective-permute-start.7 = (bf16[16,4096]{1,0:T(8,128)(2,1)S(1)}, bf16[16,4096]{1,0:T(8,128)(2,1)S(1)}, u32[]{:S(2)}, u32[]{:S(2)}) collective-permute-start(bf16[16,4096]{1,0:T(8,128)(2,1)S(1)} %get-tuple-element.55), channel_id=1, source_target_pairs={{0,88},{8,80},{16,72},{24,64},{32,120},{40,112},{48,104},{56,96},{... | collective-permute-start | bytes 393224 | tf_op jit(solution)/shard_map/ppermute | solution.py:44
  17.2 2.1 %collective-permute-done.2 = bf16[16,4096]{1,0:T(8,128)(2,1)S(1)} collective-permute-done((bf16[16,4096]{1,0:T(8,128)(2,1)S(1)}, bf16[16,4096]{1,0:T(8,128)(2,1)S(1)}, u32[]{:S(2)}, u32[]{:S(2)}) %collective-permute-start.2) | collective-permute-done | bytes 131104 | tf_op jit(solution)/shard_map/ppermute | solution.py:44
  19.4 4.4 %collective-permute-start.5 = (bf16[16,4096]{1,0:T(8,128)(2,1)S(1)}, bf16[16,4096]{1,0:T(8,128)(2,1)S(1)}, u32[]{:S(2)}, u32[]{:S(2)}) collective-permute-start(bf16[16,4096]{1,0:T(8,128)(2,1)S(1)} %get-tuple-element.53), channel_id=1, source_target_pairs={{0,24},{8,16},{16,8},{24,0},{32,56},{40,48},{48,40},{56,32},{64,88... | collective-permute-start | bytes 393224 | tf_op jit(solution)/shard_map/ppermute | solution.py:44
  24.3 6.9 %collective-permute-done.6 = bf16[16,4096]{1,0:T(8,128)(2,1)S(1)} collective-permute-done((bf16[16,4096]{1,0:T(8,128)(2,1)S(1)}, bf16[16,4096]{1,0:T(8,128)(2,1)S(1)}, u32[]{:S(2)}, u32[]{:S(2)}) %collective-permute-start.6) | collective-permute-done | bytes 131104 | tf_op jit(solution)/shard_map/ppermute | solution.py:44
  31.7 0.5 collective-permute-start.11
  32.3 2.8 %collective-permute-start.13 = (bf16[48,4096]{1,0:T(8,128)(2,1)S(1)}, bf16[48,4096]{1,0:T(8,128)(2,1)S(1)}, u32[]{:S(2)}, u32[]{:S(2)}) collective-permute-start(bf16[48,4096]{1,0:T(8,128)(2,1)S(1)} %convolution_convert_fusion.refs_1_), channel_id=1, source_target_pairs={{0,6},{2,0},{4,2},{6,4},{1,7},{3,1},{5,3},{7,5},{8,14},{10,8},{12,... | collective-permute-start | bytes 1179656 | tf_op jit(solution)/shard_map/ppermute | solution.py:27
  35.0 0.8 collective-permute-start.18
  35.8 5.4 %collective-permute-done.9.refs_7_ = bf16[48,4096]{1,0:T(8,128)(2,1)S(1)} collective-permute-done((bf16[48,4096]{1,0:T(8,128)(2,1)S(1)}, bf16[48,4096]{1,0:T(8,128)(2,1)S(1)}, u32[]{:S(2)}, u32[]{:S(2)}) %collective-permute-start.9) | collective-permute-done | bytes 393248 | tf_op jit(solution)/shard_map/ppermute | solution.py:31
  41.2 2.6 %collective-permute-done.11.refs_4_ = bf16[48,4096]{1,0:T(8,128)(2,1)S(1)} collective-permute-done((bf16[48,4096]{1,0:T(8,128)(2,1)S(1)}, bf16[48,4096]{1,0:T(8,128)(2,1)S(1)}, u32[]{:S(2)}, u32[]{:S(2)}) %collective-permute-start.11) | collective-permute-done | bytes 393248 | tf_op jit(solution)/shard_map/ppermute | solution.py:27
  43.7 5.3 %collective-permute-done.13.refs_5_ = bf16[48,4096]{1,0:T(8,128)(2,1)S(1)} collective-permute-done((bf16[48,4096]{1,0:T(8,128)(2,1)S(1)}, bf16[48,4096]{1,0:T(8,128)(2,1)S(1)}, u32[]{:S(2)}, u32[]{:S(2)}) %collective-permute-start.13) | collective-permute-done | bytes 393248 | tf_op jit(solution)/shard_map/ppermute | solution.py:27
  49.1 1.5 collective-permute-start.4
  50.6 4.3 %collective-permute-done.18.refs_3_ = bf16[48,4096]{1,0:T(8,128)(2,1)S(1)} collective-permute-done((bf16[48,4096]{1,0:T(8,128)(2,1)S(1)}, bf16[48,4096]{1,0:T(8,128)(2,1)S(1)}, u32[]{:S(2)}, u32[]{:S(2)}) %collective-permute-start.18) | collective-permute-done | bytes 393248 | tf_op jit(solution)/shard_map/ppermute | solution.py:27
  54.9 0.5 collective-permute-start.23
  55.5 4.7 %collective-permute-done.4.refs_0_.refs_8_ = bf16[48,4096]{1,0:T(8,128)(2,1)S(1)} collective-permute-done((bf16[48,4096]{1,0:T(8,128)(2,1)S(1)}, bf16[48,4096]{1,0:T(8,128)(2,1)S(1)}, u32[]{:S(2)}, u32[]{:S(2)}) %collective-permute-start.4) | collective-permute-done | bytes 393248 | tf_op jit(solution)/shard_map/ppermute | solution.py:27
  60.2 0.5 collective-permute-start.26
  61.0 1.7 collective-permute-start.12
  63.0 1.9 %collective-permute-start.15 = (bf16[48,4096]{1,0:T(8,128)(2,1)S(1)}, bf16[48,4096]{1,0:T(8,128)(2,1)S(1)}, u32[]{:S(2)}, u32[]{:S(2)}) collective-permute-start(bf16[48,4096]{1,0:T(8,128)(2,1)S(1)} %collective-permute-done.11.refs_4_), channel_id=1, source_target_pairs={{0,6},{2,0},{4,2},{6,4},{1,7},{3,1},{5,3},{7,5},{8,14},{10,8},{12,... | collective-permute-start | bytes 1179656 | tf_op jit(solution)/shard_map/ppermute | solution.py:27
  64.9 3.1 %collective-permute-start.16 = (bf16[48,4096]{1,0:T(8,128)(2,1)S(1)}, bf16[48,4096]{1,0:T(8,128)(2,1)S(1)}, u32[]{:S(2)}, u32[]{:S(2)}) collective-permute-start(bf16[48,4096]{1,0:T(8,128)(2,1)S(1)} %collective-permute-done.13.refs_5_), channel_id=1, source_target_pairs={{0,6},{2,0},{4,2},{6,4},{1,7},{3,1},{5,3},{7,5},{8,14},{10,8},{12,... | collective-permute-start | bytes 1179656 | tf_op jit(solution)/shard_map/ppermute | solution.py:27
  68.1 12.4 %group.2 = (bf16[384,2176]{1,0:T(8,128)(2,1)S(1)}, bf16[384,2176]{1,0:T(8,128)(2,1)S(1)}, bf16[384,384]{1,0:T(8,128)(2,1)S(1)}, bf16[384,384]{1,0:T(8,128)(2,1)S(1)}, bf16[384,384]{1,0:T(8,128)(2,1)S(1)}) custom-call(s32[3]{0:T(128)S(1)} %pad_add_fusion.place_ref, bf16[48,4096]{1,0:T(8,128)(2,1)S(1)} %convolution_convert_fusion.1.refs_0_, ...), custom_call_target="tpu_custom_call" | custom-call | flops 5410652160 | bytes 16777216 | tf_op jit(solution)/shard_map/group/pallas_call | solution.py:143
  80.6 1.3 collective-permute-done.16.refs_5_.refs_13_
  81.9 2.6 %collective-permute-start.29 = (bf16[32,4096]{1,0:T(8,128)(2,1)S(1)}, bf16[32,4096]{1,0:T(8,128)(2,1)S(1)}, u32[]{:S(2)}, u32[]{:S(2)}) collective-permute-start(bf16[32,4096]{1,0:T(8,128)(2,1)S(1)} %slice.108), channel_id=1, source_target_pairs={{0,2},{2,4},{4,6},{6,0},{1,3},{3,5},{5,7},{7,1},{8,10},{10,12},{12... | collective-permute-start | bytes 786440 | tf_op jit(solution)/shard_map/ppermute | solution.py:27
  84.8 1.7 collective-permute-start.31
  86.7 2.5 %collective-permute-done.29.refs_6_.refs_14_ = bf16[32,4096]{1,0:T(8,128)(2,1)S(1)} collective-permute-done((bf16[32,4096]{1,0:T(8,128)(2,1)S(1)}, bf16[32,4096]{1,0:T(8,128)(2,1)S(1)}, u32[]{:S(2)}, u32[]{:S(2)}) %collective-permute-start.29) | collective-permute-done | bytes 262176 | tf_op jit(solution)/shard_map/ppermute | solution.py:27
  89.3 2.9 %collective-permute-done.30.refs_7_.refs_15_ = bf16[32,4096]{1,0:T(8,128)(2,1)S(1)} collective-permute-done((bf16[32,4096]{1,0:T(8,128)(2,1)S(1)}, bf16[32,4096]{1,0:T(8,128)(2,1)S(1)}, u32[]{:S(2)}, u32[]{:S(2)}) %collective-permute-start.30) | collective-permute-done | bytes 262176 | tf_op jit(solution)/shard_map/ppermute | solution.py:27
  92.2 1.4 collective-permute-done.31.refs_8_.refs_16_
  93.6 0.5 collective-permute-start.37
  94.2 0.4 collective-permute-start.39
  94.9 0.4 collective-permute-done.36.refs_13_.refs_29_
  95.3 0.6 collective-permute-done.37.refs_14_.refs_30_
  97.0 12.4 %group.3 = (bf16[384,2176]{1,0:T(8,128)(2,1)S(1)}, bf16[384,2176]{1,0:T(8,128)(2,1)S(1)}, bf16[384,384]{1,0:T(8,128)(2,1)S(1)}, bf16[384,384]{1,0:T(8,128)(2,1)S(1)}, bf16[384,384]{1,0:T(8,128)(2,1)S(1)}) custom-call(s32[3]{0:T(128)S(1)} %pad_add_fusion.place_ref, bf16[48,4096]{1,0:T(8,128)(2,1)S(1)} %collective-permute-done.4.refs_0_.refs_8_, ...), custom_call_target="tpu_custom_call" | custom-call | flops 5410652160 | bytes 16777216 | tf_op jit(solution)/shard_map/group/pallas_call | solution.py:143
  110.0 3.0 %collective-permute-done.41 = bf16[384,2176]{1,0:T(8,128)(2,1)S(1)} collective-permute-done((bf16[384,2176]{1,0:T(8,128)(2,1)S(1)}, bf16[384,2176]{1,0:T(8,128)(2,1)S(1)}, u32[]{:S(2)}, u32[]{:S(2)}) %collective-permute-start.41) | collective-permute-done | bytes 1671200 | tf_op jit(solution)/shard_map/ppermute | solution.py:35
  113.1 1.7 collective-permute-start.46
  114.9 3.0 %collective-permute-start.44 = (bf16[32,2176]{1,0:T(8,128)(2,1)S(1)}, bf16[32,2176]{1,0:T(8,128)(2,1)S(1)}, u32[]{:S(2)}, u32[]{:S(2)}) collective-permute-start(bf16[32,2176]{1,0:T(8,128)(2,1)S(1)} %get-tuple-element.101), channel_id=1, source_target_pairs={{0,2},{2,4},{4,6},{6,0},{1,3},{3,5},{5,7},{7,1},{8,10},{10,12},{12... | collective-permute-start | bytes 417800 | tf_op jit(solution)/shard_map/ppermute | solution.py:27
  117.8 0.5 collective-permute-start.42
  118.4 0.6 collective-permute-done.46
  118.9 3.1 %collective-permute-done.44 = bf16[32,2176]{1,0:T(8,128)(2,1)S(1)} collective-permute-done((bf16[32,2176]{1,0:T(8,128)(2,1)S(1)}, bf16[32,2176]{1,0:T(8,128)(2,1)S(1)}, u32[]{:S(2)}, u32[]{:S(2)}) %collective-permute-start.44) | collective-permute-done | bytes 139296 | tf_op jit(solution)/shard_map/ppermute | solution.py:27
  122.1 1.1 collective-permute-done.42
  123.2 0.4 add_convert_fusion.4
  123.6 1.9 %collective-permute-start.43 = (bf16[96,2176]{1,0:T(8,128)(2,1)S(1)}, bf16[96,2176]{1,0:T(8,128)(2,1)S(1)}, u32[]{:S(2)}, u32[]{:S(2)}) collective-permute-start(bf16[96,2176]{1,0:T(8,128)(2,1)S(1)} %get-tuple-element.99), channel_id=1, source_target_pairs={{0,6},{2,0},{4,2},{6,4},{1,7},{3,1},{5,3},{7,5},{8,14},{10,8},{12,... | collective-permute-start | bytes 1253384 | tf_op jit(solution)/shard_map/ppermute | solution.py:27
  126.0 18.1 %weight_grads.1 = (bf16[344,4096]{1,0:T(8,128)(2,1)}, bf16[344,4096]{1,0:T(8,128)(2,1)}, bf16[344,4096]{1,0:T(8,128)(2,1)}) custom-call(s32[3]{0:T(128)S(1)} %pad_add_fusion.place_ref, bf16[48,4096]{1,0:T(8,128)(2,1)S(1)} %convolution_convert_fusion.1.refs_0_, bf16[48,4096]{1,0:T(8,128)(2,1)S(1)} %convolution_convert_fusion.refs_1_, ...), custom_call_target="tpu_custom_call" | custom-call | flops 6492782592 | bytes 23068672 | tf_op jit(solution)/shard_map/weight_grads/pallas_call | solution.py:218
  144.2 0.5 add_convert_fusion.11
  144.6 1.7 collective-permute-start.49
  146.4 2.3 %collective-permute-start.48 = (bf16[96,2176]{1,0:T(8,128)(2,1)S(1)}, bf16[96,2176]{1,0:T(8,128)(2,1)S(1)}, u32[]{:S(2)}, u32[]{:S(2)}) collective-permute-start(bf16[96,2176]{1,0:T(8,128)(2,1)S(1)} %get-tuple-element.96), channel_id=1, source_target_pairs={{0,2},{2,4},{4,6},{6,0},{1,3},{3,5},{5,7},{7,1},{8,10},{10,12},{12... | collective-permute-start | bytes 1253384 | tf_op jit(solution)/shard_map/ppermute | solution.py:27
  148.6 0.6 collective-permute-start.28
  149.2 5.4 %collective-permute-done.49 = bf16[96,2176]{1,0:T(8,128)(2,1)S(1)} collective-permute-done((bf16[96,2176]{1,0:T(8,128)(2,1)S(1)}, bf16[96,2176]{1,0:T(8,128)(2,1)S(1)}, u32[]{:S(2)}, u32[]{:S(2)}) %collective-permute-start.49) | collective-permute-done | bytes 417824 | tf_op jit(solution)/shard_map/ppermute | solution.py:31
  154.6 2.3 %collective-permute-done.48 = bf16[96,2176]{1,0:T(8,128)(2,1)S(1)} collective-permute-done((bf16[96,2176]{1,0:T(8,128)(2,1)S(1)}, bf16[96,2176]{1,0:T(8,128)(2,1)S(1)}, u32[]{:S(2)}, u32[]{:S(2)}) %collective-permute-start.48) | collective-permute-done | bytes 417824 | tf_op jit(solution)/shard_map/ppermute | solution.py:27
  156.9 2.0 %collective-permute-done.28 = bf16[96,2176]{1,0:T(8,128)(2,1)S(1)} collective-permute-done((bf16[96,2176]{1,0:T(8,128)(2,1)S(1)}, bf16[96,2176]{1,0:T(8,128)(2,1)S(1)}, u32[]{:S(2)}, u32[]{:S(2)}) %collective-permute-start.28) | collective-permute-done | bytes 417824 | tf_op jit(solution)/shard_map/ppermute | solution.py:27
  160.1 4.3 %collective-permute-start.51 = (bf16[16,2176]{1,0:T(8,128)(2,1)S(1)}, bf16[16,2176]{1,0:T(8,128)(2,1)S(1)}, u32[]{:S(2)}, u32[]{:S(2)}) collective-permute-start(bf16[16,2176]{1,0:T(8,128)(2,1)S(1)} %get-tuple-element.109), channel_id=1, source_target_pairs={{0,96},{8,104},{16,112},{24,120},{32,0},{40,8},{48,16},{56,24},{64... | collective-permute-start | bytes 208904 | tf_op jit(solution)/shard_map/ppermute | solution.py:44
  164.3 2.8 %collective-permute-start.52 = (bf16[16,2176]{1,0:T(8,128)(2,1)S(1)}, bf16[16,2176]{1,0:T(8,128)(2,1)S(1)}, u32[]{:S(2)}, u32[]{:S(2)}) collective-permute-start(bf16[16,2176]{1,0:T(8,128)(2,1)S(1)} %get-tuple-element.105), channel_id=1, source_target_pairs={{0,120},{8,112},{16,104},{24,96},{32,24},{40,16},{48,8},{56,0},{64... | collective-permute-start | bytes 208904 | tf_op jit(solution)/shard_map/ppermute | solution.py:44
  167.2 6.0 %collective-permute-start.54 = (bf16[16,2176]{1,0:T(8,128)(2,1)S(1)}, bf16[16,2176]{1,0:T(8,128)(2,1)S(1)}, u32[]{:S(2)}, u32[]{:S(2)}) collective-permute-start(bf16[16,2176]{1,0:T(8,128)(2,1)S(1)} %get-tuple-element.104), channel_id=1, source_target_pairs={{0,88},{8,80},{16,72},{24,64},{32,120},{40,112},{48,104},{56,96},{... | collective-permute-start | bytes 208904 | tf_op jit(solution)/shard_map/ppermute | solution.py:44
  173.3 0.6 collective-permute-start.56
  173.9 2.0 %collective-permute-done.54.refs_5_ = bf16[16,2176]{1,0:T(8,128)(2,1)S(1)} collective-permute-done((bf16[16,2176]{1,0:T(8,128)(2,1)S(1)}, bf16[16,2176]{1,0:T(8,128)(2,1)S(1)}, u32[]{:S(2)}, u32[]{:S(2)}) %collective-permute-start.54) | collective-permute-done | bytes 69664 | tf_op jit(solution)/shard_map/ppermute | solution.py:44
  175.9 2.9 %collective-permute-done.55.refs_6_ = bf16[16,2176]{1,0:T(8,128)(2,1)S(1)} collective-permute-done((bf16[16,2176]{1,0:T(8,128)(2,1)S(1)}, bf16[16,2176]{1,0:T(8,128)(2,1)S(1)}, u32[]{:S(2)}, u32[]{:S(2)}) %collective-permute-start.55) | collective-permute-done | bytes 69664 | tf_op jit(solution)/shard_map/ppermute | solution.py:44
  178.8 2.2 %collective-permute-done.56.refs_7_ = bf16[16,2176]{1,0:T(8,128)(2,1)S(1)} collective-permute-done((bf16[16,2176]{1,0:T(8,128)(2,1)S(1)}, bf16[16,2176]{1,0:T(8,128)(2,1)S(1)}, u32[]{:S(2)}, u32[]{:S(2)}) %collective-permute-start.56) | collective-permute-done | bytes 69664 | tf_op jit(solution)/shard_map/ppermute | solution.py:44
  181.0 0.9 combine.1
  181.9 0.6 copy.15
  (89 shorter events, 6.5 us)
Async XLA Ops:
  2.2 0.9 copy-start
  3.2 0.9 copy-start.1
  5.4 13.9 %collective-permute-start.2 = (bf16[16,4096]{1,0:T(8,128)(2,1)S(1)}, bf16[16,4096]{1,0:T(8,128)(2,1)S(1)}, u32[]{:S(2)}, u32[]{:S(2)}) collective-permute-start(bf16[16,4096]{1,0:T(8,128)(2,1)S(1)} %get-tuple-element.52), channel_id=1, source_target_pairs={{0,96},{8,104},{16,112},{24,120},{32,0},{40,8},{48,16},{56,24},{64... | collective-permute-start | bytes 393224 | tf_op jit(solution)/shard_map/ppermute | solution.py:44
  9.5 9.8 %collective-permute-start.1 = (bf16[16,4096]{1,0:T(8,128)(2,1)S(1)}, bf16[16,4096]{1,0:T(8,128)(2,1)S(1)}, u32[]{:S(2)}, u32[]{:S(2)}) collective-permute-start(bf16[16,4096]{1,0:T(8,128)(2,1)S(1)} %get-tuple-element.51), channel_id=1, source_target_pairs={{0,64},{8,72},{16,80},{24,88},{32,96},{40,104},{48,112},{56,120},{... | collective-permute-start | bytes 393224 | tf_op jit(solution)/shard_map/ppermute | solution.py:44
  9.5 14.2 %collective-permute-start = (bf16[16,4096]{1,0:T(8,128)(2,1)S(1)}, bf16[16,4096]{1,0:T(8,128)(2,1)S(1)}, u32[]{:S(2)}, u32[]{:S(2)}) collective-permute-start(bf16[16,4096]{1,0:T(8,128)(2,1)S(1)} %get-tuple-element.50), channel_id=1, source_target_pairs={{0,32},{8,40},{16,48},{24,56},{32,64},{40,72},{48,80},{56,88},{64,... | collective-permute-start | bytes 393224 | tf_op jit(solution)/shard_map/ppermute | solution.py:44
  10.8 13.5 %collective-permute-start.8 = (bf16[16,4096]{1,0:T(8,128)(2,1)S(1)}, bf16[16,4096]{1,0:T(8,128)(2,1)S(1)}, u32[]{:S(2)}, u32[]{:S(2)}) collective-permute-start(bf16[16,4096]{1,0:T(8,128)(2,1)S(1)} %get-tuple-element.56), channel_id=1, source_target_pairs={{0,120},{8,112},{16,104},{24,96},{32,24},{40,16},{48,8},{56,0},{64... | collective-permute-start | bytes 393224 | tf_op jit(solution)/shard_map/ppermute | solution.py:44
  15.2 9.0 %collective-permute-start.7 = (bf16[16,4096]{1,0:T(8,128)(2,1)S(1)}, bf16[16,4096]{1,0:T(8,128)(2,1)S(1)}, u32[]{:S(2)}, u32[]{:S(2)}) collective-permute-start(bf16[16,4096]{1,0:T(8,128)(2,1)S(1)} %get-tuple-element.55), channel_id=1, source_target_pairs={{0,88},{8,80},{16,72},{24,64},{32,120},{40,112},{48,104},{56,96},{... | collective-permute-start | bytes 393224 | tf_op jit(solution)/shard_map/ppermute | solution.py:44
  19.3 11.9 %collective-permute-start.6 = (bf16[16,4096]{1,0:T(8,128)(2,1)S(1)}, bf16[16,4096]{1,0:T(8,128)(2,1)S(1)}, u32[]{:S(2)}, u32[]{:S(2)}) collective-permute-start(bf16[16,4096]{1,0:T(8,128)(2,1)S(1)} %get-tuple-element.54), channel_id=1, source_target_pairs={{0,56},{8,48},{16,40},{24,32},{32,88},{40,80},{48,72},{56,64},{64,... | collective-permute-start | bytes 393224 | tf_op jit(solution)/shard_map/ppermute | solution.py:44
  19.4 11.8 %collective-permute-start.5 = (bf16[16,4096]{1,0:T(8,128)(2,1)S(1)}, bf16[16,4096]{1,0:T(8,128)(2,1)S(1)}, u32[]{:S(2)}, u32[]{:S(2)}) collective-permute-start(bf16[16,4096]{1,0:T(8,128)(2,1)S(1)} %get-tuple-element.53), channel_id=1, source_target_pairs={{0,24},{8,16},{16,8},{24,0},{32,56},{40,48},{48,40},{56,32},{64,88... | collective-permute-start | bytes 393224 | tf_op jit(solution)/shard_map/ppermute | solution.py:44
  23.8 44.3 %copy-start.2 = (bf16[1,4096,344]{1,2,0:T(8,128)(2,1)S(1)}, bf16[1,4096,344]{1,2,0:T(8,128)(2,1)}, u32[]{:S(2)}) copy-start(bf16[1,4096,344]{1,2,0:T(8,128)(2,1)} %param.11) | copy-start | bytes 8454148
  24.1 10.9 %collective-permute-start.3 = (bf16[48,4096]{1,0:T(8,128)(2,1)S(1)}, bf16[48,4096]{1,0:T(8,128)(2,1)S(1)}, u32[]{:S(2)}, u32[]{:S(2)}) collective-permute-start(bf16[48,4096]{1,0:T(8,128)(2,1)S(1)} %convolution_convert_fusion.1.refs_0_), channel_id=1, source_target_pairs={{0,8},{8,0},{1,9},{9,1},{2,10},{10,2},{3,11},{11,3},{4,12},{12,4},... | collective-permute-start | bytes 1179656 | tf_op jit(solution)/shard_map/ppermute | solution.py:31
  31.5 9.6 %collective-permute-start.9 = (bf16[48,4096]{1,0:T(8,128)(2,1)S(1)}, bf16[48,4096]{1,0:T(8,128)(2,1)S(1)}, u32[]{:S(2)}, u32[]{:S(2)}) collective-permute-start(bf16[48,4096]{1,0:T(8,128)(2,1)S(1)} %convolution_convert_fusion.refs_1_), channel_id=1, source_target_pairs={{0,8},{8,0},{1,9},{9,1},{2,10},{10,2},{3,11},{11,3},{4,12},{12,4},... | collective-permute-start | bytes 1179656 | tf_op jit(solution)/shard_map/ppermute | solution.py:31
  31.7 12.0 %collective-permute-start.11 = (bf16[48,4096]{1,0:T(8,128)(2,1)S(1)}, bf16[48,4096]{1,0:T(8,128)(2,1)S(1)}, u32[]{:S(2)}, u32[]{:S(2)}) collective-permute-start(bf16[48,4096]{1,0:T(8,128)(2,1)S(1)} %convolution_convert_fusion.1.refs_0_), channel_id=1, source_target_pairs={{0,6},{2,0},{4,2},{6,4},{1,7},{3,1},{5,3},{7,5},{8,14},{10,8},{12,... | collective-permute-start | bytes 1179656 | tf_op jit(solution)/shard_map/ppermute | solution.py:27
  32.3 16.8 %collective-permute-start.13 = (bf16[48,4096]{1,0:T(8,128)(2,1)S(1)}, bf16[48,4096]{1,0:T(8,128)(2,1)S(1)}, u32[]{:S(2)}, u32[]{:S(2)}) collective-permute-start(bf16[48,4096]{1,0:T(8,128)(2,1)S(1)} %convolution_convert_fusion.refs_1_), channel_id=1, source_target_pairs={{0,6},{2,0},{4,2},{6,4},{1,7},{3,1},{5,3},{7,5},{8,14},{10,8},{12,... | collective-permute-start | bytes 1179656 | tf_op jit(solution)/shard_map/ppermute | solution.py:27
  35.0 15.6 %collective-permute-start.17 = (bf16[48,4096]{1,0:T(8,128)(2,1)S(1)}, bf16[48,4096]{1,0:T(8,128)(2,1)S(1)}, u32[]{:S(2)}, u32[]{:S(2)}) collective-permute-start(bf16[48,4096]{1,0:T(8,128)(2,1)S(1)} %convolution_convert_fusion.1.refs_0_), channel_id=1, source_target_pairs={{0,2},{2,4},{4,6},{6,0},{1,3},{3,5},{5,7},{7,1},{8,10},{10,12},{12... | collective-permute-start | bytes 1179656 | tf_op jit(solution)/shard_map/ppermute | solution.py:27
  35.0 19.8 %collective-permute-start.18 = (bf16[48,4096]{1,0:T(8,128)(2,1)S(1)}, bf16[48,4096]{1,0:T(8,128)(2,1)S(1)}, u32[]{:S(2)}, u32[]{:S(2)}) collective-permute-start(bf16[48,4096]{1,0:T(8,128)(2,1)S(1)} %convolution_convert_fusion.refs_1_), channel_id=1, source_target_pairs={{0,2},{2,4},{4,6},{6,0},{1,3},{3,5},{5,7},{7,1},{8,10},{10,12},{12... | collective-permute-start | bytes 1179656 | tf_op jit(solution)/shard_map/ppermute | solution.py:27
  41.1 13.7 %collective-permute-start.19 = (bf16[48,4096]{1,0:T(8,128)(2,1)S(1)}, bf16[48,4096]{1,0:T(8,128)(2,1)S(1)}, u32[]{:S(2)}, u32[]{:S(2)}) collective-permute-start(bf16[48,4096]{1,0:T(8,128)(2,1)S(1)} %convolution_convert_fusion.1.refs_0_), channel_id=1, source_target_pairs={{0,1},{1,0},{2,3},{3,2},{4,5},{5,4},{6,7},{7,6},{8,9},{9,8},{10,11... | collective-permute-start | bytes 1179656 | tf_op jit(solution)/shard_map/ppermute | solution.py:35
  43.7 11.7 %collective-permute-start.20 = (bf16[48,4096]{1,0:T(8,128)(2,1)S(1)}, bf16[48,4096]{1,0:T(8,128)(2,1)S(1)}, u32[]{:S(2)}, u32[]{:S(2)}) collective-permute-start(bf16[48,4096]{1,0:T(8,128)(2,1)S(1)} %convolution_convert_fusion.refs_1_), channel_id=1, source_target_pairs={{0,1},{1,0},{2,3},{3,2},{4,5},{5,4},{6,7},{7,6},{8,9},{9,8},{10,11... | collective-permute-start | bytes 1179656 | tf_op jit(solution)/shard_map/ppermute | solution.py:35
  49.1 11.1 %collective-permute-start.4 = (bf16[48,4096]{1,0:T(8,128)(2,1)S(1)}, bf16[48,4096]{1,0:T(8,128)(2,1)S(1)}, u32[]{:S(2)}, u32[]{:S(2)}) collective-permute-start(bf16[48,4096]{1,0:T(8,128)(2,1)S(1)} %collective-permute-done.3.refs_6_), channel_id=1, source_target_pairs={{0,2},{2,4},{4,6},{6,0},{1,3},{3,5},{5,7},{7,1},{8,10},{10,12},{12... | collective-permute-start | bytes 1179656 | tf_op jit(solution)/shard_map/ppermute | solution.py:27
  50.6 9.6 %collective-permute-start.21 = (bf16[48,4096]{1,0:T(8,128)(2,1)S(1)}, bf16[48,4096]{1,0:T(8,128)(2,1)S(1)}, u32[]{:S(2)}, u32[]{:S(2)}) collective-permute-start(bf16[48,4096]{1,0:T(8,128)(2,1)S(1)} %collective-permute-done.17.refs_2_), channel_id=1, source_target_pairs={{0,1},{1,0},{2,3},{3,2},{4,5},{5,4},{6,7},{7,6},{8,9},{9,8},{10,11... | collective-permute-start | bytes 1179656 | tf_op jit(solution)/shard_map/ppermute | solution.py:35
  54.9 5.9 %collective-permute-start.22 = (bf16[48,4096]{1,0:T(8,128)(2,1)S(1)}, bf16[48,4096]{1,0:T(8,128)(2,1)S(1)}, u32[]{:S(2)}, u32[]{:S(2)}) collective-permute-start(bf16[48,4096]{1,0:T(8,128)(2,1)S(1)} %collective-permute-done.18.refs_3_), channel_id=1, source_target_pairs={{0,1},{1,0},{2,3},{3,2},{4,5},{5,4},{6,7},{7,6},{8,9},{9,8},{10,11... | collective-permute-start | bytes 1179656 | tf_op jit(solution)/shard_map/ppermute | solution.py:35
  54.9 6.1 %collective-permute-start.23 = (bf16[48,4096]{1,0:T(8,128)(2,1)S(1)}, bf16[48,4096]{1,0:T(8,128)(2,1)S(1)}, u32[]{:S(2)}, u32[]{:S(2)}) collective-permute-start(bf16[48,4096]{1,0:T(8,128)(2,1)S(1)} %collective-permute-done.11.refs_4_), channel_id=1, source_target_pairs={{0,1},{1,0},{2,3},{3,2},{4,5},{5,4},{6,7},{7,6},{8,9},{9,8},{10,11... | collective-permute-start | bytes 1179656 | tf_op jit(solution)/shard_map/ppermute | solution.py:35
  55.4 7.3 %collective-permute-start.24 = (bf16[48,4096]{1,0:T(8,128)(2,1)S(1)}, bf16[48,4096]{1,0:T(8,128)(2,1)S(1)}, u32[]{:S(2)}, u32[]{:S(2)}) collective-permute-start(bf16[48,4096]{1,0:T(8,128)(2,1)S(1)} %collective-permute-done.13.refs_5_), channel_id=1, source_target_pairs={{0,1},{1,0},{2,3},{3,2},{4,5},{5,4},{6,7},{7,6},{8,9},{9,8},{10,11... | collective-permute-start | bytes 1179656 | tf_op jit(solution)/shard_map/ppermute | solution.py:35
  60.2 2.8 %collective-permute-start.25 = (bf16[48,4096]{1,0:T(8,128)(2,1)S(1)}, bf16[48,4096]{1,0:T(8,128)(2,1)S(1)}, u32[]{:S(2)}, u32[]{:S(2)}) collective-permute-start(bf16[48,4096]{1,0:T(8,128)(2,1)S(1)} %collective-permute-done.3.refs_6_), channel_id=1, source_target_pairs={{0,1},{1,0},{2,3},{3,2},{4,5},{5,4},{6,7},{7,6},{8,9},{9,8},{10,11... | collective-permute-start | bytes 1179656 | tf_op jit(solution)/shard_map/ppermute | solution.py:35
  60.2 20.3 %copy-start.3 = (bf16[48,4096]{1,0:T(8,128)(2,1)}, bf16[48,4096]{1,0:T(8,128)(2,1)S(1)}, u32[]{:S(2)}) copy-start(bf16[48,4096]{1,0:T(8,128)(2,1)S(1)} %collective-permute-done.21.refs_10_.refs_19_) | copy-start | bytes 1179652
  60.2 4.7 %collective-permute-start.26 = (bf16[48,4096]{1,0:T(8,128)(2,1)S(1)}, bf16[48,4096]{1,0:T(8,128)(2,1)S(1)}, u32[]{:S(2)}, u32[]{:S(2)}) collective-permute-start(bf16[48,4096]{1,0:T(8,128)(2,1)S(1)} %collective-permute-done.9.refs_7_), channel_id=1, source_target_pairs={{0,1},{1,0},{2,3},{3,2},{4,5},{5,4},{6,7},{7,6},{8,9},{9,8},{10,11... | collective-permute-start | bytes 1179656 | tf_op jit(solution)/shard_map/ppermute | solution.py:35
  60.7 19.8 %collective-permute-start.10 = (bf16[48,4096]{1,0:T(8,128)(2,1)S(1)}, bf16[48,4096]{1,0:T(8,128)(2,1)S(1)}, u32[]{:S(2)}, u32[]{:S(2)}) collective-permute-start(bf16[48,4096]{1,0:T(8,128)(2,1)S(1)} %collective-permute-done.9.refs_7_), channel_id=1, source_target_pairs={{0,2},{2,4},{4,6},{6,0},{1,3},{3,5},{5,7},{7,1},{8,10},{10,12},{12... | collective-permute-start | bytes 1179656 | tf_op jit(solution)/shard_map/ppermute | solution.py:27
  61.0 19.5 %copy-start.5 = (bf16[48,4096]{1,0:T(8,128)(2,1)}, bf16[48,4096]{1,0:T(8,128)(2,1)S(1)}, u32[]{:S(2)}) copy-start(bf16[48,4096]{1,0:T(8,128)(2,1)S(1)} %collective-permute-done.23.refs_12_.refs_21_) | copy-start | bytes 1179652
  61.0 19.5 %collective-permute-start.12 = (bf16[48,4096]{1,0:T(8,128)(2,1)S(1)}, bf16[48,4096]{1,0:T(8,128)(2,1)S(1)}, u32[]{:S(2)}, u32[]{:S(2)}) collective-permute-start(bf16[48,4096]{1,0:T(8,128)(2,1)S(1)} %collective-permute-done.11.refs_4_), channel_id=1, source_target_pairs={{0,8},{8,0},{1,9},{9,1},{2,10},{10,2},{3,11},{11,3},{4,12},{12,4},... | collective-permute-start | bytes 1179656 | tf_op jit(solution)/shard_map/ppermute | solution.py:31
  62.7 17.9 %collective-permute-start.14 = (bf16[48,4096]{1,0:T(8,128)(2,1)S(1)}, bf16[48,4096]{1,0:T(8,128)(2,1)S(1)}, u32[]{:S(2)}, u32[]{:S(2)}) collective-permute-start(bf16[48,4096]{1,0:T(8,128)(2,1)S(1)} %collective-permute-done.13.refs_5_), channel_id=1, source_target_pairs={{0,8},{8,0},{1,9},{9,1},{2,10},{10,2},{3,11},{11,3},{4,12},{12,4},... | collective-permute-start | bytes 1179656 | tf_op jit(solution)/shard_map/ppermute | solution.py:31
  63.0 17.5 %collective-permute-start.15 = (bf16[48,4096]{1,0:T(8,128)(2,1)S(1)}, bf16[48,4096]{1,0:T(8,128)(2,1)S(1)}, u32[]{:S(2)}, u32[]{:S(2)}) collective-permute-start(bf16[48,4096]{1,0:T(8,128)(2,1)S(1)} %collective-permute-done.11.refs_4_), channel_id=1, source_target_pairs={{0,6},{2,0},{4,2},{6,4},{1,7},{3,1},{5,3},{7,5},{8,14},{10,8},{12,... | collective-permute-start | bytes 1179656 | tf_op jit(solution)/shard_map/ppermute | solution.py:27
  64.9 16.9 %collective-permute-start.16 = (bf16[48,4096]{1,0:T(8,128)(2,1)S(1)}, bf16[48,4096]{1,0:T(8,128)(2,1)S(1)}, u32[]{:S(2)}, u32[]{:S(2)}) collective-permute-start(bf16[48,4096]{1,0:T(8,128)(2,1)S(1)} %collective-permute-done.13.refs_5_), channel_id=1, source_target_pairs={{0,6},{2,0},{4,2},{6,4},{1,7},{3,1},{5,3},{7,5},{8,14},{10,8},{12,... | collective-permute-start | bytes 1179656 | tf_op jit(solution)/shard_map/ppermute | solution.py:27
  81.9 7.4 %collective-permute-start.29 = (bf16[32,4096]{1,0:T(8,128)(2,1)S(1)}, bf16[32,4096]{1,0:T(8,128)(2,1)S(1)}, u32[]{:S(2)}, u32[]{:S(2)}) collective-permute-start(bf16[32,4096]{1,0:T(8,128)(2,1)S(1)} %slice.108), channel_id=1, source_target_pairs={{0,2},{2,4},{4,6},{6,0},{1,3},{3,5},{5,7},{7,1},{8,10},{10,12},{12... | collective-permute-start | bytes 786440 | tf_op jit(solution)/shard_map/ppermute | solution.py:27
  84.6 7.6 %collective-permute-start.30 = (bf16[32,4096]{1,0:T(8,128)(2,1)S(1)}, bf16[32,4096]{1,0:T(8,128)(2,1)S(1)}, u32[]{:S(2)}, u32[]{:S(2)}) collective-permute-start(bf16[32,4096]{1,0:T(8,128)(2,1)S(1)} %pad_maximum_fusion), channel_id=1, source_target_pairs={{0,6},{2,0},{4,2},{6,4},{1,7},{3,1},{5,3},{7,5},{8,14},{10,8},{12,... | collective-permute-start | bytes 786440 | tf_op jit(solution)/shard_map/ppermute | solution.py:27
  84.7 8.9 %collective-permute-start.32 = (bf16[48,4096]{1,0:T(8,128)(2,1)S(1)}, bf16[48,4096]{1,0:T(8,128)(2,1)S(1)}, u32[]{:S(2)}, u32[]{:S(2)}) collective-permute-start(bf16[48,4096]{1,0:T(8,128)(2,1)S(1)} %collective-permute-done.4.refs_0_.refs_8_), channel_id=1, source_target_pairs={{0,1},{1,0},{2,3},{3,2},{4,5},{5,4},{6,7},{7,6},{8,9},{9,8},{10,11... | collective-permute-start | bytes 1179656 | tf_op jit(solution)/shard_map/ppermute | solution.py:35
  84.8 8.8 %collective-permute-start.31 = (bf16[32,4096]{1,0:T(8,128)(2,1)S(1)}, bf16[32,4096]{1,0:T(8,128)(2,1)S(1)}, u32[]{:S(2)}, u32[]{:S(2)}) collective-permute-start(bf16[32,4096]{1,0:T(8,128)(2,1)S(1)} %slice.111), channel_id=1, source_target_pairs={{0,8},{8,0},{1,9},{9,1},{2,10},{10,2},{3,11},{11,3},{4,12},{12,4},... | collective-permute-start | bytes 786440 | tf_op jit(solution)/shard_map/ppermute | solution.py:31
  86.5 7.6 %collective-permute-start.33 = (bf16[48,4096]{1,0:T(8,128)(2,1)S(1)}, bf16[48,4096]{1,0:T(8,128)(2,1)S(1)}, u32[]{:S(2)}, u32[]{:S(2)}) collective-permute-start(bf16[48,4096]{1,0:T(8,128)(2,1)S(1)} %collective-permute-done.10.refs_1_.refs_9_), channel_id=1, source_target_pairs={{0,1},{1,0},{2,3},{3,2},{4,5},{5,4},{6,7},{7,6},{8,9},{9,8},{10,11... | collective-permute-start | bytes 1179656 | tf_op jit(solution)/shard_map/ppermute | solution.py:35
  89.3 4.9 %collective-permute-start.34 = (bf16[48,4096]{1,0:T(8,128)(2,1)S(1)}, bf16[48,4096]{1,0:T(8,128)(2,1)S(1)}, u32[]{:S(2)}, u32[]{:S(2)}) collective-permute-start(bf16[48,4096]{1,0:T(8,128)(2,1)S(1)} %collective-permute-done.12.refs_2_.refs_10_), channel_id=1, source_target_pairs={{0,1},{1,0},{2,3},{3,2},{4,5},{5,4},{6,7},{7,6},{8,9},{9,8},{10,11... | collective-permute-start | bytes 1179656 | tf_op jit(solution)/shard_map/ppermute | solution.py:35
  92.2 2.4 %collective-permute-start.35 = (bf16[48,4096]{1,0:T(8,128)(2,1)S(1)}, bf16[48,4096]{1,0:T(8,128)(2,1)S(1)}, u32[]{:S(2)}, u32[]{:S(2)}) collective-permute-start(bf16[48,4096]{1,0:T(8,128)(2,1)S(1)} %collective-permute-done.14.refs_3_.refs_11_), channel_id=1, source_target_pairs={{0,1},{1,0},{2,3},{3,2},{4,5},{5,4},{6,7},{7,6},{8,9},{9,8},{10,11... | collective-permute-start | bytes 1179656 | tf_op jit(solution)/shard_map/ppermute | solution.py:35
  93.6 1.7 collective-permute-start.36
  93.6 2.3 %collective-permute-start.37 = (bf16[48,4096]{1,0:T(8,128)(2,1)S(1)}, bf16[48,4096]{1,0:T(8,128)(2,1)S(1)}, u32[]{:S(2)}, u32[]{:S(2)}) collective-permute-start(bf16[48,4096]{1,0:T(8,128)(2,1)S(1)} %collective-permute-done.16.refs_5_.refs_13_), channel_id=1, source_target_pairs={{0,1},{1,0},{2,3},{3,2},{4,5},{5,4},{6,7},{7,6},{8,9},{9,8},{10,11... | collective-permute-start | bytes 1179656 | tf_op jit(solution)/shard_map/ppermute | solution.py:35
  94.1 2.1 %collective-permute-start.38 = (bf16[32,4096]{1,0:T(8,128)(2,1)S(1)}, bf16[32,4096]{1,0:T(8,128)(2,1)S(1)}, u32[]{:S(2)}, u32[]{:S(2)}) collective-permute-start(bf16[32,4096]{1,0:T(8,128)(2,1)S(1)} %collective-permute-done.29.refs_6_.refs_14_), channel_id=1, source_target_pairs={{0,1},{1,0},{2,3},{3,2},{4,5},{5,4},{6,7},{7,6},{8,9},{9,8},{10,11... | collective-permute-start | bytes 786440 | tf_op jit(solution)/shard_map/ppermute | solution.py:35
  94.2 2.4 %collective-permute-start.39 = (bf16[32,4096]{1,0:T(8,128)(2,1)S(1)}, bf16[32,4096]{1,0:T(8,128)(2,1)S(1)}, u32[]{:S(2)}, u32[]{:S(2)}) collective-permute-start(bf16[32,4096]{1,0:T(8,128)(2,1)S(1)} %collective-permute-done.30.refs_7_.refs_15_), channel_id=1, source_target_pairs={{0,1},{1,0},{2,3},{3,2},{4,5},{5,4},{6,7},{7,6},{8,9},{9,8},{10,11... | collective-permute-start | bytes 786440 | tf_op jit(solution)/shard_map/ppermute | solution.py:35
  94.6 2.4 %collective-permute-start.40 = (bf16[32,4096]{1,0:T(8,128)(2,1)S(1)}, bf16[32,4096]{1,0:T(8,128)(2,1)S(1)}, u32[]{:S(2)}, u32[]{:S(2)}) collective-permute-start(bf16[32,4096]{1,0:T(8,128)(2,1)S(1)} %collective-permute-done.31.refs_8_.refs_16_), channel_id=1, source_target_pairs={{0,1},{1,0},{2,3},{3,2},{4,5},{5,4},{6,7},{7,6},{8,9},{9,8},{10,11... | collective-permute-start | bytes 786440 | tf_op jit(solution)/shard_map/ppermute | solution.py:35
  109.4 3.6 %collective-permute-start.41 = (bf16[384,2176]{1,0:T(8,128)(2,1)S(1)}, bf16[384,2176]{1,0:T(8,128)(2,1)S(1)}, u32[]{:S(2)}, u32[]{:S(2)}) collective-permute-start(bf16[384,2176]{1,0:T(8,128)(2,1)S(1)} %get-tuple-element.71), channel_id=1, source_target_pairs={{0,1},{1,0},{2,3},{3,2},{4,5},{5,4},{6,7},{7,6},{8,9},{9,8},{10,11... | collective-permute-start | bytes 5013512 | tf_op jit(solution)/shard_map/ppermute | solution.py:35
  109.6 34.5 %collective-permute-start.27 = (bf16[384,2176]{1,0:T(8,128)(2,1)S(1)}, bf16[384,2176]{1,0:T(8,128)(2,1)S(1)}, u32[]{:S(2)}, u32[]{:S(2)}) collective-permute-start(bf16[384,2176]{1,0:T(8,128)(2,1)S(1)} %get-tuple-element.63), channel_id=1, source_target_pairs={{0,1},{1,0},{2,3},{3,2},{4,5},{5,4},{6,7},{7,6},{8,9},{9,8},{10,11... | collective-permute-start | bytes 5013512 | tf_op jit(solution)/shard_map/ppermute | solution.py:35
  113.1 5.8 %collective-permute-start.46 = (bf16[32,2176]{1,0:T(8,128)(2,1)S(1)}, bf16[32,2176]{1,0:T(8,128)(2,1)S(1)}, u32[]{:S(2)}, u32[]{:S(2)}) collective-permute-start(bf16[32,2176]{1,0:T(8,128)(2,1)S(1)} %get-tuple-element.100), channel_id=1, source_target_pairs={{0,8},{8,0},{1,9},{9,1},{2,10},{10,2},{3,11},{11,3},{4,12},{12,4},... | collective-permute-start | bytes 417800 | tf_op jit(solution)/shard_map/ppermute | solution.py:31
  114.9 7.2 %collective-permute-start.44 = (bf16[32,2176]{1,0:T(8,128)(2,1)S(1)}, bf16[32,2176]{1,0:T(8,128)(2,1)S(1)}, u32[]{:S(2)}, u32[]{:S(2)}) collective-permute-start(bf16[32,2176]{1,0:T(8,128)(2,1)S(1)} %get-tuple-element.101), channel_id=1, source_target_pairs={{0,2},{2,4},{4,6},{6,0},{1,3},{3,5},{5,7},{7,1},{8,10},{10,12},{12... | collective-permute-start | bytes 417800 | tf_op jit(solution)/shard_map/ppermute | solution.py:27
  117.8 8.2 %copy-start.4 = (bf16[48,4096]{1,0:T(8,128)(2,1)S(1)}, bf16[48,4096]{1,0:T(8,128)(2,1)}, u32[]{:S(2)}) copy-start(bf16[48,4096]{1,0:T(8,128)(2,1)} %copy-done.3) | copy-start | bytes 1179652
  117.8 8.2 %copy-start.6 = (bf16[48,4096]{1,0:T(8,128)(2,1)S(1)}, bf16[48,4096]{1,0:T(8,128)(2,1)}, u32[]{:S(2)}) copy-start(bf16[48,4096]{1,0:T(8,128)(2,1)} %copy-done.5) | copy-start | bytes 1179652
  117.8 5.3 %collective-permute-start.42 = (bf16[32,2176]{1,0:T(8,128)(2,1)S(1)}, bf16[32,2176]{1,0:T(8,128)(2,1)S(1)}, u32[]{:S(2)}, u32[]{:S(2)}) collective-permute-start(bf16[32,2176]{1,0:T(8,128)(2,1)S(1)} %get-tuple-element.102), channel_id=1, source_target_pairs={{0,6},{2,0},{4,2},{6,4},{1,7},{3,1},{5,3},{7,5},{8,14},{10,8},{12,... | collective-permute-start | bytes 417800 | tf_op jit(solution)/shard_map/ppermute | solution.py:27
  123.6 20.5 %collective-permute-start.43 = (bf16[96,2176]{1,0:T(8,128)(2,1)S(1)}, bf16[96,2176]{1,0:T(8,128)(2,1)S(1)}, u32[]{:S(2)}, u32[]{:S(2)}) collective-permute-start(bf16[96,2176]{1,0:T(8,128)(2,1)S(1)} %get-tuple-element.99), channel_id=1, source_target_pairs={{0,6},{2,0},{4,2},{6,4},{1,7},{3,1},{5,3},{7,5},{8,14},{10,8},{12,... | collective-permute-start | bytes 1253384 | tf_op jit(solution)/shard_map/ppermute | solution.py:27
  125.5 18.7 %collective-permute-start.45 = (bf16[96,2176]{1,0:T(8,128)(2,1)S(1)}, bf16[96,2176]{1,0:T(8,128)(2,1)S(1)}, u32[]{:S(2)}, u32[]{:S(2)}) collective-permute-start(bf16[96,2176]{1,0:T(8,128)(2,1)S(1)} %get-tuple-element.98), channel_id=1, source_target_pairs={{0,8},{8,0},{1,9},{9,1},{2,10},{10,2},{3,11},{11,3},{4,12},{12,4},... | collective-permute-start | bytes 1253384 | tf_op jit(solution)/shard_map/ppermute | solution.py:31
  125.8 18.3 %collective-permute-start.47 = (bf16[96,2176]{1,0:T(8,128)(2,1)S(1)}, bf16[96,2176]{1,0:T(8,128)(2,1)S(1)}, u32[]{:S(2)}, u32[]{:S(2)}) collective-permute-start(bf16[96,2176]{1,0:T(8,128)(2,1)S(1)} %get-tuple-element.97), channel_id=1, source_target_pairs={{0,2},{2,4},{4,6},{6,0},{1,3},{3,5},{5,7},{7,1},{8,10},{10,12},{12... | collective-permute-start | bytes 1253384 | tf_op jit(solution)/shard_map/ppermute | solution.py:27
  144.6 9.9 %collective-permute-start.49 = (bf16[96,2176]{1,0:T(8,128)(2,1)S(1)}, bf16[96,2176]{1,0:T(8,128)(2,1)S(1)}, u32[]{:S(2)}, u32[]{:S(2)}) collective-permute-start(bf16[96,2176]{1,0:T(8,128)(2,1)S(1)} %get-tuple-element.95), channel_id=1, source_target_pairs={{0,8},{8,0},{1,9},{9,1},{2,10},{10,2},{3,11},{11,3},{4,12},{12,4},... | collective-permute-start | bytes 1253384 | tf_op jit(solution)/shard_map/ppermute | solution.py:31
  146.4 10.5 %collective-permute-start.48 = (bf16[96,2176]{1,0:T(8,128)(2,1)S(1)}, bf16[96,2176]{1,0:T(8,128)(2,1)S(1)}, u32[]{:S(2)}, u32[]{:S(2)}) collective-permute-start(bf16[96,2176]{1,0:T(8,128)(2,1)S(1)} %get-tuple-element.96), channel_id=1, source_target_pairs={{0,2},{2,4},{4,6},{6,0},{1,3},{3,5},{5,7},{7,1},{8,10},{10,12},{12... | collective-permute-start | bytes 1253384 | tf_op jit(solution)/shard_map/ppermute | solution.py:27
  148.6 10.3 %collective-permute-start.28 = (bf16[96,2176]{1,0:T(8,128)(2,1)S(1)}, bf16[96,2176]{1,0:T(8,128)(2,1)S(1)}, u32[]{:S(2)}, u32[]{:S(2)}) collective-permute-start(bf16[96,2176]{1,0:T(8,128)(2,1)S(1)} %get-tuple-element.94), channel_id=1, source_target_pairs={{0,6},{2,0},{4,2},{6,4},{1,7},{3,1},{5,3},{7,5},{8,14},{10,8},{12,... | collective-permute-start | bytes 1253384 | tf_op jit(solution)/shard_map/ppermute | solution.py:27
  159.9 13.3 %collective-permute-start.50 = (bf16[16,2176]{1,0:T(8,128)(2,1)S(1)}, bf16[16,2176]{1,0:T(8,128)(2,1)S(1)}, u32[]{:S(2)}, u32[]{:S(2)}) collective-permute-start(bf16[16,2176]{1,0:T(8,128)(2,1)S(1)} %get-tuple-element.106), channel_id=1, source_target_pairs={{0,24},{8,16},{16,8},{24,0},{32,56},{40,48},{48,40},{56,32},{64,88... | collective-permute-start | bytes 208904 | tf_op jit(solution)/shard_map/ppermute | solution.py:44
  160.1 13.2 %collective-permute-start.51 = (bf16[16,2176]{1,0:T(8,128)(2,1)S(1)}, bf16[16,2176]{1,0:T(8,128)(2,1)S(1)}, u32[]{:S(2)}, u32[]{:S(2)}) collective-permute-start(bf16[16,2176]{1,0:T(8,128)(2,1)S(1)} %get-tuple-element.109), channel_id=1, source_target_pairs={{0,96},{8,104},{16,112},{24,120},{32,0},{40,8},{48,16},{56,24},{64... | collective-permute-start | bytes 208904 | tf_op jit(solution)/shard_map/ppermute | solution.py:44
  164.3 9.6 %collective-permute-start.52 = (bf16[16,2176]{1,0:T(8,128)(2,1)S(1)}, bf16[16,2176]{1,0:T(8,128)(2,1)S(1)}, u32[]{:S(2)}, u32[]{:S(2)}) collective-permute-start(bf16[16,2176]{1,0:T(8,128)(2,1)S(1)} %get-tuple-element.105), channel_id=1, source_target_pairs={{0,120},{8,112},{16,104},{24,96},{32,24},{40,16},{48,8},{56,0},{64... | collective-permute-start | bytes 208904 | tf_op jit(solution)/shard_map/ppermute | solution.py:44
  167.1 6.8 %collective-permute-start.53 = (bf16[16,2176]{1,0:T(8,128)(2,1)S(1)}, bf16[16,2176]{1,0:T(8,128)(2,1)S(1)}, u32[]{:S(2)}, u32[]{:S(2)}) collective-permute-start(bf16[16,2176]{1,0:T(8,128)(2,1)S(1)} %get-tuple-element.108), channel_id=1, source_target_pairs={{0,64},{8,72},{16,80},{24,88},{32,96},{40,104},{48,112},{56,120},{... | collective-permute-start | bytes 208904 | tf_op jit(solution)/shard_map/ppermute | solution.py:44
  167.2 8.7 %collective-permute-start.54 = (bf16[16,2176]{1,0:T(8,128)(2,1)S(1)}, bf16[16,2176]{1,0:T(8,128)(2,1)S(1)}, u32[]{:S(2)}, u32[]{:S(2)}) collective-permute-start(bf16[16,2176]{1,0:T(8,128)(2,1)S(1)} %get-tuple-element.104), channel_id=1, source_target_pairs={{0,88},{8,80},{16,72},{24,64},{32,120},{40,112},{48,104},{56,96},{... | collective-permute-start | bytes 208904 | tf_op jit(solution)/shard_map/ppermute | solution.py:44
  173.3 5.5 %collective-permute-start.55 = (bf16[16,2176]{1,0:T(8,128)(2,1)S(1)}, bf16[16,2176]{1,0:T(8,128)(2,1)S(1)}, u32[]{:S(2)}, u32[]{:S(2)}) collective-permute-start(bf16[16,2176]{1,0:T(8,128)(2,1)S(1)} %get-tuple-element.107), channel_id=1, source_target_pairs={{0,32},{8,40},{16,48},{24,56},{32,64},{40,72},{48,80},{56,88},{64,... | collective-permute-start | bytes 208904 | tf_op jit(solution)/shard_map/ppermute | solution.py:44
  173.3 7.7 %collective-permute-start.56 = (bf16[16,2176]{1,0:T(8,128)(2,1)S(1)}, bf16[16,2176]{1,0:T(8,128)(2,1)S(1)}, u32[]{:S(2)}, u32[]{:S(2)}) collective-permute-start(bf16[16,2176]{1,0:T(8,128)(2,1)S(1)} %get-tuple-element.103), channel_id=1, source_target_pairs={{0,56},{8,48},{16,40},{24,32},{32,88},{40,80},{48,72},{56,64},{64,... | collective-permute-start | bytes 208904 | tf_op jit(solution)/shard_map/ppermute | solution.py:44
where the time goes:
time: 183 us; the launch traced here: 182 us
  waiting for transfers between devices  66.2 us (36%)
  starting transfers between devices  63.4 us (35%)
  Pallas kernels  45.1 us (25%)
  local copies, waits for them, and re-layouts  4.13 us (2%)
    ppermute x16, waiting for transfers between devices, along_x(): return lax.ppermute(value, 'x', [(i, (i + step) % 4) for i in range(4)])  32.2 us
    ppermute x14, starting transfers between devices, to_expert(): return lax.ppermute(value, ('z', 'yh', 'yl'), perm)  30.1 us
    pallas_call x2, Pallas kernels, run_group(): pl.pallas_call(functools.partial(group_kernel, len(ours), half), out_shap...  24.8 us
    ppermute x16, starting transfers between devices, along_x(): return lax.ppermute(value, 'x', [(i, (i + step) % 4) for i in range(4)])  22 us
    pallas_call x1, Pallas kernels, weight_grads(): pl.pallas_call(functools.partial(weight_kernel, sizes, width // 2, hid, 5...  18.1 us
    ppermute x14, waiting for transfers between devices, to_expert(): return lax.ppermute(value, ('z', 'yh', 'yl'), perm)  16.2 us
    ppermute x8, waiting for transfers between devices, pair_y(): return lax.ppermute(value, 'yl', [(0, 1), (1, 0)])  12.7 us
    ppermute x8, starting transfers between devices, pair_y(): return lax.ppermute(value, 'yl', [(0, 1), (1, 0)])  8 us
  transfers between devices with their start and end apart: 57, of which 26 were waited for; matrix products, arithmetic and copies ran while one was open for 1% of the time, Pallas kernels for 17%

commit v1 on v0

--- a/solution.py
+++ b/solution.py
@@ -153,12 +153,13 @@
     )(place, *ours, *theirs, gate, up, down)
 
 
-def weight_kernel(sizes, half, hid, tile, place_ref, *refs):
+def weight_kernel(sizes, offset, half, hid, tile, place_ref, *refs):
     count = len(sizes)
+    kinds = (len(refs) - 2 * count - 5) // 3
     ours, theirs = refs[:count], refs[count : 2 * count]
-    sides = refs[2 * count : 2 * count + 6]
-    outs = refs[2 * count + 6 : 2 * count + 9]
-    rows_ref, pair_t, hidden_t, stage, in_sem, out_sem = refs[2 * count + 9 :]
+    sides = refs[2 * count : 2 * count + 2 * kinds]
+    outs = refs[2 * count + 2 * kinds : 2 * count + 3 * kinds]
+    rows_ref, sides_t, stage, in_sem, out_sem = refs[2 * count + 3 * kinds :]
     core = place_ref[0]
     loads = []
     for s, group in enumerate((ours, theirs)):
@@ -167,7 +168,9 @@
         for i, size in enumerate(sizes):
             copies.append(
                 pltpu.make_async_copy(
-                    group[i], rows_ref.at[s, pl.ds(at, size), :], in_sem.at[s, i]
+                    group[i].at[:, pl.ds(offset, half)],
+                    rows_ref.at[s, pl.ds(at, size), :],
+                    in_sem.at[s, i],
                 )
             )
             at += size
@@ -175,13 +178,10 @@
     for copies in loads:
         for c in copies:
             c.start()
-    wide = sides[0].shape[1]
-    depth = sides[0].shape[0]
-    for i in range(2):
-        columns = slice(depth * i, depth * (i + 1))
-        pair_t[:wide, columns] = sides[i][...].T
-        pair_t[wide:, columns] = sides[2 + i][...].T
-        hidden_t[:, columns] = sides[4 + i][...].T
+    depth, wide = sides[0].shape
+    for k in range(kinds):
+        for i in range(2):
+            sides_t[wide * k : wide * (k + 1), depth * i : depth * (i + 1)] = sides[2 * k + i][...].T
     stores = []
     for s in range(2):
         for c in loads[s]:
@@ -192,16 +192,14 @@
         def _(j):
             to = pl.ds(pl.multiple_of(base + j * tile, tile), tile)
             block = rows_ref[s, :, pl.ds(pl.multiple_of(j * tile, tile), tile)]
-            pair = dot_f32(pair_t[...], block, 1, 0).astype(BF)
-            stage[0, :, to] = pair[:hid]
-            stage[1, :, to] = pair[wide : wide + hid]
-            block = rows_ref[s, :, pl.ds(pl.multiple_of(half + j * tile, tile), tile)]
-            stage[2, :, to] = dot_f32(hidden_t[...], block, 1, 0).astype(BF)[:hid]
+            grads = dot_f32(sides_t[...], block, 1, 0).astype(BF)
+            for k in range(kinds):
+                stage[k, :, to] = grads[wide * k : wide * k + hid]
 
         whole = pl.ds(pl.multiple_of(base, half), half)
-        for t in range(3):
+        for k in range(kinds):
             copy = pltpu.make_async_copy(
-                stage.at[t, :, whole], outs[t].at[:, whole], out_sem.at[s, t]
+                stage.at[k, :, whole], outs[k].at[:, whole], out_sem.at[s, k]
             )
             copy.start()
             stores.append(copy)
@@ -209,28 +207,28 @@
         copy.wait()
 
 
-def weight_grads(place, ours, theirs, sides, hid):
+def weight_grads(place, ours, theirs, sides, offset, hid, tile=1024):
     sizes = [r.shape[0] for r in ours]
     rows = sum(sizes)
     width = ours[0].shape[1]
     wide = sides[0].shape[1]
+    kinds = len(sides) // 2
     anywhere = pl.BlockSpec(memory_space=pl.ANY)
     return pl.pallas_call(
-        functools.partial(weight_kernel, sizes, width // 2, hid, 512),
-        out_shape=[jax.ShapeDtypeStruct((hid, width), BF)] * 3,
-        in_specs=[SMEM] + [anywhere] * (2 * len(sizes)) + [VMEM] * 6,
-        out_specs=[anywhere] * 3,
+        functools.partial(weight_kernel, sizes, offset, width // 2, hid, tile),
+        out_shape=[jax.ShapeDtypeStruct((hid, width), BF)] * kinds,
+        in_specs=[SMEM] + [anywhere] * (2 * len(sizes)) + [VMEM] * len(sides),
+        out_specs=[anywhere] * kinds,
         scratch_shapes=[
-            pltpu.VMEM((2, rows, width), BF),
-            pltpu.VMEM((2 * wide, rows), BF),
-            pltpu.VMEM((wide, rows), BF),
-            pltpu.VMEM((3, hid, width), BF),
+            pltpu.VMEM((2, rows, width // 2), BF),
+            pltpu.VMEM((kinds * wide, rows), BF),
+            pltpu.VMEM((kinds, hid, width), BF),
             pltpu.SemaphoreType.DMA((2, len(sizes))),
-            pltpu.SemaphoreType.DMA((2, 3)),
+            pltpu.SemaphoreType.DMA((2, kinds)),
         ],
-        compiler_params=pltpu.CompilerParams(vmem_limit_bytes=36 * MIB),
+        compiler_params=pltpu.CompilerParams(vmem_limit_bytes=28 * MIB),
         cost_estimate=pl.CostEstimate(
-            flops=6 * rows * hid * width, bytes_accessed=22 * MIB, transcendentals=0
+            flops=2 * kinds * rows * hid * width, bytes_accessed=14 * MIB, transcendentals=0
         ),
         name="weight_grads",
     )(place, *ours, *theirs, *sides)
@@ -338,13 +336,18 @@
     b_right_pair = pair_y(t_far_right)
     b_right = along_x(t_across, 1)
     hid = gate_t.shape[0]
-    sides = [g for t in (2, 3, 4) for g in (near_out[t], far_out[t])]
-    grads = weight_grads(place, near + far, near_other + far_other, sides, hid)
-    tied = lax.optimization_barrier((b_partner, b_right_pair, b_right, *grads))
-    b_partner, b_right_pair, b_right, gate_grad, up_grad, down_grad = tied
+    rows = (near + far, near_other + far_other)
+    sides = [g for t in (2, 3) for g in (near_out[t], far_out[t])]
+    gate_grad, up_grad = weight_grads(place, *rows, sides, 0, hid)
+    tied = lax.optimization_barrier((b_partner, b_right_pair, b_right, gate_grad, up_grad))
+    b_partner, b_right_pair, b_right, gate_grad, up_grad = tied
     c_left = along_x(chunk(near_out, near_got, 1), -1)
     c_right = along_x(add(chunk(near_out, near_got, 2), b_right_pair, b_right), 1)
     c_pair = pair_y(add(chunk(near_out, near_got, 3), b_partner))
+    half = tokens.shape[1] // 2
+    (down_grad,) = weight_grads(place, *rows, [near_out[4], far_out[4]], half, hid)
+    tied = lax.optimization_barrier((c_left, c_right, c_pair, down_grad))
+    c_left, c_right, c_pair, down_grad = tied
     home = add(chunk(near_out, near_got, 0), c_left, c_right, c_pair)
 
     backs = [None] * EXPERTS

time: 183 us -> 176 us (0.962); the launches traced: 182 us -> 174 us
  waiting for transfers between devices: 66.2 us -> 58.1 us
    ppermute x8, waiting for transfers between devices: 12.7 us -> 7.34 us  [pair_y(): return lax.ppermute(value, 'yl', [(0, 1), (1, 0)])]
    ppermute x16, waiting for transfers between devices: 32.2 us -> 29.5 us  [along_x(): return lax.ppermute(value, 'x', [(i, (i + step) % 4) for i in range(4)])]
    pallas_call x1 -> x2, Pallas kernels: 18.1 us -> 16.9 us  [weight_grads(): pl.pallas_call(functools.partial(weight_kernel, sizes, offset, width // 2...]
    unnamed x17 -> x13, local copies, waits for them, and re-layouts: 4.02 us -> 4.02 us
  transfers between devices with their start and end apart: 57 -> 57, of which waited for: 26 -> 25; matrix products, arithmetic and copies ran while one was open for 1% -> 1% of each run, Pallas kernels for 17% -> 17%
where the time goes in v1:
time: 176 us; the launch traced here: 174 us
  starting transfers between devices  63.6 us (36%)
  waiting for transfers between devices  58.1 us (33%)
  Pallas kernels  44.2 us (25%)
  local copies, waits for them, and re-layouts  4.12 us (2%)
    ppermute x14, starting transfers between devices, to_expert(): return lax.ppermute(value, ('z', 'yh', 'yl'), perm)  30.1 us
    ppermute x16, waiting for transfers between devices, along_x(): return lax.ppermute(value, 'x', [(i, (i + step) % 4) for i in range(4)])  29.5 us
    pallas_call x2, Pallas kernels, run_group(): pl.pallas_call(functools.partial(group_kernel, len(ours), half), out_shap...  25 us
    ppermute x16, starting transfers between devices, along_x(): return lax.ppermute(value, 'x', [(i, (i + step) % 4) for i in range(4)])  22.2 us
    pallas_call x2, Pallas kernels, weight_grads(): pl.pallas_call(functools.partial(weight_kernel, sizes, offset, width // 2...  16.9 us
    ppermute x14, waiting for transfers between devices, to_expert(): return lax.ppermute(value, ('z', 'yh', 'yl'), perm)  16.2 us
    ppermute x8, starting transfers between devices, pair_y(): return lax.ppermute(value, 'yl', [(0, 1), (1, 0)])  7.94 us
    ppermute x8, waiting for transfers between devices, pair_y(): return lax.ppermute(value, 'yl', [(0, 1), (1, 0)])  7.34 us
  transfers between devices with their start and end apart: 57, of which 25 were waited for; matrix products, arithmetic and copies ran while one was open for 1% of the time, Pallas kernels for 17%

profile of v1, /device:TPU:2, one launch (start us, length us, event | category | flops | bytes accessed | tf_op | source)
XLA Modules:
  0.0 173.5 jit_solution(3495420069806769352)
XLA Ops:
  0.6 0.8 copy.14.weights_ref
  1.4 0.8 copy.12.routes_ref
  2.2 0.9 copy-done
  3.2 0.9 copy-done.1
  4.1 1.3 slots.1
  5.4 4.1 %collective-permute-start.2 = (bf16[16,4096]{1,0:T(8,128)(2,1)S(1)}, bf16[16,4096]{1,0:T(8,128)(2,1)S(1)}, u32[]{:S(2)}, u32[]{:S(2)}) collective-permute-start(bf16[16,4096]{1,0:T(8,128)(2,1)S(1)} %get-tuple-element.54), channel_id=1, source_target_pairs={{0,96},{8,104},{16,112},{24,120},{32,0},{40,8},{48,16},{56,24},{64... | collective-permute-start | bytes 393224 | tf_op jit(solution)/shard_map/ppermute | solution.py:44
  9.5 1.3 collective-permute-start
  10.8 4.4 %collective-permute-start.8 = (bf16[16,4096]{1,0:T(8,128)(2,1)S(1)}, bf16[16,4096]{1,0:T(8,128)(2,1)S(1)}, u32[]{:S(2)}, u32[]{:S(2)}) collective-permute-start(bf16[16,4096]{1,0:T(8,128)(2,1)S(1)} %get-tuple-element.58), channel_id=1, source_target_pairs={{0,120},{8,112},{16,104},{24,96},{32,24},{40,16},{48,8},{56,0},{64... | collective-permute-start | bytes 393224 | tf_op jit(solution)/shard_map/ppermute | solution.py:44
  15.2 2.0 %collective-permute-start.7 = (bf16[16,4096]{1,0:T(8,128)(2,1)S(1)}, bf16[16,4096]{1,0:T(8,128)(2,1)S(1)}, u32[]{:S(2)}, u32[]{:S(2)}) collective-permute-start(bf16[16,4096]{1,0:T(8,128)(2,1)S(1)} %get-tuple-element.57), channel_id=1, source_target_pairs={{0,88},{8,80},{16,72},{24,64},{32,120},{40,112},{48,104},{56,96},{... | collective-permute-start | bytes 393224 | tf_op jit(solution)/shard_map/ppermute | solution.py:44
  17.2 2.1 %collective-permute-done.2 = bf16[16,4096]{1,0:T(8,128)(2,1)S(1)} collective-permute-done((bf16[16,4096]{1,0:T(8,128)(2,1)S(1)}, bf16[16,4096]{1,0:T(8,128)(2,1)S(1)}, u32[]{:S(2)}, u32[]{:S(2)}) %collective-permute-start.2) | collective-permute-done | bytes 131104 | tf_op jit(solution)/shard_map/ppermute | solution.py:44
  19.4 4.4 %collective-permute-start.5 = (bf16[16,4096]{1,0:T(8,128)(2,1)S(1)}, bf16[16,4096]{1,0:T(8,128)(2,1)S(1)}, u32[]{:S(2)}, u32[]{:S(2)}) collective-permute-start(bf16[16,4096]{1,0:T(8,128)(2,1)S(1)} %get-tuple-element.55), channel_id=1, source_target_pairs={{0,24},{8,16},{16,8},{24,0},{32,56},{40,48},{48,40},{56,32},{64,88... | collective-permute-start | bytes 393224 | tf_op jit(solution)/shard_map/ppermute | solution.py:44
  24.3 6.9 %collective-permute-done.6 = bf16[16,4096]{1,0:T(8,128)(2,1)S(1)} collective-permute-done((bf16[16,4096]{1,0:T(8,128)(2,1)S(1)}, bf16[16,4096]{1,0:T(8,128)(2,1)S(1)}, u32[]{:S(2)}, u32[]{:S(2)}) %collective-permute-start.6) | collective-permute-done | bytes 131104 | tf_op jit(solution)/shard_map/ppermute | solution.py:44
  31.7 0.5 collective-permute-start.11
  32.3 2.8 %collective-permute-start.13 = (bf16[48,4096]{1,0:T(8,128)(2,1)S(1)}, bf16[48,4096]{1,0:T(8,128)(2,1)S(1)}, u32[]{:S(2)}, u32[]{:S(2)}) collective-permute-start(bf16[48,4096]{1,0:T(8,128)(2,1)S(1)} %convolution_convert_fusion.refs_1_), channel_id=1, source_target_pairs={{0,6},{2,0},{4,2},{6,4},{1,7},{3,1},{5,3},{7,5},{8,14},{10,8},{12,... | collective-permute-start | bytes 1179656 | tf_op jit(solution)/shard_map/ppermute | solution.py:27
  35.0 0.8 collective-permute-start.18
  35.8 5.4 %collective-permute-done.9.refs_7_ = bf16[48,4096]{1,0:T(8,128)(2,1)S(1)} collective-permute-done((bf16[48,4096]{1,0:T(8,128)(2,1)S(1)}, bf16[48,4096]{1,0:T(8,128)(2,1)S(1)}, u32[]{:S(2)}, u32[]{:S(2)}) %collective-permute-start.9) | collective-permute-done | bytes 393248 | tf_op jit(solution)/shard_map/ppermute | solution.py:31
  41.2 2.6 %collective-permute-done.11.refs_4_ = bf16[48,4096]{1,0:T(8,128)(2,1)S(1)} collective-permute-done((bf16[48,4096]{1,0:T(8,128)(2,1)S(1)}, bf16[48,4096]{1,0:T(8,128)(2,1)S(1)}, u32[]{:S(2)}, u32[]{:S(2)}) %collective-permute-start.11) | collective-permute-done | bytes 393248 | tf_op jit(solution)/shard_map/ppermute | solution.py:27
  43.7 5.3 %collective-permute-done.13.refs_5_ = bf16[48,4096]{1,0:T(8,128)(2,1)S(1)} collective-permute-done((bf16[48,4096]{1,0:T(8,128)(2,1)S(1)}, bf16[48,4096]{1,0:T(8,128)(2,1)S(1)}, u32[]{:S(2)}, u32[]{:S(2)}) %collective-permute-start.13) | collective-permute-done | bytes 393248 | tf_op jit(solution)/shard_map/ppermute | solution.py:27
  49.1 1.5 collective-permute-start.4
  50.6 4.3 %collective-permute-done.18.refs_3_ = bf16[48,4096]{1,0:T(8,128)(2,1)S(1)} collective-permute-done((bf16[48,4096]{1,0:T(8,128)(2,1)S(1)}, bf16[48,4096]{1,0:T(8,128)(2,1)S(1)}, u32[]{:S(2)}, u32[]{:S(2)}) %collective-permute-start.18) | collective-permute-done | bytes 393248 | tf_op jit(solution)/shard_map/ppermute | solution.py:27
  54.9 0.5 collective-permute-start.23
  55.5 4.7 %collective-permute-done.4.refs_0_.refs_8_ = bf16[48,4096]{1,0:T(8,128)(2,1)S(1)} collective-permute-done((bf16[48,4096]{1,0:T(8,128)(2,1)S(1)}, bf16[48,4096]{1,0:T(8,128)(2,1)S(1)}, u32[]{:S(2)}, u32[]{:S(2)}) %collective-permute-start.4) | collective-permute-done | bytes 393248 | tf_op jit(solution)/shard_map/ppermute | solution.py:27
  60.2 0.5 collective-permute-start.26
  61.0 1.7 collective-permute-start.12
  63.0 1.9 %collective-permute-start.15 = (bf16[48,4096]{1,0:T(8,128)(2,1)S(1)}, bf16[48,4096]{1,0:T(8,128)(2,1)S(1)}, u32[]{:S(2)}, u32[]{:S(2)}) collective-permute-start(bf16[48,4096]{1,0:T(8,128)(2,1)S(1)} %collective-permute-done.11.refs_4_), channel_id=1, source_target_pairs={{0,6},{2,0},{4,2},{6,4},{1,7},{3,1},{5,3},{7,5},{8,14},{10,8},{12,... | collective-permute-start | bytes 1179656 | tf_op jit(solution)/shard_map/ppermute | solution.py:27
  64.9 3.2 %collective-permute-start.16 = (bf16[48,4096]{1,0:T(8,128)(2,1)S(1)}, bf16[48,4096]{1,0:T(8,128)(2,1)S(1)}, u32[]{:S(2)}, u32[]{:S(2)}) collective-permute-start(bf16[48,4096]{1,0:T(8,128)(2,1)S(1)} %collective-permute-done.13.refs_5_), channel_id=1, source_target_pairs={{0,6},{2,0},{4,2},{6,4},{1,7},{3,1},{5,3},{7,5},{8,14},{10,8},{12,... | collective-permute-start | bytes 1179656 | tf_op jit(solution)/shard_map/ppermute | solution.py:27
  68.1 12.6 %group.2 = (bf16[384,2176]{1,0:T(8,128)(2,1)S(1)}, bf16[384,2176]{1,0:T(8,128)(2,1)S(1)}, bf16[384,384]{1,0:T(8,128)(2,1)S(1)}, bf16[384,384]{1,0:T(8,128)(2,1)S(1)}, bf16[384,384]{1,0:T(8,128)(2,1)S(1)}) custom-call(s32[3]{0:T(128)S(1)} %pad_add_fusion.place_ref, bf16[48,4096]{1,0:T(8,128)(2,1)S(1)} %convolution_convert_fusion.1.refs_0_, ...), custom_call_target="tpu_custom_call" | custom-call | flops 5410652160 | bytes 16777216 | tf_op jit(solution)/shard_map/group/pallas_call | solution.py:143
  80.7 1.1 collective-permute-done.16.refs_5_.refs_13_
  81.8 2.6 %collective-permute-start.29 = (bf16[32,4096]{1,0:T(8,128)(2,1)S(1)}, bf16[32,4096]{1,0:T(8,128)(2,1)S(1)}, u32[]{:S(2)}, u32[]{:S(2)}) collective-permute-start(bf16[32,4096]{1,0:T(8,128)(2,1)S(1)} %slice.108), channel_id=1, source_target_pairs={{0,2},{2,4},{4,6},{6,0},{1,3},{3,5},{5,7},{7,1},{8,10},{10,12},{12... | collective-permute-start | bytes 786440 | tf_op jit(solution)/shard_map/ppermute | solution.py:27
  84.8 1.7 %collective-permute-start.31 = (bf16[32,4096]{1,0:T(8,128)(2,1)S(1)}, bf16[32,4096]{1,0:T(8,128)(2,1)S(1)}, u32[]{:S(2)}, u32[]{:S(2)}) collective-permute-start(bf16[32,4096]{1,0:T(8,128)(2,1)S(1)} %slice.111), channel_id=1, source_target_pairs={{0,8},{8,0},{1,9},{9,1},{2,10},{10,2},{3,11},{11,3},{4,12},{12,4},... | collective-permute-start | bytes 786440 | tf_op jit(solution)/shard_map/ppermute | solution.py:31
  86.7 2.5 %collective-permute-done.29.refs_6_.refs_14_ = bf16[32,4096]{1,0:T(8,128)(2,1)S(1)} collective-permute-done((bf16[32,4096]{1,0:T(8,128)(2,1)S(1)}, bf16[32,4096]{1,0:T(8,128)(2,1)S(1)}, u32[]{:S(2)}, u32[]{:S(2)}) %collective-permute-start.29) | collective-permute-done | bytes 262176 | tf_op jit(solution)/shard_map/ppermute | solution.py:27
  89.2 2.9 %collective-permute-done.30.refs_7_.refs_15_ = bf16[32,4096]{1,0:T(8,128)(2,1)S(1)} collective-permute-done((bf16[32,4096]{1,0:T(8,128)(2,1)S(1)}, bf16[32,4096]{1,0:T(8,128)(2,1)S(1)}, u32[]{:S(2)}, u32[]{:S(2)}) %collective-permute-start.30) | collective-permute-done | bytes 262176 | tf_op jit(solution)/shard_map/ppermute | solution.py:27
  92.1 1.4 collective-permute-done.31.refs_8_.refs_16_
  93.6 0.5 collective-permute-start.37
  94.2 0.4 collective-permute-start.39
  94.9 0.4 collective-permute-done.36.refs_13_.refs_29_
  95.3 0.6 collective-permute-done.37.refs_14_.refs_30_
  97.0 12.4 %group.3 = (bf16[384,2176]{1,0:T(8,128)(2,1)S(1)}, bf16[384,2176]{1,0:T(8,128)(2,1)S(1)}, bf16[384,384]{1,0:T(8,128)(2,1)S(1)}, bf16[384,384]{1,0:T(8,128)(2,1)S(1)}, bf16[384,384]{1,0:T(8,128)(2,1)S(1)}) custom-call(s32[3]{0:T(128)S(1)} %pad_add_fusion.place_ref, bf16[48,4096]{1,0:T(8,128)(2,1)S(1)} %collective-permute-done.4.refs_0_.refs_8_, ...), custom_call_target="tpu_custom_call" | custom-call | flops 5410652160 | bytes 16777216 | tf_op jit(solution)/shard_map/group/pallas_call | solution.py:143
  110.0 3.0 %collective-permute-done.41 = bf16[384,2176]{1,0:T(8,128)(2,1)S(1)} collective-permute-done((bf16[384,2176]{1,0:T(8,128)(2,1)S(1)}, bf16[384,2176]{1,0:T(8,128)(2,1)S(1)}, u32[]{:S(2)}, u32[]{:S(2)}) %collective-permute-start.41) | collective-permute-done | bytes 1671200 | tf_op jit(solution)/shard_map/ppermute | solution.py:35
  113.1 1.7 %collective-permute-start.46 = (bf16[32,2176]{1,0:T(8,128)(2,1)S(1)}, bf16[32,2176]{1,0:T(8,128)(2,1)S(1)}, u32[]{:S(2)}, u32[]{:S(2)}) collective-permute-start(bf16[32,2176]{1,0:T(8,128)(2,1)S(1)} %get-tuple-element.104), channel_id=1, source_target_pairs={{0,8},{8,0},{1,9},{9,1},{2,10},{10,2},{3,11},{11,3},{4,12},{12,4},... | collective-permute-start | bytes 417800 | tf_op jit(solution)/shard_map/ppermute | solution.py:31
  114.9 3.0 %collective-permute-start.44 = (bf16[32,2176]{1,0:T(8,128)(2,1)S(1)}, bf16[32,2176]{1,0:T(8,128)(2,1)S(1)}, u32[]{:S(2)}, u32[]{:S(2)}) collective-permute-start(bf16[32,2176]{1,0:T(8,128)(2,1)S(1)} %get-tuple-element.105), channel_id=1, source_target_pairs={{0,2},{2,4},{4,6},{6,0},{1,3},{3,5},{5,7},{7,1},{8,10},{10,12},{12... | collective-permute-start | bytes 417800 | tf_op jit(solution)/shard_map/ppermute | solution.py:27
  117.8 0.5 collective-permute-start.42
  118.4 0.6 collective-permute-done.46
  118.9 3.1 %collective-permute-done.44 = bf16[32,2176]{1,0:T(8,128)(2,1)S(1)} collective-permute-done((bf16[32,2176]{1,0:T(8,128)(2,1)S(1)}, bf16[32,2176]{1,0:T(8,128)(2,1)S(1)}, u32[]{:S(2)}, u32[]{:S(2)}) %collective-permute-start.44) | collective-permute-done | bytes 139296 | tf_op jit(solution)/shard_map/ppermute | solution.py:27
  122.1 1.1 collective-permute-done.42
  123.2 0.4 add_convert_fusion.4
  123.6 1.9 %collective-permute-start.43 = (bf16[96,2176]{1,0:T(8,128)(2,1)S(1)}, bf16[96,2176]{1,0:T(8,128)(2,1)S(1)}, u32[]{:S(2)}, u32[]{:S(2)}) collective-permute-start(bf16[96,2176]{1,0:T(8,128)(2,1)S(1)} %get-tuple-element.103), channel_id=1, source_target_pairs={{0,6},{2,0},{4,2},{6,4},{1,7},{3,1},{5,3},{7,5},{8,14},{10,8},{12,... | collective-permute-start | bytes 1253384 | tf_op jit(solution)/shard_map/ppermute | solution.py:27
  126.0 10.0 %weight_grads.2 = (bf16[344,4096]{1,0:T(8,128)(2,1)}, bf16[344,4096]{1,0:T(8,128)(2,1)}) custom-call(s32[3]{0:T(128)S(1)} %pad_add_fusion.place_ref, bf16[48,4096]{1,0:T(8,128)(2,1)S(1)} %convolution_convert_fusion.1.refs_0_, bf16[48,4096]{1,0:T(8,128)(2,1)S(1)} %convolution_convert_fusion.refs_1_, bf16[48,4096]{1,0:T(8,128)(2,1)S(1)} %collective-permute-done.17.refs_2_, ...), custom_call_target="tpu_custom_call" | custom-call | flops 4328521728 | bytes 14680064 | tf_op jit(solution)/shard_map/weight_grads/pallas_call | solution.py:217
  136.0 0.7 collective-permute-done.47
  136.8 0.5 add_convert_fusion.1
  137.2 3.0 %collective-permute-start.28 = (bf16[96,2176]{1,0:T(8,128)(2,1)S(1)}, bf16[96,2176]{1,0:T(8,128)(2,1)S(1)}, u32[]{:S(2)}, u32[]{:S(2)}) collective-permute-start(bf16[96,2176]{1,0:T(8,128)(2,1)S(1)} %get-tuple-element.100), channel_id=1, source_target_pairs={{0,6},{2,0},{4,2},{6,4},{1,7},{3,1},{5,3},{7,5},{8,14},{10,8},{12,... | collective-permute-start | bytes 1253384 | tf_op jit(solution)/shard_map/ppermute | solution.py:27
  140.2 1.7 collective-permute-start.49
  141.9 7.0 %weight_grads.3 = bf16[344,4096]{1,0:T(8,128)(2,1)} custom-call(s32[3]{0:T(128)S(1)} %pad_add_fusion.place_ref, bf16[48,4096]{1,0:T(8,128)(2,1)S(1)} %convolution_convert_fusion.1.refs_0_, bf16[48,4096]{1,0:T(8,128)(2,1)S(1)} %convolution_convert_fusion.refs_1_, bf16[48,4096]{1,0:T(8,128)(2,1)S(1)} %collective-permute-done.17.refs_2_, ...), custom_call_target="tpu_custom_call" | custom-call | flops 2164260864 | bytes 14680064 | tf_op jit(solution)/shard_map/weight_grads/pallas_call | solution.py:217
  148.9 1.1 collective-permute-done.48
  151.0 0.4 collective-permute-start.50
  151.5 3.9 %collective-permute-start.51 = (bf16[16,2176]{1,0:T(8,128)(2,1)S(1)}, bf16[16,2176]{1,0:T(8,128)(2,1)S(1)}, u32[]{:S(2)}, u32[]{:S(2)}) collective-permute-start(bf16[16,2176]{1,0:T(8,128)(2,1)S(1)} %get-tuple-element.113), channel_id=1, source_target_pairs={{0,96},{8,104},{16,112},{24,120},{32,0},{40,8},{48,16},{56,24},{64... | collective-permute-start | bytes 208904 | tf_op jit(solution)/shard_map/ppermute | solution.py:44
  155.4 2.9 %collective-permute-start.52 = (bf16[16,2176]{1,0:T(8,128)(2,1)S(1)}, bf16[16,2176]{1,0:T(8,128)(2,1)S(1)}, u32[]{:S(2)}, u32[]{:S(2)}) collective-permute-start(bf16[16,2176]{1,0:T(8,128)(2,1)S(1)} %get-tuple-element.109), channel_id=1, source_target_pairs={{0,120},{8,112},{16,104},{24,96},{32,24},{40,16},{48,8},{56,0},{64... | collective-permute-start | bytes 208904 | tf_op jit(solution)/shard_map/ppermute | solution.py:44
  158.3 6.0 %collective-permute-start.54 = (bf16[16,2176]{1,0:T(8,128)(2,1)S(1)}, bf16[16,2176]{1,0:T(8,128)(2,1)S(1)}, u32[]{:S(2)}, u32[]{:S(2)}) collective-permute-start(bf16[16,2176]{1,0:T(8,128)(2,1)S(1)} %get-tuple-element.108), channel_id=1, source_target_pairs={{0,88},{8,80},{16,72},{24,64},{32,120},{40,112},{48,104},{56,96},{... | collective-permute-start | bytes 208904 | tf_op jit(solution)/shard_map/ppermute | solution.py:44
  164.3 0.6 collective-permute-start.56
  165.0 2.0 %collective-permute-done.54.refs_5_ = bf16[16,2176]{1,0:T(8,128)(2,1)S(1)} collective-permute-done((bf16[16,2176]{1,0:T(8,128)(2,1)S(1)}, bf16[16,2176]{1,0:T(8,128)(2,1)S(1)}, u32[]{:S(2)}, u32[]{:S(2)}) %collective-permute-start.54) | collective-permute-done | bytes 69664 | tf_op jit(solution)/shard_map/ppermute | solution.py:44
  166.9 2.9 %collective-permute-done.55.refs_6_ = bf16[16,2176]{1,0:T(8,128)(2,1)S(1)} collective-permute-done((bf16[16,2176]{1,0:T(8,128)(2,1)S(1)}, bf16[16,2176]{1,0:T(8,128)(2,1)S(1)}, u32[]{:S(2)}, u32[]{:S(2)}) %collective-permute-start.55) | collective-permute-done | bytes 69664 | tf_op jit(solution)/shard_map/ppermute | solution.py:44
  169.8 2.2 %collective-permute-done.56.refs_7_ = bf16[16,2176]{1,0:T(8,128)(2,1)S(1)} collective-permute-done((bf16[16,2176]{1,0:T(8,128)(2,1)S(1)}, bf16[16,2176]{1,0:T(8,128)(2,1)S(1)}, u32[]{:S(2)}, u32[]{:S(2)}) %collective-permute-start.56) | collective-permute-done | bytes 69664 | tf_op jit(solution)/shard_map/ppermute | solution.py:44
  172.0 0.9 combine.1
  172.9 0.6 copy.15
  (86 shorter events, 6.2 us)
Async XLA Ops:
  2.2 0.9 copy-start
  3.2 0.9 copy-start.1
  5.4 13.9 %collective-permute-start.2 = (bf16[16,4096]{1,0:T(8,128)(2,1)S(1)}, bf16[16,4096]{1,0:T(8,128)(2,1)S(1)}, u32[]{:S(2)}, u32[]{:S(2)}) collective-permute-start(bf16[16,4096]{1,0:T(8,128)(2,1)S(1)} %get-tuple-element.54), channel_id=1, source_target_pairs={{0,96},{8,104},{16,112},{24,120},{32,0},{40,8},{48,16},{56,24},{64... | collective-permute-start | bytes 393224 | tf_op jit(solution)/shard_map/ppermute | solution.py:44
  9.5 9.8 %collective-permute-start.1 = (bf16[16,4096]{1,0:T(8,128)(2,1)S(1)}, bf16[16,4096]{1,0:T(8,128)(2,1)S(1)}, u32[]{:S(2)}, u32[]{:S(2)}) collective-permute-start(bf16[16,4096]{1,0:T(8,128)(2,1)S(1)} %get-tuple-element.53), channel_id=1, source_target_pairs={{0,64},{8,72},{16,80},{24,88},{32,96},{40,104},{48,112},{56,120},{... | collective-permute-start | bytes 393224 | tf_op jit(solution)/shard_map/ppermute | solution.py:44
  9.5 14.2 %collective-permute-start = (bf16[16,4096]{1,0:T(8,128)(2,1)S(1)}, bf16[16,4096]{1,0:T(8,128)(2,1)S(1)}, u32[]{:S(2)}, u32[]{:S(2)}) collective-permute-start(bf16[16,4096]{1,0:T(8,128)(2,1)S(1)} %get-tuple-element.52), channel_id=1, source_target_pairs={{0,32},{8,40},{16,48},{24,56},{32,64},{40,72},{48,80},{56,88},{64,... | collective-permute-start | bytes 393224 | tf_op jit(solution)/shard_map/ppermute | solution.py:44
  10.8 13.5 %collective-permute-start.8 = (bf16[16,4096]{1,0:T(8,128)(2,1)S(1)}, bf16[16,4096]{1,0:T(8,128)(2,1)S(1)}, u32[]{:S(2)}, u32[]{:S(2)}) collective-permute-start(bf16[16,4096]{1,0:T(8,128)(2,1)S(1)} %get-tuple-element.58), channel_id=1, source_target_pairs={{0,120},{8,112},{16,104},{24,96},{32,24},{40,16},{48,8},{56,0},{64... | collective-permute-start | bytes 393224 | tf_op jit(solution)/shard_map/ppermute | solution.py:44
  15.2 9.0 %collective-permute-start.7 = (bf16[16,4096]{1,0:T(8,128)(2,1)S(1)}, bf16[16,4096]{1,0:T(8,128)(2,1)S(1)}, u32[]{:S(2)}, u32[]{:S(2)}) collective-permute-start(bf16[16,4096]{1,0:T(8,128)(2,1)S(1)} %get-tuple-element.57), channel_id=1, source_target_pairs={{0,88},{8,80},{16,72},{24,64},{32,120},{40,112},{48,104},{56,96},{... | collective-permute-start | bytes 393224 | tf_op jit(solution)/shard_map/ppermute | solution.py:44
  19.3 11.9 %collective-permute-start.6 = (bf16[16,4096]{1,0:T(8,128)(2,1)S(1)}, bf16[16,4096]{1,0:T(8,128)(2,1)S(1)}, u32[]{:S(2)}, u32[]{:S(2)}) collective-permute-start(bf16[16,4096]{1,0:T(8,128)(2,1)S(1)} %get-tuple-element.56), channel_id=1, source_target_pairs={{0,56},{8,48},{16,40},{24,32},{32,88},{40,80},{48,72},{56,64},{64,... | collective-permute-start | bytes 393224 | tf_op jit(solution)/shard_map/ppermute | solution.py:44
  19.4 11.8 %collective-permute-start.5 = (bf16[16,4096]{1,0:T(8,128)(2,1)S(1)}, bf16[16,4096]{1,0:T(8,128)(2,1)S(1)}, u32[]{:S(2)}, u32[]{:S(2)}) collective-permute-start(bf16[16,4096]{1,0:T(8,128)(2,1)S(1)} %get-tuple-element.55), channel_id=1, source_target_pairs={{0,24},{8,16},{16,8},{24,0},{32,56},{40,48},{48,40},{56,32},{64,88... | collective-permute-start | bytes 393224 | tf_op jit(solution)/shard_map/ppermute | solution.py:44
  23.8 44.3 %copy-start.2 = (bf16[1,4096,344]{1,2,0:T(8,128)(2,1)S(1)}, bf16[1,4096,344]{1,2,0:T(8,128)(2,1)}, u32[]{:S(2)}) copy-start(bf16[1,4096,344]{1,2,0:T(8,128)(2,1)} %param.11) | copy-start | bytes 8454148
  24.1 10.9 %collective-permute-start.3 = (bf16[48,4096]{1,0:T(8,128)(2,1)S(1)}, bf16[48,4096]{1,0:T(8,128)(2,1)S(1)}, u32[]{:S(2)}, u32[]{:S(2)}) collective-permute-start(bf16[48,4096]{1,0:T(8,128)(2,1)S(1)} %convolution_convert_fusion.1.refs_0_), channel_id=1, source_target_pairs={{0,8},{8,0},{1,9},{9,1},{2,10},{10,2},{3,11},{11,3},{4,12},{12,4},... | collective-permute-start | bytes 1179656 | tf_op jit(solution)/shard_map/ppermute | solution.py:31
  31.5 9.6 %collective-permute-start.9 = (bf16[48,4096]{1,0:T(8,128)(2,1)S(1)}, bf16[48,4096]{1,0:T(8,128)(2,1)S(1)}, u32[]{:S(2)}, u32[]{:S(2)}) collective-permute-start(bf16[48,4096]{1,0:T(8,128)(2,1)S(1)} %convolution_convert_fusion.refs_1_), channel_id=1, source_target_pairs={{0,8},{8,0},{1,9},{9,1},{2,10},{10,2},{3,11},{11,3},{4,12},{12,4},... | collective-permute-start | bytes 1179656 | tf_op jit(solution)/shard_map/ppermute | solution.py:31
  31.7 12.0 %collective-permute-start.11 = (bf16[48,4096]{1,0:T(8,128)(2,1)S(1)}, bf16[48,4096]{1,0:T(8,128)(2,1)S(1)}, u32[]{:S(2)}, u32[]{:S(2)}) collective-permute-start(bf16[48,4096]{1,0:T(8,128)(2,1)S(1)} %convolution_convert_fusion.1.refs_0_), channel_id=1, source_target_pairs={{0,6},{2,0},{4,2},{6,4},{1,7},{3,1},{5,3},{7,5},{8,14},{10,8},{12,... | collective-permute-start | bytes 1179656 | tf_op jit(solution)/shard_map/ppermute | solution.py:27
  32.3 16.8 %collective-permute-start.13 = (bf16[48,4096]{1,0:T(8,128)(2,1)S(1)}, bf16[48,4096]{1,0:T(8,128)(2,1)S(1)}, u32[]{:S(2)}, u32[]{:S(2)}) collective-permute-start(bf16[48,4096]{1,0:T(8,128)(2,1)S(1)} %convolution_convert_fusion.refs_1_), channel_id=1, source_target_pairs={{0,6},{2,0},{4,2},{6,4},{1,7},{3,1},{5,3},{7,5},{8,14},{10,8},{12,... | collective-permute-start | bytes 1179656 | tf_op jit(solution)/shard_map/ppermute | solution.py:27
  35.0 15.6 %collective-permute-start.17 = (bf16[48,4096]{1,0:T(8,128)(2,1)S(1)}, bf16[48,4096]{1,0:T(8,128)(2,1)S(1)}, u32[]{:S(2)}, u32[]{:S(2)}) collective-permute-start(bf16[48,4096]{1,0:T(8,128)(2,1)S(1)} %convolution_convert_fusion.1.refs_0_), channel_id=1, source_target_pairs={{0,2},{2,4},{4,6},{6,0},{1,3},{3,5},{5,7},{7,1},{8,10},{10,12},{12... | collective-permute-start | bytes 1179656 | tf_op jit(solution)/shard_map/ppermute | solution.py:27
  35.0 19.8 %collective-permute-start.18 = (bf16[48,4096]{1,0:T(8,128)(2,1)S(1)}, bf16[48,4096]{1,0:T(8,128)(2,1)S(1)}, u32[]{:S(2)}, u32[]{:S(2)}) collective-permute-start(bf16[48,4096]{1,0:T(8,128)(2,1)S(1)} %convolution_convert_fusion.refs_1_), channel_id=1, source_target_pairs={{0,2},{2,4},{4,6},{6,0},{1,3},{3,5},{5,7},{7,1},{8,10},{10,12},{12... | collective-permute-start | bytes 1179656 | tf_op jit(solution)/shard_map/ppermute | solution.py:27
  41.1 13.7 %collective-permute-start.19 = (bf16[48,4096]{1,0:T(8,128)(2,1)S(1)}, bf16[48,4096]{1,0:T(8,128)(2,1)S(1)}, u32[]{:S(2)}, u32[]{:S(2)}) collective-permute-start(bf16[48,4096]{1,0:T(8,128)(2,1)S(1)} %convolution_convert_fusion.1.refs_0_), channel_id=1, source_target_pairs={{0,1},{1,0},{2,3},{3,2},{4,5},{5,4},{6,7},{7,6},{8,9},{9,8},{10,11... | collective-permute-start | bytes 1179656 | tf_op jit(solution)/shard_map/ppermute | solution.py:35
  43.7 11.7 %collective-permute-start.20 = (bf16[48,4096]{1,0:T(8,128)(2,1)S(1)}, bf16[48,4096]{1,0:T(8,128)(2,1)S(1)}, u32[]{:S(2)}, u32[]{:S(2)}) collective-permute-start(bf16[48,4096]{1,0:T(8,128)(2,1)S(1)} %convolution_convert_fusion.refs_1_), channel_id=1, source_target_pairs={{0,1},{1,0},{2,3},{3,2},{4,5},{5,4},{6,7},{7,6},{8,9},{9,8},{10,11... | collective-permute-start | bytes 1179656 | tf_op jit(solution)/shard_map/ppermute | solution.py:35
  49.1 11.1 %collective-permute-start.4 = (bf16[48,4096]{1,0:T(8,128)(2,1)S(1)}, bf16[48,4096]{1,0:T(8,128)(2,1)S(1)}, u32[]{:S(2)}, u32[]{:S(2)}) collective-permute-start(bf16[48,4096]{1,0:T(8,128)(2,1)S(1)} %collective-permute-done.3.refs_6_), channel_id=1, source_target_pairs={{0,2},{2,4},{4,6},{6,0},{1,3},{3,5},{5,7},{7,1},{8,10},{10,12},{12... | collective-permute-start | bytes 1179656 | tf_op jit(solution)/shard_map/ppermute | solution.py:27
  50.6 9.6 %collective-permute-start.21 = (bf16[48,4096]{1,0:T(8,128)(2,1)S(1)}, bf16[48,4096]{1,0:T(8,128)(2,1)S(1)}, u32[]{:S(2)}, u32[]{:S(2)}) collective-permute-start(bf16[48,4096]{1,0:T(8,128)(2,1)S(1)} %collective-permute-done.17.refs_2_), channel_id=1, source_target_pairs={{0,1},{1,0},{2,3},{3,2},{4,5},{5,4},{6,7},{7,6},{8,9},{9,8},{10,11... | collective-permute-start | bytes 1179656 | tf_op jit(solution)/shard_map/ppermute | solution.py:35
  54.9 5.9 %collective-permute-start.22 = (bf16[48,4096]{1,0:T(8,128)(2,1)S(1)}, bf16[48,4096]{1,0:T(8,128)(2,1)S(1)}, u32[]{:S(2)}, u32[]{:S(2)}) collective-permute-start(bf16[48,4096]{1,0:T(8,128)(2,1)S(1)} %collective-permute-done.18.refs_3_), channel_id=1, source_target_pairs={{0,1},{1,0},{2,3},{3,2},{4,5},{5,4},{6,7},{7,6},{8,9},{9,8},{10,11... | collective-permute-start | bytes 1179656 | tf_op jit(solution)/shard_map/ppermute | solution.py:35
  54.9 6.1 %collective-permute-start.23 = (bf16[48,4096]{1,0:T(8,128)(2,1)S(1)}, bf16[48,4096]{1,0:T(8,128)(2,1)S(1)}, u32[]{:S(2)}, u32[]{:S(2)}) collective-permute-start(bf16[48,4096]{1,0:T(8,128)(2,1)S(1)} %collective-permute-done.11.refs_4_), channel_id=1, source_target_pairs={{0,1},{1,0},{2,3},{3,2},{4,5},{5,4},{6,7},{7,6},{8,9},{9,8},{10,11... | collective-permute-start | bytes 1179656 | tf_op jit(solution)/shard_map/ppermute | solution.py:35
  55.4 7.3 %collective-permute-start.24 = (bf16[48,4096]{1,0:T(8,128)(2,1)S(1)}, bf16[48,4096]{1,0:T(8,128)(2,1)S(1)}, u32[]{:S(2)}, u32[]{:S(2)}) collective-permute-start(bf16[48,4096]{1,0:T(8,128)(2,1)S(1)} %collective-permute-done.13.refs_5_), channel_id=1, source_target_pairs={{0,1},{1,0},{2,3},{3,2},{4,5},{5,4},{6,7},{7,6},{8,9},{9,8},{10,11... | collective-permute-start | bytes 1179656 | tf_op jit(solution)/shard_map/ppermute | solution.py:35
  60.2 2.8 %collective-permute-start.25 = (bf16[48,4096]{1,0:T(8,128)(2,1)S(1)}, bf16[48,4096]{1,0:T(8,128)(2,1)S(1)}, u32[]{:S(2)}, u32[]{:S(2)}) collective-permute-start(bf16[48,4096]{1,0:T(8,128)(2,1)S(1)} %collective-permute-done.3.refs_6_), channel_id=1, source_target_pairs={{0,1},{1,0},{2,3},{3,2},{4,5},{5,4},{6,7},{7,6},{8,9},{9,8},{10,11... | collective-permute-start | bytes 1179656 | tf_op jit(solution)/shard_map/ppermute | solution.py:35
  60.2 4.7 %collective-permute-start.26 = (bf16[48,4096]{1,0:T(8,128)(2,1)S(1)}, bf16[48,4096]{1,0:T(8,128)(2,1)S(1)}, u32[]{:S(2)}, u32[]{:S(2)}) collective-permute-start(bf16[48,4096]{1,0:T(8,128)(2,1)S(1)} %collective-permute-done.9.refs_7_), channel_id=1, source_target_pairs={{0,1},{1,0},{2,3},{3,2},{4,5},{5,4},{6,7},{7,6},{8,9},{9,8},{10,11... | collective-permute-start | bytes 1179656 | tf_op jit(solution)/shard_map/ppermute | solution.py:35
  60.7 20.0 %collective-permute-start.10 = (bf16[48,4096]{1,0:T(8,128)(2,1)S(1)}, bf16[48,4096]{1,0:T(8,128)(2,1)S(1)}, u32[]{:S(2)}, u32[]{:S(2)}) collective-permute-start(bf16[48,4096]{1,0:T(8,128)(2,1)S(1)} %collective-permute-done.9.refs_7_), channel_id=1, source_target_pairs={{0,2},{2,4},{4,6},{6,0},{1,3},{3,5},{5,7},{7,1},{8,10},{10,12},{12... | collective-permute-start | bytes 1179656 | tf_op jit(solution)/shard_map/ppermute | solution.py:27
  61.0 19.7 %collective-permute-start.12 = (bf16[48,4096]{1,0:T(8,128)(2,1)S(1)}, bf16[48,4096]{1,0:T(8,128)(2,1)S(1)}, u32[]{:S(2)}, u32[]{:S(2)}) collective-permute-start(bf16[48,4096]{1,0:T(8,128)(2,1)S(1)} %collective-permute-done.11.refs_4_), channel_id=1, source_target_pairs={{0,8},{8,0},{1,9},{9,1},{2,10},{10,2},{3,11},{11,3},{4,12},{12,4},... | collective-permute-start | bytes 1179656 | tf_op jit(solution)/shard_map/ppermute | solution.py:31
  62.7 18.1 %collective-permute-start.14 = (bf16[48,4096]{1,0:T(8,128)(2,1)S(1)}, bf16[48,4096]{1,0:T(8,128)(2,1)S(1)}, u32[]{:S(2)}, u32[]{:S(2)}) collective-permute-start(bf16[48,4096]{1,0:T(8,128)(2,1)S(1)} %collective-permute-done.13.refs_5_), channel_id=1, source_target_pairs={{0,8},{8,0},{1,9},{9,1},{2,10},{10,2},{3,11},{11,3},{4,12},{12,4},... | collective-permute-start | bytes 1179656 | tf_op jit(solution)/shard_map/ppermute | solution.py:31
  63.0 17.7 %collective-permute-start.15 = (bf16[48,4096]{1,0:T(8,128)(2,1)S(1)}, bf16[48,4096]{1,0:T(8,128)(2,1)S(1)}, u32[]{:S(2)}, u32[]{:S(2)}) collective-permute-start(bf16[48,4096]{1,0:T(8,128)(2,1)S(1)} %collective-permute-done.11.refs_4_), channel_id=1, source_target_pairs={{0,6},{2,0},{4,2},{6,4},{1,7},{3,1},{5,3},{7,5},{8,14},{10,8},{12,... | collective-permute-start | bytes 1179656 | tf_op jit(solution)/shard_map/ppermute | solution.py:27
  64.9 16.9 %collective-permute-start.16 = (bf16[48,4096]{1,0:T(8,128)(2,1)S(1)}, bf16[48,4096]{1,0:T(8,128)(2,1)S(1)}, u32[]{:S(2)}, u32[]{:S(2)}) collective-permute-start(bf16[48,4096]{1,0:T(8,128)(2,1)S(1)} %collective-permute-done.13.refs_5_), channel_id=1, source_target_pairs={{0,6},{2,0},{4,2},{6,4},{1,7},{3,1},{5,3},{7,5},{8,14},{10,8},{12,... | collective-permute-start | bytes 1179656 | tf_op jit(solution)/shard_map/ppermute | solution.py:27
  68.1 28.9 %copy-start.3 = (bf16[1,4096,344]{1,2,0:T(8,128)(2,1)S(1)}, bf16[1,4096,344]{1,2,0:T(8,128)(2,1)}, u32[]{:S(2)}) copy-start(bf16[1,4096,344]{1,2,0:T(8,128)(2,1)} %param.11) | copy-start | bytes 8454148
  80.7 4.1 %copy-start.4 = (bf16[384,2176]{1,0:T(8,128)(2,1)}, bf16[384,2176]{1,0:T(8,128)(2,1)S(1)}, u32[]{:S(2)}) copy-start(bf16[384,2176]{1,0:T(8,128)(2,1)S(1)} %get-tuple-element.65) | copy-start | bytes 5013508
  81.8 7.4 %collective-permute-start.29 = (bf16[32,4096]{1,0:T(8,128)(2,1)S(1)}, bf16[32,4096]{1,0:T(8,128)(2,1)S(1)}, u32[]{:S(2)}, u32[]{:S(2)}) collective-permute-start(bf16[32,4096]{1,0:T(8,128)(2,1)S(1)} %slice.108), channel_id=1, source_target_pairs={{0,2},{2,4},{4,6},{6,0},{1,3},{3,5},{5,7},{7,1},{8,10},{10,12},{12... | collective-permute-start | bytes 786440 | tf_op jit(solution)/shard_map/ppermute | solution.py:27
  84.6 7.6 %collective-permute-start.30 = (bf16[32,4096]{1,0:T(8,128)(2,1)S(1)}, bf16[32,4096]{1,0:T(8,128)(2,1)S(1)}, u32[]{:S(2)}, u32[]{:S(2)}) collective-permute-start(bf16[32,4096]{1,0:T(8,128)(2,1)S(1)} %pad_maximum_fusion), channel_id=1, source_target_pairs={{0,6},{2,0},{4,2},{6,4},{1,7},{3,1},{5,3},{7,5},{8,14},{10,8},{12,... | collective-permute-start | bytes 786440 | tf_op jit(solution)/shard_map/ppermute | solution.py:27
  84.6 8.9 %collective-permute-start.32 = (bf16[48,4096]{1,0:T(8,128)(2,1)S(1)}, bf16[48,4096]{1,0:T(8,128)(2,1)S(1)}, u32[]{:S(2)}, u32[]{:S(2)}) collective-permute-start(bf16[48,4096]{1,0:T(8,128)(2,1)S(1)} %collective-permute-done.4.refs_0_.refs_8_), channel_id=1, source_target_pairs={{0,1},{1,0},{2,3},{3,2},{4,5},{5,4},{6,7},{7,6},{8,9},{9,8},{10,11... | collective-permute-start | bytes 1179656 | tf_op jit(solution)/shard_map/ppermute | solution.py:35
  84.8 8.8 %collective-permute-start.31 = (bf16[32,4096]{1,0:T(8,128)(2,1)S(1)}, bf16[32,4096]{1,0:T(8,128)(2,1)S(1)}, u32[]{:S(2)}, u32[]{:S(2)}) collective-permute-start(bf16[32,4096]{1,0:T(8,128)(2,1)S(1)} %slice.111), channel_id=1, source_target_pairs={{0,8},{8,0},{1,9},{9,1},{2,10},{10,2},{3,11},{11,3},{4,12},{12,4},... | collective-permute-start | bytes 786440 | tf_op jit(solution)/shard_map/ppermute | solution.py:31
  86.5 7.6 %collective-permute-start.33 = (bf16[48,4096]{1,0:T(8,128)(2,1)S(1)}, bf16[48,4096]{1,0:T(8,128)(2,1)S(1)}, u32[]{:S(2)}, u32[]{:S(2)}) collective-permute-start(bf16[48,4096]{1,0:T(8,128)(2,1)S(1)} %collective-permute-done.10.refs_1_.refs_9_), channel_id=1, source_target_pairs={{0,1},{1,0},{2,3},{3,2},{4,5},{5,4},{6,7},{7,6},{8,9},{9,8},{10,11... | collective-permute-start | bytes 1179656 | tf_op jit(solution)/shard_map/ppermute | solution.py:35
  89.2 4.9 %collective-permute-start.34 = (bf16[48,4096]{1,0:T(8,128)(2,1)S(1)}, bf16[48,4096]{1,0:T(8,128)(2,1)S(1)}, u32[]{:S(2)}, u32[]{:S(2)}) collective-permute-start(bf16[48,4096]{1,0:T(8,128)(2,1)S(1)} %collective-permute-done.12.refs_2_.refs_10_), channel_id=1, source_target_pairs={{0,1},{1,0},{2,3},{3,2},{4,5},{5,4},{6,7},{7,6},{8,9},{9,8},{10,11... | collective-permute-start | bytes 1179656 | tf_op jit(solution)/shard_map/ppermute | solution.py:35
  92.1 2.4 %collective-permute-start.35 = (bf16[48,4096]{1,0:T(8,128)(2,1)S(1)}, bf16[48,4096]{1,0:T(8,128)(2,1)S(1)}, u32[]{:S(2)}, u32[]{:S(2)}) collective-permute-start(bf16[48,4096]{1,0:T(8,128)(2,1)S(1)} %collective-permute-done.14.refs_3_.refs_11_), channel_id=1, source_target_pairs={{0,1},{1,0},{2,3},{3,2},{4,5},{5,4},{6,7},{7,6},{8,9},{9,8},{10,11... | collective-permute-start | bytes 1179656 | tf_op jit(solution)/shard_map/ppermute | solution.py:35
  93.5 1.7 collective-permute-start.36
  93.6 2.3 %collective-permute-start.37 = (bf16[48,4096]{1,0:T(8,128)(2,1)S(1)}, bf16[48,4096]{1,0:T(8,128)(2,1)S(1)}, u32[]{:S(2)}, u32[]{:S(2)}) collective-permute-start(bf16[48,4096]{1,0:T(8,128)(2,1)S(1)} %collective-permute-done.16.refs_5_.refs_13_), channel_id=1, source_target_pairs={{0,1},{1,0},{2,3},{3,2},{4,5},{5,4},{6,7},{7,6},{8,9},{9,8},{10,11... | collective-permute-start | bytes 1179656 | tf_op jit(solution)/shard_map/ppermute | solution.py:35
  94.1 2.1 %collective-permute-start.38 = (bf16[32,4096]{1,0:T(8,128)(2,1)S(1)}, bf16[32,4096]{1,0:T(8,128)(2,1)S(1)}, u32[]{:S(2)}, u32[]{:S(2)}) collective-permute-start(bf16[32,4096]{1,0:T(8,128)(2,1)S(1)} %collective-permute-done.29.refs_6_.refs_14_), channel_id=1, source_target_pairs={{0,1},{1,0},{2,3},{3,2},{4,5},{5,4},{6,7},{7,6},{8,9},{9,8},{10,11... | collective-permute-start | bytes 786440 | tf_op jit(solution)/shard_map/ppermute | solution.py:35
  94.2 2.4 %collective-permute-start.39 = (bf16[32,4096]{1,0:T(8,128)(2,1)S(1)}, bf16[32,4096]{1,0:T(8,128)(2,1)S(1)}, u32[]{:S(2)}, u32[]{:S(2)}) collective-permute-start(bf16[32,4096]{1,0:T(8,128)(2,1)S(1)} %collective-permute-done.30.refs_7_.refs_15_), channel_id=1, source_target_pairs={{0,1},{1,0},{2,3},{3,2},{4,5},{5,4},{6,7},{7,6},{8,9},{9,8},{10,11... | collective-permute-start | bytes 786440 | tf_op jit(solution)/shard_map/ppermute | solution.py:35
  94.6 2.4 %collective-permute-start.40 = (bf16[32,4096]{1,0:T(8,128)(2,1)S(1)}, bf16[32,4096]{1,0:T(8,128)(2,1)S(1)}, u32[]{:S(2)}, u32[]{:S(2)}) collective-permute-start(bf16[32,4096]{1,0:T(8,128)(2,1)S(1)} %collective-permute-done.31.refs_8_.refs_16_), channel_id=1, source_target_pairs={{0,1},{1,0},{2,3},{3,2},{4,5},{5,4},{6,7},{7,6},{8,9},{9,8},{10,11... | collective-permute-start | bytes 786440 | tf_op jit(solution)/shard_map/ppermute | solution.py:35
  109.4 3.6 %collective-permute-start.41 = (bf16[384,2176]{1,0:T(8,128)(2,1)S(1)}, bf16[384,2176]{1,0:T(8,128)(2,1)S(1)}, u32[]{:S(2)}, u32[]{:S(2)}) collective-permute-start(bf16[384,2176]{1,0:T(8,128)(2,1)S(1)} %get-tuple-element.73), channel_id=1, source_target_pairs={{0,1},{1,0},{2,3},{3,2},{4,5},{5,4},{6,7},{7,6},{8,9},{9,8},{10,11... | collective-permute-start | bytes 5013512 | tf_op jit(solution)/shard_map/ppermute | solution.py:35
  109.6 27.1 %collective-permute-start.27 = (bf16[384,2176]{1,0:T(8,128)(2,1)}, bf16[384,2176]{1,0:T(8,128)(2,1)S(1)}, u32[]{:S(2)}, u32[]{:S(2)}) collective-permute-start(bf16[384,2176]{1,0:T(8,128)(2,1)} %copy-done.4), channel_id=1, source_target_pairs={{0,1},{1,0},{2,3},{3,2},{4,5},{5,4},{6,7},{7,6},{8,9},{9,8},{10,11... | collective-permute-start | bytes 5013512 | tf_op jit(solution)/shard_map/ppermute | solution.py:35
  113.1 5.8 %collective-permute-start.46 = (bf16[32,2176]{1,0:T(8,128)(2,1)S(1)}, bf16[32,2176]{1,0:T(8,128)(2,1)S(1)}, u32[]{:S(2)}, u32[]{:S(2)}) collective-permute-start(bf16[32,2176]{1,0:T(8,128)(2,1)S(1)} %get-tuple-element.104), channel_id=1, source_target_pairs={{0,8},{8,0},{1,9},{9,1},{2,10},{10,2},{3,11},{11,3},{4,12},{12,4},... | collective-permute-start | bytes 417800 | tf_op jit(solution)/shard_map/ppermute | solution.py:31
  114.9 7.2 %collective-permute-start.44 = (bf16[32,2176]{1,0:T(8,128)(2,1)S(1)}, bf16[32,2176]{1,0:T(8,128)(2,1)S(1)}, u32[]{:S(2)}, u32[]{:S(2)}) collective-permute-start(bf16[32,2176]{1,0:T(8,128)(2,1)S(1)} %get-tuple-element.105), channel_id=1, source_target_pairs={{0,2},{2,4},{4,6},{6,0},{1,3},{3,5},{5,7},{7,1},{8,10},{10,12},{12... | collective-permute-start | bytes 417800 | tf_op jit(solution)/shard_map/ppermute | solution.py:27
  117.8 5.3 %collective-permute-start.42 = (bf16[32,2176]{1,0:T(8,128)(2,1)S(1)}, bf16[32,2176]{1,0:T(8,128)(2,1)S(1)}, u32[]{:S(2)}, u32[]{:S(2)}) collective-permute-start(bf16[32,2176]{1,0:T(8,128)(2,1)S(1)} %get-tuple-element.106), channel_id=1, source_target_pairs={{0,6},{2,0},{4,2},{6,4},{1,7},{3,1},{5,3},{7,5},{8,14},{10,8},{12,... | collective-permute-start | bytes 417800 | tf_op jit(solution)/shard_map/ppermute | solution.py:27
  123.6 12.5 %collective-permute-start.43 = (bf16[96,2176]{1,0:T(8,128)(2,1)S(1)}, bf16[96,2176]{1,0:T(8,128)(2,1)S(1)}, u32[]{:S(2)}, u32[]{:S(2)}) collective-permute-start(bf16[96,2176]{1,0:T(8,128)(2,1)S(1)} %get-tuple-element.103), channel_id=1, source_target_pairs={{0,6},{2,0},{4,2},{6,4},{1,7},{3,1},{5,3},{7,5},{8,14},{10,8},{12,... | collective-permute-start | bytes 1253384 | tf_op jit(solution)/shard_map/ppermute | solution.py:27
  125.5 10.6 %collective-permute-start.45 = (bf16[96,2176]{1,0:T(8,128)(2,1)S(1)}, bf16[96,2176]{1,0:T(8,128)(2,1)S(1)}, u32[]{:S(2)}, u32[]{:S(2)}) collective-permute-start(bf16[96,2176]{1,0:T(8,128)(2,1)S(1)} %get-tuple-element.102), channel_id=1, source_target_pairs={{0,8},{8,0},{1,9},{9,1},{2,10},{10,2},{3,11},{11,3},{4,12},{12,4},... | collective-permute-start | bytes 1253384 | tf_op jit(solution)/shard_map/ppermute | solution.py:31
  125.8 10.9 %collective-permute-start.47 = (bf16[96,2176]{1,0:T(8,128)(2,1)S(1)}, bf16[96,2176]{1,0:T(8,128)(2,1)S(1)}, u32[]{:S(2)}, u32[]{:S(2)}) collective-permute-start(bf16[96,2176]{1,0:T(8,128)(2,1)S(1)} %get-tuple-element.101), channel_id=1, source_target_pairs={{0,2},{2,4},{4,6},{6,0},{1,3},{3,5},{5,7},{7,1},{8,10},{10,12},{12... | collective-permute-start | bytes 1253384 | tf_op jit(solution)/shard_map/ppermute | solution.py:27
  137.2 11.7 %collective-permute-start.28 = (bf16[96,2176]{1,0:T(8,128)(2,1)S(1)}, bf16[96,2176]{1,0:T(8,128)(2,1)S(1)}, u32[]{:S(2)}, u32[]{:S(2)}) collective-permute-start(bf16[96,2176]{1,0:T(8,128)(2,1)S(1)} %get-tuple-element.100), channel_id=1, source_target_pairs={{0,6},{2,0},{4,2},{6,4},{1,7},{3,1},{5,3},{7,5},{8,14},{10,8},{12,... | collective-permute-start | bytes 1253384 | tf_op jit(solution)/shard_map/ppermute | solution.py:27
  140.2 9.8 %collective-permute-start.48 = (bf16[96,2176]{1,0:T(8,128)(2,1)S(1)}, bf16[96,2176]{1,0:T(8,128)(2,1)S(1)}, u32[]{:S(2)}, u32[]{:S(2)}) collective-permute-start(bf16[96,2176]{1,0:T(8,128)(2,1)S(1)} %get-tuple-element.99), channel_id=1, source_target_pairs={{0,2},{2,4},{4,6},{6,0},{1,3},{3,5},{5,7},{7,1},{8,10},{10,12},{12... | collective-permute-start | bytes 1253384 | tf_op jit(solution)/shard_map/ppermute | solution.py:27
  140.2 9.8 %collective-permute-start.49 = (bf16[96,2176]{1,0:T(8,128)(2,1)S(1)}, bf16[96,2176]{1,0:T(8,128)(2,1)S(1)}, u32[]{:S(2)}, u32[]{:S(2)}) collective-permute-start(bf16[96,2176]{1,0:T(8,128)(2,1)S(1)} %get-tuple-element.98), channel_id=1, source_target_pairs={{0,8},{8,0},{1,9},{9,1},{2,10},{10,2},{3,11},{11,3},{4,12},{12,4},... | collective-permute-start | bytes 1253384 | tf_op jit(solution)/shard_map/ppermute | solution.py:31
  151.0 13.3 %collective-permute-start.50 = (bf16[16,2176]{1,0:T(8,128)(2,1)S(1)}, bf16[16,2176]{1,0:T(8,128)(2,1)S(1)}, u32[]{:S(2)}, u32[]{:S(2)}) collective-permute-start(bf16[16,2176]{1,0:T(8,128)(2,1)S(1)} %get-tuple-element.110), channel_id=1, source_target_pairs={{0,24},{8,16},{16,8},{24,0},{32,56},{40,48},{48,40},{56,32},{64,88... | collective-permute-start | bytes 208904 | tf_op jit(solution)/shard_map/ppermute | solution.py:44
  151.5 12.9 %collective-permute-start.51 = (bf16[16,2176]{1,0:T(8,128)(2,1)S(1)}, bf16[16,2176]{1,0:T(8,128)(2,1)S(1)}, u32[]{:S(2)}, u32[]{:S(2)}) collective-permute-start(bf16[16,2176]{1,0:T(8,128)(2,1)S(1)} %get-tuple-element.113), channel_id=1, source_target_pairs={{0,96},{8,104},{16,112},{24,120},{32,0},{40,8},{48,16},{56,24},{64... | collective-permute-start | bytes 208904 | tf_op jit(solution)/shard_map/ppermute | solution.py:44
  155.4 9.6 %collective-permute-start.52 = (bf16[16,2176]{1,0:T(8,128)(2,1)S(1)}, bf16[16,2176]{1,0:T(8,128)(2,1)S(1)}, u32[]{:S(2)}, u32[]{:S(2)}) collective-permute-start(bf16[16,2176]{1,0:T(8,128)(2,1)S(1)} %get-tuple-element.109), channel_id=1, source_target_pairs={{0,120},{8,112},{16,104},{24,96},{32,24},{40,16},{48,8},{56,0},{64... | collective-permute-start | bytes 208904 | tf_op jit(solution)/shard_map/ppermute | solution.py:44
  158.3 6.7 %collective-permute-start.53 = (bf16[16,2176]{1,0:T(8,128)(2,1)S(1)}, bf16[16,2176]{1,0:T(8,128)(2,1)S(1)}, u32[]{:S(2)}, u32[]{:S(2)}) collective-permute-start(bf16[16,2176]{1,0:T(8,128)(2,1)S(1)} %get-tuple-element.112), channel_id=1, source_target_pairs={{0,64},{8,72},{16,80},{24,88},{32,96},{40,104},{48,112},{56,120},{... | collective-permute-start | bytes 208904 | tf_op jit(solution)/shard_map/ppermute | solution.py:44
  158.3 8.6 %collective-permute-start.54 = (bf16[16,2176]{1,0:T(8,128)(2,1)S(1)}, bf16[16,2176]{1,0:T(8,128)(2,1)S(1)}, u32[]{:S(2)}, u32[]{:S(2)}) collective-permute-start(bf16[16,2176]{1,0:T(8,128)(2,1)S(1)} %get-tuple-element.108), channel_id=1, source_target_pairs={{0,88},{8,80},{16,72},{24,64},{32,120},{40,112},{48,104},{56,96},{... | collective-permute-start | bytes 208904 | tf_op jit(solution)/shard_map/ppermute | solution.py:44
  164.3 5.5 %collective-permute-start.55 = (bf16[16,2176]{1,0:T(8,128)(2,1)S(1)}, bf16[16,2176]{1,0:T(8,128)(2,1)S(1)}, u32[]{:S(2)}, u32[]{:S(2)}) collective-permute-start(bf16[16,2176]{1,0:T(8,128)(2,1)S(1)} %get-tuple-element.111), channel_id=1, source_target_pairs={{0,32},{8,40},{16,48},{24,56},{32,64},{40,72},{48,80},{56,88},{64,... | collective-permute-start | bytes 208904 | tf_op jit(solution)/shard_map/ppermute | solution.py:44
  164.3 7.7 %collective-permute-start.56 = (bf16[16,2176]{1,0:T(8,128)(2,1)S(1)}, bf16[16,2176]{1,0:T(8,128)(2,1)S(1)}, u32[]{:S(2)}, u32[]{:S(2)}) collective-permute-start(bf16[16,2176]{1,0:T(8,128)(2,1)S(1)} %get-tuple-element.107), channel_id=1, source_target_pairs={{0,56},{8,48},{16,40},{24,32},{32,88},{40,80},{48,72},{56,64},{64,... | collective-permute-start | bytes 208904 | tf_op jit(solution)/shard_map/ppermute | solution.py:44

commit v2 on v1

--- a/solution.py
+++ b/solution.py
@@ -48,15 +48,25 @@
     return lax.dot_general(a, b, (((left,), (right,)), ((), ())), preferred_element_type=F32)
 
 
-def slots_kernel(half, place_ref, tok_ref, cot_ref, routes_ref, weights_ref, *outs):
+def slots_kernel(half, place_ref, tok_ref, cot_ref, routes_ref, weights_ref, *refs):
     core, z, yh = place_ref[0], place_ref[1], place_ref[2]
-    first_ref, second_ref = outs[EXPERTS:]
-    rows = tok_ref.shape[0]
+    outs = refs[:EXPERTS]
+    first_ref, second_ref, tok_half, cot_half, sems = refs[EXPERTS:]
+    here = pl.ds(pl.multiple_of(core * half, half), half)
+    loads = [
+        pltpu.make_async_copy(tok_ref.at[:, here], tok_half, sems.at[0]),
+        pltpu.make_async_copy(cot_ref.at[:, here], cot_half, sems.at[1]),
+    ]
+    for c in loads:
+        c.start()
+    rows = tok_half.shape[0]
+    routes = routes_ref[...].T
+    weights = weights_ref[...].T
     slot = lax.broadcasted_iota(jnp.int32, (rows, EXPERTS * ROOM), 1)
     index = slot // ROOM
     expert = 2 * ((z + index // 2) % 4) + (yh + index % 2) % 2
-    is_first = routes_ref[:, 0:1] == expert
-    is_second = routes_ref[:, 1:2] == expert
+    is_first = routes[:, 0:1] == expert
+    is_second = routes[:, 1:2] == expert
     hot = jnp.where(is_first | is_second, 1.0, 0.0).astype(BF)
     below = lax.broadcasted_iota(jnp.int32, (rows, rows), 1) < lax.broadcasted_iota(
         jnp.int32, (rows, rows), 0
@@ -67,11 +77,12 @@
     second = jnp.where(is_second & fits, 1.0, 0.0).astype(BF)
     first_ref[...] = first
     second_ref[...] = second
-    here = pl.ds(pl.multiple_of(core * half, half), half)
-    slot_tok = dot_f32(first + second, tok_ref[:, here], 0, 0).astype(BF)
-    cot = cot_ref[:, here].astype(F32)
-    scaled = dot_f32(first, (cot * weights_ref[:, 0:1]).astype(BF), 0, 0)
-    scaled = scaled + dot_f32(second, (cot * weights_ref[:, 1:2]).astype(BF), 0, 0)
+    for c in loads:
+        c.wait()
+    slot_tok = dot_f32(first + second, tok_half[...], 0, 0).astype(BF)
+    cot = cot_half[...].astype(F32)
+    scaled = dot_f32(first, (cot * weights[:, 0:1]).astype(BF), 0, 0)
+    scaled = scaled + dot_f32(second, (cot * weights[:, 1:2]).astype(BF), 0, 0)
     scaled = scaled.astype(BF)
     for k in range(EXPERTS):
         outs[k][:, :half] = slot_tok[k * ROOM : (k + 1) * ROOM]
@@ -82,17 +93,44 @@
     rows, width = tokens.shape
     shapes = [jax.ShapeDtypeStruct((ROOM, width), BF)] * EXPERTS
     shapes += [jax.ShapeDtypeStruct((rows, EXPERTS * ROOM), BF)] * 2
+    anywhere = pl.BlockSpec(memory_space=pl.ANY)
     return pl.pallas_call(
         functools.partial(slots_kernel, width // 2),
         out_shape=shapes,
-        in_specs=[SMEM] + [VMEM] * 4,
+        in_specs=[SMEM, anywhere, anywhere, VMEM, VMEM],
         out_specs=[VMEM] * len(shapes),
-        compiler_params=pltpu.CompilerParams(vmem_limit_bytes=8 * MIB),
+        scratch_shapes=[
+            pltpu.VMEM((rows, width // 2), BF),
+            pltpu.VMEM((rows, width // 2), BF),
+            pltpu.SemaphoreType.DMA((2,)),
+        ],
+        compiler_params=pltpu.CompilerParams(vmem_limit_bytes=60 * MIB),
         cost_estimate=pl.CostEstimate(
             flops=2 * 128 * 24 * width * 2, bytes_accessed=3 * MIB, transcendentals=0
         ),
         name="slots",
     )(place, tokens, cotangent, routes, weights)
+
+
+def stack_kernel(gate_ref, up_ref, out_ref):
+    hid = gate_ref.shape[0]
+    wide = out_ref.shape[0] // 2
+    for i, ref in enumerate((gate_ref, up_ref)):
+        out_ref[wide * i : wide * i + hid] = ref[...]
+        out_ref[wide * i + hid : wide * (i + 1)] = jnp.zeros((wide - hid, ref.shape[1]), BF)
+
+
+def stack_weights(gate, up):
+    hid, width = gate.shape
+    return pl.pallas_call(
+        stack_kernel,
+        out_shape=jax.ShapeDtypeStruct((2 * padded(hid), width), BF),
+        in_specs=[VMEM] * 2,
+        out_specs=VMEM,
+        compiler_params=pltpu.CompilerParams(vmem_limit_bytes=16 * MIB),
+        cost_estimate=pl.CostEstimate(flops=1000, bytes_accessed=12 * MIB, transcendentals=0),
+        name="stack",
+    )(gate, up)
 
 
 def padded(n):
@@ -102,24 +140,29 @@
 def group_kernel(count, half, place_ref, *refs):
     core = place_ref[0]
     ours, theirs = refs[:count], refs[count : 2 * count]
-    gate_ref, up_ref, down_ref = refs[2 * count : 2 * count + 3]
-    keep_ref, send_ref, gate_out, up_out, hidden_out = refs[2 * count + 3 :]
+    pair_ref, down_ref = refs[2 * count : 2 * count + 2]
+    keep_ref, send_ref, sides_out, hidden_out = refs[2 * count + 2 :]
+    hid = down_ref.shape[0]
+    wide = hidden_out.shape[1]
     here = pl.ds(pl.multiple_of(core * half, half), half)
     there = pl.ds(pl.multiple_of((1 - core) * half, half), half)
     tok = [jnp.concatenate([r[:, :half] for r in side], axis=0) for side in (ours, theirs)]
-    gate = dot_f32(tok[0], gate_ref[:, here], 1, 1) + dot_f32(tok[1], gate_ref[:, there], 1, 1)
-    up = dot_f32(tok[0], up_ref[:, here], 1, 1) + dot_f32(tok[1], up_ref[:, there], 1, 1)
+    pair = dot_f32(tok[0], pair_ref[:, here], 1, 1) + dot_f32(tok[1], pair_ref[:, there], 1, 1)
     cot = [jnp.concatenate([r[:, half:] for r in side], axis=0) for side in (ours, theirs)]
     grad = dot_f32(cot[0], down_ref[:, here], 1, 1) + dot_f32(cot[1], down_ref[:, there], 1, 1)
+    gate, up = pair[:, :hid], pair[:, wide : wide + hid]
     sigma = 1.0 / (1.0 + jnp.exp(-gate))
     active = gate * sigma
     hidden = (active * up).astype(BF)
     gate_side = (grad * up * (sigma * (1.0 + gate * (1.0 - sigma)))).astype(BF)
     up_side = (grad * active).astype(BF)
-    hid = hidden.shape[1]
-    for out, value in ((hidden_out, hidden), (gate_out, gate_side), (up_out, up_side)):
-        out[:, :hid] = value
-        out[:, hid:] = jnp.zeros((out.shape[0], out.shape[1] - hid), BF)
+    rest = jnp.zeros((hidden.shape[0], wide - hid), BF)
+    hidden_out[:, :hid] = hidden
+    hidden_out[:, hid:] = rest
+    sides_out[:, :hid] = gate_side
+    sides_out[:, hid:wide] = rest
+    sides_out[:, wide : wide + hid] = up_side
+    sides_out[:, wide + hid :] = rest
     share = jnp.sum(hidden.astype(F32) * grad, axis=1, keepdims=True).astype(BF)
     share = jnp.broadcast_to(share, (share.shape[0], LANES))
     tile = 512
@@ -129,37 +172,36 @@
         @pl.loop(0, half // tile)
         def _(j):
             where = pl.ds(pl.multiple_of(base + j * tile, tile), tile)
-            term = dot_f32(gate_out[:, :hid], gate_ref[:, where], 1, 0)
-            term = term + dot_f32(up_out[:, :hid], up_ref[:, where], 1, 0)
+            term = dot_f32(sides_out[...], pair_ref[:, where], 1, 0)
             out[:, pl.ds(pl.multiple_of(j * tile, tile), tile)] = term.astype(BF)
 
 
-def run_group(place, ours, theirs, gate, up, down):
+def run_group(place, ours, theirs, pair, down):
     rows = sum(r.shape[0] for r in ours)
-    hid, width = gate.shape
+    hid, width = down.shape
     half = width // 2
     shapes = [jax.ShapeDtypeStruct((rows, half + LANES), BF)] * 2
-    shapes += [jax.ShapeDtypeStruct((rows, padded(hid)), BF)] * 3
+    shapes += [jax.ShapeDtypeStruct((rows, n * padded(hid)), BF) for n in (2, 1)]
     return pl.pallas_call(
         functools.partial(group_kernel, len(ours), half),
         out_shape=shapes,
-        in_specs=[SMEM] + [VMEM] * (2 * len(ours) + 3),
+        in_specs=[SMEM] + [VMEM] * (2 * len(ours) + 2),
         out_specs=[VMEM] * len(shapes),
         compiler_params=pltpu.CompilerParams(vmem_limit_bytes=40 * MIB),
         cost_estimate=pl.CostEstimate(
             flops=10 * rows * hid * width, bytes_accessed=16 * MIB, transcendentals=rows * hid
         ),
         name="group",
-    )(place, *ours, *theirs, gate, up, down)
+    )(place, *ours, *theirs, pair, down)
 
 
 def weight_kernel(sizes, offset, half, hid, tile, place_ref, *refs):
     count = len(sizes)
-    kinds = (len(refs) - 2 * count - 5) // 3
+    kinds = len(refs) - 2 * count - 7
     ours, theirs = refs[:count], refs[count : 2 * count]
-    sides = refs[2 * count : 2 * count + 2 * kinds]
-    outs = refs[2 * count + 2 * kinds : 2 * count + 3 * kinds]
-    rows_ref, sides_t, stage, in_sem, out_sem = refs[2 * count + 3 * kinds :]
+    sides = refs[2 * count : 2 * count + 2]
+    outs = refs[2 * count + 2 : 2 * count + 2 + kinds]
+    rows_ref, sides_t, stage, in_sem, out_sem = refs[2 * count + 2 + kinds :]
     core = place_ref[0]
     loads = []
     for s, group in enumerate((ours, theirs)):
@@ -178,10 +220,10 @@
     for copies in loads:
         for c in copies:
             c.start()
-    depth, wide = sides[0].shape
-    for k in range(kinds):
-        for i in range(2):
-            sides_t[wide * k : wide * (k + 1), depth * i : depth * (i + 1)] = sides[2 * k + i][...].T
+    depth = sides[0].shape[0]
+    wide = sides[0].shape[1] // kinds
+    for i in range(2):
+        sides_t[:, depth * i : depth * (i + 1)] = sides[i][...].T
     stores = []
     for s in range(2):
         for c in loads[s]:
@@ -211,8 +253,8 @@
     sizes = [r.shape[0] for r in ours]
     rows = sum(sizes)
     width = ours[0].shape[1]
-    wide = sides[0].shape[1]
-    kinds = len(sides) // 2
+    wide = padded(hid)
+    kinds = sides[0].shape[1] // wide
     anywhere = pl.BlockSpec(memory_space=pl.ANY)
     return pl.pallas_call(
         functools.partial(weight_kernel, sizes, offset, width // 2, hid, tile),
@@ -241,18 +283,18 @@
     first, second = first_ref[...], second_ref[...]
     token_ref[...] = dot_f32(first + second, back[:, :half], 1, 0).astype(BF)
     share = back[:, half:]
-    route_ref[:, 0:1] = dot_f32(first, share, 1, 0)[:, 0:1] / weights_ref[:, 0:1]
-    route_ref[:, 1:2] = dot_f32(second, share, 1, 0)[:, 0:1] / weights_ref[:, 1:2]
+    route_ref[0:1] = dot_f32(share, first, 0, 1)[0:1] / weights_ref[0:1]
+    route_ref[1:2] = dot_f32(share, second, 0, 1)[0:1] / weights_ref[1:2]
 
 
 def combine(weights, first, second, backs):
-    rows = weights.shape[0]
+    rows = weights.shape[1]
     half = backs[0].shape[1] - LANES
     return pl.pallas_call(
         functools.partial(final_kernel, half),
         out_shape=[
             jax.ShapeDtypeStruct((rows, half), BF),
-            jax.ShapeDtypeStruct((rows, TOP), F32),
+            jax.ShapeDtypeStruct((TOP, rows), F32),
         ],
         in_specs=[VMEM] * (3 + EXPERTS),
         out_specs=[VMEM] * 2,
@@ -270,7 +312,7 @@
     packed = EXPERTS * CAP
     third = packed // 3
 
-    made = make_slots(place, tokens, cotangent, routes, route_weights)
+    made = make_slots(place, tokens, cotangent, routes.T, route_weights.T)
     first, second = made[EXPERTS:]
     part = packed // 2
     row_of = jnp.arange(part)
@@ -296,12 +338,12 @@
         far_right.append(pair_y(right[h]))
         across.append(along_x(right[h], -1))
 
-    gate_t = gate_weight[0].T
-    up_t = up_weight[0].T
     down_t = down_weight[0]
+    hid = down_t.shape[0]
+    pair_t = stack_weights(gate_weight[0].T, up_weight[0].T)
     near = own + left + right + partner
     near_other = [pair_core(v) for v in near]
-    near_out = run_group(place, near, near_other, gate_t, up_t, down_t)
+    near_out = run_group(place, near, near_other, pair_t, down_t)
     far = far_left + far_right + across
     tied = lax.optimization_barrier((*far, *near_out))
     far = list(tied[: len(far)])
@@ -310,7 +352,7 @@
     last = [along_x(far[0][:third], 1), along_x(middle, -1), pair_y(far[5][2 * third - part :])]
     far = far + last
     far_other = [pair_core(v) for v in far]
-    far_out = run_group(place, far, far_other, gate_t, up_t, down_t)
+    far_out = run_group(place, far, far_other, pair_t, down_t)
 
     def add(a, *more):
         total = a.astype(F32)
@@ -335,9 +377,8 @@
     b_partner = along_x(t_far_left, -1)
     b_right_pair = pair_y(t_far_right)
     b_right = along_x(t_across, 1)
-    hid = gate_t.shape[0]
     rows = (near + far, near_other + far_other)
-    sides = [g for t in (2, 3) for g in (near_out[t], far_out[t])]
+    sides = [near_out[2], far_out[2]]
     gate_grad, up_grad = weight_grads(place, *rows, sides, 0, hid)
     tied = lax.optimization_barrier((b_partner, b_right_pair, b_right, gate_grad, up_grad))
     b_partner, b_right_pair, b_right, gate_grad, up_grad = tied
@@ -345,7 +386,7 @@
     c_right = along_x(add(chunk(near_out, near_got, 2), b_right_pair, b_right), 1)
     c_pair = pair_y(add(chunk(near_out, near_got, 3), b_partner))
     half = tokens.shape[1] // 2
-    (down_grad,) = weight_grads(place, *rows, [near_out[4], far_out[4]], half, hid)
+    (down_grad,) = weight_grads(place, *rows, [near_out[3], far_out[3]], half, hid)
     tied = lax.optimization_barrier((c_left, c_right, c_pair, down_grad))
     c_left, c_right, c_pair, down_grad = tied
     home = add(chunk(near_out, near_got, 0), c_left, c_right, c_pair)
@@ -359,9 +400,9 @@
             if k:
                 piece = to_expert(piece, dz, dy, -1)
             backs[k] = piece
-    token_grad, route_grad = combine(route_weights, first, second, backs)
-
-    return token_grad, route_grad, gate_grad.T[None], up_grad.T[None], down_grad[None]
+    token_grad, route_grad = combine(route_weights.T, first, second, backs)
+
+    return token_grad, route_grad.T, gate_grad.T[None], up_grad.T[None], down_grad[None]
 
 
 def solution(mesh):

time: 176 us -> 158 us (0.90)
  waiting for transfers between devices: 58.1 us -> 43.4 us
  starting transfers between devices: 63.6 us -> 60.4 us
    ppermute x14, waiting for transfers between devices: 16.2 us -> 8.69 us  [to_expert(): return lax.ppermute(value, ('z', 'yh', 'yl'), perm)]
    ppermute x16, waiting for transfers between devices: 29.5 us -> 22.2 us  [along_x(): return lax.ppermute(value, 'x', [(i, (i + step) % 4) for i in range(4)])]
    pallas_call x2, Pallas kernels: 25 us -> 22.5 us  [run_group(): pl.pallas_call(functools.partial(group_kernel, len(ours), half), out_shap...]
    ppermute x16, starting transfers between devices: 22.2 us -> 20.2 us  [along_x(): return lax.ppermute(value, 'x', [(i, (i + step) % 4) for i in range(4)])]
    pallas_call x1, Pallas kernels: 1.34 us -> 3.18 us  [make_slots(): pl.pallas_call(functools.partial(slots_kernel, width // 2), out_shape=sha...]
    unnamed x13 -> x22, local copies, waits for them, and re-layouts: 4.02 us -> 4.46 us
  transfers between devices with their start and end apart: 57 -> 57, of which waited for: 25 -> 29; matrix products, arithmetic and copies ran while one was open for 1% -> 1% of each run, Pallas kernels for 17% -> 18%
where the time goes in v2:
time: 158 us; the launch traced here: 156 us
  starting transfers between devices  60.4 us (38%)
  Pallas kernels  43.9 us (28%)
  waiting for transfers between devices  43.4 us (27%)
  local copies, waits for them, and re-layouts  4.56 us (3%)
  other arithmetic  1.8 us (1%)
    ppermute x14, starting transfers between devices, to_expert(): return lax.ppermute(value, ('z', 'yh', 'yl'), perm)  28.7 us
    pallas_call x2, Pallas kernels, run_group(): pl.pallas_call(functools.partial(group_kernel, len(ours), half), out_shap...  22.5 us
    ppermute x16, waiting for transfers between devices, along_x(): return lax.ppermute(value, 'x', [(i, (i + step) % 4) for i in range(4)])  22.2 us
    ppermute x16, starting transfers between devices, along_x(): return lax.ppermute(value, 'x', [(i, (i + step) % 4) for i in range(4)])  20.2 us
    pallas_call x2, Pallas kernels, weight_grads(): pl.pallas_call(functools.partial(weight_kernel, sizes, offset, width // 2...  16.9 us
    ppermute x14, waiting for transfers between devices, to_expert(): return lax.ppermute(value, ('z', 'yh', 'yl'), perm)  8.69 us
    ppermute x8, starting transfers between devices, pair_y(): return lax.ppermute(value, 'yl', [(0, 1), (1, 0)])  8.24 us
    ppermute x8, waiting for transfers between devices, pair_y(): return lax.ppermute(value, 'yl', [(0, 1), (1, 0)])  7.16 us
  transfers between devices with their start and end apart: 57, of which 29 were waited for; matrix products, arithmetic and copies ran while one was open for 1% of the time, Pallas kernels for 18%

profile of v2, /device:TPU:2, one launch (start us, length us, event | category | flops | bytes accessed | tf_op | source)
XLA Modules:
  0.0 156.3 jit_solution(13193669407038704817)
XLA Ops:
  0.6 0.6 pad_add_fusion.place_ref
  1.2 3.2 %slots.1 = (bf16[16,4096]{1,0:T(8,128)(2,1)}, bf16[16,4096]{1,0:T(8,128)(2,1)}, bf16[16,4096]{1,0:T(8,128)(2,1)}, bf16[16,4096]{1,0:T(8,128)(2,1)}, bf16[16,4096...) custom-call(s32[3]{0:T(128)} %pad_add_fusion.place_ref, ...), custom_call_target="tpu_custom_call" | custom-call | flops 50331648 | bytes 3145728 | tf_op jit(solution)/shard_map/slots/pallas_call | solution.py:97
  4.4 3.1 %collective-permute-start.5 = (bf16[16,4096]{1,0:T(8,128)(2,1)}, bf16[16,4096]{1,0:T(8,128)(2,1)S(1)}, u32[]{:S(2)}, u32[]{:S(2)}) collective-permute-start(bf16[16,4096]{1,0:T(8,128)(2,1)} %get-tuple-element.52), channel_id=1, source_target_pairs={{0,24},{8,16},{16,8},{24,0},{32,56},{40,48},{48,40},{56,32},{64,88... | collective-permute-start | bytes 393224 | tf_op jit(solution)/shard_map/ppermute | solution.py:44
  7.5 1.6 %collective-permute-start.6 = (bf16[16,4096]{1,0:T(8,128)(2,1)}, bf16[16,4096]{1,0:T(8,128)(2,1)S(1)}, u32[]{:S(2)}, u32[]{:S(2)}) collective-permute-start(bf16[16,4096]{1,0:T(8,128)(2,1)} %get-tuple-element.53), channel_id=1, source_target_pairs={{0,56},{8,48},{16,40},{24,32},{32,88},{40,80},{48,72},{56,64},{64,... | collective-permute-start | bytes 393224 | tf_op jit(solution)/shard_map/ppermute | solution.py:44
  9.1 6.0 %collective-permute-start.7 = (bf16[16,4096]{1,0:T(8,128)(2,1)}, bf16[16,4096]{1,0:T(8,128)(2,1)S(1)}, u32[]{:S(2)}, u32[]{:S(2)}) collective-permute-start(bf16[16,4096]{1,0:T(8,128)(2,1)} %get-tuple-element.54), channel_id=1, source_target_pairs={{0,88},{8,80},{16,72},{24,64},{32,120},{40,112},{48,104},{56,96},{... | collective-permute-start | bytes 393224 | tf_op jit(solution)/shard_map/ppermute | solution.py:44
  15.1 0.7 collective-permute-start.8
  15.8 1.0 collective-permute-start
  16.8 0.9 collective-permute-start.1
  17.7 0.9 collective-permute-done.6
  18.6 1.8 %collective-permute-start.2 = (bf16[16,4096]{1,0:T(8,128)(2,1)}, bf16[16,4096]{1,0:T(8,128)(2,1)S(1)}, u32[]{:S(2)}, u32[]{:S(2)}) collective-permute-start(bf16[16,4096]{1,0:T(8,128)(2,1)} %get-tuple-element.51), channel_id=1, source_target_pairs={{0,96},{8,104},{16,112},{24,120},{32,0},{40,8},{48,16},{56,24},{64... | collective-permute-start | bytes 393224 | tf_op jit(solution)/shard_map/ppermute | solution.py:44
  20.3 2.1 %collective-permute-done.7 = bf16[16,4096]{1,0:T(8,128)(2,1)S(1)} collective-permute-done((bf16[16,4096]{1,0:T(8,128)(2,1)}, bf16[16,4096]{1,0:T(8,128)(2,1)S(1)}, u32[]{:S(2)}, u32[]{:S(2)}) %collective-permute-start.7) | collective-permute-done | bytes 131104 | tf_op jit(solution)/shard_map/ppermute | solution.py:44
  22.9 1.6 collective-permute-start.18
  25.0 1.7 %collective-permute-done.1 = bf16[16,4096]{1,0:T(8,128)(2,1)S(1)} collective-permute-done((bf16[16,4096]{1,0:T(8,128)(2,1)}, bf16[16,4096]{1,0:T(8,128)(2,1)S(1)}, u32[]{:S(2)}, u32[]{:S(2)}) %collective-permute-start.1) | collective-permute-done | bytes 131104 | tf_op jit(solution)/shard_map/ppermute | solution.py:44
  26.8 1.1 collective-permute-done.2
  28.3 1.6 %collective-permute-start.17 = (bf16[48,4096]{1,0:T(8,128)(2,1)S(1)}, bf16[48,4096]{1,0:T(8,128)(2,1)S(1)}, u32[]{:S(2)}, u32[]{:S(2)}) collective-permute-start(bf16[48,4096]{1,0:T(8,128)(2,1)S(1)} %convolution_convert_fusion.1.refs_0_), channel_id=1, source_target_pairs={{0,2},{2,4},{4,6},{6,0},{1,3},{3,5},{5,7},{7,1},{8,10},{10,12},{12... | collective-permute-start | bytes 1179656 | tf_op jit(solution)/shard_map/ppermute | solution.py:27
  29.8 5.1 %collective-permute-done.18.refs_3_ = bf16[48,4096]{1,0:T(8,128)(2,1)S(1)} collective-permute-done((bf16[48,4096]{1,0:T(8,128)(2,1)S(1)}, bf16[48,4096]{1,0:T(8,128)(2,1)S(1)}, u32[]{:S(2)}, u32[]{:S(2)}) %collective-permute-start.18) | collective-permute-done | bytes 393248 | tf_op jit(solution)/shard_map/ppermute | solution.py:27
  34.9 1.7 %collective-permute-start.11 = (bf16[48,4096]{1,0:T(8,128)(2,1)S(1)}, bf16[48,4096]{1,0:T(8,128)(2,1)S(1)}, u32[]{:S(2)}, u32[]{:S(2)}) collective-permute-start(bf16[48,4096]{1,0:T(8,128)(2,1)S(1)} %convolution_convert_fusion.1.refs_0_), channel_id=1, source_target_pairs={{0,6},{2,0},{4,2},{6,4},{1,7},{3,1},{5,3},{7,5},{8,14},{10,8},{12,... | collective-permute-start | bytes 1179656 | tf_op jit(solution)/shard_map/ppermute | solution.py:27
  36.7 1.6 %collective-permute-start.3 = (bf16[48,4096]{1,0:T(8,128)(2,1)S(1)}, bf16[48,4096]{1,0:T(8,128)(2,1)S(1)}, u32[]{:S(2)}, u32[]{:S(2)}) collective-permute-start(bf16[48,4096]{1,0:T(8,128)(2,1)S(1)} %convolution_convert_fusion.1.refs_0_), channel_id=1, source_target_pairs={{0,8},{8,0},{1,9},{9,1},{2,10},{10,2},{3,11},{11,3},{4,12},{12,4},... | collective-permute-start | bytes 1179656 | tf_op jit(solution)/shard_map/ppermute | solution.py:31
  38.8 4.0 %collective-permute-done.17.refs_2_ = bf16[48,4096]{1,0:T(8,128)(2,1)S(1)} collective-permute-done((bf16[48,4096]{1,0:T(8,128)(2,1)S(1)}, bf16[48,4096]{1,0:T(8,128)(2,1)S(1)}, u32[]{:S(2)}, u32[]{:S(2)}) %collective-permute-start.17) | collective-permute-done | bytes 393248 | tf_op jit(solution)/shard_map/ppermute | solution.py:27
  42.8 1.7 %collective-permute-start.16 = (bf16[48,4096]{1,0:T(8,128)(2,1)S(1)}, bf16[48,4096]{1,0:T(8,128)(2,1)S(1)}, u32[]{:S(2)}, u32[]{:S(2)}) collective-permute-start(bf16[48,4096]{1,0:T(8,128)(2,1)S(1)} %collective-permute-done.13.refs_5_), channel_id=1, source_target_pairs={{0,6},{2,0},{4,2},{6,4},{1,7},{3,1},{5,3},{7,5},{8,14},{10,8},{12,... | collective-permute-start | bytes 1179656 | tf_op jit(solution)/shard_map/ppermute | solution.py:27
  45.0 1.5 collective-permute-done.3.refs_6_
  47.1 1.8 %copy-done.2 = bf16[1,4096,344]{1,2,0:T(8,128)(2,1)S(1)} copy-done((bf16[1,4096,344]{1,2,0:T(8,128)(2,1)S(1)}, bf16[1,4096,344]{1,2,0:T(8,128)(2,1)}, u32[]{:S(2)}) %copy-start.2) | copy-done | bytes 2818072
  49.3 2.6 %copy-done = bf16[768,4096]{1,0:T(8,128)(2,1)} copy-done((bf16[768,4096]{1,0:T(8,128)(2,1)}, bf16[768,4096]{1,0:T(8,128)(2,1)S(1)}, u32[]{:S(2)}) %copy-start) | copy-done | bytes 6291480
  51.9 1.5 collective-permute-done.16.refs_5_.refs_13_
  53.4 0.8 collective-permute-start.14
  54.2 1.5 collective-permute-start.10
  56.2 1.3 collective-permute-start.12
  57.5 2.0 %collective-permute-start.4 = (bf16[48,4096]{1,0:T(8,128)(2,1)S(1)}, bf16[48,4096]{1,0:T(8,128)(2,1)S(1)}, u32[]{:S(2)}, u32[]{:S(2)}) collective-permute-start(bf16[48,4096]{1,0:T(8,128)(2,1)S(1)} %collective-permute-done.3.refs_6_), channel_id=1, source_target_pairs={{0,2},{2,4},{4,6},{6,0},{1,3},{3,5},{5,7},{7,1},{8,10},{10,12},{12... | collective-permute-start | bytes 1179656 | tf_op jit(solution)/shard_map/ppermute | solution.py:27
  59.4 11.3 %group.2 = (bf16[384,2176]{1,0:T(8,128)(2,1)S(1)}, bf16[384,2176]{1,0:T(8,128)(2,1)S(1)}, bf16[384,768]{1,0:T(8,128)(2,1)S(1)}, bf16[384,384]{1,0:T(8,128)(2,1)S(1)}) custom-call(s32[3]{0:T(128)S(1)} %copy-done.5, bf16[48,4096]{1,0:T(8,128)(2,1)S(1)} %convolution_convert_fusion.1.refs_0_, bf16[48,4096]{1,0:T(8,128)(2,1)S(1)} %convolution_convert_fusion.refs_1_, ...), custom_call_target="tpu_custom_call" | custom-call | flops 5410652160 | bytes 16777216 | tf_op jit(solution)/shard_map/group/pallas_call | solution.py:185
  70.8 0.9 collective-permute-done.12.refs_2_.refs_10_
  71.8 0.8 collective-permute-done.4.refs_0_.refs_8_
  72.6 1.1 collective-permute-start.31
  73.7 1.3 collective-permute-start.29
  75.0 1.5 collective-permute-start.30
  76.8 2.3 %collective-permute-done.31.refs_8_.refs_16_ = bf16[32,4096]{1,0:T(8,128)(2,1)S(1)} collective-permute-done((bf16[32,4096]{1,0:T(8,128)(2,1)S(1)}, bf16[32,4096]{1,0:T(8,128)(2,1)S(1)}, u32[]{:S(2)}, u32[]{:S(2)}) %collective-permute-start.31) | collective-permute-done | bytes 262176 | tf_op jit(solution)/shard_map/ppermute | solution.py:31
  79.1 1.7 %collective-permute-done.29.refs_6_.refs_14_ = bf16[32,4096]{1,0:T(8,128)(2,1)S(1)} collective-permute-done((bf16[32,4096]{1,0:T(8,128)(2,1)S(1)}, bf16[32,4096]{1,0:T(8,128)(2,1)S(1)}, u32[]{:S(2)}, u32[]{:S(2)}) %collective-permute-start.29) | collective-permute-done | bytes 262176 | tf_op jit(solution)/shard_map/ppermute | solution.py:27
  80.8 3.7 %collective-permute-done.30.refs_7_.refs_15_ = bf16[32,4096]{1,0:T(8,128)(2,1)S(1)} collective-permute-done((bf16[32,4096]{1,0:T(8,128)(2,1)S(1)}, bf16[32,4096]{1,0:T(8,128)(2,1)S(1)}, u32[]{:S(2)}, u32[]{:S(2)}) %collective-permute-start.30) | collective-permute-done | bytes 262176 | tf_op jit(solution)/shard_map/ppermute | solution.py:27
  85.6 0.6 collective-permute-done.35.refs_12_.refs_28_
  86.2 0.6 collective-permute-done.37.refs_14_.refs_30_
  87.9 11.1 %group.3 = (bf16[384,2176]{1,0:T(8,128)(2,1)S(1)}, bf16[384,2176]{1,0:T(8,128)(2,1)S(1)}, bf16[384,768]{1,0:T(8,128)(2,1)S(1)}, bf16[384,384]{1,0:T(8,128)(2,1)S(1)}) custom-call(s32[3]{0:T(128)S(1)} %copy-done.5, bf16[48,4096]{1,0:T(8,128)(2,1)S(1)} %collective-permute-done.4.refs_0_.refs_8_, bf16[48,4096]{1,0:T(8,128)(2,1)S(1)} %collective-permute-done.10.refs_1_.refs_9_, ...), custom_call_target="tpu_custom_call" | custom-call | flops 5410652160 | bytes 16777216 | tf_op jit(solution)/shard_map/group/pallas_call | solution.py:185
  99.6 3.0 %collective-permute-done.41 = bf16[384,2176]{1,0:T(8,128)(2,1)S(1)} collective-permute-done((bf16[384,2176]{1,0:T(8,128)(2,1)S(1)}, bf16[384,2176]{1,0:T(8,128)(2,1)S(1)}, u32[]{:S(2)}, u32[]{:S(2)}) %collective-permute-start.41) | collective-permute-done | bytes 1671200 | tf_op jit(solution)/shard_map/ppermute | solution.py:35
  102.8 1.3 collective-permute-start.46
  104.1 1.7 %collective-permute-start.44 = (bf16[32,2176]{1,0:T(8,128)(2,1)S(1)}, bf16[32,2176]{1,0:T(8,128)(2,1)S(1)}, u32[]{:S(2)}, u32[]{:S(2)}) collective-permute-start(bf16[32,2176]{1,0:T(8,128)(2,1)S(1)} %get-tuple-element.94), channel_id=1, source_target_pairs={{0,2},{2,4},{4,6},{6,0},{1,3},{3,5},{5,7},{7,1},{8,10},{10,12},{12... | collective-permute-start | bytes 417800 | tf_op jit(solution)/shard_map/ppermute | solution.py:27
  106.1 2.4 %collective-permute-done.46 = bf16[32,2176]{1,0:T(8,128)(2,1)S(1)} collective-permute-done((bf16[32,2176]{1,0:T(8,128)(2,1)S(1)}, bf16[32,2176]{1,0:T(8,128)(2,1)S(1)}, u32[]{:S(2)}, u32[]{:S(2)}) %collective-permute-start.46) | collective-permute-done | bytes 139296 | tf_op jit(solution)/shard_map/ppermute | solution.py:31
  108.6 1.0 collective-permute-done.44
  109.5 2.4 %collective-permute-done.42 = bf16[32,2176]{1,0:T(8,128)(2,1)S(1)} collective-permute-done((bf16[32,2176]{1,0:T(8,128)(2,1)S(1)}, bf16[32,2176]{1,0:T(8,128)(2,1)S(1)}, u32[]{:S(2)}, u32[]{:S(2)}) %collective-permute-start.42) | collective-permute-done | bytes 139296 | tf_op jit(solution)/shard_map/ppermute | solution.py:27
  112.3 1.8 %collective-permute-start.47 = (bf16[96,2176]{1,0:T(8,128)(2,1)S(1)}, bf16[96,2176]{1,0:T(8,128)(2,1)S(1)}, u32[]{:S(2)}, u32[]{:S(2)}) collective-permute-start(bf16[96,2176]{1,0:T(8,128)(2,1)S(1)} %get-tuple-element.90), channel_id=1, source_target_pairs={{0,2},{2,4},{4,6},{6,0},{1,3},{3,5},{5,7},{7,1},{8,10},{10,12},{12... | collective-permute-start | bytes 1253384 | tf_op jit(solution)/shard_map/ppermute | solution.py:27
  114.2 1.0 collective-permute-start.45
  115.4 10.0 %weight_grads.2 = (bf16[344,4096]{1,0:T(8,128)(2,1)}, bf16[344,4096]{1,0:T(8,128)(2,1)}) custom-call(s32[3]{0:T(128)S(1)} %copy-done.5, bf16[48,4096]{1,0:T(8,128)(2,1)S(1)} %convolution_convert_fusion.1.refs_0_, bf16[48,4096]{1,0:T(8,128)(2,1)S(1)} %convolution_convert_fusion.refs_1_, bf16[48,4096]{1,0:T(8,128)(2,1)S(1)} %collective-permute-done.17.refs_2_, ...), custom_call_target="tpu_custom_call" | custom-call | flops 4328521728 | bytes 14680064 | tf_op jit(solution)/shard_map/weight_grads/pallas_call | solution.py:259
  125.9 1.1 collective-permute-start.49
  127.0 1.7 %collective-permute-start.48 = (bf16[96,2176]{1,0:T(8,128)(2,1)S(1)}, bf16[96,2176]{1,0:T(8,128)(2,1)S(1)}, u32[]{:S(2)}, u32[]{:S(2)}) collective-permute-start(bf16[96,2176]{1,0:T(8,128)(2,1)S(1)} %get-tuple-element.88), channel_id=1, source_target_pairs={{0,2},{2,4},{4,6},{6,0},{1,3},{3,5},{5,7},{7,1},{8,10},{10,12},{12... | collective-permute-start | bytes 1253384 | tf_op jit(solution)/shard_map/ppermute | solution.py:27
  129.1 7.0 %weight_grads.3 = bf16[344,4096]{1,0:T(8,128)(2,1)} custom-call(s32[3]{0:T(128)S(1)} %copy-done.5, bf16[48,4096]{1,0:T(8,128)(2,1)S(1)} %convolution_convert_fusion.1.refs_0_, bf16[48,4096]{1,0:T(8,128)(2,1)S(1)} %convolution_convert_fusion.refs_1_, bf16[48,4096]{1,0:T(8,128)(2,1)S(1)} %collective-permute-done.17.refs_2_, ...), custom_call_target="tpu_custom_call" | custom-call | flops 2164260864 | bytes 14680064 | tf_op jit(solution)/shard_map/weight_grads/pallas_call | solution.py:259
  136.1 1.0 collective-permute-done.48
  137.1 0.6 collective-permute-done.28
  138.7 3.4 %collective-permute-start.56 = (bf16[16,2176]{1,0:T(8,128)(2,1)S(1)}, bf16[16,2176]{1,0:T(8,128)(2,1)S(1)}, u32[]{:S(2)}, u32[]{:S(2)}) collective-permute-start(bf16[16,2176]{1,0:T(8,128)(2,1)S(1)} %get-tuple-element.96), channel_id=1, source_target_pairs={{0,56},{8,48},{16,40},{24,32},{32,88},{40,80},{48,72},{56,64},{64,... | collective-permute-start | bytes 208904 | tf_op jit(solution)/shard_map/ppermute | solution.py:44
  142.1 2.5 %collective-permute-start.54 = (bf16[16,2176]{1,0:T(8,128)(2,1)S(1)}, bf16[16,2176]{1,0:T(8,128)(2,1)S(1)}, u32[]{:S(2)}, u32[]{:S(2)}) collective-permute-start(bf16[16,2176]{1,0:T(8,128)(2,1)S(1)} %get-tuple-element.97), channel_id=1, source_target_pairs={{0,88},{8,80},{16,72},{24,64},{32,120},{40,112},{48,104},{56,96},{... | collective-permute-start | bytes 208904 | tf_op jit(solution)/shard_map/ppermute | solution.py:44
  144.6 3.1 %collective-permute-start.52 = (bf16[16,2176]{1,0:T(8,128)(2,1)S(1)}, bf16[16,2176]{1,0:T(8,128)(2,1)S(1)}, u32[]{:S(2)}, u32[]{:S(2)}) collective-permute-start(bf16[16,2176]{1,0:T(8,128)(2,1)S(1)} %get-tuple-element.98), channel_id=1, source_target_pairs={{0,120},{8,112},{16,104},{24,96},{32,24},{40,16},{48,8},{56,0},{64... | collective-permute-start | bytes 208904 | tf_op jit(solution)/shard_map/ppermute | solution.py:44
  147.7 0.6 collective-permute-start.50
  148.2 1.1 collective-permute-start.55
  149.4 1.1 collective-permute-start.53
  150.4 2.1 %collective-permute-start.51 = (bf16[16,2176]{1,0:T(8,128)(2,1)S(1)}, bf16[16,2176]{1,0:T(8,128)(2,1)S(1)}, u32[]{:S(2)}, u32[]{:S(2)}) collective-permute-start(bf16[16,2176]{1,0:T(8,128)(2,1)S(1)} %get-tuple-element.102), channel_id=1, source_target_pairs={{0,96},{8,104},{16,112},{24,120},{32,0},{40,8},{48,16},{56,24},{64... | collective-permute-start | bytes 208904 | tf_op jit(solution)/shard_map/ppermute | solution.py:44
  152.5 0.7 collective-permute-done.50.refs_1_
  153.8 1.4 collective-permute-done.53.refs_4_
  155.4 0.9 combine.1
  (96 shorter events, 10.8 us)
Async XLA Ops:
  4.4 23.5 %copy-start.10 = (bf16[16,4096]{1,0:T(8,128)(2,1)S(1)}, bf16[16,4096]{1,0:T(8,128)(2,1)}, u32[]{:S(2)}) copy-start(bf16[16,4096]{1,0:T(8,128)(2,1)} %get-tuple-element.48) | copy-start | bytes 393220
  4.4 12.4 %collective-permute-start.5 = (bf16[16,4096]{1,0:T(8,128)(2,1)}, bf16[16,4096]{1,0:T(8,128)(2,1)S(1)}, u32[]{:S(2)}, u32[]{:S(2)}) collective-permute-start(bf16[16,4096]{1,0:T(8,128)(2,1)} %get-tuple-element.52), channel_id=1, source_target_pairs={{0,24},{8,16},{16,8},{24,0},{32,56},{40,48},{48,40},{56,32},{64,88... | collective-permute-start | bytes 393224 | tf_op jit(solution)/shard_map/ppermute | solution.py:44
  7.5 11.0 %collective-permute-start.6 = (bf16[16,4096]{1,0:T(8,128)(2,1)}, bf16[16,4096]{1,0:T(8,128)(2,1)S(1)}, u32[]{:S(2)}, u32[]{:S(2)}) collective-permute-start(bf16[16,4096]{1,0:T(8,128)(2,1)} %get-tuple-element.53), channel_id=1, source_target_pairs={{0,56},{8,48},{16,40},{24,32},{32,88},{40,80},{48,72},{56,64},{64,... | collective-permute-start | bytes 393224 | tf_op jit(solution)/shard_map/ppermute | solution.py:44
  9.1 13.4 %collective-permute-start.7 = (bf16[16,4096]{1,0:T(8,128)(2,1)}, bf16[16,4096]{1,0:T(8,128)(2,1)S(1)}, u32[]{:S(2)}, u32[]{:S(2)}) collective-permute-start(bf16[16,4096]{1,0:T(8,128)(2,1)} %get-tuple-element.54), channel_id=1, source_target_pairs={{0,88},{8,80},{16,72},{24,64},{32,120},{40,112},{48,104},{56,96},{... | collective-permute-start | bytes 393224 | tf_op jit(solution)/shard_map/ppermute | solution.py:44
  15.1 7.4 %collective-permute-start.8 = (bf16[16,4096]{1,0:T(8,128)(2,1)}, bf16[16,4096]{1,0:T(8,128)(2,1)S(1)}, u32[]{:S(2)}, u32[]{:S(2)}) collective-permute-start(bf16[16,4096]{1,0:T(8,128)(2,1)} %get-tuple-element.55), channel_id=1, source_target_pairs={{0,120},{8,112},{16,104},{24,96},{32,24},{40,16},{48,8},{56,0},{64... | collective-permute-start | bytes 393224 | tf_op jit(solution)/shard_map/ppermute | solution.py:44
  15.8 8.6 %collective-permute-start = (bf16[16,4096]{1,0:T(8,128)(2,1)}, bf16[16,4096]{1,0:T(8,128)(2,1)S(1)}, u32[]{:S(2)}, u32[]{:S(2)}) collective-permute-start(bf16[16,4096]{1,0:T(8,128)(2,1)} %get-tuple-element.49), channel_id=1, source_target_pairs={{0,32},{8,40},{16,48},{24,56},{32,64},{40,72},{48,80},{56,88},{64,... | collective-permute-start | bytes 393224 | tf_op jit(solution)/shard_map/ppermute | solution.py:44
  16.8 9.9 %collective-permute-start.1 = (bf16[16,4096]{1,0:T(8,128)(2,1)}, bf16[16,4096]{1,0:T(8,128)(2,1)S(1)}, u32[]{:S(2)}, u32[]{:S(2)}) collective-permute-start(bf16[16,4096]{1,0:T(8,128)(2,1)} %get-tuple-element.50), channel_id=1, source_target_pairs={{0,64},{8,72},{16,80},{24,88},{32,96},{40,104},{48,112},{56,120},{... | collective-permute-start | bytes 393224 | tf_op jit(solution)/shard_map/ppermute | solution.py:44
  18.5 28.5 %copy-start.1 = (bf16[1,4096,344]{1,2,0:T(8,128)(2,1)S(1)}, bf16[1,4096,344]{1,2,0:T(8,128)(2,1)}, u32[]{:S(2)}) copy-start(bf16[1,4096,344]{1,2,0:T(8,128)(2,1)} %param.11) | copy-start | bytes 8454148
  18.6 9.3 %collective-permute-start.2 = (bf16[16,4096]{1,0:T(8,128)(2,1)}, bf16[16,4096]{1,0:T(8,128)(2,1)S(1)}, u32[]{:S(2)}, u32[]{:S(2)}) collective-permute-start(bf16[16,4096]{1,0:T(8,128)(2,1)} %get-tuple-element.51), channel_id=1, source_target_pairs={{0,96},{8,104},{16,112},{24,120},{32,0},{40,8},{48,16},{56,24},{64... | collective-permute-start | bytes 393224 | tf_op jit(solution)/shard_map/ppermute | solution.py:44
  22.8 5.5 %collective-permute-start.20 = (bf16[48,4096]{1,0:T(8,128)(2,1)S(1)}, bf16[48,4096]{1,0:T(8,128)(2,1)S(1)}, u32[]{:S(2)}, u32[]{:S(2)}) collective-permute-start(bf16[48,4096]{1,0:T(8,128)(2,1)S(1)} %convolution_convert_fusion.refs_1_), channel_id=1, source_target_pairs={{0,1},{1,0},{2,3},{3,2},{4,5},{5,4},{6,7},{7,6},{8,9},{9,8},{10,11... | collective-permute-start | bytes 1179656 | tf_op jit(solution)/shard_map/ppermute | solution.py:35
  22.9 12.1 %collective-permute-start.18 = (bf16[48,4096]{1,0:T(8,128)(2,1)S(1)}, bf16[48,4096]{1,0:T(8,128)(2,1)S(1)}, u32[]{:S(2)}, u32[]{:S(2)}) collective-permute-start(bf16[48,4096]{1,0:T(8,128)(2,1)S(1)} %convolution_convert_fusion.refs_1_), channel_id=1, source_target_pairs={{0,2},{2,4},{4,6},{6,0},{1,3},{3,5},{5,7},{7,1},{8,10},{10,12},{12... | collective-permute-start | bytes 1179656 | tf_op jit(solution)/shard_map/ppermute | solution.py:27
  24.4 12.2 %collective-permute-start.13 = (bf16[48,4096]{1,0:T(8,128)(2,1)S(1)}, bf16[48,4096]{1,0:T(8,128)(2,1)S(1)}, u32[]{:S(2)}, u32[]{:S(2)}) collective-permute-start(bf16[48,4096]{1,0:T(8,128)(2,1)S(1)} %convolution_convert_fusion.refs_1_), channel_id=1, source_target_pairs={{0,6},{2,0},{4,2},{6,4},{1,7},{3,1},{5,3},{7,5},{8,14},{10,8},{12,... | collective-permute-start | bytes 1179656 | tf_op jit(solution)/shard_map/ppermute | solution.py:27
  26.7 11.6 %collective-permute-start.9 = (bf16[48,4096]{1,0:T(8,128)(2,1)S(1)}, bf16[48,4096]{1,0:T(8,128)(2,1)S(1)}, u32[]{:S(2)}, u32[]{:S(2)}) collective-permute-start(bf16[48,4096]{1,0:T(8,128)(2,1)S(1)} %convolution_convert_fusion.refs_1_), channel_id=1, source_target_pairs={{0,8},{8,0},{1,9},{9,1},{2,10},{10,2},{3,11},{11,3},{4,12},{12,4},... | collective-permute-start | bytes 1179656 | tf_op jit(solution)/shard_map/ppermute | solution.py:31
  28.2 10.1 %collective-permute-start.19 = (bf16[48,4096]{1,0:T(8,128)(2,1)S(1)}, bf16[48,4096]{1,0:T(8,128)(2,1)S(1)}, u32[]{:S(2)}, u32[]{:S(2)}) collective-permute-start(bf16[48,4096]{1,0:T(8,128)(2,1)S(1)} %convolution_convert_fusion.1.refs_0_), channel_id=1, source_target_pairs={{0,1},{1,0},{2,3},{3,2},{4,5},{5,4},{6,7},{7,6},{8,9},{9,8},{10,11... | collective-permute-start | bytes 1179656 | tf_op jit(solution)/shard_map/ppermute | solution.py:35
  28.3 14.5 %collective-permute-start.17 = (bf16[48,4096]{1,0:T(8,128)(2,1)S(1)}, bf16[48,4096]{1,0:T(8,128)(2,1)S(1)}, u32[]{:S(2)}, u32[]{:S(2)}) collective-permute-start(bf16[48,4096]{1,0:T(8,128)(2,1)S(1)} %convolution_convert_fusion.1.refs_0_), channel_id=1, source_target_pairs={{0,2},{2,4},{4,6},{6,0},{1,3},{3,5},{5,7},{7,1},{8,10},{10,12},{12... | collective-permute-start | bytes 1179656 | tf_op jit(solution)/shard_map/ppermute | solution.py:27
  34.9 10.1 %collective-permute-start.11 = (bf16[48,4096]{1,0:T(8,128)(2,1)S(1)}, bf16[48,4096]{1,0:T(8,128)(2,1)S(1)}, u32[]{:S(2)}, u32[]{:S(2)}) collective-permute-start(bf16[48,4096]{1,0:T(8,128)(2,1)S(1)} %convolution_convert_fusion.1.refs_0_), channel_id=1, source_target_pairs={{0,6},{2,0},{4,2},{6,4},{1,7},{3,1},{5,3},{7,5},{8,14},{10,8},{12,... | collective-permute-start | bytes 1179656 | tf_op jit(solution)/shard_map/ppermute | solution.py:27
  36.7 9.8 %collective-permute-start.3 = (bf16[48,4096]{1,0:T(8,128)(2,1)S(1)}, bf16[48,4096]{1,0:T(8,128)(2,1)S(1)}, u32[]{:S(2)}, u32[]{:S(2)}) collective-permute-start(bf16[48,4096]{1,0:T(8,128)(2,1)S(1)} %convolution_convert_fusion.1.refs_0_), channel_id=1, source_target_pairs={{0,8},{8,0},{1,9},{9,1},{2,10},{10,2},{3,11},{11,3},{4,12},{12,4},... | collective-permute-start | bytes 1179656 | tf_op jit(solution)/shard_map/ppermute | solution.py:31
  38.3 8.2 %collective-permute-start.22 = (bf16[48,4096]{1,0:T(8,128)(2,1)S(1)}, bf16[48,4096]{1,0:T(8,128)(2,1)S(1)}, u32[]{:S(2)}, u32[]{:S(2)}) collective-permute-start(bf16[48,4096]{1,0:T(8,128)(2,1)S(1)} %collective-permute-done.18.refs_3_), channel_id=1, source_target_pairs={{0,1},{1,0},{2,3},{3,2},{4,5},{5,4},{6,7},{7,6},{8,9},{9,8},{10,11... | collective-permute-start | bytes 1179656 | tf_op jit(solution)/shard_map/ppermute | solution.py:35
  38.3 8.7 %collective-permute-start.24 = (bf16[48,4096]{1,0:T(8,128)(2,1)S(1)}, bf16[48,4096]{1,0:T(8,128)(2,1)S(1)}, u32[]{:S(2)}, u32[]{:S(2)}) collective-permute-start(bf16[48,4096]{1,0:T(8,128)(2,1)S(1)} %collective-permute-done.13.refs_5_), channel_id=1, source_target_pairs={{0,1},{1,0},{2,3},{3,2},{4,5},{5,4},{6,7},{7,6},{8,9},{9,8},{10,11... | collective-permute-start | bytes 1179656 | tf_op jit(solution)/shard_map/ppermute | solution.py:35
  42.8 10.6 %collective-permute-start.16 = (bf16[48,4096]{1,0:T(8,128)(2,1)S(1)}, bf16[48,4096]{1,0:T(8,128)(2,1)S(1)}, u32[]{:S(2)}, u32[]{:S(2)}) collective-permute-start(bf16[48,4096]{1,0:T(8,128)(2,1)S(1)} %collective-permute-done.13.refs_5_), channel_id=1, source_target_pairs={{0,6},{2,0},{4,2},{6,4},{1,7},{3,1},{5,3},{7,5},{8,14},{10,8},{12,... | collective-permute-start | bytes 1179656 | tf_op jit(solution)/shard_map/ppermute | solution.py:27
  45.0 9.2 %collective-permute-start.26 = (bf16[48,4096]{1,0:T(8,128)(2,1)S(1)}, bf16[48,4096]{1,0:T(8,128)(2,1)S(1)}, u32[]{:S(2)}, u32[]{:S(2)}) collective-permute-start(bf16[48,4096]{1,0:T(8,128)(2,1)S(1)} %collective-permute-done.9.refs_7_), channel_id=1, source_target_pairs={{0,1},{1,0},{2,3},{3,2},{4,5},{5,4},{6,7},{7,6},{8,9},{9,8},{10,11... | collective-permute-start | bytes 1179656 | tf_op jit(solution)/shard_map/ppermute | solution.py:35
  46.4 9.2 %collective-permute-start.21 = (bf16[48,4096]{1,0:T(8,128)(2,1)S(1)}, bf16[48,4096]{1,0:T(8,128)(2,1)S(1)}, u32[]{:S(2)}, u32[]{:S(2)}) collective-permute-start(bf16[48,4096]{1,0:T(8,128)(2,1)S(1)} %collective-permute-done.17.refs_2_), channel_id=1, source_target_pairs={{0,1},{1,0},{2,3},{3,2},{4,5},{5,4},{6,7},{7,6},{8,9},{9,8},{10,11... | collective-permute-start | bytes 1179656 | tf_op jit(solution)/shard_map/ppermute | solution.py:35
  46.5 9.7 %collective-permute-start.23 = (bf16[48,4096]{1,0:T(8,128)(2,1)S(1)}, bf16[48,4096]{1,0:T(8,128)(2,1)S(1)}, u32[]{:S(2)}, u32[]{:S(2)}) collective-permute-start(bf16[48,4096]{1,0:T(8,128)(2,1)S(1)} %collective-permute-done.11.refs_4_), channel_id=1, source_target_pairs={{0,1},{1,0},{2,3},{3,2},{4,5},{5,4},{6,7},{7,6},{8,9},{9,8},{10,11... | collective-permute-start | bytes 1179656 | tf_op jit(solution)/shard_map/ppermute | solution.py:35
  47.0 10.5 %collective-permute-start.25 = (bf16[48,4096]{1,0:T(8,128)(2,1)S(1)}, bf16[48,4096]{1,0:T(8,128)(2,1)S(1)}, u32[]{:S(2)}, u32[]{:S(2)}) collective-permute-start(bf16[48,4096]{1,0:T(8,128)(2,1)S(1)} %collective-permute-done.3.refs_6_), channel_id=1, source_target_pairs={{0,1},{1,0},{2,3},{3,2},{4,5},{5,4},{6,7},{7,6},{8,9},{9,8},{10,11... | collective-permute-start | bytes 1179656 | tf_op jit(solution)/shard_map/ppermute | solution.py:35
  48.8 10.6 %copy-start.7 = (bf16[1,344,4096]{2,1,0:T(8,128)(2,1)S(1)}, bf16[1,344,4096]{2,1,0:T(8,128)(2,1)}, u32[]{:S(2)}) copy-start(bf16[1,344,4096]{2,1,0:T(8,128)(2,1)} %param.13) | copy-start | bytes 8454148
  53.4 17.4 %collective-permute-start.14 = (bf16[48,4096]{1,0:T(8,128)(2,1)S(1)}, bf16[48,4096]{1,0:T(8,128)(2,1)S(1)}, u32[]{:S(2)}, u32[]{:S(2)}) collective-permute-start(bf16[48,4096]{1,0:T(8,128)(2,1)S(1)} %collective-permute-done.13.refs_5_), channel_id=1, source_target_pairs={{0,8},{8,0},{1,9},{9,1},{2,10},{10,2},{3,11},{11,3},{4,12},{12,4},... | collective-permute-start | bytes 1179656 | tf_op jit(solution)/shard_map/ppermute | solution.py:31
  54.2 16.7 %collective-permute-start.10 = (bf16[48,4096]{1,0:T(8,128)(2,1)S(1)}, bf16[48,4096]{1,0:T(8,128)(2,1)S(1)}, u32[]{:S(2)}, u32[]{:S(2)}) collective-permute-start(bf16[48,4096]{1,0:T(8,128)(2,1)S(1)} %collective-permute-done.9.refs_7_), channel_id=1, source_target_pairs={{0,2},{2,4},{4,6},{6,0},{1,3},{3,5},{5,7},{7,1},{8,10},{10,12},{12... | collective-permute-start | bytes 1179656 | tf_op jit(solution)/shard_map/ppermute | solution.py:27
  55.7 15.2 %collective-permute-start.15 = (bf16[48,4096]{1,0:T(8,128)(2,1)S(1)}, bf16[48,4096]{1,0:T(8,128)(2,1)S(1)}, u32[]{:S(2)}, u32[]{:S(2)}) collective-permute-start(bf16[48,4096]{1,0:T(8,128)(2,1)S(1)} %collective-permute-done.11.refs_4_), channel_id=1, source_target_pairs={{0,6},{2,0},{4,2},{6,4},{1,7},{3,1},{5,3},{7,5},{8,14},{10,8},{12,... | collective-permute-start | bytes 1179656 | tf_op jit(solution)/shard_map/ppermute | solution.py:27
  56.2 15.6 %collective-permute-start.12 = (bf16[48,4096]{1,0:T(8,128)(2,1)S(1)}, bf16[48,4096]{1,0:T(8,128)(2,1)S(1)}, u32[]{:S(2)}, u32[]{:S(2)}) collective-permute-start(bf16[48,4096]{1,0:T(8,128)(2,1)S(1)} %collective-permute-done.11.refs_4_), channel_id=1, source_target_pairs={{0,8},{8,0},{1,9},{9,1},{2,10},{10,2},{3,11},{11,3},{4,12},{12,4},... | collective-permute-start | bytes 1179656 | tf_op jit(solution)/shard_map/ppermute | solution.py:31
  57.5 15.1 %collective-permute-start.4 = (bf16[48,4096]{1,0:T(8,128)(2,1)S(1)}, bf16[48,4096]{1,0:T(8,128)(2,1)S(1)}, u32[]{:S(2)}, u32[]{:S(2)}) collective-permute-start(bf16[48,4096]{1,0:T(8,128)(2,1)S(1)} %collective-permute-done.3.refs_6_), channel_id=1, source_target_pairs={{0,2},{2,4},{4,6},{6,0},{1,3},{3,5},{5,7},{7,1},{8,10},{10,12},{12... | collective-permute-start | bytes 1179656 | tf_op jit(solution)/shard_map/ppermute | solution.py:27
  59.4 28.4 %copy-start.8 = (bf16[1,344,4096]{2,1,0:T(8,128)(2,1)S(1)}, bf16[1,344,4096]{2,1,0:T(8,128)(2,1)}, u32[]{:S(2)}) copy-start(bf16[1,344,4096]{2,1,0:T(8,128)(2,1)} %param.13) | copy-start | bytes 8454148
  72.6 6.5 %collective-permute-start.31 = (bf16[32,4096]{1,0:T(8,128)(2,1)S(1)}, bf16[32,4096]{1,0:T(8,128)(2,1)S(1)}, u32[]{:S(2)}, u32[]{:S(2)}) collective-permute-start(bf16[32,4096]{1,0:T(8,128)(2,1)S(1)} %slice.111), channel_id=1, source_target_pairs={{0,8},{8,0},{1,9},{9,1},{2,10},{10,2},{3,11},{11,3},{4,12},{12,4},... | collective-permute-start | bytes 786440 | tf_op jit(solution)/shard_map/ppermute | solution.py:31
  73.7 7.1 %collective-permute-start.29 = (bf16[32,4096]{1,0:T(8,128)(2,1)S(1)}, bf16[32,4096]{1,0:T(8,128)(2,1)S(1)}, u32[]{:S(2)}, u32[]{:S(2)}) collective-permute-start(bf16[32,4096]{1,0:T(8,128)(2,1)S(1)} %slice.108), channel_id=1, source_target_pairs={{0,2},{2,4},{4,6},{6,0},{1,3},{3,5},{5,7},{7,1},{8,10},{10,12},{12... | collective-permute-start | bytes 786440 | tf_op jit(solution)/shard_map/ppermute | solution.py:27
  75.0 9.5 %collective-permute-start.33 = (bf16[48,4096]{1,0:T(8,128)(2,1)S(1)}, bf16[48,4096]{1,0:T(8,128)(2,1)S(1)}, u32[]{:S(2)}, u32[]{:S(2)}) collective-permute-start(bf16[48,4096]{1,0:T(8,128)(2,1)S(1)} %collective-permute-done.10.refs_1_.refs_9_), channel_id=1, source_target_pairs={{0,1},{1,0},{2,3},{3,2},{4,5},{5,4},{6,7},{7,6},{8,9},{9,8},{10,11... | collective-permute-start | bytes 1179656 | tf_op jit(solution)/shard_map/ppermute | solution.py:35
  75.0 9.5 %collective-permute-start.30 = (bf16[32,4096]{1,0:T(8,128)(2,1)S(1)}, bf16[32,4096]{1,0:T(8,128)(2,1)S(1)}, u32[]{:S(2)}, u32[]{:S(2)}) collective-permute-start(bf16[32,4096]{1,0:T(8,128)(2,1)S(1)} %pad_maximum_fusion), channel_id=1, source_target_pairs={{0,6},{2,0},{4,2},{6,4},{1,7},{3,1},{5,3},{7,5},{8,14},{10,8},{12,... | collective-permute-start | bytes 786440 | tf_op jit(solution)/shard_map/ppermute | solution.py:27
  76.5 8.4 %collective-permute-start.36 = (bf16[48,4096]{1,0:T(8,128)(2,1)S(1)}, bf16[48,4096]{1,0:T(8,128)(2,1)S(1)}, u32[]{:S(2)}, u32[]{:S(2)}) collective-permute-start(bf16[48,4096]{1,0:T(8,128)(2,1)S(1)} %collective-permute-done.15.refs_4_.refs_12_), channel_id=1, source_target_pairs={{0,1},{1,0},{2,3},{3,2},{4,5},{5,4},{6,7},{7,6},{8,9},{9,8},{10,11... | collective-permute-start | bytes 1179656 | tf_op jit(solution)/shard_map/ppermute | solution.py:35
  79.1 6.0 %collective-permute-start.32 = (bf16[48,4096]{1,0:T(8,128)(2,1)S(1)}, bf16[48,4096]{1,0:T(8,128)(2,1)S(1)}, u32[]{:S(2)}, u32[]{:S(2)}) collective-permute-start(bf16[48,4096]{1,0:T(8,128)(2,1)S(1)} %collective-permute-done.4.refs_0_.refs_8_), channel_id=1, source_target_pairs={{0,1},{1,0},{2,3},{3,2},{4,5},{5,4},{6,7},{7,6},{8,9},{9,8},{10,11... | collective-permute-start | bytes 1179656 | tf_op jit(solution)/shard_map/ppermute | solution.py:35
  80.8 4.7 %collective-permute-start.34 = (bf16[48,4096]{1,0:T(8,128)(2,1)S(1)}, bf16[48,4096]{1,0:T(8,128)(2,1)S(1)}, u32[]{:S(2)}, u32[]{:S(2)}) collective-permute-start(bf16[48,4096]{1,0:T(8,128)(2,1)S(1)} %collective-permute-done.12.refs_2_.refs_10_), channel_id=1, source_target_pairs={{0,1},{1,0},{2,3},{3,2},{4,5},{5,4},{6,7},{7,6},{8,9},{9,8},{10,11... | collective-permute-start | bytes 1179656 | tf_op jit(solution)/shard_map/ppermute | solution.py:35
  84.5 1.7 %collective-permute-start.35 = (bf16[48,4096]{1,0:T(8,128)(2,1)S(1)}, bf16[48,4096]{1,0:T(8,128)(2,1)S(1)}, u32[]{:S(2)}, u32[]{:S(2)}) collective-permute-start(bf16[48,4096]{1,0:T(8,128)(2,1)S(1)} %collective-permute-done.14.refs_3_.refs_11_), channel_id=1, source_target_pairs={{0,1},{1,0},{2,3},{3,2},{4,5},{5,4},{6,7},{7,6},{8,9},{9,8},{10,11... | collective-permute-start | bytes 1179656 | tf_op jit(solution)/shard_map/ppermute | solution.py:35
  84.5 2.3 %collective-permute-start.37 = (bf16[48,4096]{1,0:T(8,128)(2,1)S(1)}, bf16[48,4096]{1,0:T(8,128)(2,1)S(1)}, u32[]{:S(2)}, u32[]{:S(2)}) collective-permute-start(bf16[48,4096]{1,0:T(8,128)(2,1)S(1)} %collective-permute-done.16.refs_5_.refs_13_), channel_id=1, source_target_pairs={{0,1},{1,0},{2,3},{3,2},{4,5},{5,4},{6,7},{7,6},{8,9},{9,8},{10,11... | collective-permute-start | bytes 1179656 | tf_op jit(solution)/shard_map/ppermute | solution.py:35
  85.0 2.1 %collective-permute-start.40 = (bf16[32,4096]{1,0:T(8,128)(2,1)S(1)}, bf16[32,4096]{1,0:T(8,128)(2,1)S(1)}, u32[]{:S(2)}, u32[]{:S(2)}) collective-permute-start(bf16[32,4096]{1,0:T(8,128)(2,1)S(1)} %collective-permute-done.31.refs_8_.refs_16_), channel_id=1, source_target_pairs={{0,1},{1,0},{2,3},{3,2},{4,5},{5,4},{6,7},{7,6},{8,9},{9,8},{10,11... | collective-permute-start | bytes 786440 | tf_op jit(solution)/shard_map/ppermute | solution.py:35
  85.1 2.4 %collective-permute-start.38 = (bf16[32,4096]{1,0:T(8,128)(2,1)S(1)}, bf16[32,4096]{1,0:T(8,128)(2,1)S(1)}, u32[]{:S(2)}, u32[]{:S(2)}) collective-permute-start(bf16[32,4096]{1,0:T(8,128)(2,1)S(1)} %collective-permute-done.29.refs_6_.refs_14_), channel_id=1, source_target_pairs={{0,1},{1,0},{2,3},{3,2},{4,5},{5,4},{6,7},{7,6},{8,9},{9,8},{10,11... | collective-permute-start | bytes 786440 | tf_op jit(solution)/shard_map/ppermute | solution.py:35
  85.5 2.4 %collective-permute-start.39 = (bf16[32,4096]{1,0:T(8,128)(2,1)S(1)}, bf16[32,4096]{1,0:T(8,128)(2,1)S(1)}, u32[]{:S(2)}, u32[]{:S(2)}) collective-permute-start(bf16[32,4096]{1,0:T(8,128)(2,1)S(1)} %collective-permute-done.30.refs_7_.refs_15_), channel_id=1, source_target_pairs={{0,1},{1,0},{2,3},{3,2},{4,5},{5,4},{6,7},{7,6},{8,9},{9,8},{10,11... | collective-permute-start | bytes 786440 | tf_op jit(solution)/shard_map/ppermute | solution.py:35
  99.0 3.6 %collective-permute-start.41 = (bf16[384,2176]{1,0:T(8,128)(2,1)S(1)}, bf16[384,2176]{1,0:T(8,128)(2,1)S(1)}, u32[]{:S(2)}, u32[]{:S(2)}) collective-permute-start(bf16[384,2176]{1,0:T(8,128)(2,1)S(1)} %get-tuple-element.69), channel_id=1, source_target_pairs={{0,1},{1,0},{2,3},{3,2},{4,5},{5,4},{6,7},{7,6},{8,9},{9,8},{10,11... | collective-permute-start | bytes 5013512 | tf_op jit(solution)/shard_map/ppermute | solution.py:35
  99.3 26.2 %collective-permute-start.27 = (bf16[384,2176]{1,0:T(8,128)(2,1)}, bf16[384,2176]{1,0:T(8,128)(2,1)S(1)}, u32[]{:S(2)}, u32[]{:S(2)}) collective-permute-start(bf16[384,2176]{1,0:T(8,128)(2,1)} %copy-done.9), channel_id=1, source_target_pairs={{0,1},{1,0},{2,3},{3,2},{4,5},{5,4},{6,7},{7,6},{8,9},{9,8},{10,11... | collective-permute-start | bytes 5013512 | tf_op jit(solution)/shard_map/ppermute | solution.py:35
  102.8 5.8 %collective-permute-start.46 = (bf16[32,2176]{1,0:T(8,128)(2,1)S(1)}, bf16[32,2176]{1,0:T(8,128)(2,1)S(1)}, u32[]{:S(2)}, u32[]{:S(2)}) collective-permute-start(bf16[32,2176]{1,0:T(8,128)(2,1)S(1)} %get-tuple-element.93), channel_id=1, source_target_pairs={{0,8},{8,0},{1,9},{9,1},{2,10},{10,2},{3,11},{11,3},{4,12},{12,4},... | collective-permute-start | bytes 417800 | tf_op jit(solution)/shard_map/ppermute | solution.py:31
  104.1 5.4 %collective-permute-start.44 = (bf16[32,2176]{1,0:T(8,128)(2,1)S(1)}, bf16[32,2176]{1,0:T(8,128)(2,1)S(1)}, u32[]{:S(2)}, u32[]{:S(2)}) collective-permute-start(bf16[32,2176]{1,0:T(8,128)(2,1)S(1)} %get-tuple-element.94), channel_id=1, source_target_pairs={{0,2},{2,4},{4,6},{6,0},{1,3},{3,5},{5,7},{7,1},{8,10},{10,12},{12... | collective-permute-start | bytes 417800 | tf_op jit(solution)/shard_map/ppermute | solution.py:27
  105.8 6.1 %collective-permute-start.42 = (bf16[32,2176]{1,0:T(8,128)(2,1)S(1)}, bf16[32,2176]{1,0:T(8,128)(2,1)S(1)}, u32[]{:S(2)}, u32[]{:S(2)}) collective-permute-start(bf16[32,2176]{1,0:T(8,128)(2,1)S(1)} %get-tuple-element.95), channel_id=1, source_target_pairs={{0,6},{2,0},{4,2},{6,4},{1,7},{3,1},{5,3},{7,5},{8,14},{10,8},{12,... | collective-permute-start | bytes 417800 | tf_op jit(solution)/shard_map/ppermute | solution.py:27
  112.3 13.1 %collective-permute-start.47 = (bf16[96,2176]{1,0:T(8,128)(2,1)S(1)}, bf16[96,2176]{1,0:T(8,128)(2,1)S(1)}, u32[]{:S(2)}, u32[]{:S(2)}) collective-permute-start(bf16[96,2176]{1,0:T(8,128)(2,1)S(1)} %get-tuple-element.90), channel_id=1, source_target_pairs={{0,2},{2,4},{4,6},{6,0},{1,3},{3,5},{5,7},{7,1},{8,10},{10,12},{12... | collective-permute-start | bytes 1253384 | tf_op jit(solution)/shard_map/ppermute | solution.py:27
  114.2 11.3 %collective-permute-start.45 = (bf16[96,2176]{1,0:T(8,128)(2,1)S(1)}, bf16[96,2176]{1,0:T(8,128)(2,1)S(1)}, u32[]{:S(2)}, u32[]{:S(2)}) collective-permute-start(bf16[96,2176]{1,0:T(8,128)(2,1)S(1)} %get-tuple-element.91), channel_id=1, source_target_pairs={{0,8},{8,0},{1,9},{9,1},{2,10},{10,2},{3,11},{11,3},{4,12},{12,4},... | collective-permute-start | bytes 1253384 | tf_op jit(solution)/shard_map/ppermute | solution.py:31
  115.1 10.3 %collective-permute-start.43 = (bf16[96,2176]{1,0:T(8,128)(2,1)S(1)}, bf16[96,2176]{1,0:T(8,128)(2,1)S(1)}, u32[]{:S(2)}, u32[]{:S(2)}) collective-permute-start(bf16[96,2176]{1,0:T(8,128)(2,1)S(1)} %get-tuple-element.92), channel_id=1, source_target_pairs={{0,6},{2,0},{4,2},{6,4},{1,7},{3,1},{5,3},{7,5},{8,14},{10,8},{12,... | collective-permute-start | bytes 1253384 | tf_op jit(solution)/shard_map/ppermute | solution.py:27
  125.9 10.2 %collective-permute-start.49 = (bf16[96,2176]{1,0:T(8,128)(2,1)S(1)}, bf16[96,2176]{1,0:T(8,128)(2,1)S(1)}, u32[]{:S(2)}, u32[]{:S(2)}) collective-permute-start(bf16[96,2176]{1,0:T(8,128)(2,1)S(1)} %get-tuple-element.87), channel_id=1, source_target_pairs={{0,8},{8,0},{1,9},{9,1},{2,10},{10,2},{3,11},{11,3},{4,12},{12,4},... | collective-permute-start | bytes 1253384 | tf_op jit(solution)/shard_map/ppermute | solution.py:31
  127.0 10.1 %collective-permute-start.48 = (bf16[96,2176]{1,0:T(8,128)(2,1)S(1)}, bf16[96,2176]{1,0:T(8,128)(2,1)S(1)}, u32[]{:S(2)}, u32[]{:S(2)}) collective-permute-start(bf16[96,2176]{1,0:T(8,128)(2,1)S(1)} %get-tuple-element.88), channel_id=1, source_target_pairs={{0,2},{2,4},{4,6},{6,0},{1,3},{3,5},{5,7},{7,1},{8,10},{10,12},{12... | collective-permute-start | bytes 1253384 | tf_op jit(solution)/shard_map/ppermute | solution.py:27
  128.8 8.9 %collective-permute-start.28 = (bf16[96,2176]{1,0:T(8,128)(2,1)S(1)}, bf16[96,2176]{1,0:T(8,128)(2,1)S(1)}, u32[]{:S(2)}, u32[]{:S(2)}) collective-permute-start(bf16[96,2176]{1,0:T(8,128)(2,1)S(1)} %get-tuple-element.89), channel_id=1, source_target_pairs={{0,6},{2,0},{4,2},{6,4},{1,7},{3,1},{5,3},{7,5},{8,14},{10,8},{12,... | collective-permute-start | bytes 1253384 | tf_op jit(solution)/shard_map/ppermute | solution.py:27
  137.9 17.4 %copy-start.3 = (bf16[24,128]{1,0:T(8,128)(2,1)S(1)}, bf16[24,128]{1,0:T(8,128)(2,1)}, u32[]{:S(2)}) copy-start(bf16[24,128]{1,0:T(8,128)(2,1)} %get-tuple-element.46.first_ref) | copy-start | bytes 18436
  138.0 17.4 %copy-start.4 = (bf16[24,128]{1,0:T(8,128)(2,1)S(1)}, bf16[24,128]{1,0:T(8,128)(2,1)}, u32[]{:S(2)}) copy-start(bf16[24,128]{1,0:T(8,128)(2,1)} %get-tuple-element.47.second_ref) | copy-start | bytes 18436
  138.0 17.4 %copy-start.6 = (f32[24,2]{0,1:T(2,128)S(1)}, f32[24,2]{0,1:T(2,128)}, u32[]{:S(2)}) copy-start(f32[24,2]{0,1:T(2,128)} %param.10) | copy-start | bytes 580
  138.7 10.6 %collective-permute-start.56 = (bf16[16,2176]{1,0:T(8,128)(2,1)S(1)}, bf16[16,2176]{1,0:T(8,128)(2,1)S(1)}, u32[]{:S(2)}, u32[]{:S(2)}) collective-permute-start(bf16[16,2176]{1,0:T(8,128)(2,1)S(1)} %get-tuple-element.96), channel_id=1, source_target_pairs={{0,56},{8,48},{16,40},{24,32},{32,88},{40,80},{48,72},{56,64},{64,... | collective-permute-start | bytes 208904 | tf_op jit(solution)/shard_map/ppermute | solution.py:44
  142.1 8.3 %collective-permute-start.54 = (bf16[16,2176]{1,0:T(8,128)(2,1)S(1)}, bf16[16,2176]{1,0:T(8,128)(2,1)S(1)}, u32[]{:S(2)}, u32[]{:S(2)}) collective-permute-start(bf16[16,2176]{1,0:T(8,128)(2,1)S(1)} %get-tuple-element.97), channel_id=1, source_target_pairs={{0,88},{8,80},{16,72},{24,64},{32,120},{40,112},{48,104},{56,96},{... | collective-permute-start | bytes 208904 | tf_op jit(solution)/shard_map/ppermute | solution.py:44
  144.6 7.9 %collective-permute-start.52 = (bf16[16,2176]{1,0:T(8,128)(2,1)S(1)}, bf16[16,2176]{1,0:T(8,128)(2,1)S(1)}, u32[]{:S(2)}, u32[]{:S(2)}) collective-permute-start(bf16[16,2176]{1,0:T(8,128)(2,1)S(1)} %get-tuple-element.98), channel_id=1, source_target_pairs={{0,120},{8,112},{16,104},{24,96},{32,24},{40,16},{48,8},{56,0},{64... | collective-permute-start | bytes 208904 | tf_op jit(solution)/shard_map/ppermute | solution.py:44
  147.7 5.5 %collective-permute-start.50 = (bf16[16,2176]{1,0:T(8,128)(2,1)S(1)}, bf16[16,2176]{1,0:T(8,128)(2,1)S(1)}, u32[]{:S(2)}, u32[]{:S(2)}) collective-permute-start(bf16[16,2176]{1,0:T(8,128)(2,1)S(1)} %get-tuple-element.99), channel_id=1, source_target_pairs={{0,24},{8,16},{16,8},{24,0},{32,56},{40,48},{48,40},{56,32},{64,88... | collective-permute-start | bytes 208904 | tf_op jit(solution)/shard_map/ppermute | solution.py:44
  148.2 5.5 %collective-permute-start.55 = (bf16[16,2176]{1,0:T(8,128)(2,1)S(1)}, bf16[16,2176]{1,0:T(8,128)(2,1)S(1)}, u32[]{:S(2)}, u32[]{:S(2)}) collective-permute-start(bf16[16,2176]{1,0:T(8,128)(2,1)S(1)} %get-tuple-element.100), channel_id=1, source_target_pairs={{0,32},{8,40},{16,48},{24,56},{32,64},{40,72},{48,80},{56,88},{64,... | collective-permute-start | bytes 208904 | tf_op jit(solution)/shard_map/ppermute | solution.py:44
  149.4 5.8 %collective-permute-start.53 = (bf16[16,2176]{1,0:T(8,128)(2,1)S(1)}, bf16[16,2176]{1,0:T(8,128)(2,1)S(1)}, u32[]{:S(2)}, u32[]{:S(2)}) collective-permute-start(bf16[16,2176]{1,0:T(8,128)(2,1)S(1)} %get-tuple-element.101), channel_id=1, source_target_pairs={{0,64},{8,72},{16,80},{24,88},{32,96},{40,104},{48,112},{56,120},{... | collective-permute-start | bytes 208904 | tf_op jit(solution)/shard_map/ppermute | solution.py:44
  150.4 5.0 %collective-permute-start.51 = (bf16[16,2176]{1,0:T(8,128)(2,1)S(1)}, bf16[16,2176]{1,0:T(8,128)(2,1)S(1)}, u32[]{:S(2)}, u32[]{:S(2)}) collective-permute-start(bf16[16,2176]{1,0:T(8,128)(2,1)S(1)} %get-tuple-element.102), channel_id=1, source_target_pairs={{0,96},{8,104},{16,112},{24,120},{32,0},{40,8},{48,16},{56,24},{64... | collective-permute-start | bytes 208904 | tf_op jit(solution)/shard_map/ppermute | solution.py:44
  (4 other events, 16.8 us)

commit v3 on v2

--- a/solution.py
+++ b/solution.py
@@ -141,7 +141,7 @@
     core = place_ref[0]
     ours, theirs = refs[:count], refs[count : 2 * count]
     pair_ref, down_ref = refs[2 * count : 2 * count + 2]
-    keep_ref, send_ref, sides_out, hidden_out = refs[2 * count + 2 :]
+    send_ref, share_out, sides_out, hidden_out = refs[2 * count + 2 :]
     hid = down_ref.shape[0]
     wide = hidden_out.shape[1]
     here = pl.ds(pl.multiple_of(core * half, half), half)
@@ -165,31 +165,56 @@
     sides_out[:, wide + hid :] = rest
     share = jnp.sum(hidden.astype(F32) * grad, axis=1, keepdims=True).astype(BF)
     share = jnp.broadcast_to(share, (share.shape[0], LANES))
-    tile = 512
-    for base, out in ((core * half, keep_ref), ((1 - core) * half, send_ref)):
-        out[:, half:] = share
-
-        @pl.loop(0, half // tile)
-        def _(j):
-            where = pl.ds(pl.multiple_of(base + j * tile, tile), tile)
-            term = dot_f32(sides_out[...], pair_ref[:, where], 1, 0)
-            out[:, pl.ds(pl.multiple_of(j * tile, tile), tile)] = term.astype(BF)
+    share_out[...] = share
+    token_terms(sides_out, pair_ref, share, (1 - core) * half, send_ref)
+
+
+def token_terms(sides_ref, pair_ref, share, base, out):
+    half = out.shape[1] - LANES
+    tile = 1024
+    out[:, half:] = share
+
+    @pl.loop(0, half // tile)
+    def _(j):
+        where = pl.ds(pl.multiple_of(base + j * tile, tile), tile)
+        term = dot_f32(sides_ref[...], pair_ref[:, where], 1, 0)
+        out[:, pl.ds(pl.multiple_of(j * tile, tile), tile)] = term.astype(BF)
+
+
+def keep_kernel(half, place_ref, sides_ref, share_ref, pair_ref, out_ref):
+    token_terms(sides_ref, pair_ref, share_ref[...], place_ref[0] * half, out_ref)
+
+
+def keep_half(place, sides, share, pair):
+    rows = sides.shape[0]
+    half = pair.shape[1] // 2
+    return pl.pallas_call(
+        functools.partial(keep_kernel, half),
+        out_shape=jax.ShapeDtypeStruct((rows, half + LANES), BF),
+        in_specs=[SMEM] + [VMEM] * 3,
+        out_specs=VMEM,
+        compiler_params=pltpu.CompilerParams(vmem_limit_bytes=12 * MIB),
+        cost_estimate=pl.CostEstimate(
+            flops=2 * rows * pair.shape[0] * half, bytes_accessed=8 * MIB, transcendentals=0
+        ),
+        name="keep",
+    )(place, sides, share, pair)
 
 
 def run_group(place, ours, theirs, pair, down):
     rows = sum(r.shape[0] for r in ours)
     hid, width = down.shape
     half = width // 2
-    shapes = [jax.ShapeDtypeStruct((rows, half + LANES), BF)] * 2
-    shapes += [jax.ShapeDtypeStruct((rows, n * padded(hid)), BF) for n in (2, 1)]
+    lanes = (half + LANES, LANES, 2 * padded(hid), padded(hid))
+    shapes = [jax.ShapeDtypeStruct((rows, n), BF) for n in lanes]
     return pl.pallas_call(
         functools.partial(group_kernel, len(ours), half),
         out_shape=shapes,
         in_specs=[SMEM] + [VMEM] * (2 * len(ours) + 2),
         out_specs=[VMEM] * len(shapes),
-        compiler_params=pltpu.CompilerParams(vmem_limit_bytes=40 * MIB),
+        compiler_params=pltpu.CompilerParams(vmem_limit_bytes=20 * MIB),
         cost_estimate=pl.CostEstimate(
-            flops=10 * rows * hid * width, bytes_accessed=16 * MIB, transcendentals=rows * hid
+            flops=8 * rows * hid * width, bytes_accessed=16 * MIB, transcendentals=rows * hid
         ),
         name="group",
     )(place, *ours, *theirs, pair, down)
@@ -268,7 +293,7 @@
             pltpu.SemaphoreType.DMA((2, len(sizes))),
             pltpu.SemaphoreType.DMA((2, kinds)),
         ],
-        compiler_params=pltpu.CompilerParams(vmem_limit_bytes=28 * MIB),
+        compiler_params=pltpu.CompilerParams(vmem_limit_bytes=22 * MIB),
         cost_estimate=pl.CostEstimate(
             flops=2 * kinds * rows * hid * width, bytes_accessed=14 * MIB, transcendentals=0
         ),
@@ -360,20 +385,22 @@
             total = total + m.astype(F32)
         return total.astype(BF)
 
-    near_got = pair_core(near_out[1])
-    far_got = pair_core(far_out[1])
-
-    def chunk(out, got, i, a=0, b=packed):
-        return add(out[0][packed * i + a : packed * i + b], got[packed * i + a : packed * i + b])
-
-    t_last = [chunk(far_out, far_got, 3, third * i, third * (i + 1)) for i in range(3)]
+    far_got = pair_core(far_out[0])
+    near_got = pair_core(near_out[0])
+    far_keep = keep_half(place, far_out[2], far_out[1], pair_t)
+    near_keep = keep_half(place, near_out[2], near_out[1], pair_t)
+
+    def chunk(keep, got, i, a=0, b=packed):
+        return add(keep[packed * i + a : packed * i + b], got[packed * i + a : packed * i + b])
+
+    t_last = [chunk(far_keep, far_got, 3, third * i, third * (i + 1)) for i in range(3)]
     a_left = along_x(t_last[0], -1)
     a_right = along_x(t_last[1], 1)
     a_pair = pair_y(t_last[2])
     pads = [[(third * i, packed - third * (i + 1)), (0, 0)] for i in range(3)]
-    t_far_left = add(chunk(far_out, far_got, 0), jnp.pad(a_left, pads[0]))
-    t_far_right = add(chunk(far_out, far_got, 1), jnp.pad(a_right, pads[1]))
-    t_across = add(chunk(far_out, far_got, 2), jnp.pad(a_pair, pads[2]))
+    t_far_left = add(chunk(far_keep, far_got, 0), jnp.pad(a_left, pads[0]))
+    t_far_right = add(chunk(far_keep, far_got, 1), jnp.pad(a_right, pads[1]))
+    t_across = add(chunk(far_keep, far_got, 2), jnp.pad(a_pair, pads[2]))
     b_partner = along_x(t_far_left, -1)
     b_right_pair = pair_y(t_far_right)
     b_right = along_x(t_across, 1)
@@ -382,14 +409,14 @@
     gate_grad, up_grad = weight_grads(place, *rows, sides, 0, hid)
     tied = lax.optimization_barrier((b_partner, b_right_pair, b_right, gate_grad, up_grad))
     b_partner, b_right_pair, b_right, gate_grad, up_grad = tied
-    c_left = along_x(chunk(near_out, near_got, 1), -1)
-    c_right = along_x(add(chunk(near_out, near_got, 2), b_right_pair, b_right), 1)
-    c_pair = pair_y(add(chunk(near_out, near_got, 3), b_partner))
+    c_left = along_x(chunk(near_keep, near_got, 1), -1)
+    c_right = along_x(add(chunk(near_keep, near_got, 2), b_right_pair, b_right), 1)
+    c_pair = pair_y(add(chunk(near_keep, near_got, 3), b_partner))
     half = tokens.shape[1] // 2
     (down_grad,) = weight_grads(place, *rows, [near_out[3], far_out[3]], half, hid)
     tied = lax.optimization_barrier((c_left, c_right, c_pair, down_grad))
     c_left, c_right, c_pair, down_grad = tied
-    home = add(chunk(near_out, near_got, 0), c_left, c_right, c_pair)
+    home = add(chunk(near_keep, near_got, 0), c_left, c_right, c_pair)
 
     backs = [None] * EXPERTS
     for dy in range(2):

time: 158 us -> 156 us (0.987)
  waiting for transfers between devices: 43.4 us -> 48.6 us
  Pallas kernels: 43.9 us -> 38.8 us
  local copies, waits for them, and re-layouts: 4.56 us -> 1.93 us
    pallas_call x2, Pallas kernels: 22.5 us -> 13.1 us  [run_group(): pl.pallas_call(functools.partial(group_kernel, len(ours), half), out_shap...]
    ppermute x8, waiting for transfers between devices: 7.16 us -> 11.6 us  [pair_y(): return lax.ppermute(value, 'yl', [(0, 1), (1, 0)])]
    pallas_call x0 -> x2, Pallas kernels: none -> 4.22 us  [keep_half(): pl.pallas_call(functools.partial(keep_kernel, half), out_shape=jax.ShapeD...]
    ppermute x16, waiting for transfers between devices: 22.2 us -> 25.1 us  [along_x(): return lax.ppermute(value, 'x', [(i, (i + step) % 4) for i in range(4)])]
    unnamed x22 -> x16, local copies, waits for them, and re-layouts: 4.46 us -> 1.83 us
    ppermute x19, waiting for transfers between devices: 5.36 us -> 3.24 us  [pair_core(): return lax.ppermute(value, 'core', [(0, 1), (1, 0)])]
where the time goes in v3:
time: 156 us; the launch traced here: 154 us
  starting transfers between devices  60.3 us (39%)
  waiting for transfers between devices  48.6 us (31%)
  Pallas kernels  38.8 us (25%)
  local copies, waits for them, and re-layouts  1.93 us (1%)
  other arithmetic  1.89 us (1%)
    ppermute x14, starting transfers between devices, to_expert(): return lax.ppermute(value, ('z', 'yh', 'yl'), perm)  28.7 us
    ppermute x16, waiting for transfers between devices, along_x(): return lax.ppermute(value, 'x', [(i, (i + step) % 4) for i in range(4)])  25.1 us
    ppermute x16, starting transfers between devices, along_x(): return lax.ppermute(value, 'x', [(i, (i + step) % 4) for i in range(4)])  20.4 us
    pallas_call x2, Pallas kernels, weight_grads(): pl.pallas_call(functools.partial(weight_kernel, sizes, offset, width // 2...  17 us
    pallas_call x2, Pallas kernels, run_group(): pl.pallas_call(functools.partial(group_kernel, len(ours), half), out_shap...  13.1 us
    ppermute x8, waiting for transfers between devices, pair_y(): return lax.ppermute(value, 'yl', [(0, 1), (1, 0)])  11.6 us
    ppermute x14, waiting for transfers between devices, to_expert(): return lax.ppermute(value, ('z', 'yh', 'yl'), perm)  8.6 us
    ppermute x8, starting transfers between devices, pair_y(): return lax.ppermute(value, 'yl', [(0, 1), (1, 0)])  8.04 us
  transfers between devices with their start and end apart: 57, of which 29 were waited for; matrix products, arithmetic and copies ran while one was open for 1% of the time, Pallas kernels for 18%

profile of v3, /device:TPU:2, one launch (start us, length us, event | category | flops | bytes accessed | tf_op | source)
XLA Modules:
  0.0 153.8 jit_solution(18244833189620216547)
XLA Ops:
  0.6 0.7 pad_add_fusion.place_ref
  1.3 3.2 %slots.1 = (bf16[16,4096]{1,0:T(8,128)(2,1)}, bf16[16,4096]{1,0:T(8,128)(2,1)}, bf16[16,4096]{1,0:T(8,128)(2,1)}, bf16[16,4096]{1,0:T(8,128)(2,1)}, bf16[16,4096...) custom-call(s32[3]{0:T(128)} %pad_add_fusion.place_ref, ...), custom_call_target="tpu_custom_call" | custom-call | flops 50331648 | bytes 3145728 | tf_op jit(solution)/shard_map/slots/pallas_call | solution.py:97
  4.5 3.1 %collective-permute-start.5 = (bf16[16,4096]{1,0:T(8,128)(2,1)}, bf16[16,4096]{1,0:T(8,128)(2,1)S(1)}, u32[]{:S(2)}, u32[]{:S(2)}) collective-permute-start(bf16[16,4096]{1,0:T(8,128)(2,1)} %get-tuple-element.52), channel_id=1, source_target_pairs={{0,24},{8,16},{16,8},{24,0},{32,56},{40,48},{48,40},{56,32},{64,88... | collective-permute-start | bytes 393224 | tf_op jit(solution)/shard_map/ppermute | solution.py:44
  7.6 1.6 %collective-permute-start.6 = (bf16[16,4096]{1,0:T(8,128)(2,1)}, bf16[16,4096]{1,0:T(8,128)(2,1)S(1)}, u32[]{:S(2)}, u32[]{:S(2)}) collective-permute-start(bf16[16,4096]{1,0:T(8,128)(2,1)} %get-tuple-element.53), channel_id=1, source_target_pairs={{0,56},{8,48},{16,40},{24,32},{32,88},{40,80},{48,72},{56,64},{64,... | collective-permute-start | bytes 393224 | tf_op jit(solution)/shard_map/ppermute | solution.py:44
  9.2 6.0 %collective-permute-start.7 = (bf16[16,4096]{1,0:T(8,128)(2,1)}, bf16[16,4096]{1,0:T(8,128)(2,1)S(1)}, u32[]{:S(2)}, u32[]{:S(2)}) collective-permute-start(bf16[16,4096]{1,0:T(8,128)(2,1)} %get-tuple-element.54), channel_id=1, source_target_pairs={{0,88},{8,80},{16,72},{24,64},{32,120},{40,112},{48,104},{56,96},{... | collective-permute-start | bytes 393224 | tf_op jit(solution)/shard_map/ppermute | solution.py:44
  15.2 0.7 collective-permute-start.8
  15.9 1.0 collective-permute-start
  16.9 0.9 collective-permute-start.1
  17.8 0.9 collective-permute-done.6
  18.7 1.7 %collective-permute-start.2 = (bf16[16,4096]{1,0:T(8,128)(2,1)}, bf16[16,4096]{1,0:T(8,128)(2,1)S(1)}, u32[]{:S(2)}, u32[]{:S(2)}) collective-permute-start(bf16[16,4096]{1,0:T(8,128)(2,1)} %get-tuple-element.51), channel_id=1, source_target_pairs={{0,96},{8,104},{16,112},{24,120},{32,0},{40,8},{48,16},{56,24},{64... | collective-permute-start | bytes 393224 | tf_op jit(solution)/shard_map/ppermute | solution.py:44
  20.4 2.1 %collective-permute-done.7 = bf16[16,4096]{1,0:T(8,128)(2,1)S(1)} collective-permute-done((bf16[16,4096]{1,0:T(8,128)(2,1)}, bf16[16,4096]{1,0:T(8,128)(2,1)S(1)}, u32[]{:S(2)}, u32[]{:S(2)}) %collective-permute-start.7) | collective-permute-done | bytes 131104 | tf_op jit(solution)/shard_map/ppermute | solution.py:44
  23.0 1.6 %collective-permute-start.18 = (bf16[48,4096]{1,0:T(8,128)(2,1)S(1)}, bf16[48,4096]{1,0:T(8,128)(2,1)S(1)}, u32[]{:S(2)}, u32[]{:S(2)}) collective-permute-start(bf16[48,4096]{1,0:T(8,128)(2,1)S(1)} %convolution_convert_fusion.refs_1_), channel_id=1, source_target_pairs={{0,2},{2,4},{4,6},{6,0},{1,3},{3,5},{5,7},{7,1},{8,10},{10,12},{12... | collective-permute-start | bytes 1179656 | tf_op jit(solution)/shard_map/ppermute | solution.py:27
  25.1 1.7 %collective-permute-done.1 = bf16[16,4096]{1,0:T(8,128)(2,1)S(1)} collective-permute-done((bf16[16,4096]{1,0:T(8,128)(2,1)}, bf16[16,4096]{1,0:T(8,128)(2,1)S(1)}, u32[]{:S(2)}, u32[]{:S(2)}) %collective-permute-start.1) | collective-permute-done | bytes 131104 | tf_op jit(solution)/shard_map/ppermute | solution.py:44
  26.9 1.1 collective-permute-done.2
  28.4 1.5 %collective-permute-start.17 = (bf16[48,4096]{1,0:T(8,128)(2,1)S(1)}, bf16[48,4096]{1,0:T(8,128)(2,1)S(1)}, u32[]{:S(2)}, u32[]{:S(2)}) collective-permute-start(bf16[48,4096]{1,0:T(8,128)(2,1)S(1)} %convolution_convert_fusion.1.refs_0_), channel_id=1, source_target_pairs={{0,2},{2,4},{4,6},{6,0},{1,3},{3,5},{5,7},{7,1},{8,10},{10,12},{12... | collective-permute-start | bytes 1179656 | tf_op jit(solution)/shard_map/ppermute | solution.py:27
  29.9 5.1 %collective-permute-done.18.refs_3_ = bf16[48,4096]{1,0:T(8,128)(2,1)S(1)} collective-permute-done((bf16[48,4096]{1,0:T(8,128)(2,1)S(1)}, bf16[48,4096]{1,0:T(8,128)(2,1)S(1)}, u32[]{:S(2)}, u32[]{:S(2)}) %collective-permute-start.18) | collective-permute-done | bytes 393248 | tf_op jit(solution)/shard_map/ppermute | solution.py:27
  35.0 1.7 %collective-permute-start.11 = (bf16[48,4096]{1,0:T(8,128)(2,1)S(1)}, bf16[48,4096]{1,0:T(8,128)(2,1)S(1)}, u32[]{:S(2)}, u32[]{:S(2)}) collective-permute-start(bf16[48,4096]{1,0:T(8,128)(2,1)S(1)} %convolution_convert_fusion.1.refs_0_), channel_id=1, source_target_pairs={{0,6},{2,0},{4,2},{6,4},{1,7},{3,1},{5,3},{7,5},{8,14},{10,8},{12,... | collective-permute-start | bytes 1179656 | tf_op jit(solution)/shard_map/ppermute | solution.py:27
  36.8 1.6 %collective-permute-start.3 = (bf16[48,4096]{1,0:T(8,128)(2,1)S(1)}, bf16[48,4096]{1,0:T(8,128)(2,1)S(1)}, u32[]{:S(2)}, u32[]{:S(2)}) collective-permute-start(bf16[48,4096]{1,0:T(8,128)(2,1)S(1)} %convolution_convert_fusion.1.refs_0_), channel_id=1, source_target_pairs={{0,8},{8,0},{1,9},{9,1},{2,10},{10,2},{3,11},{11,3},{4,12},{12,4},... | collective-permute-start | bytes 1179656 | tf_op jit(solution)/shard_map/ppermute | solution.py:31
  38.9 4.0 %collective-permute-done.17.refs_2_ = bf16[48,4096]{1,0:T(8,128)(2,1)S(1)} collective-permute-done((bf16[48,4096]{1,0:T(8,128)(2,1)S(1)}, bf16[48,4096]{1,0:T(8,128)(2,1)S(1)}, u32[]{:S(2)}, u32[]{:S(2)}) %collective-permute-start.17) | collective-permute-done | bytes 393248 | tf_op jit(solution)/shard_map/ppermute | solution.py:27
  42.9 1.7 %collective-permute-start.16 = (bf16[48,4096]{1,0:T(8,128)(2,1)S(1)}, bf16[48,4096]{1,0:T(8,128)(2,1)S(1)}, u32[]{:S(2)}, u32[]{:S(2)}) collective-permute-start(bf16[48,4096]{1,0:T(8,128)(2,1)S(1)} %collective-permute-done.13.refs_5_), channel_id=1, source_target_pairs={{0,6},{2,0},{4,2},{6,4},{1,7},{3,1},{5,3},{7,5},{8,14},{10,8},{12,... | collective-permute-start | bytes 1179656 | tf_op jit(solution)/shard_map/ppermute | solution.py:27
  45.1 1.5 collective-permute-done.3.refs_6_
  47.2 1.8 %copy-done.1 = bf16[1,4096,344]{1,2,0:T(8,128)(2,1)S(1)} copy-done((bf16[1,4096,344]{1,2,0:T(8,128)(2,1)S(1)}, bf16[1,4096,344]{1,2,0:T(8,128)(2,1)}, u32[]{:S(2)}) %copy-start.1) | copy-done | bytes 2818072
  49.4 4.1 %collective-permute-done.16.refs_5_.refs_13_ = bf16[48,4096]{1,0:T(8,128)(2,1)S(1)} collective-permute-done((bf16[48,4096]{1,0:T(8,128)(2,1)S(1)}, bf16[48,4096]{1,0:T(8,128)(2,1)S(1)}, u32[]{:S(2)}, u32[]{:S(2)}) %collective-permute-start.16) | collective-permute-done | bytes 393248 | tf_op jit(solution)/shard_map/ppermute | solution.py:27
  53.5 0.8 collective-permute-start.14
  54.3 1.5 collective-permute-start.10
  56.3 1.3 collective-permute-start.12
  57.6 2.0 %collective-permute-start.4 = (bf16[48,4096]{1,0:T(8,128)(2,1)S(1)}, bf16[48,4096]{1,0:T(8,128)(2,1)S(1)}, u32[]{:S(2)}, u32[]{:S(2)}) collective-permute-start(bf16[48,4096]{1,0:T(8,128)(2,1)S(1)} %collective-permute-done.3.refs_6_), channel_id=1, source_target_pairs={{0,2},{2,4},{4,6},{6,0},{1,3},{3,5},{5,7},{7,1},{8,10},{10,12},{12... | collective-permute-start | bytes 1179656 | tf_op jit(solution)/shard_map/ppermute | solution.py:27
  59.5 6.6 %group.2 = (bf16[384,2176]{1,0:T(8,128)(2,1)S(1)}, bf16[384,128]{1,0:T(8,128)(2,1)S(1)}, bf16[384,768]{1,0:T(8,128)(2,1)S(1)}, bf16[384,384]{1,0:T(8,128)(2,1)S(1)}) custom-call(s32[3]{0:T(128)S(1)} %copy-done.2, bf16[48,4096]{1,0:T(8,128)(2,1)S(1)} %convolution_convert_fusion.1.refs_0_, bf16[48,4096]{1,0:T(8,128)(2,1)S(1)} %convolution_convert_fusion.refs_1_, ...), custom_call_target="tpu_custom_call" | custom-call | flops 4328521728 | bytes 16777216 | tf_op jit(solution)/shard_map/group/pallas_call | solution.py:210
  66.3 5.4 %collective-permute-done.12.refs_2_.refs_10_ = bf16[48,4096]{1,0:T(8,128)(2,1)S(1)} collective-permute-done((bf16[48,4096]{1,0:T(8,128)(2,1)S(1)}, bf16[48,4096]{1,0:T(8,128)(2,1)S(1)}, u32[]{:S(2)}, u32[]{:S(2)}) %collective-permute-start.12) | collective-permute-done | bytes 393248 | tf_op jit(solution)/shard_map/ppermute | solution.py:31
  71.7 0.9 collective-permute-done.4.refs_0_.refs_8_
  72.7 0.9 collective-permute-start.31
  73.6 1.5 collective-permute-start.29
  75.1 1.5 collective-permute-start.30
  76.9 2.3 %collective-permute-done.31.refs_8_.refs_16_ = bf16[32,4096]{1,0:T(8,128)(2,1)S(1)} collective-permute-done((bf16[32,4096]{1,0:T(8,128)(2,1)S(1)}, bf16[32,4096]{1,0:T(8,128)(2,1)S(1)}, u32[]{:S(2)}, u32[]{:S(2)}) %collective-permute-start.31) | collective-permute-done | bytes 262176 | tf_op jit(solution)/shard_map/ppermute | solution.py:31
  79.1 1.8 %collective-permute-done.29.refs_6_.refs_14_ = bf16[32,4096]{1,0:T(8,128)(2,1)S(1)} collective-permute-done((bf16[32,4096]{1,0:T(8,128)(2,1)S(1)}, bf16[32,4096]{1,0:T(8,128)(2,1)S(1)}, u32[]{:S(2)}, u32[]{:S(2)}) %collective-permute-start.29) | collective-permute-done | bytes 262176 | tf_op jit(solution)/shard_map/ppermute | solution.py:27
  80.9 3.7 %collective-permute-done.30.refs_7_.refs_15_ = bf16[32,4096]{1,0:T(8,128)(2,1)S(1)} collective-permute-done((bf16[32,4096]{1,0:T(8,128)(2,1)S(1)}, bf16[32,4096]{1,0:T(8,128)(2,1)S(1)}, u32[]{:S(2)}, u32[]{:S(2)}) %collective-permute-start.30) | collective-permute-done | bytes 262176 | tf_op jit(solution)/shard_map/ppermute | solution.py:27
  85.7 0.6 collective-permute-done.35.refs_12_.refs_28_
  86.3 0.6 collective-permute-done.37.refs_14_.refs_30_
  88.0 6.6 %group.3 = (bf16[384,2176]{1,0:T(8,128)(2,1)S(1)}, bf16[384,128]{1,0:T(8,128)(2,1)S(1)}, bf16[384,768]{1,0:T(8,128)(2,1)S(1)}, bf16[384,384]{1,0:T(8,128)(2,1)S(1)}) custom-call(s32[3]{0:T(128)S(1)} %copy-done.2, bf16[48,4096]{1,0:T(8,128)(2,1)S(1)} %collective-permute-done.4.refs_0_.refs_8_, bf16[48,4096]{1,0:T(8,128)(2,1)S(1)} %collective-permute-done.10.refs_1_.refs_9_, ...), custom_call_target="tpu_custom_call" | custom-call | flops 4328521728 | bytes 16777216 | tf_op jit(solution)/shard_map/group/pallas_call | solution.py:210
  95.1 2.1 %keep.3 = bf16[384,2176]{1,0:T(8,128)(2,1)S(1)} custom-call(s32[3]{0:T(128)S(1)} %copy-done.2, bf16[384,768]{1,0:T(8,128)(2,1)S(1)} %get-tuple-element.69.sides_ref.refs_35_, bf16[384,128]{1,0:T(8,128)(2,1)S(1)} %get-tuple-element.70.share_ref, bf16[768,4096]{1,0:T(8,128)(2,1)S(1)} %stack.17.refs_16_.pair_ref.refs_18_), custom_call_target="tpu_custom_call" | custom-call | flops 1207959552 | bytes 8388608 | tf_op jit(solution)/shard_map/keep/pallas_call | solution.py:191
  97.2 0.9 collective-permute-done.41
  98.3 1.3 collective-permute-start.46
  99.6 1.7 %collective-permute-start.44 = (bf16[32,2176]{1,0:T(8,128)(2,1)S(1)}, bf16[32,2176]{1,0:T(8,128)(2,1)S(1)}, u32[]{:S(2)}, u32[]{:S(2)}) collective-permute-start(bf16[32,2176]{1,0:T(8,128)(2,1)S(1)} %get-tuple-element.94), channel_id=1, source_target_pairs={{0,2},{2,4},{4,6},{6,0},{1,3},{3,5},{5,7},{7,1},{8,10},{10,12},{12... | collective-permute-start | bytes 417800 | tf_op jit(solution)/shard_map/ppermute | solution.py:27
  101.6 2.5 %collective-permute-done.46 = bf16[32,2176]{1,0:T(8,128)(2,1)S(1)} collective-permute-done((bf16[32,2176]{1,0:T(8,128)(2,1)S(1)}, bf16[32,2176]{1,0:T(8,128)(2,1)S(1)}, u32[]{:S(2)}, u32[]{:S(2)}) %collective-permute-start.46) | collective-permute-done | bytes 139296 | tf_op jit(solution)/shard_map/ppermute | solution.py:31
  104.1 0.9 collective-permute-done.44
  105.0 2.4 %collective-permute-done.42 = bf16[32,2176]{1,0:T(8,128)(2,1)S(1)} collective-permute-done((bf16[32,2176]{1,0:T(8,128)(2,1)S(1)}, bf16[32,2176]{1,0:T(8,128)(2,1)S(1)}, u32[]{:S(2)}, u32[]{:S(2)}) %collective-permute-start.42) | collective-permute-done | bytes 139296 | tf_op jit(solution)/shard_map/ppermute | solution.py:27
  107.8 1.8 %collective-permute-start.47 = (bf16[96,2176]{1,0:T(8,128)(2,1)S(1)}, bf16[96,2176]{1,0:T(8,128)(2,1)S(1)}, u32[]{:S(2)}, u32[]{:S(2)}) collective-permute-start(bf16[96,2176]{1,0:T(8,128)(2,1)S(1)} %get-tuple-element.90), channel_id=1, source_target_pairs={{0,2},{2,4},{4,6},{6,0},{1,3},{3,5},{5,7},{7,1},{8,10},{10,12},{12... | collective-permute-start | bytes 1253384 | tf_op jit(solution)/shard_map/ppermute | solution.py:27
  109.6 1.0 collective-permute-start.45
  110.9 2.1 %keep.2 = bf16[384,2176]{1,0:T(8,128)(2,1)S(1)} custom-call(s32[3]{0:T(128)S(1)} %copy-done.2, bf16[384,768]{1,0:T(8,128)(2,1)S(1)} %get-tuple-element.60.sides_ref.refs_34_, bf16[384,128]{1,0:T(8,128)(2,1)S(1)} %get-tuple-element.61.share_ref, bf16[768,4096]{1,0:T(8,128)(2,1)S(1)} %stack.17.refs_16_.pair_ref.refs_18_), custom_call_target="tpu_custom_call" | custom-call | flops 1207959552 | bytes 8388608 | tf_op jit(solution)/shard_map/keep/pallas_call | solution.py:191
  113.0 10.0 %weight_grads.2 = (bf16[344,4096]{1,0:T(8,128)(2,1)}, bf16[344,4096]{1,0:T(8,128)(2,1)}) custom-call(s32[3]{0:T(128)S(1)} %copy-done.2, bf16[48,4096]{1,0:T(8,128)(2,1)S(1)} %convolution_convert_fusion.1.refs_0_, bf16[48,4096]{1,0:T(8,128)(2,1)S(1)} %convolution_convert_fusion.refs_1_, bf16[48,4096]{1,0:T(8,128)(2,1)S(1)} %collective-permute-done.17.refs_2_, ...), custom_call_target="tpu_custom_call" | custom-call | flops 4328521728 | bytes 14680064 | tf_op jit(solution)/shard_map/weight_grads/pallas_call | solution.py:284
  123.6 1.1 collective-permute-start.49
  124.7 1.8 %collective-permute-start.48 = (bf16[96,2176]{1,0:T(8,128)(2,1)S(1)}, bf16[96,2176]{1,0:T(8,128)(2,1)S(1)}, u32[]{:S(2)}, u32[]{:S(2)}) collective-permute-start(bf16[96,2176]{1,0:T(8,128)(2,1)S(1)} %get-tuple-element.88), channel_id=1, source_target_pairs={{0,2},{2,4},{4,6},{6,0},{1,3},{3,5},{5,7},{7,1},{8,10},{10,12},{12... | collective-permute-start | bytes 1253384 | tf_op jit(solution)/shard_map/ppermute | solution.py:27
  126.8 7.0 %weight_grads.3 = bf16[344,4096]{1,0:T(8,128)(2,1)} custom-call(s32[3]{0:T(128)S(1)} %copy-done.2, bf16[48,4096]{1,0:T(8,128)(2,1)S(1)} %convolution_convert_fusion.1.refs_0_, bf16[48,4096]{1,0:T(8,128)(2,1)S(1)} %convolution_convert_fusion.refs_1_, bf16[48,4096]{1,0:T(8,128)(2,1)S(1)} %collective-permute-done.17.refs_2_, ...), custom_call_target="tpu_custom_call" | custom-call | flops 2164260864 | bytes 14680064 | tf_op jit(solution)/shard_map/weight_grads/pallas_call | solution.py:284
  133.8 1.0 collective-permute-done.48
  134.7 0.6 collective-permute-done.28
  136.3 3.5 %collective-permute-start.56 = (bf16[16,2176]{1,0:T(8,128)(2,1)S(1)}, bf16[16,2176]{1,0:T(8,128)(2,1)S(1)}, u32[]{:S(2)}, u32[]{:S(2)}) collective-permute-start(bf16[16,2176]{1,0:T(8,128)(2,1)S(1)} %get-tuple-element.96), channel_id=1, source_target_pairs={{0,56},{8,48},{16,40},{24,32},{32,88},{40,80},{48,72},{56,64},{64,... | collective-permute-start | bytes 208904 | tf_op jit(solution)/shard_map/ppermute | solution.py:44
  139.8 2.4 %collective-permute-start.54 = (bf16[16,2176]{1,0:T(8,128)(2,1)S(1)}, bf16[16,2176]{1,0:T(8,128)(2,1)S(1)}, u32[]{:S(2)}, u32[]{:S(2)}) collective-permute-start(bf16[16,2176]{1,0:T(8,128)(2,1)S(1)} %get-tuple-element.97), channel_id=1, source_target_pairs={{0,88},{8,80},{16,72},{24,64},{32,120},{40,112},{48,104},{56,96},{... | collective-permute-start | bytes 208904 | tf_op jit(solution)/shard_map/ppermute | solution.py:44
  142.3 3.1 %collective-permute-start.52 = (bf16[16,2176]{1,0:T(8,128)(2,1)S(1)}, bf16[16,2176]{1,0:T(8,128)(2,1)S(1)}, u32[]{:S(2)}, u32[]{:S(2)}) collective-permute-start(bf16[16,2176]{1,0:T(8,128)(2,1)S(1)} %get-tuple-element.98), channel_id=1, source_target_pairs={{0,120},{8,112},{16,104},{24,96},{32,24},{40,16},{48,8},{56,0},{64... | collective-permute-start | bytes 208904 | tf_op jit(solution)/shard_map/ppermute | solution.py:44
  145.7 1.4 collective-permute-start.55
  147.1 1.0 collective-permute-start.53
  148.1 2.0 %collective-permute-start.51 = (bf16[16,2176]{1,0:T(8,128)(2,1)S(1)}, bf16[16,2176]{1,0:T(8,128)(2,1)S(1)}, u32[]{:S(2)}, u32[]{:S(2)}) collective-permute-start(bf16[16,2176]{1,0:T(8,128)(2,1)S(1)} %get-tuple-element.102), channel_id=1, source_target_pairs={{0,96},{8,104},{16,112},{24,120},{32,0},{40,8},{48,16},{56,24},{64... | collective-permute-start | bytes 208904 | tf_op jit(solution)/shard_map/ppermute | solution.py:44
  150.1 0.9 collective-permute-done.50.refs_1_
  151.2 1.7 %collective-permute-done.53.refs_4_ = bf16[16,2176]{1,0:T(8,128)(2,1)S(1)} collective-permute-done((bf16[16,2176]{1,0:T(8,128)(2,1)S(1)}, bf16[16,2176]{1,0:T(8,128)(2,1)S(1)}, u32[]{:S(2)}, u32[]{:S(2)}) %collective-permute-start.53) | collective-permute-done | bytes 69664 | tf_op jit(solution)/shard_map/ppermute | solution.py:44
  152.9 0.9 combine.1
  (92 shorter events, 10.7 us)
Async XLA Ops:
  4.5 23.5 %copy-start.7 = (bf16[16,4096]{1,0:T(8,128)(2,1)S(1)}, bf16[16,4096]{1,0:T(8,128)(2,1)}, u32[]{:S(2)}) copy-start(bf16[16,4096]{1,0:T(8,128)(2,1)} %get-tuple-element.48) | copy-start | bytes 393220
  4.5 12.4 %collective-permute-start.5 = (bf16[16,4096]{1,0:T(8,128)(2,1)}, bf16[16,4096]{1,0:T(8,128)(2,1)S(1)}, u32[]{:S(2)}, u32[]{:S(2)}) collective-permute-start(bf16[16,4096]{1,0:T(8,128)(2,1)} %get-tuple-element.52), channel_id=1, source_target_pairs={{0,24},{8,16},{16,8},{24,0},{32,56},{40,48},{48,40},{56,32},{64,88... | collective-permute-start | bytes 393224 | tf_op jit(solution)/shard_map/ppermute | solution.py:44
  7.6 11.1 %collective-permute-start.6 = (bf16[16,4096]{1,0:T(8,128)(2,1)}, bf16[16,4096]{1,0:T(8,128)(2,1)S(1)}, u32[]{:S(2)}, u32[]{:S(2)}) collective-permute-start(bf16[16,4096]{1,0:T(8,128)(2,1)} %get-tuple-element.53), channel_id=1, source_target_pairs={{0,56},{8,48},{16,40},{24,32},{32,88},{40,80},{48,72},{56,64},{64,... | collective-permute-start | bytes 393224 | tf_op jit(solution)/shard_map/ppermute | solution.py:44
  9.2 13.4 %collective-permute-start.7 = (bf16[16,4096]{1,0:T(8,128)(2,1)}, bf16[16,4096]{1,0:T(8,128)(2,1)S(1)}, u32[]{:S(2)}, u32[]{:S(2)}) collective-permute-start(bf16[16,4096]{1,0:T(8,128)(2,1)} %get-tuple-element.54), channel_id=1, source_target_pairs={{0,88},{8,80},{16,72},{24,64},{32,120},{40,112},{48,104},{56,96},{... | collective-permute-start | bytes 393224 | tf_op jit(solution)/shard_map/ppermute | solution.py:44
  15.2 7.4 %collective-permute-start.8 = (bf16[16,4096]{1,0:T(8,128)(2,1)}, bf16[16,4096]{1,0:T(8,128)(2,1)S(1)}, u32[]{:S(2)}, u32[]{:S(2)}) collective-permute-start(bf16[16,4096]{1,0:T(8,128)(2,1)} %get-tuple-element.55), channel_id=1, source_target_pairs={{0,120},{8,112},{16,104},{24,96},{32,24},{40,16},{48,8},{56,0},{64... | collective-permute-start | bytes 393224 | tf_op jit(solution)/shard_map/ppermute | solution.py:44
  15.9 8.7 %collective-permute-start = (bf16[16,4096]{1,0:T(8,128)(2,1)}, bf16[16,4096]{1,0:T(8,128)(2,1)S(1)}, u32[]{:S(2)}, u32[]{:S(2)}) collective-permute-start(bf16[16,4096]{1,0:T(8,128)(2,1)} %get-tuple-element.49), channel_id=1, source_target_pairs={{0,32},{8,40},{16,48},{24,56},{32,64},{40,72},{48,80},{56,88},{64,... | collective-permute-start | bytes 393224 | tf_op jit(solution)/shard_map/ppermute | solution.py:44
  16.9 9.8 %collective-permute-start.1 = (bf16[16,4096]{1,0:T(8,128)(2,1)}, bf16[16,4096]{1,0:T(8,128)(2,1)S(1)}, u32[]{:S(2)}, u32[]{:S(2)}) collective-permute-start(bf16[16,4096]{1,0:T(8,128)(2,1)} %get-tuple-element.50), channel_id=1, source_target_pairs={{0,64},{8,72},{16,80},{24,88},{32,96},{40,104},{48,112},{56,120},{... | collective-permute-start | bytes 393224 | tf_op jit(solution)/shard_map/ppermute | solution.py:44
  18.7 28.5 %copy-start = (bf16[1,4096,344]{1,2,0:T(8,128)(2,1)S(1)}, bf16[1,4096,344]{1,2,0:T(8,128)(2,1)}, u32[]{:S(2)}) copy-start(bf16[1,4096,344]{1,2,0:T(8,128)(2,1)} %param.11) | copy-start | bytes 8454148
  18.7 9.3 %collective-permute-start.2 = (bf16[16,4096]{1,0:T(8,128)(2,1)}, bf16[16,4096]{1,0:T(8,128)(2,1)S(1)}, u32[]{:S(2)}, u32[]{:S(2)}) collective-permute-start(bf16[16,4096]{1,0:T(8,128)(2,1)} %get-tuple-element.51), channel_id=1, source_target_pairs={{0,96},{8,104},{16,112},{24,120},{32,0},{40,8},{48,16},{56,24},{64... | collective-permute-start | bytes 393224 | tf_op jit(solution)/shard_map/ppermute | solution.py:44
  22.9 5.5 %collective-permute-start.20 = (bf16[48,4096]{1,0:T(8,128)(2,1)S(1)}, bf16[48,4096]{1,0:T(8,128)(2,1)S(1)}, u32[]{:S(2)}, u32[]{:S(2)}) collective-permute-start(bf16[48,4096]{1,0:T(8,128)(2,1)S(1)} %convolution_convert_fusion.refs_1_), channel_id=1, source_target_pairs={{0,1},{1,0},{2,3},{3,2},{4,5},{5,4},{6,7},{7,6},{8,9},{9,8},{10,11... | collective-permute-start | bytes 1179656 | tf_op jit(solution)/shard_map/ppermute | solution.py:35
  23.0 12.1 %collective-permute-start.18 = (bf16[48,4096]{1,0:T(8,128)(2,1)S(1)}, bf16[48,4096]{1,0:T(8,128)(2,1)S(1)}, u32[]{:S(2)}, u32[]{:S(2)}) collective-permute-start(bf16[48,4096]{1,0:T(8,128)(2,1)S(1)} %convolution_convert_fusion.refs_1_), channel_id=1, source_target_pairs={{0,2},{2,4},{4,6},{6,0},{1,3},{3,5},{5,7},{7,1},{8,10},{10,12},{12... | collective-permute-start | bytes 1179656 | tf_op jit(solution)/shard_map/ppermute | solution.py:27
  24.5 12.2 %collective-permute-start.13 = (bf16[48,4096]{1,0:T(8,128)(2,1)S(1)}, bf16[48,4096]{1,0:T(8,128)(2,1)S(1)}, u32[]{:S(2)}, u32[]{:S(2)}) collective-permute-start(bf16[48,4096]{1,0:T(8,128)(2,1)S(1)} %convolution_convert_fusion.refs_1_), channel_id=1, source_target_pairs={{0,6},{2,0},{4,2},{6,4},{1,7},{3,1},{5,3},{7,5},{8,14},{10,8},{12,... | collective-permute-start | bytes 1179656 | tf_op jit(solution)/shard_map/ppermute | solution.py:27
  26.8 11.6 %collective-permute-start.9 = (bf16[48,4096]{1,0:T(8,128)(2,1)S(1)}, bf16[48,4096]{1,0:T(8,128)(2,1)S(1)}, u32[]{:S(2)}, u32[]{:S(2)}) collective-permute-start(bf16[48,4096]{1,0:T(8,128)(2,1)S(1)} %convolution_convert_fusion.refs_1_), channel_id=1, source_target_pairs={{0,8},{8,0},{1,9},{9,1},{2,10},{10,2},{3,11},{11,3},{4,12},{12,4},... | collective-permute-start | bytes 1179656 | tf_op jit(solution)/shard_map/ppermute | solution.py:31
  28.3 10.1 %collective-permute-start.19 = (bf16[48,4096]{1,0:T(8,128)(2,1)S(1)}, bf16[48,4096]{1,0:T(8,128)(2,1)S(1)}, u32[]{:S(2)}, u32[]{:S(2)}) collective-permute-start(bf16[48,4096]{1,0:T(8,128)(2,1)S(1)} %convolution_convert_fusion.1.refs_0_), channel_id=1, source_target_pairs={{0,1},{1,0},{2,3},{3,2},{4,5},{5,4},{6,7},{7,6},{8,9},{9,8},{10,11... | collective-permute-start | bytes 1179656 | tf_op jit(solution)/shard_map/ppermute | solution.py:35
  28.4 14.5 %collective-permute-start.17 = (bf16[48,4096]{1,0:T(8,128)(2,1)S(1)}, bf16[48,4096]{1,0:T(8,128)(2,1)S(1)}, u32[]{:S(2)}, u32[]{:S(2)}) collective-permute-start(bf16[48,4096]{1,0:T(8,128)(2,1)S(1)} %convolution_convert_fusion.1.refs_0_), channel_id=1, source_target_pairs={{0,2},{2,4},{4,6},{6,0},{1,3},{3,5},{5,7},{7,1},{8,10},{10,12},{12... | collective-permute-start | bytes 1179656 | tf_op jit(solution)/shard_map/ppermute | solution.py:27
  35.0 10.1 %collective-permute-start.11 = (bf16[48,4096]{1,0:T(8,128)(2,1)S(1)}, bf16[48,4096]{1,0:T(8,128)(2,1)S(1)}, u32[]{:S(2)}, u32[]{:S(2)}) collective-permute-start(bf16[48,4096]{1,0:T(8,128)(2,1)S(1)} %convolution_convert_fusion.1.refs_0_), channel_id=1, source_target_pairs={{0,6},{2,0},{4,2},{6,4},{1,7},{3,1},{5,3},{7,5},{8,14},{10,8},{12,... | collective-permute-start | bytes 1179656 | tf_op jit(solution)/shard_map/ppermute | solution.py:27
  36.8 9.8 %collective-permute-start.3 = (bf16[48,4096]{1,0:T(8,128)(2,1)S(1)}, bf16[48,4096]{1,0:T(8,128)(2,1)S(1)}, u32[]{:S(2)}, u32[]{:S(2)}) collective-permute-start(bf16[48,4096]{1,0:T(8,128)(2,1)S(1)} %convolution_convert_fusion.1.refs_0_), channel_id=1, source_target_pairs={{0,8},{8,0},{1,9},{9,1},{2,10},{10,2},{3,11},{11,3},{4,12},{12,4},... | collective-permute-start | bytes 1179656 | tf_op jit(solution)/shard_map/ppermute | solution.py:31
  38.4 8.2 %collective-permute-start.22 = (bf16[48,4096]{1,0:T(8,128)(2,1)S(1)}, bf16[48,4096]{1,0:T(8,128)(2,1)S(1)}, u32[]{:S(2)}, u32[]{:S(2)}) collective-permute-start(bf16[48,4096]{1,0:T(8,128)(2,1)S(1)} %collective-permute-done.18.refs_3_), channel_id=1, source_target_pairs={{0,1},{1,0},{2,3},{3,2},{4,5},{5,4},{6,7},{7,6},{8,9},{9,8},{10,11... | collective-permute-start | bytes 1179656 | tf_op jit(solution)/shard_map/ppermute | solution.py:35
  38.4 8.7 %collective-permute-start.24 = (bf16[48,4096]{1,0:T(8,128)(2,1)S(1)}, bf16[48,4096]{1,0:T(8,128)(2,1)S(1)}, u32[]{:S(2)}, u32[]{:S(2)}) collective-permute-start(bf16[48,4096]{1,0:T(8,128)(2,1)S(1)} %collective-permute-done.13.refs_5_), channel_id=1, source_target_pairs={{0,1},{1,0},{2,3},{3,2},{4,5},{5,4},{6,7},{7,6},{8,9},{9,8},{10,11... | collective-permute-start | bytes 1179656 | tf_op jit(solution)/shard_map/ppermute | solution.py:35
  42.9 10.6 %collective-permute-start.16 = (bf16[48,4096]{1,0:T(8,128)(2,1)S(1)}, bf16[48,4096]{1,0:T(8,128)(2,1)S(1)}, u32[]{:S(2)}, u32[]{:S(2)}) collective-permute-start(bf16[48,4096]{1,0:T(8,128)(2,1)S(1)} %collective-permute-done.13.refs_5_), channel_id=1, source_target_pairs={{0,6},{2,0},{4,2},{6,4},{1,7},{3,1},{5,3},{7,5},{8,14},{10,8},{12,... | collective-permute-start | bytes 1179656 | tf_op jit(solution)/shard_map/ppermute | solution.py:27
  45.1 9.2 %collective-permute-start.26 = (bf16[48,4096]{1,0:T(8,128)(2,1)S(1)}, bf16[48,4096]{1,0:T(8,128)(2,1)S(1)}, u32[]{:S(2)}, u32[]{:S(2)}) collective-permute-start(bf16[48,4096]{1,0:T(8,128)(2,1)S(1)} %collective-permute-done.9.refs_7_), channel_id=1, source_target_pairs={{0,1},{1,0},{2,3},{3,2},{4,5},{5,4},{6,7},{7,6},{8,9},{9,8},{10,11... | collective-permute-start | bytes 1179656 | tf_op jit(solution)/shard_map/ppermute | solution.py:35
  46.5 9.2 %collective-permute-start.21 = (bf16[48,4096]{1,0:T(8,128)(2,1)S(1)}, bf16[48,4096]{1,0:T(8,128)(2,1)S(1)}, u32[]{:S(2)}, u32[]{:S(2)}) collective-permute-start(bf16[48,4096]{1,0:T(8,128)(2,1)S(1)} %collective-permute-done.17.refs_2_), channel_id=1, source_target_pairs={{0,1},{1,0},{2,3},{3,2},{4,5},{5,4},{6,7},{7,6},{8,9},{9,8},{10,11... | collective-permute-start | bytes 1179656 | tf_op jit(solution)/shard_map/ppermute | solution.py:35
  46.6 9.7 %collective-permute-start.23 = (bf16[48,4096]{1,0:T(8,128)(2,1)S(1)}, bf16[48,4096]{1,0:T(8,128)(2,1)S(1)}, u32[]{:S(2)}, u32[]{:S(2)}) collective-permute-start(bf16[48,4096]{1,0:T(8,128)(2,1)S(1)} %collective-permute-done.11.refs_4_), channel_id=1, source_target_pairs={{0,1},{1,0},{2,3},{3,2},{4,5},{5,4},{6,7},{7,6},{8,9},{9,8},{10,11... | collective-permute-start | bytes 1179656 | tf_op jit(solution)/shard_map/ppermute | solution.py:35
  47.1 10.5 %collective-permute-start.25 = (bf16[48,4096]{1,0:T(8,128)(2,1)S(1)}, bf16[48,4096]{1,0:T(8,128)(2,1)S(1)}, u32[]{:S(2)}, u32[]{:S(2)}) collective-permute-start(bf16[48,4096]{1,0:T(8,128)(2,1)S(1)} %collective-permute-done.3.refs_6_), channel_id=1, source_target_pairs={{0,1},{1,0},{2,3},{3,2},{4,5},{5,4},{6,7},{7,6},{8,9},{9,8},{10,11... | collective-permute-start | bytes 1179656 | tf_op jit(solution)/shard_map/ppermute | solution.py:35
  49.0 10.6 %copy-start.2 = (s32[3]{0:T(128)S(1)}, s32[3]{0:T(128)}, u32[]{:S(2)}) copy-start(s32[3]{0:T(128)} %pad_add_fusion.place_ref) | copy-start | bytes 40
  49.0 10.6 %copy-start.6 = (bf16[1,344,4096]{2,1,0:T(8,128)(2,1)S(1)}, bf16[1,344,4096]{2,1,0:T(8,128)(2,1)}, u32[]{:S(2)}) copy-start(bf16[1,344,4096]{2,1,0:T(8,128)(2,1)} %param.13) | copy-start | bytes 8454148
  53.5 12.6 %collective-permute-start.14 = (bf16[48,4096]{1,0:T(8,128)(2,1)S(1)}, bf16[48,4096]{1,0:T(8,128)(2,1)S(1)}, u32[]{:S(2)}, u32[]{:S(2)}) collective-permute-start(bf16[48,4096]{1,0:T(8,128)(2,1)S(1)} %collective-permute-done.13.refs_5_), channel_id=1, source_target_pairs={{0,8},{8,0},{1,9},{9,1},{2,10},{10,2},{3,11},{11,3},{4,12},{12,4},... | collective-permute-start | bytes 1179656 | tf_op jit(solution)/shard_map/ppermute | solution.py:31
  54.3 12.0 %collective-permute-start.10 = (bf16[48,4096]{1,0:T(8,128)(2,1)S(1)}, bf16[48,4096]{1,0:T(8,128)(2,1)S(1)}, u32[]{:S(2)}, u32[]{:S(2)}) collective-permute-start(bf16[48,4096]{1,0:T(8,128)(2,1)S(1)} %collective-permute-done.9.refs_7_), channel_id=1, source_target_pairs={{0,2},{2,4},{4,6},{6,0},{1,3},{3,5},{5,7},{7,1},{8,10},{10,12},{12... | collective-permute-start | bytes 1179656 | tf_op jit(solution)/shard_map/ppermute | solution.py:27
  55.8 10.5 %collective-permute-start.15 = (bf16[48,4096]{1,0:T(8,128)(2,1)S(1)}, bf16[48,4096]{1,0:T(8,128)(2,1)S(1)}, u32[]{:S(2)}, u32[]{:S(2)}) collective-permute-start(bf16[48,4096]{1,0:T(8,128)(2,1)S(1)} %collective-permute-done.11.refs_4_), channel_id=1, source_target_pairs={{0,6},{2,0},{4,2},{6,4},{1,7},{3,1},{5,3},{7,5},{8,14},{10,8},{12,... | collective-permute-start | bytes 1179656 | tf_op jit(solution)/shard_map/ppermute | solution.py:27
  56.3 15.4 %collective-permute-start.12 = (bf16[48,4096]{1,0:T(8,128)(2,1)S(1)}, bf16[48,4096]{1,0:T(8,128)(2,1)S(1)}, u32[]{:S(2)}, u32[]{:S(2)}) collective-permute-start(bf16[48,4096]{1,0:T(8,128)(2,1)S(1)} %collective-permute-done.11.refs_4_), channel_id=1, source_target_pairs={{0,8},{8,0},{1,9},{9,1},{2,10},{10,2},{3,11},{11,3},{4,12},{12,4},... | collective-permute-start | bytes 1179656 | tf_op jit(solution)/shard_map/ppermute | solution.py:31
  57.6 15.0 %collective-permute-start.4 = (bf16[48,4096]{1,0:T(8,128)(2,1)S(1)}, bf16[48,4096]{1,0:T(8,128)(2,1)S(1)}, u32[]{:S(2)}, u32[]{:S(2)}) collective-permute-start(bf16[48,4096]{1,0:T(8,128)(2,1)S(1)} %collective-permute-done.3.refs_6_), channel_id=1, source_target_pairs={{0,2},{2,4},{4,6},{6,0},{1,3},{3,5},{5,7},{7,1},{8,10},{10,12},{12... | collective-permute-start | bytes 1179656 | tf_op jit(solution)/shard_map/ppermute | solution.py:27
  72.7 6.5 %collective-permute-start.31 = (bf16[32,4096]{1,0:T(8,128)(2,1)S(1)}, bf16[32,4096]{1,0:T(8,128)(2,1)S(1)}, u32[]{:S(2)}, u32[]{:S(2)}) collective-permute-start(bf16[32,4096]{1,0:T(8,128)(2,1)S(1)} %slice.111), channel_id=1, source_target_pairs={{0,8},{8,0},{1,9},{9,1},{2,10},{10,2},{3,11},{11,3},{4,12},{12,4},... | collective-permute-start | bytes 786440 | tf_op jit(solution)/shard_map/ppermute | solution.py:31
  73.6 7.3 %collective-permute-start.29 = (bf16[32,4096]{1,0:T(8,128)(2,1)S(1)}, bf16[32,4096]{1,0:T(8,128)(2,1)S(1)}, u32[]{:S(2)}, u32[]{:S(2)}) collective-permute-start(bf16[32,4096]{1,0:T(8,128)(2,1)S(1)} %slice.108), channel_id=1, source_target_pairs={{0,2},{2,4},{4,6},{6,0},{1,3},{3,5},{5,7},{7,1},{8,10},{10,12},{12... | collective-permute-start | bytes 786440 | tf_op jit(solution)/shard_map/ppermute | solution.py:27
  75.1 9.5 %collective-permute-start.33 = (bf16[48,4096]{1,0:T(8,128)(2,1)S(1)}, bf16[48,4096]{1,0:T(8,128)(2,1)S(1)}, u32[]{:S(2)}, u32[]{:S(2)}) collective-permute-start(bf16[48,4096]{1,0:T(8,128)(2,1)S(1)} %collective-permute-done.10.refs_1_.refs_9_), channel_id=1, source_target_pairs={{0,1},{1,0},{2,3},{3,2},{4,5},{5,4},{6,7},{7,6},{8,9},{9,8},{10,11... | collective-permute-start | bytes 1179656 | tf_op jit(solution)/shard_map/ppermute | solution.py:35
  75.1 9.5 %collective-permute-start.30 = (bf16[32,4096]{1,0:T(8,128)(2,1)S(1)}, bf16[32,4096]{1,0:T(8,128)(2,1)S(1)}, u32[]{:S(2)}, u32[]{:S(2)}) collective-permute-start(bf16[32,4096]{1,0:T(8,128)(2,1)S(1)} %pad_maximum_fusion), channel_id=1, source_target_pairs={{0,6},{2,0},{4,2},{6,4},{1,7},{3,1},{5,3},{7,5},{8,14},{10,8},{12,... | collective-permute-start | bytes 786440 | tf_op jit(solution)/shard_map/ppermute | solution.py:27
  76.6 8.4 %collective-permute-start.36 = (bf16[48,4096]{1,0:T(8,128)(2,1)S(1)}, bf16[48,4096]{1,0:T(8,128)(2,1)S(1)}, u32[]{:S(2)}, u32[]{:S(2)}) collective-permute-start(bf16[48,4096]{1,0:T(8,128)(2,1)S(1)} %collective-permute-done.15.refs_4_.refs_12_), channel_id=1, source_target_pairs={{0,1},{1,0},{2,3},{3,2},{4,5},{5,4},{6,7},{7,6},{8,9},{9,8},{10,11... | collective-permute-start | bytes 1179656 | tf_op jit(solution)/shard_map/ppermute | solution.py:35
  79.1 6.0 %collective-permute-start.32 = (bf16[48,4096]{1,0:T(8,128)(2,1)S(1)}, bf16[48,4096]{1,0:T(8,128)(2,1)S(1)}, u32[]{:S(2)}, u32[]{:S(2)}) collective-permute-start(bf16[48,4096]{1,0:T(8,128)(2,1)S(1)} %collective-permute-done.4.refs_0_.refs_8_), channel_id=1, source_target_pairs={{0,1},{1,0},{2,3},{3,2},{4,5},{5,4},{6,7},{7,6},{8,9},{9,8},{10,11... | collective-permute-start | bytes 1179656 | tf_op jit(solution)/shard_map/ppermute | solution.py:35
  80.9 4.7 %collective-permute-start.34 = (bf16[48,4096]{1,0:T(8,128)(2,1)S(1)}, bf16[48,4096]{1,0:T(8,128)(2,1)S(1)}, u32[]{:S(2)}, u32[]{:S(2)}) collective-permute-start(bf16[48,4096]{1,0:T(8,128)(2,1)S(1)} %collective-permute-done.12.refs_2_.refs_10_), channel_id=1, source_target_pairs={{0,1},{1,0},{2,3},{3,2},{4,5},{5,4},{6,7},{7,6},{8,9},{9,8},{10,11... | collective-permute-start | bytes 1179656 | tf_op jit(solution)/shard_map/ppermute | solution.py:35
  84.6 1.7 %collective-permute-start.35 = (bf16[48,4096]{1,0:T(8,128)(2,1)S(1)}, bf16[48,4096]{1,0:T(8,128)(2,1)S(1)}, u32[]{:S(2)}, u32[]{:S(2)}) collective-permute-start(bf16[48,4096]{1,0:T(8,128)(2,1)S(1)} %collective-permute-done.14.refs_3_.refs_11_), channel_id=1, source_target_pairs={{0,1},{1,0},{2,3},{3,2},{4,5},{5,4},{6,7},{7,6},{8,9},{9,8},{10,11... | collective-permute-start | bytes 1179656 | tf_op jit(solution)/shard_map/ppermute | solution.py:35
  84.6 2.3 %collective-permute-start.37 = (bf16[48,4096]{1,0:T(8,128)(2,1)S(1)}, bf16[48,4096]{1,0:T(8,128)(2,1)S(1)}, u32[]{:S(2)}, u32[]{:S(2)}) collective-permute-start(bf16[48,4096]{1,0:T(8,128)(2,1)S(1)} %collective-permute-done.16.refs_5_.refs_13_), channel_id=1, source_target_pairs={{0,1},{1,0},{2,3},{3,2},{4,5},{5,4},{6,7},{7,6},{8,9},{9,8},{10,11... | collective-permute-start | bytes 1179656 | tf_op jit(solution)/shard_map/ppermute | solution.py:35
  85.1 2.1 %collective-permute-start.40 = (bf16[32,4096]{1,0:T(8,128)(2,1)S(1)}, bf16[32,4096]{1,0:T(8,128)(2,1)S(1)}, u32[]{:S(2)}, u32[]{:S(2)}) collective-permute-start(bf16[32,4096]{1,0:T(8,128)(2,1)S(1)} %collective-permute-done.31.refs_8_.refs_16_), channel_id=1, source_target_pairs={{0,1},{1,0},{2,3},{3,2},{4,5},{5,4},{6,7},{7,6},{8,9},{9,8},{10,11... | collective-permute-start | bytes 786440 | tf_op jit(solution)/shard_map/ppermute | solution.py:35
  85.2 2.4 %collective-permute-start.38 = (bf16[32,4096]{1,0:T(8,128)(2,1)S(1)}, bf16[32,4096]{1,0:T(8,128)(2,1)S(1)}, u32[]{:S(2)}, u32[]{:S(2)}) collective-permute-start(bf16[32,4096]{1,0:T(8,128)(2,1)S(1)} %collective-permute-done.29.refs_6_.refs_14_), channel_id=1, source_target_pairs={{0,1},{1,0},{2,3},{3,2},{4,5},{5,4},{6,7},{7,6},{8,9},{9,8},{10,11... | collective-permute-start | bytes 786440 | tf_op jit(solution)/shard_map/ppermute | solution.py:35
  85.6 2.4 %collective-permute-start.39 = (bf16[32,4096]{1,0:T(8,128)(2,1)S(1)}, bf16[32,4096]{1,0:T(8,128)(2,1)S(1)}, u32[]{:S(2)}, u32[]{:S(2)}) collective-permute-start(bf16[32,4096]{1,0:T(8,128)(2,1)S(1)} %collective-permute-done.30.refs_7_.refs_15_), channel_id=1, source_target_pairs={{0,1},{1,0},{2,3},{3,2},{4,5},{5,4},{6,7},{7,6},{8,9},{9,8},{10,11... | collective-permute-start | bytes 786440 | tf_op jit(solution)/shard_map/ppermute | solution.py:35
  94.5 3.6 %collective-permute-start.41 = (bf16[384,2176]{1,0:T(8,128)(2,1)S(1)}, bf16[384,2176]{1,0:T(8,128)(2,1)S(1)}, u32[]{:S(2)}, u32[]{:S(2)}) collective-permute-start(bf16[384,2176]{1,0:T(8,128)(2,1)S(1)} %get-tuple-element.71), channel_id=1, source_target_pairs={{0,1},{1,0},{2,3},{3,2},{4,5},{5,4},{6,7},{7,6},{8,9},{9,8},{10,11... | collective-permute-start | bytes 5013512 | tf_op jit(solution)/shard_map/ppermute | solution.py:35
  94.8 28.4 %collective-permute-start.27 = (bf16[384,2176]{1,0:T(8,128)(2,1)S(1)}, bf16[384,2176]{1,0:T(8,128)(2,1)S(1)}, u32[]{:S(2)}, u32[]{:S(2)}) collective-permute-start(bf16[384,2176]{1,0:T(8,128)(2,1)S(1)} %get-tuple-element.62), channel_id=1, source_target_pairs={{0,1},{1,0},{2,3},{3,2},{4,5},{5,4},{6,7},{7,6},{8,9},{9,8},{10,11... | collective-permute-start | bytes 5013512 | tf_op jit(solution)/shard_map/ppermute | solution.py:35
  98.3 5.8 %collective-permute-start.46 = (bf16[32,2176]{1,0:T(8,128)(2,1)S(1)}, bf16[32,2176]{1,0:T(8,128)(2,1)S(1)}, u32[]{:S(2)}, u32[]{:S(2)}) collective-permute-start(bf16[32,2176]{1,0:T(8,128)(2,1)S(1)} %get-tuple-element.93), channel_id=1, source_target_pairs={{0,8},{8,0},{1,9},{9,1},{2,10},{10,2},{3,11},{11,3},{4,12},{12,4},... | collective-permute-start | bytes 417800 | tf_op jit(solution)/shard_map/ppermute | solution.py:31
  99.6 5.4 %collective-permute-start.44 = (bf16[32,2176]{1,0:T(8,128)(2,1)S(1)}, bf16[32,2176]{1,0:T(8,128)(2,1)S(1)}, u32[]{:S(2)}, u32[]{:S(2)}) collective-permute-start(bf16[32,2176]{1,0:T(8,128)(2,1)S(1)} %get-tuple-element.94), channel_id=1, source_target_pairs={{0,2},{2,4},{4,6},{6,0},{1,3},{3,5},{5,7},{7,1},{8,10},{10,12},{12... | collective-permute-start | bytes 417800 | tf_op jit(solution)/shard_map/ppermute | solution.py:27
  101.3 6.1 %collective-permute-start.42 = (bf16[32,2176]{1,0:T(8,128)(2,1)S(1)}, bf16[32,2176]{1,0:T(8,128)(2,1)S(1)}, u32[]{:S(2)}, u32[]{:S(2)}) collective-permute-start(bf16[32,2176]{1,0:T(8,128)(2,1)S(1)} %get-tuple-element.95), channel_id=1, source_target_pairs={{0,6},{2,0},{4,2},{6,4},{1,7},{3,1},{5,3},{7,5},{8,14},{10,8},{12,... | collective-permute-start | bytes 417800 | tf_op jit(solution)/shard_map/ppermute | solution.py:27
  107.8 15.3 %collective-permute-start.47 = (bf16[96,2176]{1,0:T(8,128)(2,1)S(1)}, bf16[96,2176]{1,0:T(8,128)(2,1)S(1)}, u32[]{:S(2)}, u32[]{:S(2)}) collective-permute-start(bf16[96,2176]{1,0:T(8,128)(2,1)S(1)} %get-tuple-element.90), channel_id=1, source_target_pairs={{0,2},{2,4},{4,6},{6,0},{1,3},{3,5},{5,7},{7,1},{8,10},{10,12},{12... | collective-permute-start | bytes 1253384 | tf_op jit(solution)/shard_map/ppermute | solution.py:27
  109.6 13.5 %collective-permute-start.45 = (bf16[96,2176]{1,0:T(8,128)(2,1)S(1)}, bf16[96,2176]{1,0:T(8,128)(2,1)S(1)}, u32[]{:S(2)}, u32[]{:S(2)}) collective-permute-start(bf16[96,2176]{1,0:T(8,128)(2,1)S(1)} %get-tuple-element.91), channel_id=1, source_target_pairs={{0,8},{8,0},{1,9},{9,1},{2,10},{10,2},{3,11},{11,3},{4,12},{12,4},... | collective-permute-start | bytes 1253384 | tf_op jit(solution)/shard_map/ppermute | solution.py:31
  110.6 12.5 %collective-permute-start.43 = (bf16[96,2176]{1,0:T(8,128)(2,1)S(1)}, bf16[96,2176]{1,0:T(8,128)(2,1)S(1)}, u32[]{:S(2)}, u32[]{:S(2)}) collective-permute-start(bf16[96,2176]{1,0:T(8,128)(2,1)S(1)} %get-tuple-element.92), channel_id=1, source_target_pairs={{0,6},{2,0},{4,2},{6,4},{1,7},{3,1},{5,3},{7,5},{8,14},{10,8},{12,... | collective-permute-start | bytes 1253384 | tf_op jit(solution)/shard_map/ppermute | solution.py:27
  123.6 10.2 %collective-permute-start.49 = (bf16[96,2176]{1,0:T(8,128)(2,1)S(1)}, bf16[96,2176]{1,0:T(8,128)(2,1)S(1)}, u32[]{:S(2)}, u32[]{:S(2)}) collective-permute-start(bf16[96,2176]{1,0:T(8,128)(2,1)S(1)} %get-tuple-element.87), channel_id=1, source_target_pairs={{0,8},{8,0},{1,9},{9,1},{2,10},{10,2},{3,11},{11,3},{4,12},{12,4},... | collective-permute-start | bytes 1253384 | tf_op jit(solution)/shard_map/ppermute | solution.py:31
  124.7 10.1 %collective-permute-start.48 = (bf16[96,2176]{1,0:T(8,128)(2,1)S(1)}, bf16[96,2176]{1,0:T(8,128)(2,1)S(1)}, u32[]{:S(2)}, u32[]{:S(2)}) collective-permute-start(bf16[96,2176]{1,0:T(8,128)(2,1)S(1)} %get-tuple-element.88), channel_id=1, source_target_pairs={{0,2},{2,4},{4,6},{6,0},{1,3},{3,5},{5,7},{7,1},{8,10},{10,12},{12... | collective-permute-start | bytes 1253384 | tf_op jit(solution)/shard_map/ppermute | solution.py:27
  126.4 8.9 %collective-permute-start.28 = (bf16[96,2176]{1,0:T(8,128)(2,1)S(1)}, bf16[96,2176]{1,0:T(8,128)(2,1)S(1)}, u32[]{:S(2)}, u32[]{:S(2)}) collective-permute-start(bf16[96,2176]{1,0:T(8,128)(2,1)S(1)} %get-tuple-element.89), channel_id=1, source_target_pairs={{0,6},{2,0},{4,2},{6,4},{1,7},{3,1},{5,3},{7,5},{8,14},{10,8},{12,... | collective-permute-start | bytes 1253384 | tf_op jit(solution)/shard_map/ppermute | solution.py:27
  135.6 17.3 %copy-start.3 = (bf16[24,128]{1,0:T(8,128)(2,1)S(1)}, bf16[24,128]{1,0:T(8,128)(2,1)}, u32[]{:S(2)}) copy-start(bf16[24,128]{1,0:T(8,128)(2,1)} %get-tuple-element.46.first_ref) | copy-start | bytes 18436
  135.6 17.3 %copy-start.4 = (bf16[24,128]{1,0:T(8,128)(2,1)S(1)}, bf16[24,128]{1,0:T(8,128)(2,1)}, u32[]{:S(2)}) copy-start(bf16[24,128]{1,0:T(8,128)(2,1)} %get-tuple-element.47.second_ref) | copy-start | bytes 18436
  135.6 17.3 %copy-start.5 = (f32[24,2]{0,1:T(2,128)S(1)}, f32[24,2]{0,1:T(2,128)}, u32[]{:S(2)}) copy-start(f32[24,2]{0,1:T(2,128)} %param.10) | copy-start | bytes 580
  136.3 10.7 %collective-permute-start.56 = (bf16[16,2176]{1,0:T(8,128)(2,1)S(1)}, bf16[16,2176]{1,0:T(8,128)(2,1)S(1)}, u32[]{:S(2)}, u32[]{:S(2)}) collective-permute-start(bf16[16,2176]{1,0:T(8,128)(2,1)S(1)} %get-tuple-element.96), channel_id=1, source_target_pairs={{0,56},{8,48},{16,40},{24,32},{32,88},{40,80},{48,72},{56,64},{64,... | collective-permute-start | bytes 208904 | tf_op jit(solution)/shard_map/ppermute | solution.py:44
  139.8 8.3 %collective-permute-start.54 = (bf16[16,2176]{1,0:T(8,128)(2,1)S(1)}, bf16[16,2176]{1,0:T(8,128)(2,1)S(1)}, u32[]{:S(2)}, u32[]{:S(2)}) collective-permute-start(bf16[16,2176]{1,0:T(8,128)(2,1)S(1)} %get-tuple-element.97), channel_id=1, source_target_pairs={{0,88},{8,80},{16,72},{24,64},{32,120},{40,112},{48,104},{56,96},{... | collective-permute-start | bytes 208904 | tf_op jit(solution)/shard_map/ppermute | solution.py:44
  142.3 7.8 %collective-permute-start.52 = (bf16[16,2176]{1,0:T(8,128)(2,1)S(1)}, bf16[16,2176]{1,0:T(8,128)(2,1)S(1)}, u32[]{:S(2)}, u32[]{:S(2)}) collective-permute-start(bf16[16,2176]{1,0:T(8,128)(2,1)S(1)} %get-tuple-element.98), channel_id=1, source_target_pairs={{0,120},{8,112},{16,104},{24,96},{32,24},{40,16},{48,8},{56,0},{64... | collective-permute-start | bytes 208904 | tf_op jit(solution)/shard_map/ppermute | solution.py:44
  145.4 5.5 %collective-permute-start.50 = (bf16[16,2176]{1,0:T(8,128)(2,1)S(1)}, bf16[16,2176]{1,0:T(8,128)(2,1)S(1)}, u32[]{:S(2)}, u32[]{:S(2)}) collective-permute-start(bf16[16,2176]{1,0:T(8,128)(2,1)S(1)} %get-tuple-element.99), channel_id=1, source_target_pairs={{0,24},{8,16},{16,8},{24,0},{32,56},{40,48},{48,40},{56,32},{64,88... | collective-permute-start | bytes 208904 | tf_op jit(solution)/shard_map/ppermute | solution.py:44
  145.7 5.5 %collective-permute-start.55 = (bf16[16,2176]{1,0:T(8,128)(2,1)S(1)}, bf16[16,2176]{1,0:T(8,128)(2,1)S(1)}, u32[]{:S(2)}, u32[]{:S(2)}) collective-permute-start(bf16[16,2176]{1,0:T(8,128)(2,1)S(1)} %get-tuple-element.100), channel_id=1, source_target_pairs={{0,32},{8,40},{16,48},{24,56},{32,64},{40,72},{48,80},{56,88},{64,... | collective-permute-start | bytes 208904 | tf_op jit(solution)/shard_map/ppermute | solution.py:44
  147.1 5.8 %collective-permute-start.53 = (bf16[16,2176]{1,0:T(8,128)(2,1)S(1)}, bf16[16,2176]{1,0:T(8,128)(2,1)S(1)}, u32[]{:S(2)}, u32[]{:S(2)}) collective-permute-start(bf16[16,2176]{1,0:T(8,128)(2,1)S(1)} %get-tuple-element.101), channel_id=1, source_target_pairs={{0,64},{8,72},{16,80},{24,88},{32,96},{40,104},{48,112},{56,120},{... | collective-permute-start | bytes 208904 | tf_op jit(solution)/shard_map/ppermute | solution.py:44
  148.1 4.8 %collective-permute-start.51 = (bf16[16,2176]{1,0:T(8,128)(2,1)S(1)}, bf16[16,2176]{1,0:T(8,128)(2,1)S(1)}, u32[]{:S(2)}, u32[]{:S(2)}) collective-permute-start(bf16[16,2176]{1,0:T(8,128)(2,1)S(1)} %get-tuple-element.102), channel_id=1, source_target_pairs={{0,96},{8,104},{16,112},{24,120},{32,0},{40,8},{48,16},{56,24},{64... | collective-permute-start | bytes 208904 | tf_op jit(solution)/shard_map/ppermute | solution.py:44
  (1 other events, 1.8 us)

commit v4 on v3

--- a/solution.py
+++ b/solution.py
@@ -369,12 +369,13 @@
     near = own + left + right + partner
     near_other = [pair_core(v) for v in near]
     near_out = run_group(place, near, near_other, pair_t, down_t)
+    tied = lax.optimization_barrier((far_left[0], far_right[0], *near_out))
+    far_left[0], far_right[0] = tied[:2]
+    near_out = tied[2:]
+    early = [along_x(far_left[0][:third], 1), along_x(far_right[0][third:], -1)]
     far = far_left + far_right + across
-    tied = lax.optimization_barrier((*far, *near_out))
-    far = list(tied[: len(far)])
-    near_out = tied[len(far) :]
-    middle = jnp.concatenate([far[2][third:], far[3][: 2 * third - part]], axis=0)
-    last = [along_x(far[0][:third], 1), along_x(middle, -1), pair_y(far[5][2 * third - part :])]
+    rest = packed - 2 * third - third // 2
+    last = early + [along_x(far_left[1][:rest], 1), pair_y(across[1][rest:])]
     far = far + last
     far_other = [pair_core(v) for v in far]
     far_out = run_group(place, far, far_other, pair_t, down_t)

time: 156 us -> 167 us (1.071)
  waiting for transfers between devices: 48.6 us -> 56.5 us
  starting transfers between devices: 60.3 us -> 62.7 us
    ppermute x8, waiting for transfers between devices: 11.6 us -> 20.4 us  [pair_y(): return lax.ppermute(value, 'yl', [(0, 1), (1, 0)])]
    ppermute x8, starting transfers between devices: 8.04 us -> 10.6 us  [pair_y(): return lax.ppermute(value, 'yl', [(0, 1), (1, 0)])]
    ppermute x16 -> x17, waiting for transfers between devices: 25.1 us -> 23.5 us  [along_x(): return lax.ppermute(value, 'x', [(i, (i + step) % 4) for i in range(4)])]
    ppermute x16 -> x17, starting transfers between devices: 20.4 us -> 19.5 us  [along_x(): return lax.ppermute(value, 'x', [(i, (i + step) % 4) for i in range(4)])]
    ppermute x19 -> x20, starting transfers between devices: 3.21 us -> 3.83 us  [pair_core(): return lax.ppermute(value, 'core', [(0, 1), (1, 0)])]
  transfers between devices with their start and end apart: 57 -> 59, of which waited for: 29 -> 25; matrix products, arithmetic and copies ran while one was open for 1% -> 1% of each run, Pallas kernels for 18% -> 17%
where the time goes in v4:
time: 167 us; the launch traced here: 164 us
  starting transfers between devices  62.7 us (38%)
  waiting for transfers between devices  56.5 us (34%)
  Pallas kernels  39 us (23%)
  local copies, waits for them, and re-layouts  1.93 us (1%)
  other arithmetic  1.8 us (1%)
    ppermute x14, starting transfers between devices, to_expert(): return lax.ppermute(value, ('z', 'yh', 'yl'), perm)  28.7 us
    ppermute x17, waiting for transfers between devices, along_x(): return lax.ppermute(value, 'x', [(i, (i + step) % 4) for i in range(4)])  23.5 us
    ppermute x8, waiting for transfers between devices, pair_y(): return lax.ppermute(value, 'yl', [(0, 1), (1, 0)])  20.4 us
    ppermute x17, starting transfers between devices, along_x(): return lax.ppermute(value, 'x', [(i, (i + step) % 4) for i in range(4)])  19.5 us
    pallas_call x2, Pallas kernels, weight_grads(): pl.pallas_call(functools.partial(weight_kernel, sizes, offset, width // 2...  17.3 us
    pallas_call x2, Pallas kernels, run_group(): pl.pallas_call(functools.partial(group_kernel, len(ours), half), out_shap...  13.1 us
    ppermute x8, starting transfers between devices, pair_y(): return lax.ppermute(value, 'yl', [(0, 1), (1, 0)])  10.6 us
    ppermute x14, waiting for transfers between devices, to_expert(): return lax.ppermute(value, ('z', 'yh', 'yl'), perm)  9.65 us
  transfers between devices with their start and end apart: 59, of which 25 were waited for; matrix products, arithmetic and copies ran while one was open for 1% of the time, Pallas kernels for 17%

profile of v4, /device:TPU:2, one launch (start us, length us, event | category | flops | bytes accessed | tf_op | source)
XLA Modules:
  0.0 164.3 jit_solution(7632939460456180259)
XLA Ops:
  0.6 0.6 pad_add_fusion.place_ref
  1.2 3.2 %slots.1 = (bf16[16,4096]{1,0:T(8,128)(2,1)}, bf16[16,4096]{1,0:T(8,128)(2,1)}, bf16[16,4096]{1,0:T(8,128)(2,1)}, bf16[16,4096]{1,0:T(8,128)(2,1)}, bf16[16,4096...) custom-call(s32[3]{0:T(128)} %pad_add_fusion.place_ref, ...), custom_call_target="tpu_custom_call" | custom-call | flops 50331648 | bytes 3145728 | tf_op jit(solution)/shard_map/slots/pallas_call | solution.py:97
  4.4 3.1 %collective-permute-start.7 = (bf16[16,4096]{1,0:T(8,128)(2,1)}, bf16[16,4096]{1,0:T(8,128)(2,1)S(1)}, u32[]{:S(2)}, u32[]{:S(2)}) collective-permute-start(bf16[16,4096]{1,0:T(8,128)(2,1)} %get-tuple-element.48), channel_id=1, source_target_pairs={{0,24},{8,16},{16,8},{24,0},{32,56},{40,48},{48,40},{56,32},{64,88... | collective-permute-start | bytes 393224 | tf_op jit(solution)/shard_map/ppermute | solution.py:44
  7.5 1.6 collective-permute-start.8
  9.1 6.0 %collective-permute-start.9 = (bf16[16,4096]{1,0:T(8,128)(2,1)}, bf16[16,4096]{1,0:T(8,128)(2,1)S(1)}, u32[]{:S(2)}, u32[]{:S(2)}) collective-permute-start(bf16[16,4096]{1,0:T(8,128)(2,1)} %get-tuple-element.50), channel_id=1, source_target_pairs={{0,88},{8,80},{16,72},{24,64},{32,120},{40,112},{48,104},{56,96},{... | collective-permute-start | bytes 393224 | tf_op jit(solution)/shard_map/ppermute | solution.py:44
  15.1 0.7 collective-permute-start.10
  15.8 1.0 collective-permute-start
  16.8 0.9 collective-permute-start.1
  17.7 0.9 collective-permute-done.8
  18.6 1.8 %collective-permute-start.2 = (bf16[16,4096]{1,0:T(8,128)(2,1)}, bf16[16,4096]{1,0:T(8,128)(2,1)S(1)}, u32[]{:S(2)}, u32[]{:S(2)}) collective-permute-start(bf16[16,4096]{1,0:T(8,128)(2,1)} %get-tuple-element.47), channel_id=1, source_target_pairs={{0,96},{8,104},{16,112},{24,120},{32,0},{40,8},{48,16},{56,24},{64... | collective-permute-start | bytes 393224 | tf_op jit(solution)/shard_map/ppermute | solution.py:44
  20.4 2.1 %collective-permute-done.9 = bf16[16,4096]{1,0:T(8,128)(2,1)S(1)} collective-permute-done((bf16[16,4096]{1,0:T(8,128)(2,1)}, bf16[16,4096]{1,0:T(8,128)(2,1)S(1)}, u32[]{:S(2)}, u32[]{:S(2)}) %collective-permute-start.9) | collective-permute-done | bytes 131104 | tf_op jit(solution)/shard_map/ppermute | solution.py:44
  24.0 2.7 %collective-permute-done.1 = bf16[16,4096]{1,0:T(8,128)(2,1)S(1)} collective-permute-done((bf16[16,4096]{1,0:T(8,128)(2,1)}, bf16[16,4096]{1,0:T(8,128)(2,1)S(1)}, u32[]{:S(2)}, u32[]{:S(2)}) %collective-permute-start.1) | collective-permute-done | bytes 131104 | tf_op jit(solution)/shard_map/ppermute | solution.py:44
  26.7 1.5 collective-permute-start.12
  28.6 1.3 collective-permute-start.11
  29.9 4.5 %collective-permute-done.14.refs_7_ = bf16[48,4096]{1,0:T(8,128)(2,1)S(1)} collective-permute-done((bf16[48,4096]{1,0:T(8,128)(2,1)S(1)}, bf16[48,4096]{1,0:T(8,128)(2,1)S(1)}, u32[]{:S(2)}, u32[]{:S(2)}) %collective-permute-start.14) | collective-permute-done | bytes 393248 | tf_op jit(solution)/shard_map/ppermute | solution.py:31
  35.0 2.6 %collective-permute-start.3 = (bf16[48,4096]{1,0:T(8,128)(2,1)S(1)}, bf16[48,4096]{1,0:T(8,128)(2,1)S(1)}, u32[]{:S(2)}, u32[]{:S(2)}) collective-permute-start(bf16[48,4096]{1,0:T(8,128)(2,1)S(1)} %convolution_convert_fusion.1.refs_0_), channel_id=1, source_target_pairs={{0,8},{8,0},{1,9},{9,1},{2,10},{10,2},{3,11},{11,3},{4,12},{12,4},... | collective-permute-start | bytes 1179656 | tf_op jit(solution)/shard_map/ppermute | solution.py:31
  37.6 1.1 collective-permute-done.12.refs_3_
  38.7 1.5 collective-permute-start.25
  40.2 6.9 %collective-permute-done.11.refs_2_ = bf16[48,4096]{1,0:T(8,128)(2,1)S(1)} collective-permute-done((bf16[48,4096]{1,0:T(8,128)(2,1)S(1)}, bf16[48,4096]{1,0:T(8,128)(2,1)S(1)}, u32[]{:S(2)}, u32[]{:S(2)}) %collective-permute-start.11) | collective-permute-done | bytes 393248 | tf_op jit(solution)/shard_map/ppermute | solution.py:27
  47.7 6.9 %collective-permute-done.25.refs_1_.refs_9_ = bf16[48,4096]{1,0:T(8,128)(2,1)S(1)} collective-permute-done((bf16[48,4096]{1,0:T(8,128)(2,1)S(1)}, bf16[48,4096]{1,0:T(8,128)(2,1)S(1)}, u32[]{:S(2)}, u32[]{:S(2)}) %collective-permute-start.25) | collective-permute-done | bytes 393248 | tf_op jit(solution)/shard_map/ppermute | solution.py:27
  55.1 1.8 %copy-done.1 = bf16[1,4096,344]{1,2,0:T(8,128)(2,1)S(1)} copy-done((bf16[1,4096,344]{1,2,0:T(8,128)(2,1)S(1)}, bf16[1,4096,344]{1,2,0:T(8,128)(2,1)}, u32[]{:S(2)}) %copy-start.1) | copy-done | bytes 2818072
  57.3 1.8 %collective-permute-start.28 = (bf16[48,4096]{1,0:T(8,128)(2,1)S(1)}, bf16[48,4096]{1,0:T(8,128)(2,1)S(1)}, u32[]{:S(2)}, u32[]{:S(2)}) collective-permute-start(bf16[48,4096]{1,0:T(8,128)(2,1)S(1)} %collective-permute-done.13.refs_5_), channel_id=1, source_target_pairs={{0,6},{2,0},{4,2},{6,4},{1,7},{3,1},{5,3},{7,5},{8,14},{10,8},{12,... | collective-permute-start | bytes 1179656 | tf_op jit(solution)/shard_map/ppermute | solution.py:27
  59.2 2.1 %collective-permute-start.26 = (bf16[48,4096]{1,0:T(8,128)(2,1)S(1)}, bf16[48,4096]{1,0:T(8,128)(2,1)S(1)}, u32[]{:S(2)}, u32[]{:S(2)}) collective-permute-start(bf16[48,4096]{1,0:T(8,128)(2,1)S(1)} %collective-permute-done.13.refs_5_), channel_id=1, source_target_pairs={{0,8},{8,0},{1,9},{9,1},{2,10},{10,2},{3,11},{11,3},{4,12},{12,4},... | collective-permute-start | bytes 1179656 | tf_op jit(solution)/shard_map/ppermute | solution.py:31
  61.3 1.4 collective-permute-start.6
  62.7 0.8 collective-permute-start.4
  63.5 6.6 %group.2 = (bf16[384,2176]{1,0:T(8,128)(2,1)S(1)}, bf16[384,128]{1,0:T(8,128)(2,1)S(1)}, bf16[384,768]{1,0:T(8,128)(2,1)S(1)}, bf16[384,384]{1,0:T(8,128)(2,1)S(1)}) custom-call(s32[3]{0:T(128)S(1)} %copy-done.2, bf16[48,4096]{1,0:T(8,128)(2,1)S(1)} %convolution_convert_fusion.1.refs_0_, bf16[48,4096]{1,0:T(8,128)(2,1)S(1)} %convolution_convert_fusion.refs_1_, ...), custom_call_target="tpu_custom_call" | custom-call | flops 4328521728 | bytes 16777216 | tf_op jit(solution)/shard_map/group/pallas_call | solution.py:210
  70.1 8.5 %collective-permute-done.6.refs_2_.refs_10_ = bf16[48,4096]{1,0:T(8,128)(2,1)S(1)} collective-permute-done((bf16[48,4096]{1,0:T(8,128)(2,1)S(1)}, bf16[48,4096]{1,0:T(8,128)(2,1)S(1)}, u32[]{:S(2)}, u32[]{:S(2)}) %collective-permute-start.6) | collective-permute-done | bytes 393248 | tf_op jit(solution)/shard_map/ppermute | solution.py:31
  78.7 2.1 %collective-permute-start.30 = (bf16[16,4096]{1,0:T(8,128)(2,1)S(1)}, bf16[16,4096]{1,0:T(8,128)(2,1)S(1)}, u32[]{:S(2)}, u32[]{:S(2)}) collective-permute-start(bf16[16,4096]{1,0:T(8,128)(2,1)S(1)} %slice.109), channel_id=1, source_target_pairs={{0,6},{2,0},{4,2},{6,4},{1,7},{3,1},{5,3},{7,5},{8,14},{10,8},{12,... | collective-permute-start | bytes 393224 | tf_op jit(solution)/shard_map/ppermute | solution.py:27
  80.8 2.8 %collective-permute-done.31.refs_8_.refs_16_ = bf16[16,4096]{1,0:T(8,128)(2,1)S(1)} collective-permute-done((bf16[16,4096]{1,0:T(8,128)(2,1)S(1)}, bf16[16,4096]{1,0:T(8,128)(2,1)S(1)}, u32[]{:S(2)}, u32[]{:S(2)}) %collective-permute-start.31) | collective-permute-done | bytes 131104 | tf_op jit(solution)/shard_map/ppermute | solution.py:27
  84.2 1.8 %collective-permute-start.32 = (bf16[32,4096]{1,0:T(8,128)(2,1)S(1)}, bf16[32,4096]{1,0:T(8,128)(2,1)S(1)}, u32[]{:S(2)}, u32[]{:S(2)}) collective-permute-start(bf16[32,4096]{1,0:T(8,128)(2,1)S(1)} %slice.143), channel_id=1, source_target_pairs={{0,8},{8,0},{1,9},{9,1},{2,10},{10,2},{3,11},{11,3},{4,12},{12,4},... | collective-permute-start | bytes 786440 | tf_op jit(solution)/shard_map/ppermute | solution.py:31
  86.0 0.6 collective-permute-start.29
  87.1 5.5 %collective-permute-done.32.refs_9_.refs_17_ = bf16[32,4096]{1,0:T(8,128)(2,1)S(1)} collective-permute-done((bf16[32,4096]{1,0:T(8,128)(2,1)S(1)}, bf16[32,4096]{1,0:T(8,128)(2,1)S(1)}, u32[]{:S(2)}, u32[]{:S(2)}) %collective-permute-start.32) | collective-permute-done | bytes 262176 | tf_op jit(solution)/shard_map/ppermute | solution.py:31
  92.6 1.7 %collective-permute-done.29.refs_6_.refs_14_ = bf16[32,4096]{1,0:T(8,128)(2,1)S(1)} collective-permute-done((bf16[32,4096]{1,0:T(8,128)(2,1)S(1)}, bf16[32,4096]{1,0:T(8,128)(2,1)S(1)}, u32[]{:S(2)}, u32[]{:S(2)}) %collective-permute-start.29) | collective-permute-done | bytes 262176 | tf_op jit(solution)/shard_map/ppermute | solution.py:27
  95.4 0.7 collective-permute-done.37.refs_14_.refs_30_
  96.1 0.6 collective-permute-done.35.refs_12_.refs_28_
  97.4 6.6 %group.3 = (bf16[384,2176]{1,0:T(8,128)(2,1)S(1)}, bf16[384,128]{1,0:T(8,128)(2,1)S(1)}, bf16[384,768]{1,0:T(8,128)(2,1)S(1)}, bf16[384,384]{1,0:T(8,128)(2,1)S(1)}) custom-call(s32[3]{0:T(128)S(1)} %copy-done.2, bf16[48,4096]{1,0:T(8,128)(2,1)S(1)} %collective-permute-done.4.refs_0_.refs_8_, bf16[48,4096]{1,0:T(8,128)(2,1)S(1)} %collective-permute-done.25.refs_1_.refs_9_, ...), custom_call_target="tpu_custom_call" | custom-call | flops 4328521728 | bytes 16777216 | tf_op jit(solution)/shard_map/group/pallas_call | solution.py:210
  104.5 2.1 %keep.3 = bf16[384,2176]{1,0:T(8,128)(2,1)S(1)} custom-call(s32[3]{0:T(128)S(1)} %copy-done.2, bf16[384,768]{1,0:T(8,128)(2,1)S(1)} %get-tuple-element.61.sides_ref.refs_37_, bf16[384,128]{1,0:T(8,128)(2,1)S(1)} %get-tuple-element.62.share_ref, bf16[768,4096]{1,0:T(8,128)(2,1)S(1)} %stack.17.refs_16_.pair_ref.refs_20_), custom_call_target="tpu_custom_call" | custom-call | flops 1207959552 | bytes 8388608 | tf_op jit(solution)/shard_map/keep/pallas_call | solution.py:191
  106.6 0.9 collective-permute-done.43
  107.7 0.7 collective-permute-start.48
  108.4 2.0 %collective-permute-start.46 = (bf16[32,2176]{1,0:T(8,128)(2,1)S(1)}, bf16[32,2176]{1,0:T(8,128)(2,1)S(1)}, u32[]{:S(2)}, u32[]{:S(2)}) collective-permute-start(bf16[32,2176]{1,0:T(8,128)(2,1)S(1)} %get-tuple-element.86), channel_id=1, source_target_pairs={{0,2},{2,4},{4,6},{6,0},{1,3},{3,5},{5,7},{7,1},{8,10},{10,12},{12... | collective-permute-start | bytes 417800 | tf_op jit(solution)/shard_map/ppermute | solution.py:27
  110.3 1.3 collective-permute-start.44
  111.7 1.8 %collective-permute-done.48 = bf16[32,2176]{1,0:T(8,128)(2,1)S(1)} collective-permute-done((bf16[32,2176]{1,0:T(8,128)(2,1)S(1)}, bf16[32,2176]{1,0:T(8,128)(2,1)S(1)}, u32[]{:S(2)}, u32[]{:S(2)}) %collective-permute-start.48) | collective-permute-done | bytes 139296 | tf_op jit(solution)/shard_map/ppermute | solution.py:31
  113.5 1.9 %collective-permute-done.46 = bf16[32,2176]{1,0:T(8,128)(2,1)S(1)} collective-permute-done((bf16[32,2176]{1,0:T(8,128)(2,1)S(1)}, bf16[32,2176]{1,0:T(8,128)(2,1)S(1)}, u32[]{:S(2)}, u32[]{:S(2)}) %collective-permute-start.46) | collective-permute-done | bytes 139296 | tf_op jit(solution)/shard_map/ppermute | solution.py:27
  115.4 0.9 collective-permute-done.44
  116.6 1.8 %collective-permute-start.49 = (bf16[96,2176]{1,0:T(8,128)(2,1)S(1)}, bf16[96,2176]{1,0:T(8,128)(2,1)S(1)}, u32[]{:S(2)}, u32[]{:S(2)}) collective-permute-start(bf16[96,2176]{1,0:T(8,128)(2,1)S(1)} %get-tuple-element.82), channel_id=1, source_target_pairs={{0,2},{2,4},{4,6},{6,0},{1,3},{3,5},{5,7},{7,1},{8,10},{10,12},{12... | collective-permute-start | bytes 1253384 | tf_op jit(solution)/shard_map/ppermute | solution.py:27
  118.4 0.9 collective-permute-start.47
  119.3 0.6 collective-permute-start.45
  119.9 2.1 %keep.2 = bf16[384,2176]{1,0:T(8,128)(2,1)S(1)} custom-call(s32[3]{0:T(128)S(1)} %copy-done.2, bf16[384,768]{1,0:T(8,128)(2,1)S(1)} %get-tuple-element.56.sides_ref.refs_36_, bf16[384,128]{1,0:T(8,128)(2,1)S(1)} %get-tuple-element.57.share_ref, bf16[768,4096]{1,0:T(8,128)(2,1)S(1)} %stack.17.refs_16_.pair_ref.refs_20_), custom_call_target="tpu_custom_call" | custom-call | flops 1207959552 | bytes 8388608 | tf_op jit(solution)/shard_map/keep/pallas_call | solution.py:191
  122.0 10.2 %weight_grads.2 = (bf16[344,4096]{1,0:T(8,128)(2,1)}, bf16[344,4096]{1,0:T(8,128)(2,1)}) custom-call(s32[3]{0:T(128)S(1)} %copy-done.2, bf16[48,4096]{1,0:T(8,128)(2,1)S(1)} %convolution_convert_fusion.1.refs_0_, bf16[48,4096]{1,0:T(8,128)(2,1)S(1)} %convolution_convert_fusion.refs_1_, bf16[48,4096]{1,0:T(8,128)(2,1)S(1)} %collective-permute-done.11.refs_2_, ...), custom_call_target="tpu_custom_call" | custom-call | flops 4328521728 | bytes 14680064 | tf_op jit(solution)/shard_map/weight_grads/pallas_call | solution.py:284
  132.7 1.1 collective-permute-start.51
  133.8 2.2 %collective-permute-start.50 = (bf16[96,2176]{1,0:T(8,128)(2,1)S(1)}, bf16[96,2176]{1,0:T(8,128)(2,1)S(1)}, u32[]{:S(2)}, u32[]{:S(2)}) collective-permute-start(bf16[96,2176]{1,0:T(8,128)(2,1)S(1)} %get-tuple-element.80), channel_id=1, source_target_pairs={{0,2},{2,4},{4,6},{6,0},{1,3},{3,5},{5,7},{7,1},{8,10},{10,12},{12... | collective-permute-start | bytes 1253384 | tf_op jit(solution)/shard_map/ppermute | solution.py:27
  136.0 0.9 collective-permute-start.24
  136.9 7.1 %weight_grads.3 = bf16[344,4096]{1,0:T(8,128)(2,1)} custom-call(s32[3]{0:T(128)S(1)} %copy-done.2, bf16[48,4096]{1,0:T(8,128)(2,1)S(1)} %convolution_convert_fusion.1.refs_0_, bf16[48,4096]{1,0:T(8,128)(2,1)S(1)} %convolution_convert_fusion.refs_1_, bf16[48,4096]{1,0:T(8,128)(2,1)S(1)} %collective-permute-done.11.refs_2_, ...), custom_call_target="tpu_custom_call" | custom-call | flops 2164260864 | bytes 14680064 | tf_op jit(solution)/shard_map/weight_grads/pallas_call | solution.py:284
  144.0 0.6 collective-permute-done.50
  144.6 0.6 collective-permute-done.24
  146.2 2.5 %collective-permute-start.58 = (bf16[16,2176]{1,0:T(8,128)(2,1)S(1)}, bf16[16,2176]{1,0:T(8,128)(2,1)S(1)}, u32[]{:S(2)}, u32[]{:S(2)}) collective-permute-start(bf16[16,2176]{1,0:T(8,128)(2,1)S(1)} %get-tuple-element.88), channel_id=1, source_target_pairs={{0,56},{8,48},{16,40},{24,32},{32,88},{40,80},{48,72},{56,64},{64,... | collective-permute-start | bytes 208904 | tf_op jit(solution)/shard_map/ppermute | solution.py:44
  148.8 2.1 %collective-permute-start.56 = (bf16[16,2176]{1,0:T(8,128)(2,1)S(1)}, bf16[16,2176]{1,0:T(8,128)(2,1)S(1)}, u32[]{:S(2)}, u32[]{:S(2)}) collective-permute-start(bf16[16,2176]{1,0:T(8,128)(2,1)S(1)} %get-tuple-element.89), channel_id=1, source_target_pairs={{0,88},{8,80},{16,72},{24,64},{32,120},{40,112},{48,104},{56,96},{... | collective-permute-start | bytes 208904 | tf_op jit(solution)/shard_map/ppermute | solution.py:44
  150.8 3.1 %collective-permute-start.54 = (bf16[16,2176]{1,0:T(8,128)(2,1)S(1)}, bf16[16,2176]{1,0:T(8,128)(2,1)S(1)}, u32[]{:S(2)}, u32[]{:S(2)}) collective-permute-start(bf16[16,2176]{1,0:T(8,128)(2,1)S(1)} %get-tuple-element.90), channel_id=1, source_target_pairs={{0,120},{8,112},{16,104},{24,96},{32,24},{40,16},{48,8},{56,0},{64... | collective-permute-start | bytes 208904 | tf_op jit(solution)/shard_map/ppermute | solution.py:44
  153.9 2.3 %collective-permute-start.52 = (bf16[16,2176]{1,0:T(8,128)(2,1)S(1)}, bf16[16,2176]{1,0:T(8,128)(2,1)S(1)}, u32[]{:S(2)}, u32[]{:S(2)}) collective-permute-start(bf16[16,2176]{1,0:T(8,128)(2,1)S(1)} %get-tuple-element.91), channel_id=1, source_target_pairs={{0,24},{8,16},{16,8},{24,0},{32,56},{40,48},{48,40},{56,32},{64,88... | collective-permute-start | bytes 208904 | tf_op jit(solution)/shard_map/ppermute | solution.py:44
  156.3 1.0 collective-permute-start.55
  157.3 2.6 %collective-permute-start.53 = (bf16[16,2176]{1,0:T(8,128)(2,1)S(1)}, bf16[16,2176]{1,0:T(8,128)(2,1)S(1)}, u32[]{:S(2)}, u32[]{:S(2)}) collective-permute-start(bf16[16,2176]{1,0:T(8,128)(2,1)S(1)} %get-tuple-element.94), channel_id=1, source_target_pairs={{0,96},{8,104},{16,112},{24,120},{32,0},{40,8},{48,16},{56,24},{64... | collective-permute-start | bytes 208904 | tf_op jit(solution)/shard_map/ppermute | solution.py:44
  160.0 2.6 %collective-permute-done.57.refs_6_ = bf16[16,2176]{1,0:T(8,128)(2,1)S(1)} collective-permute-done((bf16[16,2176]{1,0:T(8,128)(2,1)S(1)}, bf16[16,2176]{1,0:T(8,128)(2,1)S(1)}, u32[]{:S(2)}, u32[]{:S(2)}) %collective-permute-start.57) | collective-permute-done | bytes 69664 | tf_op jit(solution)/shard_map/ppermute | solution.py:44
  162.6 0.9 collective-permute-done.53.refs_2_
  163.4 0.9 combine.1
  (95 shorter events, 9.5 us)
Async XLA Ops:
  4.4 23.8 %copy-start.7 = (bf16[16,4096]{1,0:T(8,128)(2,1)S(1)}, bf16[16,4096]{1,0:T(8,128)(2,1)}, u32[]{:S(2)}) copy-start(bf16[16,4096]{1,0:T(8,128)(2,1)} %get-tuple-element.44) | copy-start | bytes 393220
  4.4 12.4 %collective-permute-start.7 = (bf16[16,4096]{1,0:T(8,128)(2,1)}, bf16[16,4096]{1,0:T(8,128)(2,1)S(1)}, u32[]{:S(2)}, u32[]{:S(2)}) collective-permute-start(bf16[16,4096]{1,0:T(8,128)(2,1)} %get-tuple-element.48), channel_id=1, source_target_pairs={{0,24},{8,16},{16,8},{24,0},{32,56},{40,48},{48,40},{56,32},{64,88... | collective-permute-start | bytes 393224 | tf_op jit(solution)/shard_map/ppermute | solution.py:44
  7.5 11.0 %collective-permute-start.8 = (bf16[16,4096]{1,0:T(8,128)(2,1)}, bf16[16,4096]{1,0:T(8,128)(2,1)S(1)}, u32[]{:S(2)}, u32[]{:S(2)}) collective-permute-start(bf16[16,4096]{1,0:T(8,128)(2,1)} %get-tuple-element.49), channel_id=1, source_target_pairs={{0,56},{8,48},{16,40},{24,32},{32,88},{40,80},{48,72},{56,64},{64,... | collective-permute-start | bytes 393224 | tf_op jit(solution)/shard_map/ppermute | solution.py:44
  9.1 13.4 %collective-permute-start.9 = (bf16[16,4096]{1,0:T(8,128)(2,1)}, bf16[16,4096]{1,0:T(8,128)(2,1)S(1)}, u32[]{:S(2)}, u32[]{:S(2)}) collective-permute-start(bf16[16,4096]{1,0:T(8,128)(2,1)} %get-tuple-element.50), channel_id=1, source_target_pairs={{0,88},{8,80},{16,72},{24,64},{32,120},{40,112},{48,104},{56,96},{... | collective-permute-start | bytes 393224 | tf_op jit(solution)/shard_map/ppermute | solution.py:44
  15.1 7.4 %collective-permute-start.10 = (bf16[16,4096]{1,0:T(8,128)(2,1)}, bf16[16,4096]{1,0:T(8,128)(2,1)S(1)}, u32[]{:S(2)}, u32[]{:S(2)}) collective-permute-start(bf16[16,4096]{1,0:T(8,128)(2,1)} %get-tuple-element.51), channel_id=1, source_target_pairs={{0,120},{8,112},{16,104},{24,96},{32,24},{40,16},{48,8},{56,0},{64... | collective-permute-start | bytes 393224 | tf_op jit(solution)/shard_map/ppermute | solution.py:44
  15.8 7.6 %collective-permute-start = (bf16[16,4096]{1,0:T(8,128)(2,1)}, bf16[16,4096]{1,0:T(8,128)(2,1)S(1)}, u32[]{:S(2)}, u32[]{:S(2)}) collective-permute-start(bf16[16,4096]{1,0:T(8,128)(2,1)} %get-tuple-element.45), channel_id=1, source_target_pairs={{0,32},{8,40},{16,48},{24,56},{32,64},{40,72},{48,80},{56,88},{64,... | collective-permute-start | bytes 393224 | tf_op jit(solution)/shard_map/ppermute | solution.py:44
  16.8 9.9 %collective-permute-start.1 = (bf16[16,4096]{1,0:T(8,128)(2,1)}, bf16[16,4096]{1,0:T(8,128)(2,1)S(1)}, u32[]{:S(2)}, u32[]{:S(2)}) collective-permute-start(bf16[16,4096]{1,0:T(8,128)(2,1)} %get-tuple-element.46), channel_id=1, source_target_pairs={{0,64},{8,72},{16,80},{24,88},{32,96},{40,104},{48,112},{56,120},{... | collective-permute-start | bytes 393224 | tf_op jit(solution)/shard_map/ppermute | solution.py:44
  18.6 36.5 %copy-start = (bf16[1,4096,344]{1,2,0:T(8,128)(2,1)S(1)}, bf16[1,4096,344]{1,2,0:T(8,128)(2,1)}, u32[]{:S(2)}) copy-start(bf16[1,4096,344]{1,2,0:T(8,128)(2,1)} %param.11) | copy-start | bytes 8454148
  18.6 9.6 %collective-permute-start.2 = (bf16[16,4096]{1,0:T(8,128)(2,1)}, bf16[16,4096]{1,0:T(8,128)(2,1)S(1)}, u32[]{:S(2)}, u32[]{:S(2)}) collective-permute-start(bf16[16,4096]{1,0:T(8,128)(2,1)} %get-tuple-element.47), channel_id=1, source_target_pairs={{0,96},{8,104},{16,112},{24,120},{32,0},{40,8},{48,16},{56,24},{64... | collective-permute-start | bytes 393224 | tf_op jit(solution)/shard_map/ppermute | solution.py:44
  22.8 5.8 %collective-permute-start.16 = (bf16[48,4096]{1,0:T(8,128)(2,1)S(1)}, bf16[48,4096]{1,0:T(8,128)(2,1)S(1)}, u32[]{:S(2)}, u32[]{:S(2)}) collective-permute-start(bf16[48,4096]{1,0:T(8,128)(2,1)S(1)} %convolution_convert_fusion.refs_1_), channel_id=1, source_target_pairs={{0,1},{1,0},{2,3},{3,2},{4,5},{5,4},{6,7},{7,6},{8,9},{9,8},{10,11... | collective-permute-start | bytes 1179656 | tf_op jit(solution)/shard_map/ppermute | solution.py:35
  22.9 11.5 %collective-permute-start.14 = (bf16[48,4096]{1,0:T(8,128)(2,1)S(1)}, bf16[48,4096]{1,0:T(8,128)(2,1)S(1)}, u32[]{:S(2)}, u32[]{:S(2)}) collective-permute-start(bf16[48,4096]{1,0:T(8,128)(2,1)S(1)} %convolution_convert_fusion.refs_1_), channel_id=1, source_target_pairs={{0,8},{8,0},{1,9},{9,1},{2,10},{10,2},{3,11},{11,3},{4,12},{12,4},... | collective-permute-start | bytes 1179656 | tf_op jit(solution)/shard_map/ppermute | solution.py:31
  23.4 11.5 %collective-permute-start.13 = (bf16[48,4096]{1,0:T(8,128)(2,1)S(1)}, bf16[48,4096]{1,0:T(8,128)(2,1)S(1)}, u32[]{:S(2)}, u32[]{:S(2)}) collective-permute-start(bf16[48,4096]{1,0:T(8,128)(2,1)S(1)} %convolution_convert_fusion.refs_1_), channel_id=1, source_target_pairs={{0,6},{2,0},{4,2},{6,4},{1,7},{3,1},{5,3},{7,5},{8,14},{10,8},{12,... | collective-permute-start | bytes 1179656 | tf_op jit(solution)/shard_map/ppermute | solution.py:27
  26.7 12.0 %collective-permute-start.12 = (bf16[48,4096]{1,0:T(8,128)(2,1)S(1)}, bf16[48,4096]{1,0:T(8,128)(2,1)S(1)}, u32[]{:S(2)}, u32[]{:S(2)}) collective-permute-start(bf16[48,4096]{1,0:T(8,128)(2,1)S(1)} %convolution_convert_fusion.refs_1_), channel_id=1, source_target_pairs={{0,2},{2,4},{4,6},{6,0},{1,3},{3,5},{5,7},{7,1},{8,10},{10,12},{12... | collective-permute-start | bytes 1179656 | tf_op jit(solution)/shard_map/ppermute | solution.py:27
  28.5 11.7 %collective-permute-start.15 = (bf16[48,4096]{1,0:T(8,128)(2,1)S(1)}, bf16[48,4096]{1,0:T(8,128)(2,1)S(1)}, u32[]{:S(2)}, u32[]{:S(2)}) collective-permute-start(bf16[48,4096]{1,0:T(8,128)(2,1)S(1)} %convolution_convert_fusion.1.refs_0_), channel_id=1, source_target_pairs={{0,1},{1,0},{2,3},{3,2},{4,5},{5,4},{6,7},{7,6},{8,9},{9,8},{10,11... | collective-permute-start | bytes 1179656 | tf_op jit(solution)/shard_map/ppermute | solution.py:35
  28.6 18.5 %collective-permute-start.11 = (bf16[48,4096]{1,0:T(8,128)(2,1)S(1)}, bf16[48,4096]{1,0:T(8,128)(2,1)S(1)}, u32[]{:S(2)}, u32[]{:S(2)}) collective-permute-start(bf16[48,4096]{1,0:T(8,128)(2,1)S(1)} %convolution_convert_fusion.1.refs_0_), channel_id=1, source_target_pairs={{0,2},{2,4},{4,6},{6,0},{1,3},{3,5},{5,7},{7,1},{8,10},{10,12},{12... | collective-permute-start | bytes 1179656 | tf_op jit(solution)/shard_map/ppermute | solution.py:27
  34.4 12.7 %collective-permute-start.5 = (bf16[48,4096]{1,0:T(8,128)(2,1)S(1)}, bf16[48,4096]{1,0:T(8,128)(2,1)S(1)}, u32[]{:S(2)}, u32[]{:S(2)}) collective-permute-start(bf16[48,4096]{1,0:T(8,128)(2,1)S(1)} %convolution_convert_fusion.1.refs_0_), channel_id=1, source_target_pairs={{0,6},{2,0},{4,2},{6,4},{1,7},{3,1},{5,3},{7,5},{8,14},{10,8},{12,... | collective-permute-start | bytes 1179656 | tf_op jit(solution)/shard_map/ppermute | solution.py:27
  35.0 12.7 %collective-permute-start.3 = (bf16[48,4096]{1,0:T(8,128)(2,1)S(1)}, bf16[48,4096]{1,0:T(8,128)(2,1)S(1)}, u32[]{:S(2)}, u32[]{:S(2)}) collective-permute-start(bf16[48,4096]{1,0:T(8,128)(2,1)S(1)} %convolution_convert_fusion.1.refs_0_), channel_id=1, source_target_pairs={{0,8},{8,0},{1,9},{9,1},{2,10},{10,2},{3,11},{11,3},{4,12},{12,4},... | collective-permute-start | bytes 1179656 | tf_op jit(solution)/shard_map/ppermute | solution.py:31
  38.7 15.9 %collective-permute-start.25 = (bf16[48,4096]{1,0:T(8,128)(2,1)S(1)}, bf16[48,4096]{1,0:T(8,128)(2,1)S(1)}, u32[]{:S(2)}, u32[]{:S(2)}) collective-permute-start(bf16[48,4096]{1,0:T(8,128)(2,1)S(1)} %collective-permute-done.14.refs_7_), channel_id=1, source_target_pairs={{0,2},{2,4},{4,6},{6,0},{1,3},{3,5},{5,7},{7,1},{8,10},{10,12},{12... | collective-permute-start | bytes 1179656 | tf_op jit(solution)/shard_map/ppermute | solution.py:27
  40.2 14.4 %collective-permute-start.22 = (bf16[48,4096]{1,0:T(8,128)(2,1)S(1)}, bf16[48,4096]{1,0:T(8,128)(2,1)S(1)}, u32[]{:S(2)}, u32[]{:S(2)}) collective-permute-start(bf16[48,4096]{1,0:T(8,128)(2,1)S(1)} %collective-permute-done.14.refs_7_), channel_id=1, source_target_pairs={{0,1},{1,0},{2,3},{3,2},{4,5},{5,4},{6,7},{7,6},{8,9},{9,8},{10,11... | collective-permute-start | bytes 1179656 | tf_op jit(solution)/shard_map/ppermute | solution.py:35
  47.1 10.2 %collective-permute-start.20 = (bf16[48,4096]{1,0:T(8,128)(2,1)S(1)}, bf16[48,4096]{1,0:T(8,128)(2,1)S(1)}, u32[]{:S(2)}, u32[]{:S(2)}) collective-permute-start(bf16[48,4096]{1,0:T(8,128)(2,1)S(1)} %collective-permute-done.13.refs_5_), channel_id=1, source_target_pairs={{0,1},{1,0},{2,3},{3,2},{4,5},{5,4},{6,7},{7,6},{8,9},{9,8},{10,11... | collective-permute-start | bytes 1179656 | tf_op jit(solution)/shard_map/ppermute | solution.py:35
  47.1 12.0 %collective-permute-start.18 = (bf16[48,4096]{1,0:T(8,128)(2,1)S(1)}, bf16[48,4096]{1,0:T(8,128)(2,1)S(1)}, u32[]{:S(2)}, u32[]{:S(2)}) collective-permute-start(bf16[48,4096]{1,0:T(8,128)(2,1)S(1)} %collective-permute-done.12.refs_3_), channel_id=1, source_target_pairs={{0,1},{1,0},{2,3},{3,2},{4,5},{5,4},{6,7},{7,6},{8,9},{9,8},{10,11... | collective-permute-start | bytes 1179656 | tf_op jit(solution)/shard_map/ppermute | solution.py:35
  47.6 13.6 %collective-permute-start.17 = (bf16[48,4096]{1,0:T(8,128)(2,1)S(1)}, bf16[48,4096]{1,0:T(8,128)(2,1)S(1)}, u32[]{:S(2)}, u32[]{:S(2)}) collective-permute-start(bf16[48,4096]{1,0:T(8,128)(2,1)S(1)} %collective-permute-done.11.refs_2_), channel_id=1, source_target_pairs={{0,1},{1,0},{2,3},{3,2},{4,5},{5,4},{6,7},{7,6},{8,9},{9,8},{10,11... | collective-permute-start | bytes 1179656 | tf_op jit(solution)/shard_map/ppermute | solution.py:35
  54.6 6.7 %collective-permute-start.19 = (bf16[48,4096]{1,0:T(8,128)(2,1)S(1)}, bf16[48,4096]{1,0:T(8,128)(2,1)S(1)}, u32[]{:S(2)}, u32[]{:S(2)}) collective-permute-start(bf16[48,4096]{1,0:T(8,128)(2,1)S(1)} %collective-permute-done.5.refs_4_), channel_id=1, source_target_pairs={{0,1},{1,0},{2,3},{3,2},{4,5},{5,4},{6,7},{7,6},{8,9},{9,8},{10,11... | collective-permute-start | bytes 1179656 | tf_op jit(solution)/shard_map/ppermute | solution.py:35
  54.6 8.1 %collective-permute-start.21 = (bf16[48,4096]{1,0:T(8,128)(2,1)S(1)}, bf16[48,4096]{1,0:T(8,128)(2,1)S(1)}, u32[]{:S(2)}, u32[]{:S(2)}) collective-permute-start(bf16[48,4096]{1,0:T(8,128)(2,1)S(1)} %collective-permute-done.3.refs_6_), channel_id=1, source_target_pairs={{0,1},{1,0},{2,3},{3,2},{4,5},{5,4},{6,7},{7,6},{8,9},{9,8},{10,11... | collective-permute-start | bytes 1179656 | tf_op jit(solution)/shard_map/ppermute | solution.py:35
  57.3 23.4 %collective-permute-start.28 = (bf16[48,4096]{1,0:T(8,128)(2,1)S(1)}, bf16[48,4096]{1,0:T(8,128)(2,1)S(1)}, u32[]{:S(2)}, u32[]{:S(2)}) collective-permute-start(bf16[48,4096]{1,0:T(8,128)(2,1)S(1)} %collective-permute-done.13.refs_5_), channel_id=1, source_target_pairs={{0,6},{2,0},{4,2},{6,4},{1,7},{3,1},{5,3},{7,5},{8,14},{10,8},{12,... | collective-permute-start | bytes 1179656 | tf_op jit(solution)/shard_map/ppermute | solution.py:27
  59.2 25.0 %collective-permute-start.26 = (bf16[48,4096]{1,0:T(8,128)(2,1)S(1)}, bf16[48,4096]{1,0:T(8,128)(2,1)S(1)}, u32[]{:S(2)}, u32[]{:S(2)}) collective-permute-start(bf16[48,4096]{1,0:T(8,128)(2,1)S(1)} %collective-permute-done.13.refs_5_), channel_id=1, source_target_pairs={{0,8},{8,0},{1,9},{9,1},{2,10},{10,2},{3,11},{11,3},{4,12},{12,4},... | collective-permute-start | bytes 1179656 | tf_op jit(solution)/shard_map/ppermute | solution.py:31
  61.2 24.8 %collective-permute-start.27 = (bf16[48,4096]{1,0:T(8,128)(2,1)S(1)}, bf16[48,4096]{1,0:T(8,128)(2,1)S(1)}, u32[]{:S(2)}, u32[]{:S(2)}) collective-permute-start(bf16[48,4096]{1,0:T(8,128)(2,1)S(1)} %collective-permute-done.5.refs_4_), channel_id=1, source_target_pairs={{0,6},{2,0},{4,2},{6,4},{1,7},{3,1},{5,3},{7,5},{8,14},{10,8},{12,... | collective-permute-start | bytes 1179656 | tf_op jit(solution)/shard_map/ppermute | solution.py:27
  61.3 17.3 %collective-permute-start.6 = (bf16[48,4096]{1,0:T(8,128)(2,1)S(1)}, bf16[48,4096]{1,0:T(8,128)(2,1)S(1)}, u32[]{:S(2)}, u32[]{:S(2)}) collective-permute-start(bf16[48,4096]{1,0:T(8,128)(2,1)S(1)} %collective-permute-done.5.refs_4_), channel_id=1, source_target_pairs={{0,8},{8,0},{1,9},{9,1},{2,10},{10,2},{3,11},{11,3},{4,12},{12,4},... | collective-permute-start | bytes 1179656 | tf_op jit(solution)/shard_map/ppermute | solution.py:31
  62.7 15.9 %collective-permute-start.4 = (bf16[48,4096]{1,0:T(8,128)(2,1)S(1)}, bf16[48,4096]{1,0:T(8,128)(2,1)S(1)}, u32[]{:S(2)}, u32[]{:S(2)}) collective-permute-start(bf16[48,4096]{1,0:T(8,128)(2,1)S(1)} %collective-permute-done.3.refs_6_), channel_id=1, source_target_pairs={{0,2},{2,4},{4,6},{6,0},{1,3},{3,5},{5,7},{7,1},{8,10},{10,12},{12... | collective-permute-start | bytes 1179656 | tf_op jit(solution)/shard_map/ppermute | solution.py:27
  78.7 5.0 %collective-permute-start.31 = (bf16[16,4096]{1,0:T(8,128)(2,1)S(1)}, bf16[16,4096]{1,0:T(8,128)(2,1)S(1)}, u32[]{:S(2)}, u32[]{:S(2)}) collective-permute-start(bf16[16,4096]{1,0:T(8,128)(2,1)S(1)} %slice.142), channel_id=1, source_target_pairs={{0,2},{2,4},{4,6},{6,0},{1,3},{3,5},{5,7},{7,1},{8,10},{10,12},{12... | collective-permute-start | bytes 393224 | tf_op jit(solution)/shard_map/ppermute | solution.py:27
  78.7 5.0 %collective-permute-start.30 = (bf16[16,4096]{1,0:T(8,128)(2,1)S(1)}, bf16[16,4096]{1,0:T(8,128)(2,1)S(1)}, u32[]{:S(2)}, u32[]{:S(2)}) collective-permute-start(bf16[16,4096]{1,0:T(8,128)(2,1)S(1)} %slice.109), channel_id=1, source_target_pairs={{0,6},{2,0},{4,2},{6,4},{1,7},{3,1},{5,3},{7,5},{8,14},{10,8},{12,... | collective-permute-start | bytes 393224 | tf_op jit(solution)/shard_map/ppermute | solution.py:27
  80.8 13.6 %collective-permute-start.34 = (bf16[48,4096]{1,0:T(8,128)(2,1)S(1)}, bf16[48,4096]{1,0:T(8,128)(2,1)S(1)}, u32[]{:S(2)}, u32[]{:S(2)}) collective-permute-start(bf16[48,4096]{1,0:T(8,128)(2,1)S(1)} %collective-permute-done.25.refs_1_.refs_9_), channel_id=1, source_target_pairs={{0,1},{1,0},{2,3},{3,2},{4,5},{5,4},{6,7},{7,6},{8,9},{9,8},{10,11... | collective-permute-start | bytes 1179656 | tf_op jit(solution)/shard_map/ppermute | solution.py:35
  83.6 3.0 %collective-permute-start.41 = (bf16[16,4096]{1,0:T(8,128)(2,1)S(1)}, bf16[16,4096]{1,0:T(8,128)(2,1)S(1)}, u32[]{:S(2)}, u32[]{:S(2)}) collective-permute-start(bf16[16,4096]{1,0:T(8,128)(2,1)S(1)} %collective-permute-done.31.refs_8_.refs_16_), channel_id=1, source_target_pairs={{0,1},{1,0},{2,3},{3,2},{4,5},{5,4},{6,7},{7,6},{8,9},{9,8},{10,11... | collective-permute-start | bytes 393224 | tf_op jit(solution)/shard_map/ppermute | solution.py:35
  83.7 2.9 %collective-permute-start.40 = (bf16[16,4096]{1,0:T(8,128)(2,1)S(1)}, bf16[16,4096]{1,0:T(8,128)(2,1)S(1)}, u32[]{:S(2)}, u32[]{:S(2)}) collective-permute-start(bf16[16,4096]{1,0:T(8,128)(2,1)S(1)} %collective-permute-done.30.refs_7_.refs_15_), channel_id=1, source_target_pairs={{0,1},{1,0},{2,3},{3,2},{4,5},{5,4},{6,7},{7,6},{8,9},{9,8},{10,11... | collective-permute-start | bytes 393224 | tf_op jit(solution)/shard_map/ppermute | solution.py:35
  84.2 8.4 %collective-permute-start.32 = (bf16[32,4096]{1,0:T(8,128)(2,1)S(1)}, bf16[32,4096]{1,0:T(8,128)(2,1)S(1)}, u32[]{:S(2)}, u32[]{:S(2)}) collective-permute-start(bf16[32,4096]{1,0:T(8,128)(2,1)S(1)} %slice.143), channel_id=1, source_target_pairs={{0,8},{8,0},{1,9},{9,1},{2,10},{10,2},{3,11},{11,3},{4,12},{12,4},... | collective-permute-start | bytes 786440 | tf_op jit(solution)/shard_map/ppermute | solution.py:31
  86.0 8.3 %collective-permute-start.29 = (bf16[32,4096]{1,0:T(8,128)(2,1)S(1)}, bf16[32,4096]{1,0:T(8,128)(2,1)S(1)}, u32[]{:S(2)}, u32[]{:S(2)}) collective-permute-start(bf16[32,4096]{1,0:T(8,128)(2,1)S(1)} %slice.108), channel_id=1, source_target_pairs={{0,2},{2,4},{4,6},{6,0},{1,3},{3,5},{5,7},{7,1},{8,10},{10,12},{12... | collective-permute-start | bytes 786440 | tf_op jit(solution)/shard_map/ppermute | solution.py:27
  86.6 8.2 %collective-permute-start.38 = (bf16[48,4096]{1,0:T(8,128)(2,1)S(1)}, bf16[48,4096]{1,0:T(8,128)(2,1)S(1)}, u32[]{:S(2)}, u32[]{:S(2)}) collective-permute-start(bf16[48,4096]{1,0:T(8,128)(2,1)S(1)} %collective-permute-done.28.refs_5_.refs_13_), channel_id=1, source_target_pairs={{0,1},{1,0},{2,3},{3,2},{4,5},{5,4},{6,7},{7,6},{8,9},{9,8},{10,11... | collective-permute-start | bytes 1179656 | tf_op jit(solution)/shard_map/ppermute | solution.py:35
  86.6 8.3 %collective-permute-start.36 = (bf16[48,4096]{1,0:T(8,128)(2,1)S(1)}, bf16[48,4096]{1,0:T(8,128)(2,1)S(1)}, u32[]{:S(2)}, u32[]{:S(2)}) collective-permute-start(bf16[48,4096]{1,0:T(8,128)(2,1)S(1)} %collective-permute-done.26.refs_3_.refs_11_), channel_id=1, source_target_pairs={{0,1},{1,0},{2,3},{3,2},{4,5},{5,4},{6,7},{7,6},{8,9},{9,8},{10,11... | collective-permute-start | bytes 1179656 | tf_op jit(solution)/shard_map/ppermute | solution.py:35
  92.6 3.5 %collective-permute-start.33 = (bf16[48,4096]{1,0:T(8,128)(2,1)S(1)}, bf16[48,4096]{1,0:T(8,128)(2,1)S(1)}, u32[]{:S(2)}, u32[]{:S(2)}) collective-permute-start(bf16[48,4096]{1,0:T(8,128)(2,1)S(1)} %collective-permute-done.4.refs_0_.refs_8_), channel_id=1, source_target_pairs={{0,1},{1,0},{2,3},{3,2},{4,5},{5,4},{6,7},{7,6},{8,9},{9,8},{10,11... | collective-permute-start | bytes 1179656 | tf_op jit(solution)/shard_map/ppermute | solution.py:35
  94.3 1.7 %collective-permute-start.37 = (bf16[48,4096]{1,0:T(8,128)(2,1)S(1)}, bf16[48,4096]{1,0:T(8,128)(2,1)S(1)}, u32[]{:S(2)}, u32[]{:S(2)}) collective-permute-start(bf16[48,4096]{1,0:T(8,128)(2,1)S(1)} %collective-permute-done.27.refs_4_.refs_12_), channel_id=1, source_target_pairs={{0,1},{1,0},{2,3},{3,2},{4,5},{5,4},{6,7},{7,6},{8,9},{9,8},{10,11... | collective-permute-start | bytes 1179656 | tf_op jit(solution)/shard_map/ppermute | solution.py:35
  94.3 2.3 %collective-permute-start.35 = (bf16[48,4096]{1,0:T(8,128)(2,1)S(1)}, bf16[48,4096]{1,0:T(8,128)(2,1)S(1)}, u32[]{:S(2)}, u32[]{:S(2)}) collective-permute-start(bf16[48,4096]{1,0:T(8,128)(2,1)S(1)} %collective-permute-done.6.refs_2_.refs_10_), channel_id=1, source_target_pairs={{0,1},{1,0},{2,3},{3,2},{4,5},{5,4},{6,7},{7,6},{8,9},{9,8},{10,11... | collective-permute-start | bytes 1179656 | tf_op jit(solution)/shard_map/ppermute | solution.py:35
  94.8 2.1 %collective-permute-start.42 = (bf16[32,4096]{1,0:T(8,128)(2,1)S(1)}, bf16[32,4096]{1,0:T(8,128)(2,1)S(1)}, u32[]{:S(2)}, u32[]{:S(2)}) collective-permute-start(bf16[32,4096]{1,0:T(8,128)(2,1)S(1)} %collective-permute-done.32.refs_9_.refs_17_), channel_id=1, source_target_pairs={{0,1},{1,0},{2,3},{3,2},{4,5},{5,4},{6,7},{7,6},{8,9},{9,8},{10,11... | collective-permute-start | bytes 786440 | tf_op jit(solution)/shard_map/ppermute | solution.py:35
  94.9 2.4 %collective-permute-start.39 = (bf16[32,4096]{1,0:T(8,128)(2,1)S(1)}, bf16[32,4096]{1,0:T(8,128)(2,1)S(1)}, u32[]{:S(2)}, u32[]{:S(2)}) collective-permute-start(bf16[32,4096]{1,0:T(8,128)(2,1)S(1)} %collective-permute-done.29.refs_6_.refs_14_), channel_id=1, source_target_pairs={{0,1},{1,0},{2,3},{3,2},{4,5},{5,4},{6,7},{7,6},{8,9},{9,8},{10,11... | collective-permute-start | bytes 786440 | tf_op jit(solution)/shard_map/ppermute | solution.py:35
  103.9 3.6 %collective-permute-start.43 = (bf16[384,2176]{1,0:T(8,128)(2,1)S(1)}, bf16[384,2176]{1,0:T(8,128)(2,1)S(1)}, u32[]{:S(2)}, u32[]{:S(2)}) collective-permute-start(bf16[384,2176]{1,0:T(8,128)(2,1)S(1)} %get-tuple-element.63), channel_id=1, source_target_pairs={{0,1},{1,0},{2,3},{3,2},{4,5},{5,4},{6,7},{7,6},{8,9},{9,8},{10,11... | collective-permute-start | bytes 5013512 | tf_op jit(solution)/shard_map/ppermute | solution.py:35
  104.2 28.1 %collective-permute-start.23 = (bf16[384,2176]{1,0:T(8,128)(2,1)S(1)}, bf16[384,2176]{1,0:T(8,128)(2,1)S(1)}, u32[]{:S(2)}, u32[]{:S(2)}) collective-permute-start(bf16[384,2176]{1,0:T(8,128)(2,1)S(1)} %get-tuple-element.58), channel_id=1, source_target_pairs={{0,1},{1,0},{2,3},{3,2},{4,5},{5,4},{6,7},{7,6},{8,9},{9,8},{10,11... | collective-permute-start | bytes 5013512 | tf_op jit(solution)/shard_map/ppermute | solution.py:35
  107.7 5.8 %collective-permute-start.48 = (bf16[32,2176]{1,0:T(8,128)(2,1)S(1)}, bf16[32,2176]{1,0:T(8,128)(2,1)S(1)}, u32[]{:S(2)}, u32[]{:S(2)}) collective-permute-start(bf16[32,2176]{1,0:T(8,128)(2,1)S(1)} %get-tuple-element.85), channel_id=1, source_target_pairs={{0,8},{8,0},{1,9},{9,1},{2,10},{10,2},{3,11},{11,3},{4,12},{12,4},... | collective-permute-start | bytes 417800 | tf_op jit(solution)/shard_map/ppermute | solution.py:31
  108.4 7.0 %collective-permute-start.46 = (bf16[32,2176]{1,0:T(8,128)(2,1)S(1)}, bf16[32,2176]{1,0:T(8,128)(2,1)S(1)}, u32[]{:S(2)}, u32[]{:S(2)}) collective-permute-start(bf16[32,2176]{1,0:T(8,128)(2,1)S(1)} %get-tuple-element.86), channel_id=1, source_target_pairs={{0,2},{2,4},{4,6},{6,0},{1,3},{3,5},{5,7},{7,1},{8,10},{10,12},{12... | collective-permute-start | bytes 417800 | tf_op jit(solution)/shard_map/ppermute | solution.py:27
  110.3 5.9 %collective-permute-start.44 = (bf16[32,2176]{1,0:T(8,128)(2,1)S(1)}, bf16[32,2176]{1,0:T(8,128)(2,1)S(1)}, u32[]{:S(2)}, u32[]{:S(2)}) collective-permute-start(bf16[32,2176]{1,0:T(8,128)(2,1)S(1)} %get-tuple-element.87), channel_id=1, source_target_pairs={{0,6},{2,0},{4,2},{6,4},{1,7},{3,1},{5,3},{7,5},{8,14},{10,8},{12,... | collective-permute-start | bytes 417800 | tf_op jit(solution)/shard_map/ppermute | solution.py:27
  116.6 15.6 %collective-permute-start.49 = (bf16[96,2176]{1,0:T(8,128)(2,1)S(1)}, bf16[96,2176]{1,0:T(8,128)(2,1)S(1)}, u32[]{:S(2)}, u32[]{:S(2)}) collective-permute-start(bf16[96,2176]{1,0:T(8,128)(2,1)S(1)} %get-tuple-element.82), channel_id=1, source_target_pairs={{0,2},{2,4},{4,6},{6,0},{1,3},{3,5},{5,7},{7,1},{8,10},{10,12},{12... | collective-permute-start | bytes 1253384 | tf_op jit(solution)/shard_map/ppermute | solution.py:27
  118.4 13.8 %collective-permute-start.47 = (bf16[96,2176]{1,0:T(8,128)(2,1)S(1)}, bf16[96,2176]{1,0:T(8,128)(2,1)S(1)}, u32[]{:S(2)}, u32[]{:S(2)}) collective-permute-start(bf16[96,2176]{1,0:T(8,128)(2,1)S(1)} %get-tuple-element.83), channel_id=1, source_target_pairs={{0,8},{8,0},{1,9},{9,1},{2,10},{10,2},{3,11},{11,3},{4,12},{12,4},... | collective-permute-start | bytes 1253384 | tf_op jit(solution)/shard_map/ppermute | solution.py:31
  119.3 12.9 %collective-permute-start.45 = (bf16[96,2176]{1,0:T(8,128)(2,1)S(1)}, bf16[96,2176]{1,0:T(8,128)(2,1)S(1)}, u32[]{:S(2)}, u32[]{:S(2)}) collective-permute-start(bf16[96,2176]{1,0:T(8,128)(2,1)S(1)} %get-tuple-element.84), channel_id=1, source_target_pairs={{0,6},{2,0},{4,2},{6,4},{1,7},{3,1},{5,3},{7,5},{8,14},{10,8},{12,... | collective-permute-start | bytes 1253384 | tf_op jit(solution)/shard_map/ppermute | solution.py:27
  132.7 11.3 %collective-permute-start.51 = (bf16[96,2176]{1,0:T(8,128)(2,1)S(1)}, bf16[96,2176]{1,0:T(8,128)(2,1)S(1)}, u32[]{:S(2)}, u32[]{:S(2)}) collective-permute-start(bf16[96,2176]{1,0:T(8,128)(2,1)S(1)} %get-tuple-element.79), channel_id=1, source_target_pairs={{0,8},{8,0},{1,9},{9,1},{2,10},{10,2},{3,11},{11,3},{4,12},{12,4},... | collective-permute-start | bytes 1253384 | tf_op jit(solution)/shard_map/ppermute | solution.py:31
  133.8 10.8 %collective-permute-start.50 = (bf16[96,2176]{1,0:T(8,128)(2,1)S(1)}, bf16[96,2176]{1,0:T(8,128)(2,1)S(1)}, u32[]{:S(2)}, u32[]{:S(2)}) collective-permute-start(bf16[96,2176]{1,0:T(8,128)(2,1)S(1)} %get-tuple-element.80), channel_id=1, source_target_pairs={{0,2},{2,4},{4,6},{6,0},{1,3},{3,5},{5,7},{7,1},{8,10},{10,12},{12... | collective-permute-start | bytes 1253384 | tf_op jit(solution)/shard_map/ppermute | solution.py:27
  136.0 9.2 %collective-permute-start.24 = (bf16[96,2176]{1,0:T(8,128)(2,1)S(1)}, bf16[96,2176]{1,0:T(8,128)(2,1)S(1)}, u32[]{:S(2)}, u32[]{:S(2)}) collective-permute-start(bf16[96,2176]{1,0:T(8,128)(2,1)S(1)} %get-tuple-element.81), channel_id=1, source_target_pairs={{0,6},{2,0},{4,2},{6,4},{1,7},{3,1},{5,3},{7,5},{8,14},{10,8},{12,... | collective-permute-start | bytes 1253384 | tf_op jit(solution)/shard_map/ppermute | solution.py:27
  145.5 18.0 %copy-start.3 = (bf16[24,128]{1,0:T(8,128)(2,1)S(1)}, bf16[24,128]{1,0:T(8,128)(2,1)}, u32[]{:S(2)}) copy-start(bf16[24,128]{1,0:T(8,128)(2,1)} %get-tuple-element.42.first_ref) | copy-start | bytes 18436
  145.5 18.0 %copy-start.4 = (bf16[24,128]{1,0:T(8,128)(2,1)S(1)}, bf16[24,128]{1,0:T(8,128)(2,1)}, u32[]{:S(2)}) copy-start(bf16[24,128]{1,0:T(8,128)(2,1)} %get-tuple-element.43.second_ref) | copy-start | bytes 18436
  145.5 17.9 %copy-start.5 = (f32[24,2]{0,1:T(2,128)S(1)}, f32[24,2]{0,1:T(2,128)}, u32[]{:S(2)}) copy-start(f32[24,2]{0,1:T(2,128)} %param.10) | copy-start | bytes 580
  146.2 10.1 %collective-permute-start.58 = (bf16[16,2176]{1,0:T(8,128)(2,1)S(1)}, bf16[16,2176]{1,0:T(8,128)(2,1)S(1)}, u32[]{:S(2)}, u32[]{:S(2)}) collective-permute-start(bf16[16,2176]{1,0:T(8,128)(2,1)S(1)} %get-tuple-element.88), channel_id=1, source_target_pairs={{0,56},{8,48},{16,40},{24,32},{32,88},{40,80},{48,72},{56,64},{64,... | collective-permute-start | bytes 208904 | tf_op jit(solution)/shard_map/ppermute | solution.py:44
  148.8 8.6 %collective-permute-start.56 = (bf16[16,2176]{1,0:T(8,128)(2,1)S(1)}, bf16[16,2176]{1,0:T(8,128)(2,1)S(1)}, u32[]{:S(2)}, u32[]{:S(2)}) collective-permute-start(bf16[16,2176]{1,0:T(8,128)(2,1)S(1)} %get-tuple-element.89), channel_id=1, source_target_pairs={{0,88},{8,80},{16,72},{24,64},{32,120},{40,112},{48,104},{56,96},{... | collective-permute-start | bytes 208904 | tf_op jit(solution)/shard_map/ppermute | solution.py:44
  150.8 9.1 %collective-permute-start.54 = (bf16[16,2176]{1,0:T(8,128)(2,1)S(1)}, bf16[16,2176]{1,0:T(8,128)(2,1)S(1)}, u32[]{:S(2)}, u32[]{:S(2)}) collective-permute-start(bf16[16,2176]{1,0:T(8,128)(2,1)S(1)} %get-tuple-element.90), channel_id=1, source_target_pairs={{0,120},{8,112},{16,104},{24,96},{32,24},{40,16},{48,8},{56,0},{64... | collective-permute-start | bytes 208904 | tf_op jit(solution)/shard_map/ppermute | solution.py:44
  153.9 6.0 %collective-permute-start.52 = (bf16[16,2176]{1,0:T(8,128)(2,1)S(1)}, bf16[16,2176]{1,0:T(8,128)(2,1)S(1)}, u32[]{:S(2)}, u32[]{:S(2)}) collective-permute-start(bf16[16,2176]{1,0:T(8,128)(2,1)S(1)} %get-tuple-element.91), channel_id=1, source_target_pairs={{0,24},{8,16},{16,8},{24,0},{32,56},{40,48},{48,40},{56,32},{64,88... | collective-permute-start | bytes 208904 | tf_op jit(solution)/shard_map/ppermute | solution.py:44
  156.3 6.3 %collective-permute-start.57 = (bf16[16,2176]{1,0:T(8,128)(2,1)S(1)}, bf16[16,2176]{1,0:T(8,128)(2,1)S(1)}, u32[]{:S(2)}, u32[]{:S(2)}) collective-permute-start(bf16[16,2176]{1,0:T(8,128)(2,1)S(1)} %get-tuple-element.92), channel_id=1, source_target_pairs={{0,32},{8,40},{16,48},{24,56},{32,64},{40,72},{48,80},{56,88},{64,... | collective-permute-start | bytes 208904 | tf_op jit(solution)/shard_map/ppermute | solution.py:44
  156.3 6.3 %collective-permute-start.55 = (bf16[16,2176]{1,0:T(8,128)(2,1)S(1)}, bf16[16,2176]{1,0:T(8,128)(2,1)S(1)}, u32[]{:S(2)}, u32[]{:S(2)}) collective-permute-start(bf16[16,2176]{1,0:T(8,128)(2,1)S(1)} %get-tuple-element.93), channel_id=1, source_target_pairs={{0,64},{8,72},{16,80},{24,88},{32,96},{40,104},{48,112},{56,120},{... | collective-permute-start | bytes 208904 | tf_op jit(solution)/shard_map/ppermute | solution.py:44
  157.3 6.1 %collective-permute-start.53 = (bf16[16,2176]{1,0:T(8,128)(2,1)S(1)}, bf16[16,2176]{1,0:T(8,128)(2,1)S(1)}, u32[]{:S(2)}, u32[]{:S(2)}) collective-permute-start(bf16[16,2176]{1,0:T(8,128)(2,1)S(1)} %get-tuple-element.94), channel_id=1, source_target_pairs={{0,96},{8,104},{16,112},{24,120},{32,0},{40,8},{48,16},{56,24},{64... | collective-permute-start | bytes 208904 | tf_op jit(solution)/shard_map/ppermute | solution.py:44
  (3 other events, 15.0 us)

commit v5 on v4

--- a/solution.py
+++ b/solution.py
@@ -222,43 +222,25 @@
 
 def weight_kernel(sizes, offset, half, hid, tile, place_ref, *refs):
     count = len(sizes)
-    kinds = len(refs) - 2 * count - 7
+    kinds = len(refs) - 2 * count - 5
     ours, theirs = refs[:count], refs[count : 2 * count]
     sides = refs[2 * count : 2 * count + 2]
     outs = refs[2 * count + 2 : 2 * count + 2 + kinds]
-    rows_ref, sides_t, stage, in_sem, out_sem = refs[2 * count + 2 + kinds :]
+    sides_t, stage, out_sem = refs[2 * count + 2 + kinds :]
     core = place_ref[0]
-    loads = []
-    for s, group in enumerate((ours, theirs)):
-        at = 0
-        copies = []
-        for i, size in enumerate(sizes):
-            copies.append(
-                pltpu.make_async_copy(
-                    group[i].at[:, pl.ds(offset, half)],
-                    rows_ref.at[s, pl.ds(at, size), :],
-                    in_sem.at[s, i],
-                )
-            )
-            at += size
-        loads.append(copies)
-    for copies in loads:
-        for c in copies:
-            c.start()
     depth = sides[0].shape[0]
     wide = sides[0].shape[1] // kinds
     for i in range(2):
         sides_t[:, depth * i : depth * (i + 1)] = sides[i][...].T
     stores = []
-    for s in range(2):
-        for c in loads[s]:
-            c.wait()
+    for s, group in enumerate((ours, theirs)):
         base = (core if s == 0 else 1 - core) * half
 
         @pl.loop(0, half // tile)
         def _(j):
             to = pl.ds(pl.multiple_of(base + j * tile, tile), tile)
-            block = rows_ref[s, :, pl.ds(pl.multiple_of(j * tile, tile), tile)]
+            lanes = pl.ds(pl.multiple_of(offset + j * tile, tile), tile)
+            block = jnp.concatenate([r[:, lanes] for r in group], axis=0)
             grads = dot_f32(sides_t[...], block, 1, 0).astype(BF)
             for k in range(kinds):
                 stage[k, :, to] = grads[wide * k : wide * k + hid]
@@ -284,16 +266,14 @@
     return pl.pallas_call(
         functools.partial(weight_kernel, sizes, offset, width // 2, hid, tile),
         out_shape=[jax.ShapeDtypeStruct((hid, width), BF)] * kinds,
-        in_specs=[SMEM] + [anywhere] * (2 * len(sizes)) + [VMEM] * len(sides),
+        in_specs=[SMEM] + [VMEM] * (2 * len(sizes) + len(sides)),
         out_specs=[anywhere] * kinds,
         scratch_shapes=[
-            pltpu.VMEM((2, rows, width // 2), BF),
             pltpu.VMEM((kinds * wide, rows), BF),
             pltpu.VMEM((kinds, hid, width), BF),
-            pltpu.SemaphoreType.DMA((2, len(sizes))),
             pltpu.SemaphoreType.DMA((2, kinds)),
         ],
-        compiler_params=pltpu.CompilerParams(vmem_limit_bytes=22 * MIB),
+        compiler_params=pltpu.CompilerParams(vmem_limit_bytes=18 * MIB),
         cost_estimate=pl.CostEstimate(
             flops=2 * kinds * rows * hid * width, bytes_accessed=14 * MIB, transcendentals=0
         ),
@@ -394,6 +374,7 @@
     def chunk(keep, got, i, a=0, b=packed):
         return add(keep[packed * i + a : packed * i + b], got[packed * i + a : packed * i + b])
 
+    c_left = along_x(chunk(near_keep, near_got, 1), -1)
     t_last = [chunk(far_keep, far_got, 3, third * i, third * (i + 1)) for i in range(3)]
     a_left = along_x(t_last[0], -1)
     a_right = along_x(t_last[1], 1)
@@ -402,32 +383,37 @@
     t_far_left = add(chunk(far_keep, far_got, 0), jnp.pad(a_left, pads[0]))
     t_far_right = add(chunk(far_keep, far_got, 1), jnp.pad(a_right, pads[1]))
     t_across = add(chunk(far_keep, far_got, 2), jnp.pad(a_pair, pads[2]))
-    b_partner = along_x(t_far_left, -1)
     b_right_pair = pair_y(t_far_right)
     b_right = along_x(t_across, 1)
+    b_partner = along_x(t_far_left, -1)
     rows = (near + far, near_other + far_other)
     sides = [near_out[2], far_out[2]]
     gate_grad, up_grad = weight_grads(place, *rows, sides, 0, hid)
     tied = lax.optimization_barrier((b_partner, b_right_pair, b_right, gate_grad, up_grad))
     b_partner, b_right_pair, b_right, gate_grad, up_grad = tied
-    c_left = along_x(chunk(near_keep, near_got, 1), -1)
-    c_right = along_x(add(chunk(near_keep, near_got, 2), b_right_pair, b_right), 1)
-    c_pair = pair_y(add(chunk(near_keep, near_got, 3), b_partner))
     half = tokens.shape[1] // 2
     (down_grad,) = weight_grads(place, *rows, [near_out[3], far_out[3]], half, hid)
-    tied = lax.optimization_barrier((c_left, c_right, c_pair, down_grad))
-    c_left, c_right, c_pair, down_grad = tied
-    home = add(chunk(near_keep, near_got, 0), c_left, c_right, c_pair)
-
+    c_right, c_pair = [], []
+    for h in range(2):
+        span = (part * h, part * (h + 1))
+        cut = slice(*span)
+        value = add(chunk(near_keep, near_got, 2, *span), b_right_pair[cut], b_right[cut])
+        c_right.append(along_x(value, 1))
+        value = add(chunk(near_keep, near_got, 3, *span), b_partner[cut])
+        c_pair.append(pair_y(value))
     backs = [None] * EXPERTS
-    for dy in range(2):
-        spread = dot_f32(pack, home[part * dy : part * (dy + 1)], 0, 0).astype(BF)
+    base = (near_keep, near_got, c_left)
+    for h in range(2):
+        span = (part * h, part * (h + 1))
+        home = add(chunk(base[0], base[1], 0, *span), base[2][slice(*span)], c_right[h], c_pair[h])
+        if h == 0:
+            home, *base = lax.optimization_barrier((home, *base))
+        spread = dot_f32(pack, home, 0, 0).astype(BF)
         for dz in (2, 1, 3, 0):
-            k = 2 * dz + dy
             piece = spread[ROOM * dz : ROOM * (dz + 1)]
-            if k:
-                piece = to_expert(piece, dz, dy, -1)
-            backs[k] = piece
+            if dz or h:
+                piece = to_expert(piece, dz, h, -1)
+            backs[2 * dz + h] = piece
     token_grad, route_grad = combine(route_weights.T, first, second, backs)
 
     return token_grad, route_grad.T, gate_grad.T[None], up_grad.T[None], down_grad[None]

time: 167 us -> 171 us (1.024)
  starting transfers between devices: 62.7 us -> 70.6 us
  Pallas kernels: 39 us -> 34.9 us
    ppermute x17 -> x18, waiting for transfers between devices: 23.5 us -> 39.9 us  [along_x(): return lax.ppermute(value, 'x', [(i, (i + step) % 4) for i in range(4)])]
    ppermute x8 -> x9, waiting for transfers between devices: 20.4 us -> 5.88 us  [pair_y(): return lax.ppermute(value, 'yl', [(0, 1), (1, 0)])]
    ppermute x17 -> x18, starting transfers between devices: 19.5 us -> 26.5 us  [along_x(): return lax.ppermute(value, 'x', [(i, (i + step) % 4) for i in range(4)])]
    pallas_call x2, Pallas kernels: 17.3 us -> 13.1 us  [weight_grads(): pl.pallas_call(functools.partial(weight_kernel, sizes, offset, width // 2...]
    ppermute x14, starting transfers between devices: 28.7 us -> 32 us  [to_expert(): return lax.ppermute(value, ('z', 'yh', 'yl'), perm)]
    ppermute x8 -> x9, starting transfers between devices: 10.6 us -> 7.94 us  [pair_y(): return lax.ppermute(value, 'yl', [(0, 1), (1, 0)])]
  transfers between devices with their start and end apart: 59 -> 61, of which waited for: 25 -> 23; matrix products, arithmetic and copies ran while one was open for 1% -> 2% of each run, Pallas kernels for 17% -> 14%
where the time goes in v5:
time: 171 us; the launch traced here: 169 us
  starting transfers between devices  70.6 us (41%)
  waiting for transfers between devices  56.3 us (33%)
  Pallas kernels  34.9 us (20%)
  matrix products  2.34 us (1%)
  local copies, waits for them, and re-layouts  1.92 us (1%)
  other arithmetic  1.74 us (1%)
    ppermute x18, waiting for transfers between devices, along_x(): return lax.ppermute(value, 'x', [(i, (i + step) % 4) for i in range(4)])  39.9 us
    ppermute x14, starting transfers between devices, to_expert(): return lax.ppermute(value, ('z', 'yh', 'yl'), perm)  32 us
    ppermute x18, starting transfers between devices, along_x(): return lax.ppermute(value, 'x', [(i, (i + step) % 4) for i in range(4)])  26.5 us
    pallas_call x2, Pallas kernels, run_group(): pl.pallas_call(functools.partial(group_kernel, len(ours), half), out_shap...  13.1 us
    pallas_call x2, Pallas kernels, weight_grads(): pl.pallas_call(functools.partial(weight_kernel, sizes, offset, width // 2...  13.1 us
    ppermute x14, waiting for transfers between devices, to_expert(): return lax.ppermute(value, ('z', 'yh', 'yl'), perm)  8.41 us
    ppermute x9, starting transfers between devices, pair_y(): return lax.ppermute(value, 'yl', [(0, 1), (1, 0)])  7.94 us
    ppermute x9, waiting for transfers between devices, pair_y(): return lax.ppermute(value, 'yl', [(0, 1), (1, 0)])  5.88 us
  transfers between devices with their start and end apart: 61, of which 23 were waited for; matrix products, arithmetic and copies ran while one was open for 2% of the time, Pallas kernels for 14%

profile of v5, /device:TPU:2, one launch (start us, length us, event | category | flops | bytes accessed | tf_op | source)
XLA Modules:
  0.0 168.7 jit_solution(17271839976787964330)
XLA Ops:
  0.6 0.7 pad_add_fusion.place_ref
  1.3 3.2 %slots.1 = (bf16[16,4096]{1,0:T(8,128)(2,1)}, bf16[16,4096]{1,0:T(8,128)(2,1)}, bf16[16,4096]{1,0:T(8,128)(2,1)}, bf16[16,4096]{1,0:T(8,128)(2,1)}, bf16[16,4096...) custom-call(s32[3]{0:T(128)} %pad_add_fusion.place_ref, ...), custom_call_target="tpu_custom_call" | custom-call | flops 50331648 | bytes 3145728 | tf_op jit(solution)/shard_map/slots/pallas_call | solution.py:97
  4.5 4.1 %collective-permute-start.2 = (bf16[16,4096]{1,0:T(8,128)(2,1)}, bf16[16,4096]{1,0:T(8,128)(2,1)S(1)}, u32[]{:S(2)}, u32[]{:S(2)}) collective-permute-start(bf16[16,4096]{1,0:T(8,128)(2,1)} %get-tuple-element.47), channel_id=1, source_target_pairs={{0,96},{8,104},{16,112},{24,120},{32,0},{40,8},{48,16},{56,24},{64... | collective-permute-start | bytes 393224 | tf_op jit(solution)/shard_map/ppermute | solution.py:44
  8.6 1.2 collective-permute-start
  9.8 4.4 %collective-permute-start.10 = (bf16[16,4096]{1,0:T(8,128)(2,1)}, bf16[16,4096]{1,0:T(8,128)(2,1)S(1)}, u32[]{:S(2)}, u32[]{:S(2)}) collective-permute-start(bf16[16,4096]{1,0:T(8,128)(2,1)} %get-tuple-element.51), channel_id=1, source_target_pairs={{0,120},{8,112},{16,104},{24,96},{32,24},{40,16},{48,8},{56,0},{64... | collective-permute-start | bytes 393224 | tf_op jit(solution)/shard_map/ppermute | solution.py:44
  14.3 2.0 %collective-permute-start.9 = (bf16[16,4096]{1,0:T(8,128)(2,1)}, bf16[16,4096]{1,0:T(8,128)(2,1)S(1)}, u32[]{:S(2)}, u32[]{:S(2)}) collective-permute-start(bf16[16,4096]{1,0:T(8,128)(2,1)} %get-tuple-element.50), channel_id=1, source_target_pairs={{0,88},{8,80},{16,72},{24,64},{32,120},{40,112},{48,104},{56,96},{... | collective-permute-start | bytes 393224 | tf_op jit(solution)/shard_map/ppermute | solution.py:44
  16.3 2.4 %collective-permute-done.2 = bf16[16,4096]{1,0:T(8,128)(2,1)S(1)} collective-permute-done((bf16[16,4096]{1,0:T(8,128)(2,1)}, bf16[16,4096]{1,0:T(8,128)(2,1)S(1)}, u32[]{:S(2)}, u32[]{:S(2)}) %collective-permute-start.2) | collective-permute-done | bytes 131104 | tf_op jit(solution)/shard_map/ppermute | solution.py:44
  18.7 4.4 %collective-permute-start.7 = (bf16[16,4096]{1,0:T(8,128)(2,1)}, bf16[16,4096]{1,0:T(8,128)(2,1)S(1)}, u32[]{:S(2)}, u32[]{:S(2)}) collective-permute-start(bf16[16,4096]{1,0:T(8,128)(2,1)} %get-tuple-element.48), channel_id=1, source_target_pairs={{0,24},{8,16},{16,8},{24,0},{32,56},{40,48},{48,40},{56,32},{64,88... | collective-permute-start | bytes 393224 | tf_op jit(solution)/shard_map/ppermute | solution.py:44
  23.1 1.3 convolution_convert_fusion.1.refs_0_
  24.7 0.5 collective-permute-start.5
  25.2 1.5 collective-permute-start.11
  26.7 4.0 %collective-permute-done.8 = bf16[16,4096]{1,0:T(8,128)(2,1)S(1)} collective-permute-done((bf16[16,4096]{1,0:T(8,128)(2,1)}, bf16[16,4096]{1,0:T(8,128)(2,1)S(1)}, u32[]{:S(2)}, u32[]{:S(2)}) %collective-permute-start.8) | collective-permute-done | bytes 131104 | tf_op jit(solution)/shard_map/ppermute | solution.py:44
  31.0 1.6 collective-permute-start.12
  32.6 0.5 collective-permute-start.13
  33.1 1.7 %collective-permute-start.14 = (bf16[48,4096]{1,0:T(8,128)(2,1)S(1)}, bf16[48,4096]{1,0:T(8,128)(2,1)S(1)}, u32[]{:S(2)}, u32[]{:S(2)}) collective-permute-start(bf16[48,4096]{1,0:T(8,128)(2,1)S(1)} %convolution_convert_fusion.refs_1_), channel_id=1, source_target_pairs={{0,8},{8,0},{1,9},{9,1},{2,10},{10,2},{3,11},{11,3},{4,12},{12,4},... | collective-permute-start | bytes 1179656 | tf_op jit(solution)/shard_map/ppermute | solution.py:31
  34.9 1.5 collective-permute-done.5.refs_4_
  36.4 1.6 collective-permute-done.11.refs_2_
  38.0 6.4 %collective-permute-done.12.refs_3_ = bf16[48,4096]{1,0:T(8,128)(2,1)S(1)} collective-permute-done((bf16[48,4096]{1,0:T(8,128)(2,1)S(1)}, bf16[48,4096]{1,0:T(8,128)(2,1)S(1)}, u32[]{:S(2)}, u32[]{:S(2)}) %collective-permute-start.12) | collective-permute-done | bytes 393248 | tf_op jit(solution)/shard_map/ppermute | solution.py:27
  44.3 0.5 collective-permute-start.4
  44.8 0.5 collective-permute-start.18
  45.8 8.5 %collective-permute-done.4.refs_0_.refs_8_ = bf16[48,4096]{1,0:T(8,128)(2,1)S(1)} collective-permute-done((bf16[48,4096]{1,0:T(8,128)(2,1)S(1)}, bf16[48,4096]{1,0:T(8,128)(2,1)S(1)}, u32[]{:S(2)}, u32[]{:S(2)}) %collective-permute-start.4) | collective-permute-done | bytes 393248 | tf_op jit(solution)/shard_map/ppermute | solution.py:27
  54.3 0.5 collective-permute-start.22
  54.8 1.8 %copy-done.1 = bf16[1,4096,344]{1,2,0:T(8,128)(2,1)S(1)} copy-done((bf16[1,4096,344]{1,2,0:T(8,128)(2,1)S(1)}, bf16[1,4096,344]{1,2,0:T(8,128)(2,1)}, u32[]{:S(2)}) %copy-start.1) | copy-done | bytes 2818072
  57.2 2.0 %collective-permute-start.26 = (bf16[48,4096]{1,0:T(8,128)(2,1)S(1)}, bf16[48,4096]{1,0:T(8,128)(2,1)S(1)}, u32[]{:S(2)}, u32[]{:S(2)}) collective-permute-start(bf16[48,4096]{1,0:T(8,128)(2,1)S(1)} %collective-permute-done.13.refs_5_), channel_id=1, source_target_pairs={{0,8},{8,0},{1,9},{9,1},{2,10},{10,2},{3,11},{11,3},{4,12},{12,4},... | collective-permute-start | bytes 1179656 | tf_op jit(solution)/shard_map/ppermute | solution.py:31
  59.2 3.0 %collective-permute-start.27 = (bf16[48,4096]{1,0:T(8,128)(2,1)S(1)}, bf16[48,4096]{1,0:T(8,128)(2,1)S(1)}, u32[]{:S(2)}, u32[]{:S(2)}) collective-permute-start(bf16[48,4096]{1,0:T(8,128)(2,1)S(1)} %collective-permute-done.5.refs_4_), channel_id=1, source_target_pairs={{0,6},{2,0},{4,2},{6,4},{1,7},{3,1},{5,3},{7,5},{8,14},{10,8},{12,... | collective-permute-start | bytes 1179656 | tf_op jit(solution)/shard_map/ppermute | solution.py:27
  62.2 3.2 %collective-permute-start.28 = (bf16[48,4096]{1,0:T(8,128)(2,1)S(1)}, bf16[48,4096]{1,0:T(8,128)(2,1)S(1)}, u32[]{:S(2)}, u32[]{:S(2)}) collective-permute-start(bf16[48,4096]{1,0:T(8,128)(2,1)S(1)} %collective-permute-done.13.refs_5_), channel_id=1, source_target_pairs={{0,6},{2,0},{4,2},{6,4},{1,7},{3,1},{5,3},{7,5},{8,14},{10,8},{12,... | collective-permute-start | bytes 1179656 | tf_op jit(solution)/shard_map/ppermute | solution.py:27
  65.4 6.6 %group.2 = (bf16[384,2176]{1,0:T(8,128)(2,1)S(1)}, bf16[384,128]{1,0:T(8,128)(2,1)S(1)}, bf16[384,768]{1,0:T(8,128)(2,1)S(1)}, bf16[384,384]{1,0:T(8,128)(2,1)S(1)}) custom-call(s32[3]{0:T(128)S(1)} %copy-done.2, bf16[48,4096]{1,0:T(8,128)(2,1)S(1)} %convolution_convert_fusion.1.refs_0_, bf16[48,4096]{1,0:T(8,128)(2,1)S(1)} %convolution_convert_fusion.refs_1_, ...), custom_call_target="tpu_custom_call" | custom-call | flops 4328521728 | bytes 16777216 | tf_op jit(solution)/shard_map/group/pallas_call | solution.py:210
  72.3 1.8 %collective-permute-start.31 = (bf16[16,4096]{1,0:T(8,128)(2,1)S(1)}, bf16[16,4096]{1,0:T(8,128)(2,1)S(1)}, u32[]{:S(2)}, u32[]{:S(2)}) collective-permute-start(bf16[16,4096]{1,0:T(8,128)(2,1)S(1)} %slice.191), channel_id=1, source_target_pairs={{0,2},{2,4},{4,6},{6,0},{1,3},{3,5},{5,7},{7,1},{8,10},{10,12},{12... | collective-permute-start | bytes 393224 | tf_op jit(solution)/shard_map/ppermute | solution.py:27
  74.1 5.9 %collective-permute-done.28.refs_5_.refs_13_ = bf16[48,4096]{1,0:T(8,128)(2,1)S(1)} collective-permute-done((bf16[48,4096]{1,0:T(8,128)(2,1)S(1)}, bf16[48,4096]{1,0:T(8,128)(2,1)S(1)}, u32[]{:S(2)}, u32[]{:S(2)}) %collective-permute-start.28) | collective-permute-done | bytes 393248 | tf_op jit(solution)/shard_map/ppermute | solution.py:27
  80.0 1.4 collective-permute-done.30.refs_7_.refs_15_
  81.4 0.5 collective-permute-start.41
  82.0 3.1 %collective-permute-start.29 = (bf16[32,4096]{1,0:T(8,128)(2,1)S(1)}, bf16[32,4096]{1,0:T(8,128)(2,1)S(1)}, u32[]{:S(2)}, u32[]{:S(2)}) collective-permute-start(bf16[32,4096]{1,0:T(8,128)(2,1)S(1)} %slice.145), channel_id=1, source_target_pairs={{0,2},{2,4},{4,6},{6,0},{1,3},{3,5},{5,7},{7,1},{8,10},{10,12},{12... | collective-permute-start | bytes 786440 | tf_op jit(solution)/shard_map/ppermute | solution.py:27
  85.5 0.5 collective-permute-start.35
  86.0 5.4 %collective-permute-done.29.refs_6_.refs_14_ = bf16[32,4096]{1,0:T(8,128)(2,1)S(1)} collective-permute-done((bf16[32,4096]{1,0:T(8,128)(2,1)S(1)}, bf16[32,4096]{1,0:T(8,128)(2,1)S(1)}, u32[]{:S(2)}, u32[]{:S(2)}) %collective-permute-start.29) | collective-permute-done | bytes 262176 | tf_op jit(solution)/shard_map/ppermute | solution.py:27
  91.4 1.6 collective-permute-done.32.refs_9_.refs_17_
  93.0 0.5 collective-permute-start.38
  94.0 0.7 collective-permute-done.37.refs_14_.refs_30_
  94.7 0.6 collective-permute-done.38.refs_15_.refs_31_
  96.0 6.6 %group.3 = (bf16[384,2176]{1,0:T(8,128)(2,1)S(1)}, bf16[384,128]{1,0:T(8,128)(2,1)S(1)}, bf16[384,768]{1,0:T(8,128)(2,1)S(1)}, bf16[384,384]{1,0:T(8,128)(2,1)S(1)}) custom-call(s32[3]{0:T(128)S(1)} %copy-done.2, bf16[48,4096]{1,0:T(8,128)(2,1)S(1)} %collective-permute-done.4.refs_0_.refs_8_, bf16[48,4096]{1,0:T(8,128)(2,1)S(1)} %collective-permute-done.25.refs_1_.refs_9_, ...), custom_call_target="tpu_custom_call" | custom-call | flops 4328521728 | bytes 16777216 | tf_op jit(solution)/shard_map/group/pallas_call | solution.py:210
  103.2 2.1 %keep.2 = bf16[384,2176]{1,0:T(8,128)(2,1)S(1)} custom-call(s32[3]{0:T(128)S(1)} %copy-done.2, bf16[384,768]{1,0:T(8,128)(2,1)S(1)} %get-tuple-element.56.sides_ref.refs_36_, bf16[384,128]{1,0:T(8,128)(2,1)S(1)} %get-tuple-element.57.share_ref, bf16[768,4096]{1,0:T(8,128)(2,1)S(1)} %stack.17.refs_16_.pair_ref.refs_20_), custom_call_target="tpu_custom_call" | custom-call | flops 1207959552 | bytes 8388608 | tf_op jit(solution)/shard_map/keep/pallas_call | solution.py:191
  105.3 2.1 %keep.3 = bf16[384,2176]{1,0:T(8,128)(2,1)S(1)} custom-call(s32[3]{0:T(128)S(1)} %copy-done.2, bf16[384,768]{1,0:T(8,128)(2,1)S(1)} %get-tuple-element.61.sides_ref.refs_37_, bf16[384,128]{1,0:T(8,128)(2,1)S(1)} %get-tuple-element.62.share_ref, bf16[768,4096]{1,0:T(8,128)(2,1)S(1)} %stack.17.refs_16_.pair_ref.refs_20_), custom_call_target="tpu_custom_call" | custom-call | flops 1207959552 | bytes 8388608 | tf_op jit(solution)/shard_map/keep/pallas_call | solution.py:191
  108.0 2.9 %collective-permute-start.46 = (bf16[32,2176]{1,0:T(8,128)(2,1)S(1)}, bf16[32,2176]{1,0:T(8,128)(2,1)S(1)}, u32[]{:S(2)}, u32[]{:S(2)}) collective-permute-start(bf16[32,2176]{1,0:T(8,128)(2,1)S(1)} %get-tuple-element.89), channel_id=1, source_target_pairs={{0,2},{2,4},{4,6},{6,0},{1,3},{3,5},{5,7},{7,1},{8,10},{10,12},{12... | collective-permute-start | bytes 417800 | tf_op jit(solution)/shard_map/ppermute | solution.py:27
  111.0 8.1 %weight_grads.2 = (bf16[344,4096]{1,0:T(8,128)(2,1)}, bf16[344,4096]{1,0:T(8,128)(2,1)}) custom-call(s32[3]{0:T(128)S(1)} %copy-done.2, bf16[48,4096]{1,0:T(8,128)(2,1)S(1)} %convolution_convert_fusion.1.refs_0_, bf16[48,4096]{1,0:T(8,128)(2,1)S(1)} %convolution_convert_fusion.refs_1_, bf16[48,4096]{1,0:T(8,128)(2,1)S(1)} %collective-permute-done.11.refs_2_, ...), custom_call_target="tpu_custom_call" | custom-call | flops 4328521728 | bytes 14680064 | tf_op jit(solution)/shard_map/weight_grads/pallas_call | solution.py:266
  119.4 3.0 %collective-permute-start.45 = (bf16[96,2176]{1,0:T(8,128)(2,1)S(1)}, bf16[96,2176]{1,0:T(8,128)(2,1)S(1)}, u32[]{:S(2)}, u32[]{:S(2)}) collective-permute-start(bf16[96,2176]{1,0:T(8,128)(2,1)S(1)} %get-tuple-element.87), channel_id=1, source_target_pairs={{0,6},{2,0},{4,2},{6,4},{1,7},{3,1},{5,3},{7,5},{8,14},{10,8},{12,... | collective-permute-start | bytes 1253384 | tf_op jit(solution)/shard_map/ppermute | solution.py:27
  122.5 1.7 collective-permute-start.47
  124.2 2.1 %collective-permute-start.24 = (bf16[96,2176]{1,0:T(8,128)(2,1)S(1)}, bf16[96,2176]{1,0:T(8,128)(2,1)S(1)}, u32[]{:S(2)}, u32[]{:S(2)}) collective-permute-start(bf16[96,2176]{1,0:T(8,128)(2,1)S(1)} %add_convert_fusion.6), channel_id=1, source_target_pairs={{0,6},{2,0},{4,2},{6,4},{1,7},{3,1},{5,3},{7,5},{8,14},{10,8},{12,... | collective-permute-start | bytes 1253384 | tf_op jit(solution)/shard_map/ppermute | solution.py:27
  126.3 6.2 %collective-permute-done.45 = bf16[96,2176]{1,0:T(8,128)(2,1)S(1)} collective-permute-done((bf16[96,2176]{1,0:T(8,128)(2,1)S(1)}, bf16[96,2176]{1,0:T(8,128)(2,1)S(1)}, u32[]{:S(2)}, u32[]{:S(2)}) %collective-permute-start.45) | collective-permute-done | bytes 417824 | tf_op jit(solution)/shard_map/ppermute | solution.py:27
  132.5 0.5 collective-permute-done.47
  133.0 1.4 collective-permute-done.49
  134.8 0.5 collective-permute-start.51
  135.2 0.9 collective-permute-start.50
  136.2 1.0 collective-permute-start.53
  137.1 1.5 collective-permute-start.52
  138.6 1.2 collective-permute-done.24
  139.8 2.2 %collective-permute-done.51 = bf16[48,2176]{1,0:T(8,128)(2,1)S(1)} collective-permute-done((bf16[48,2176]{1,0:T(8,128)(2,1)S(1)}, bf16[48,2176]{1,0:T(8,128)(2,1)S(1)}, u32[]{:S(2)}, u32[]{:S(2)}) %collective-permute-start.51) | collective-permute-done | bytes 208928 | tf_op jit(solution)/shard_map/ppermute | solution.py:31
  142.8 1.5 collective-permute-done.53
  144.9 1.1 collective-permute-start.54
  146.0 4.3 %collective-permute-start.55 = (bf16[16,2176]{1,0:T(8,128)(2,1)S(1)}, bf16[16,2176]{1,0:T(8,128)(2,1)S(1)}, u32[]{:S(2)}, u32[]{:S(2)}) collective-permute-start(bf16[16,2176]{1,0:T(8,128)(2,1)S(1)} %get-tuple-element.97), channel_id=1, source_target_pairs={{0,96},{8,104},{16,112},{24,120},{32,0},{40,8},{48,16},{56,24},{64... | collective-permute-start | bytes 208904 | tf_op jit(solution)/shard_map/ppermute | solution.py:44
  150.3 4.1 %collective-permute-start.56 = (bf16[16,2176]{1,0:T(8,128)(2,1)S(1)}, bf16[16,2176]{1,0:T(8,128)(2,1)S(1)}, u32[]{:S(2)}, u32[]{:S(2)}) collective-permute-start(bf16[16,2176]{1,0:T(8,128)(2,1)S(1)} %get-tuple-element.93), channel_id=1, source_target_pairs={{0,120},{8,112},{16,104},{24,96},{32,24},{40,16},{48,8},{56,0},{64... | collective-permute-start | bytes 208904 | tf_op jit(solution)/shard_map/ppermute | solution.py:44
  154.4 5.6 %collective-permute-start.58 = (bf16[16,2176]{1,0:T(8,128)(2,1)S(1)}, bf16[16,2176]{1,0:T(8,128)(2,1)S(1)}, u32[]{:S(2)}, u32[]{:S(2)}) collective-permute-start(bf16[16,2176]{1,0:T(8,128)(2,1)S(1)} %get-tuple-element.92), channel_id=1, source_target_pairs={{0,88},{8,80},{16,72},{24,64},{32,120},{40,112},{48,104},{56,96},{... | collective-permute-start | bytes 208904 | tf_op jit(solution)/shard_map/ppermute | solution.py:44
  160.1 0.6 collective-permute-start.60
  160.7 5.0 %weight_grads.3 = bf16[344,4096]{1,0:T(8,128)(2,1)} custom-call(s32[3]{0:T(128)S(1)} %copy-done.2, bf16[48,4096]{1,0:T(8,128)(2,1)S(1)} %convolution_convert_fusion.1.refs_0_, bf16[48,4096]{1,0:T(8,128)(2,1)S(1)} %convolution_convert_fusion.refs_1_, bf16[48,4096]{1,0:T(8,128)(2,1)S(1)} %collective-permute-done.11.refs_2_, ...), custom_call_target="tpu_custom_call" | custom-call | flops 2164260864 | bytes 14680064 | tf_op jit(solution)/shard_map/weight_grads/pallas_call | solution.py:266
  165.8 2.0 %collective-permute-done.60.refs_7_ = bf16[16,2176]{1,0:T(8,128)(2,1)S(1)} collective-permute-done((bf16[16,2176]{1,0:T(8,128)(2,1)S(1)}, bf16[16,2176]{1,0:T(8,128)(2,1)S(1)}, u32[]{:S(2)}, u32[]{:S(2)}) %collective-permute-start.60) | collective-permute-done | bytes 69664 | tf_op jit(solution)/shard_map/ppermute | solution.py:44
  167.8 0.9 combine.1
  (98 shorter events, 7.2 us)
Async XLA Ops:
  4.5 14.2 %collective-permute-start.2 = (bf16[16,4096]{1,0:T(8,128)(2,1)}, bf16[16,4096]{1,0:T(8,128)(2,1)S(1)}, u32[]{:S(2)}, u32[]{:S(2)}) collective-permute-start(bf16[16,4096]{1,0:T(8,128)(2,1)} %get-tuple-element.47), channel_id=1, source_target_pairs={{0,96},{8,104},{16,112},{24,120},{32,0},{40,8},{48,16},{56,24},{64... | collective-permute-start | bytes 393224 | tf_op jit(solution)/shard_map/ppermute | solution.py:44
  8.6 10.1 %collective-permute-start.1 = (bf16[16,4096]{1,0:T(8,128)(2,1)}, bf16[16,4096]{1,0:T(8,128)(2,1)S(1)}, u32[]{:S(2)}, u32[]{:S(2)}) collective-permute-start(bf16[16,4096]{1,0:T(8,128)(2,1)} %get-tuple-element.46), channel_id=1, source_target_pairs={{0,64},{8,72},{16,80},{24,88},{32,96},{40,104},{48,112},{56,120},{... | collective-permute-start | bytes 393224 | tf_op jit(solution)/shard_map/ppermute | solution.py:44
  8.6 14.5 %collective-permute-start = (bf16[16,4096]{1,0:T(8,128)(2,1)}, bf16[16,4096]{1,0:T(8,128)(2,1)S(1)}, u32[]{:S(2)}, u32[]{:S(2)}) collective-permute-start(bf16[16,4096]{1,0:T(8,128)(2,1)} %get-tuple-element.45), channel_id=1, source_target_pairs={{0,32},{8,40},{16,48},{24,56},{32,64},{40,72},{48,80},{56,88},{64,... | collective-permute-start | bytes 393224 | tf_op jit(solution)/shard_map/ppermute | solution.py:44
  9.8 14.8 %collective-permute-start.10 = (bf16[16,4096]{1,0:T(8,128)(2,1)}, bf16[16,4096]{1,0:T(8,128)(2,1)S(1)}, u32[]{:S(2)}, u32[]{:S(2)}) collective-permute-start(bf16[16,4096]{1,0:T(8,128)(2,1)} %get-tuple-element.51), channel_id=1, source_target_pairs={{0,120},{8,112},{16,104},{24,96},{32,24},{40,16},{48,8},{56,0},{64... | collective-permute-start | bytes 393224 | tf_op jit(solution)/shard_map/ppermute | solution.py:44
  14.3 10.9 %collective-permute-start.9 = (bf16[16,4096]{1,0:T(8,128)(2,1)}, bf16[16,4096]{1,0:T(8,128)(2,1)S(1)}, u32[]{:S(2)}, u32[]{:S(2)}) collective-permute-start(bf16[16,4096]{1,0:T(8,128)(2,1)} %get-tuple-element.50), channel_id=1, source_target_pairs={{0,88},{8,80},{16,72},{24,64},{32,120},{40,112},{48,104},{56,96},{... | collective-permute-start | bytes 393224 | tf_op jit(solution)/shard_map/ppermute | solution.py:44
  18.7 12.0 %collective-permute-start.8 = (bf16[16,4096]{1,0:T(8,128)(2,1)}, bf16[16,4096]{1,0:T(8,128)(2,1)S(1)}, u32[]{:S(2)}, u32[]{:S(2)}) collective-permute-start(bf16[16,4096]{1,0:T(8,128)(2,1)} %get-tuple-element.49), channel_id=1, source_target_pairs={{0,56},{8,48},{16,40},{24,32},{32,88},{40,80},{48,72},{56,64},{64,... | collective-permute-start | bytes 393224 | tf_op jit(solution)/shard_map/ppermute | solution.py:44
  18.7 12.0 %collective-permute-start.7 = (bf16[16,4096]{1,0:T(8,128)(2,1)}, bf16[16,4096]{1,0:T(8,128)(2,1)S(1)}, u32[]{:S(2)}, u32[]{:S(2)}) collective-permute-start(bf16[16,4096]{1,0:T(8,128)(2,1)} %get-tuple-element.48), channel_id=1, source_target_pairs={{0,24},{8,16},{16,8},{24,0},{32,56},{40,48},{48,40},{56,32},{64,88... | collective-permute-start | bytes 393224 | tf_op jit(solution)/shard_map/ppermute | solution.py:44
  23.1 31.7 %copy-start = (bf16[1,4096,344]{1,2,0:T(8,128)(2,1)S(1)}, bf16[1,4096,344]{1,2,0:T(8,128)(2,1)}, u32[]{:S(2)}) copy-start(bf16[1,4096,344]{1,2,0:T(8,128)(2,1)} %param.11) | copy-start | bytes 8454148
  24.5 8.6 %collective-permute-start.3 = (bf16[48,4096]{1,0:T(8,128)(2,1)S(1)}, bf16[48,4096]{1,0:T(8,128)(2,1)S(1)}, u32[]{:S(2)}, u32[]{:S(2)}) collective-permute-start(bf16[48,4096]{1,0:T(8,128)(2,1)S(1)} %convolution_convert_fusion.1.refs_0_), channel_id=1, source_target_pairs={{0,8},{8,0},{1,9},{9,1},{2,10},{10,2},{3,11},{11,3},{4,12},{12,4},... | collective-permute-start | bytes 1179656 | tf_op jit(solution)/shard_map/ppermute | solution.py:31
  24.7 11.7 %collective-permute-start.5 = (bf16[48,4096]{1,0:T(8,128)(2,1)S(1)}, bf16[48,4096]{1,0:T(8,128)(2,1)S(1)}, u32[]{:S(2)}, u32[]{:S(2)}) collective-permute-start(bf16[48,4096]{1,0:T(8,128)(2,1)S(1)} %convolution_convert_fusion.1.refs_0_), channel_id=1, source_target_pairs={{0,6},{2,0},{4,2},{6,4},{1,7},{3,1},{5,3},{7,5},{8,14},{10,8},{12,... | collective-permute-start | bytes 1179656 | tf_op jit(solution)/shard_map/ppermute | solution.py:27
  25.2 12.7 %collective-permute-start.11 = (bf16[48,4096]{1,0:T(8,128)(2,1)S(1)}, bf16[48,4096]{1,0:T(8,128)(2,1)S(1)}, u32[]{:S(2)}, u32[]{:S(2)}) collective-permute-start(bf16[48,4096]{1,0:T(8,128)(2,1)S(1)} %convolution_convert_fusion.1.refs_0_), channel_id=1, source_target_pairs={{0,2},{2,4},{4,6},{6,0},{1,3},{3,5},{5,7},{7,1},{8,10},{10,12},{12... | collective-permute-start | bytes 1179656 | tf_op jit(solution)/shard_map/ppermute | solution.py:27
  31.0 13.3 %collective-permute-start.12 = (bf16[48,4096]{1,0:T(8,128)(2,1)S(1)}, bf16[48,4096]{1,0:T(8,128)(2,1)S(1)}, u32[]{:S(2)}, u32[]{:S(2)}) collective-permute-start(bf16[48,4096]{1,0:T(8,128)(2,1)S(1)} %convolution_convert_fusion.refs_1_), channel_id=1, source_target_pairs={{0,2},{2,4},{4,6},{6,0},{1,3},{3,5},{5,7},{7,1},{8,10},{10,12},{12... | collective-permute-start | bytes 1179656 | tf_op jit(solution)/shard_map/ppermute | solution.py:27
  32.6 12.2 %collective-permute-start.13 = (bf16[48,4096]{1,0:T(8,128)(2,1)S(1)}, bf16[48,4096]{1,0:T(8,128)(2,1)S(1)}, u32[]{:S(2)}, u32[]{:S(2)}) collective-permute-start(bf16[48,4096]{1,0:T(8,128)(2,1)S(1)} %convolution_convert_fusion.refs_1_), channel_id=1, source_target_pairs={{0,6},{2,0},{4,2},{6,4},{1,7},{3,1},{5,3},{7,5},{8,14},{10,8},{12,... | collective-permute-start | bytes 1179656 | tf_op jit(solution)/shard_map/ppermute | solution.py:27
  33.1 11.7 %collective-permute-start.14 = (bf16[48,4096]{1,0:T(8,128)(2,1)S(1)}, bf16[48,4096]{1,0:T(8,128)(2,1)S(1)}, u32[]{:S(2)}, u32[]{:S(2)}) collective-permute-start(bf16[48,4096]{1,0:T(8,128)(2,1)S(1)} %convolution_convert_fusion.refs_1_), channel_id=1, source_target_pairs={{0,8},{8,0},{1,9},{9,1},{2,10},{10,2},{3,11},{11,3},{4,12},{12,4},... | collective-permute-start | bytes 1179656 | tf_op jit(solution)/shard_map/ppermute | solution.py:31
  36.4 8.9 %collective-permute-start.15 = (bf16[48,4096]{1,0:T(8,128)(2,1)S(1)}, bf16[48,4096]{1,0:T(8,128)(2,1)S(1)}, u32[]{:S(2)}, u32[]{:S(2)}) collective-permute-start(bf16[48,4096]{1,0:T(8,128)(2,1)S(1)} %convolution_convert_fusion.1.refs_0_), channel_id=1, source_target_pairs={{0,1},{1,0},{2,3},{3,2},{4,5},{5,4},{6,7},{7,6},{8,9},{9,8},{10,11... | collective-permute-start | bytes 1179656 | tf_op jit(solution)/shard_map/ppermute | solution.py:35
  38.0 7.4 %collective-permute-start.16 = (bf16[48,4096]{1,0:T(8,128)(2,1)S(1)}, bf16[48,4096]{1,0:T(8,128)(2,1)S(1)}, u32[]{:S(2)}, u32[]{:S(2)}) collective-permute-start(bf16[48,4096]{1,0:T(8,128)(2,1)S(1)} %convolution_convert_fusion.refs_1_), channel_id=1, source_target_pairs={{0,1},{1,0},{2,3},{3,2},{4,5},{5,4},{6,7},{7,6},{8,9},{9,8},{10,11... | collective-permute-start | bytes 1179656 | tf_op jit(solution)/shard_map/ppermute | solution.py:35
  44.3 10.0 %collective-permute-start.4 = (bf16[48,4096]{1,0:T(8,128)(2,1)S(1)}, bf16[48,4096]{1,0:T(8,128)(2,1)S(1)}, u32[]{:S(2)}, u32[]{:S(2)}) collective-permute-start(bf16[48,4096]{1,0:T(8,128)(2,1)S(1)} %collective-permute-done.3.refs_6_), channel_id=1, source_target_pairs={{0,2},{2,4},{4,6},{6,0},{1,3},{3,5},{5,7},{7,1},{8,10},{10,12},{12... | collective-permute-start | bytes 1179656 | tf_op jit(solution)/shard_map/ppermute | solution.py:27
  44.8 9.5 %collective-permute-start.17 = (bf16[48,4096]{1,0:T(8,128)(2,1)S(1)}, bf16[48,4096]{1,0:T(8,128)(2,1)S(1)}, u32[]{:S(2)}, u32[]{:S(2)}) collective-permute-start(bf16[48,4096]{1,0:T(8,128)(2,1)S(1)} %collective-permute-done.11.refs_2_), channel_id=1, source_target_pairs={{0,1},{1,0},{2,3},{3,2},{4,5},{5,4},{6,7},{7,6},{8,9},{9,8},{10,11... | collective-permute-start | bytes 1179656 | tf_op jit(solution)/shard_map/ppermute | solution.py:35
  44.8 12.2 %collective-permute-start.18 = (bf16[48,4096]{1,0:T(8,128)(2,1)S(1)}, bf16[48,4096]{1,0:T(8,128)(2,1)S(1)}, u32[]{:S(2)}, u32[]{:S(2)}) collective-permute-start(bf16[48,4096]{1,0:T(8,128)(2,1)S(1)} %collective-permute-done.12.refs_3_), channel_id=1, source_target_pairs={{0,1},{1,0},{2,3},{3,2},{4,5},{5,4},{6,7},{7,6},{8,9},{9,8},{10,11... | collective-permute-start | bytes 1179656 | tf_op jit(solution)/shard_map/ppermute | solution.py:35
  45.3 11.8 %collective-permute-start.19 = (bf16[48,4096]{1,0:T(8,128)(2,1)S(1)}, bf16[48,4096]{1,0:T(8,128)(2,1)S(1)}, u32[]{:S(2)}, u32[]{:S(2)}) collective-permute-start(bf16[48,4096]{1,0:T(8,128)(2,1)S(1)} %collective-permute-done.5.refs_4_), channel_id=1, source_target_pairs={{0,1},{1,0},{2,3},{3,2},{4,5},{5,4},{6,7},{7,6},{8,9},{9,8},{10,11... | collective-permute-start | bytes 1179656 | tf_op jit(solution)/shard_map/ppermute | solution.py:35
  45.4 11.8 %collective-permute-start.20 = (bf16[48,4096]{1,0:T(8,128)(2,1)S(1)}, bf16[48,4096]{1,0:T(8,128)(2,1)S(1)}, u32[]{:S(2)}, u32[]{:S(2)}) collective-permute-start(bf16[48,4096]{1,0:T(8,128)(2,1)S(1)} %collective-permute-done.13.refs_5_), channel_id=1, source_target_pairs={{0,1},{1,0},{2,3},{3,2},{4,5},{5,4},{6,7},{7,6},{8,9},{9,8},{10,11... | collective-permute-start | bytes 1179656 | tf_op jit(solution)/shard_map/ppermute | solution.py:35
  54.3 4.9 %collective-permute-start.21 = (bf16[48,4096]{1,0:T(8,128)(2,1)S(1)}, bf16[48,4096]{1,0:T(8,128)(2,1)S(1)}, u32[]{:S(2)}, u32[]{:S(2)}) collective-permute-start(bf16[48,4096]{1,0:T(8,128)(2,1)S(1)} %collective-permute-done.3.refs_6_), channel_id=1, source_target_pairs={{0,1},{1,0},{2,3},{3,2},{4,5},{5,4},{6,7},{7,6},{8,9},{9,8},{10,11... | collective-permute-start | bytes 1179656 | tf_op jit(solution)/shard_map/ppermute | solution.py:35
  54.3 7.9 %collective-permute-start.22 = (bf16[48,4096]{1,0:T(8,128)(2,1)S(1)}, bf16[48,4096]{1,0:T(8,128)(2,1)S(1)}, u32[]{:S(2)}, u32[]{:S(2)}) collective-permute-start(bf16[48,4096]{1,0:T(8,128)(2,1)S(1)} %collective-permute-done.14.refs_7_), channel_id=1, source_target_pairs={{0,1},{1,0},{2,3},{3,2},{4,5},{5,4},{6,7},{7,6},{8,9},{9,8},{10,11... | collective-permute-start | bytes 1179656 | tf_op jit(solution)/shard_map/ppermute | solution.py:35
  56.6 8.7 %copy-start.2 = (s32[3]{0:T(128)S(1)}, s32[3]{0:T(128)}, u32[]{:S(2)}) copy-start(s32[3]{0:T(128)} %pad_add_fusion.place_ref) | copy-start | bytes 40
  56.6 8.7 %copy-start.6 = (bf16[1,344,4096]{2,1,0:T(8,128)(2,1)S(1)}, bf16[1,344,4096]{2,1,0:T(8,128)(2,1)}, u32[]{:S(2)}) copy-start(bf16[1,344,4096]{2,1,0:T(8,128)(2,1)} %param.13) | copy-start | bytes 8454148
  57.0 14.9 %collective-permute-start.6 = (bf16[48,4096]{1,0:T(8,128)(2,1)S(1)}, bf16[48,4096]{1,0:T(8,128)(2,1)S(1)}, u32[]{:S(2)}, u32[]{:S(2)}) collective-permute-start(bf16[48,4096]{1,0:T(8,128)(2,1)S(1)} %collective-permute-done.5.refs_4_), channel_id=1, source_target_pairs={{0,8},{8,0},{1,9},{9,1},{2,10},{10,2},{3,11},{11,3},{4,12},{12,4},... | collective-permute-start | bytes 1179656 | tf_op jit(solution)/shard_map/ppermute | solution.py:31
  57.1 15.1 %collective-permute-start.25 = (bf16[48,4096]{1,0:T(8,128)(2,1)S(1)}, bf16[48,4096]{1,0:T(8,128)(2,1)S(1)}, u32[]{:S(2)}, u32[]{:S(2)}) collective-permute-start(bf16[48,4096]{1,0:T(8,128)(2,1)S(1)} %collective-permute-done.14.refs_7_), channel_id=1, source_target_pairs={{0,2},{2,4},{4,6},{6,0},{1,3},{3,5},{5,7},{7,1},{8,10},{10,12},{12... | collective-permute-start | bytes 1179656 | tf_op jit(solution)/shard_map/ppermute | solution.py:27
  57.2 24.7 %collective-permute-start.26 = (bf16[48,4096]{1,0:T(8,128)(2,1)S(1)}, bf16[48,4096]{1,0:T(8,128)(2,1)S(1)}, u32[]{:S(2)}, u32[]{:S(2)}) collective-permute-start(bf16[48,4096]{1,0:T(8,128)(2,1)S(1)} %collective-permute-done.13.refs_5_), channel_id=1, source_target_pairs={{0,8},{8,0},{1,9},{9,1},{2,10},{10,2},{3,11},{11,3},{4,12},{12,4},... | collective-permute-start | bytes 1179656 | tf_op jit(solution)/shard_map/ppermute | solution.py:31
  59.2 25.8 %collective-permute-start.27 = (bf16[48,4096]{1,0:T(8,128)(2,1)S(1)}, bf16[48,4096]{1,0:T(8,128)(2,1)S(1)}, u32[]{:S(2)}, u32[]{:S(2)}) collective-permute-start(bf16[48,4096]{1,0:T(8,128)(2,1)S(1)} %collective-permute-done.5.refs_4_), channel_id=1, source_target_pairs={{0,6},{2,0},{4,2},{6,4},{1,7},{3,1},{5,3},{7,5},{8,14},{10,8},{12,... | collective-permute-start | bytes 1179656 | tf_op jit(solution)/shard_map/ppermute | solution.py:27
  62.2 17.8 %collective-permute-start.28 = (bf16[48,4096]{1,0:T(8,128)(2,1)S(1)}, bf16[48,4096]{1,0:T(8,128)(2,1)S(1)}, u32[]{:S(2)}, u32[]{:S(2)}) collective-permute-start(bf16[48,4096]{1,0:T(8,128)(2,1)S(1)} %collective-permute-done.13.refs_5_), channel_id=1, source_target_pairs={{0,6},{2,0},{4,2},{6,4},{1,7},{3,1},{5,3},{7,5},{8,14},{10,8},{12,... | collective-permute-start | bytes 1179656 | tf_op jit(solution)/shard_map/ppermute | solution.py:27
  72.0 9.5 %collective-permute-start.30 = (bf16[16,4096]{1,0:T(8,128)(2,1)S(1)}, bf16[16,4096]{1,0:T(8,128)(2,1)S(1)}, u32[]{:S(2)}, u32[]{:S(2)}) collective-permute-start(bf16[16,4096]{1,0:T(8,128)(2,1)S(1)} %slice.146), channel_id=1, source_target_pairs={{0,6},{2,0},{4,2},{6,4},{1,7},{3,1},{5,3},{7,5},{8,14},{10,8},{12,... | collective-permute-start | bytes 393224 | tf_op jit(solution)/shard_map/ppermute | solution.py:27
  72.3 9.1 %collective-permute-start.31 = (bf16[16,4096]{1,0:T(8,128)(2,1)S(1)}, bf16[16,4096]{1,0:T(8,128)(2,1)S(1)}, u32[]{:S(2)}, u32[]{:S(2)}) collective-permute-start(bf16[16,4096]{1,0:T(8,128)(2,1)S(1)} %slice.191), channel_id=1, source_target_pairs={{0,2},{2,4},{4,6},{6,0},{1,3},{3,5},{5,7},{7,1},{8,10},{10,12},{12... | collective-permute-start | bytes 393224 | tf_op jit(solution)/shard_map/ppermute | solution.py:27
  80.0 13.0 %collective-permute-start.33 = (bf16[48,4096]{1,0:T(8,128)(2,1)S(1)}, bf16[48,4096]{1,0:T(8,128)(2,1)S(1)}, u32[]{:S(2)}, u32[]{:S(2)}) collective-permute-start(bf16[48,4096]{1,0:T(8,128)(2,1)S(1)} %collective-permute-done.4.refs_0_.refs_8_), channel_id=1, source_target_pairs={{0,1},{1,0},{2,3},{3,2},{4,5},{5,4},{6,7},{7,6},{8,9},{9,8},{10,11... | collective-permute-start | bytes 1179656 | tf_op jit(solution)/shard_map/ppermute | solution.py:35
  81.4 4.0 %collective-permute-start.40 = (bf16[16,4096]{1,0:T(8,128)(2,1)S(1)}, bf16[16,4096]{1,0:T(8,128)(2,1)S(1)}, u32[]{:S(2)}, u32[]{:S(2)}) collective-permute-start(bf16[16,4096]{1,0:T(8,128)(2,1)S(1)} %collective-permute-done.30.refs_7_.refs_15_), channel_id=1, source_target_pairs={{0,1},{1,0},{2,3},{3,2},{4,5},{5,4},{6,7},{7,6},{8,9},{9,8},{10,11... | collective-permute-start | bytes 393224 | tf_op jit(solution)/shard_map/ppermute | solution.py:35
  81.4 4.0 %collective-permute-start.41 = (bf16[16,4096]{1,0:T(8,128)(2,1)S(1)}, bf16[16,4096]{1,0:T(8,128)(2,1)S(1)}, u32[]{:S(2)}, u32[]{:S(2)}) collective-permute-start(bf16[16,4096]{1,0:T(8,128)(2,1)S(1)} %collective-permute-done.31.refs_8_.refs_16_), channel_id=1, source_target_pairs={{0,1},{1,0},{2,3},{3,2},{4,5},{5,4},{6,7},{7,6},{8,9},{9,8},{10,11... | collective-permute-start | bytes 393224 | tf_op jit(solution)/shard_map/ppermute | solution.py:35
  82.0 9.4 %collective-permute-start.29 = (bf16[32,4096]{1,0:T(8,128)(2,1)S(1)}, bf16[32,4096]{1,0:T(8,128)(2,1)S(1)}, u32[]{:S(2)}, u32[]{:S(2)}) collective-permute-start(bf16[32,4096]{1,0:T(8,128)(2,1)S(1)} %slice.145), channel_id=1, source_target_pairs={{0,2},{2,4},{4,6},{6,0},{1,3},{3,5},{5,7},{7,1},{8,10},{10,12},{12... | collective-permute-start | bytes 786440 | tf_op jit(solution)/shard_map/ppermute | solution.py:27
  85.1 7.9 %collective-permute-start.32 = (bf16[32,4096]{1,0:T(8,128)(2,1)S(1)}, bf16[32,4096]{1,0:T(8,128)(2,1)S(1)}, u32[]{:S(2)}, u32[]{:S(2)}) collective-permute-start(bf16[32,4096]{1,0:T(8,128)(2,1)S(1)} %slice.192), channel_id=1, source_target_pairs={{0,8},{8,0},{1,9},{9,1},{2,10},{10,2},{3,11},{11,3},{4,12},{12,4},... | collective-permute-start | bytes 786440 | tf_op jit(solution)/shard_map/ppermute | solution.py:31
  85.4 8.1 %collective-permute-start.34 = (bf16[48,4096]{1,0:T(8,128)(2,1)S(1)}, bf16[48,4096]{1,0:T(8,128)(2,1)S(1)}, u32[]{:S(2)}, u32[]{:S(2)}) collective-permute-start(bf16[48,4096]{1,0:T(8,128)(2,1)S(1)} %collective-permute-done.25.refs_1_.refs_9_), channel_id=1, source_target_pairs={{0,1},{1,0},{2,3},{3,2},{4,5},{5,4},{6,7},{7,6},{8,9},{9,8},{10,11... | collective-permute-start | bytes 1179656 | tf_op jit(solution)/shard_map/ppermute | solution.py:35
  85.5 8.2 %collective-permute-start.35 = (bf16[48,4096]{1,0:T(8,128)(2,1)S(1)}, bf16[48,4096]{1,0:T(8,128)(2,1)S(1)}, u32[]{:S(2)}, u32[]{:S(2)}) collective-permute-start(bf16[48,4096]{1,0:T(8,128)(2,1)S(1)} %collective-permute-done.6.refs_2_.refs_10_), channel_id=1, source_target_pairs={{0,1},{1,0},{2,3},{3,2},{4,5},{5,4},{6,7},{7,6},{8,9},{9,8},{10,11... | collective-permute-start | bytes 1179656 | tf_op jit(solution)/shard_map/ppermute | solution.py:35
  91.4 2.6 %collective-permute-start.36 = (bf16[48,4096]{1,0:T(8,128)(2,1)S(1)}, bf16[48,4096]{1,0:T(8,128)(2,1)S(1)}, u32[]{:S(2)}, u32[]{:S(2)}) collective-permute-start(bf16[48,4096]{1,0:T(8,128)(2,1)S(1)} %collective-permute-done.26.refs_3_.refs_11_), channel_id=1, source_target_pairs={{0,1},{1,0},{2,3},{3,2},{4,5},{5,4},{6,7},{7,6},{8,9},{9,8},{10,11... | collective-permute-start | bytes 1179656 | tf_op jit(solution)/shard_map/ppermute | solution.py:35
  93.0 1.7 %collective-permute-start.37 = (bf16[48,4096]{1,0:T(8,128)(2,1)S(1)}, bf16[48,4096]{1,0:T(8,128)(2,1)S(1)}, u32[]{:S(2)}, u32[]{:S(2)}) collective-permute-start(bf16[48,4096]{1,0:T(8,128)(2,1)S(1)} %collective-permute-done.27.refs_4_.refs_12_), channel_id=1, source_target_pairs={{0,1},{1,0},{2,3},{3,2},{4,5},{5,4},{6,7},{7,6},{8,9},{9,8},{10,11... | collective-permute-start | bytes 1179656 | tf_op jit(solution)/shard_map/ppermute | solution.py:35
  93.0 2.3 %collective-permute-start.38 = (bf16[48,4096]{1,0:T(8,128)(2,1)S(1)}, bf16[48,4096]{1,0:T(8,128)(2,1)S(1)}, u32[]{:S(2)}, u32[]{:S(2)}) collective-permute-start(bf16[48,4096]{1,0:T(8,128)(2,1)S(1)} %collective-permute-done.28.refs_5_.refs_13_), channel_id=1, source_target_pairs={{0,1},{1,0},{2,3},{3,2},{4,5},{5,4},{6,7},{7,6},{8,9},{9,8},{10,11... | collective-permute-start | bytes 1179656 | tf_op jit(solution)/shard_map/ppermute | solution.py:35
  93.5 2.1 %collective-permute-start.39 = (bf16[32,4096]{1,0:T(8,128)(2,1)S(1)}, bf16[32,4096]{1,0:T(8,128)(2,1)S(1)}, u32[]{:S(2)}, u32[]{:S(2)}) collective-permute-start(bf16[32,4096]{1,0:T(8,128)(2,1)S(1)} %collective-permute-done.29.refs_6_.refs_14_), channel_id=1, source_target_pairs={{0,1},{1,0},{2,3},{3,2},{4,5},{5,4},{6,7},{7,6},{8,9},{9,8},{10,11... | collective-permute-start | bytes 786440 | tf_op jit(solution)/shard_map/ppermute | solution.py:35
  93.6 2.4 %collective-permute-start.42 = (bf16[32,4096]{1,0:T(8,128)(2,1)S(1)}, bf16[32,4096]{1,0:T(8,128)(2,1)S(1)}, u32[]{:S(2)}, u32[]{:S(2)}) collective-permute-start(bf16[32,4096]{1,0:T(8,128)(2,1)S(1)} %collective-permute-done.32.refs_9_.refs_17_), channel_id=1, source_target_pairs={{0,1},{1,0},{2,3},{3,2},{4,5},{5,4},{6,7},{7,6},{8,9},{9,8},{10,11... | collective-permute-start | bytes 786440 | tf_op jit(solution)/shard_map/ppermute | solution.py:35
  102.6 4.8 %collective-permute-start.43 = (bf16[384,2176]{1,0:T(8,128)(2,1)S(1)}, bf16[384,2176]{1,0:T(8,128)(2,1)S(1)}, u32[]{:S(2)}, u32[]{:S(2)}) collective-permute-start(bf16[384,2176]{1,0:T(8,128)(2,1)S(1)} %get-tuple-element.63), channel_id=1, source_target_pairs={{0,1},{1,0},{2,3},{3,2},{4,5},{5,4},{6,7},{7,6},{8,9},{9,8},{10,11... | collective-permute-start | bytes 5013512 | tf_op jit(solution)/shard_map/ppermute | solution.py:35
  102.8 21.3 %collective-permute-start.23 = (bf16[384,2176]{1,0:T(8,128)(2,1)S(1)}, bf16[384,2176]{1,0:T(8,128)(2,1)S(1)}, u32[]{:S(2)}, u32[]{:S(2)}) collective-permute-start(bf16[384,2176]{1,0:T(8,128)(2,1)S(1)} %get-tuple-element.58), channel_id=1, source_target_pairs={{0,1},{1,0},{2,3},{3,2},{4,5},{5,4},{6,7},{7,6},{8,9},{9,8},{10,11... | collective-permute-start | bytes 5013512 | tf_op jit(solution)/shard_map/ppermute | solution.py:35
  107.6 11.5 %collective-permute-start.48 = (bf16[32,2176]{1,0:T(8,128)(2,1)S(1)}, bf16[32,2176]{1,0:T(8,128)(2,1)S(1)}, u32[]{:S(2)}, u32[]{:S(2)}) collective-permute-start(bf16[32,2176]{1,0:T(8,128)(2,1)S(1)} %get-tuple-element.88), channel_id=1, source_target_pairs={{0,8},{8,0},{1,9},{9,1},{2,10},{10,2},{3,11},{11,3},{4,12},{12,4},... | collective-permute-start | bytes 417800 | tf_op jit(solution)/shard_map/ppermute | solution.py:31
  108.0 11.0 %collective-permute-start.46 = (bf16[32,2176]{1,0:T(8,128)(2,1)S(1)}, bf16[32,2176]{1,0:T(8,128)(2,1)S(1)}, u32[]{:S(2)}, u32[]{:S(2)}) collective-permute-start(bf16[32,2176]{1,0:T(8,128)(2,1)S(1)} %get-tuple-element.89), channel_id=1, source_target_pairs={{0,2},{2,4},{4,6},{6,0},{1,3},{3,5},{5,7},{7,1},{8,10},{10,12},{12... | collective-permute-start | bytes 417800 | tf_op jit(solution)/shard_map/ppermute | solution.py:27
  111.0 8.1 %collective-permute-start.44 = (bf16[32,2176]{1,0:T(8,128)(2,1)S(1)}, bf16[32,2176]{1,0:T(8,128)(2,1)S(1)}, u32[]{:S(2)}, u32[]{:S(2)}) collective-permute-start(bf16[32,2176]{1,0:T(8,128)(2,1)S(1)} %get-tuple-element.90), channel_id=1, source_target_pairs={{0,6},{2,0},{4,2},{6,4},{1,7},{3,1},{5,3},{7,5},{8,14},{10,8},{12,... | collective-permute-start | bytes 417800 | tf_op jit(solution)/shard_map/ppermute | solution.py:27
  119.4 13.0 %collective-permute-start.45 = (bf16[96,2176]{1,0:T(8,128)(2,1)S(1)}, bf16[96,2176]{1,0:T(8,128)(2,1)S(1)}, u32[]{:S(2)}, u32[]{:S(2)}) collective-permute-start(bf16[96,2176]{1,0:T(8,128)(2,1)S(1)} %get-tuple-element.87), channel_id=1, source_target_pairs={{0,6},{2,0},{4,2},{6,4},{1,7},{3,1},{5,3},{7,5},{8,14},{10,8},{12,... | collective-permute-start | bytes 1253384 | tf_op jit(solution)/shard_map/ppermute | solution.py:27
  122.5 10.6 %collective-permute-start.47 = (bf16[96,2176]{1,0:T(8,128)(2,1)S(1)}, bf16[96,2176]{1,0:T(8,128)(2,1)S(1)}, u32[]{:S(2)}, u32[]{:S(2)}) collective-permute-start(bf16[96,2176]{1,0:T(8,128)(2,1)S(1)} %get-tuple-element.86), channel_id=1, source_target_pairs={{0,8},{8,0},{1,9},{9,1},{2,10},{10,2},{3,11},{11,3},{4,12},{12,4},... | collective-permute-start | bytes 1253384 | tf_op jit(solution)/shard_map/ppermute | solution.py:31
  124.1 10.3 %collective-permute-start.49 = (bf16[96,2176]{1,0:T(8,128)(2,1)S(1)}, bf16[96,2176]{1,0:T(8,128)(2,1)S(1)}, u32[]{:S(2)}, u32[]{:S(2)}) collective-permute-start(bf16[96,2176]{1,0:T(8,128)(2,1)S(1)} %get-tuple-element.85), channel_id=1, source_target_pairs={{0,2},{2,4},{4,6},{6,0},{1,3},{3,5},{5,7},{7,1},{8,10},{10,12},{12... | collective-permute-start | bytes 1253384 | tf_op jit(solution)/shard_map/ppermute | solution.py:27
  124.2 15.5 %collective-permute-start.24 = (bf16[96,2176]{1,0:T(8,128)(2,1)S(1)}, bf16[96,2176]{1,0:T(8,128)(2,1)S(1)}, u32[]{:S(2)}, u32[]{:S(2)}) collective-permute-start(bf16[96,2176]{1,0:T(8,128)(2,1)S(1)} %add_convert_fusion.6), channel_id=1, source_target_pairs={{0,6},{2,0},{4,2},{6,4},{1,7},{3,1},{5,3},{7,5},{8,14},{10,8},{12,... | collective-permute-start | bytes 1253384 | tf_op jit(solution)/shard_map/ppermute | solution.py:27
  134.8 7.2 %collective-permute-start.51 = (bf16[48,2176]{1,0:T(8,128)(2,1)S(1)}, bf16[48,2176]{1,0:T(8,128)(2,1)S(1)}, u32[]{:S(2)}, u32[]{:S(2)}) collective-permute-start(bf16[48,2176]{1,0:T(8,128)(2,1)S(1)} %get-tuple-element.83), channel_id=1, source_target_pairs={{0,8},{8,0},{1,9},{9,1},{2,10},{10,2},{3,11},{11,3},{4,12},{12,4},... | collective-permute-start | bytes 626696 | tf_op jit(solution)/shard_map/ppermute | solution.py:31
  135.2 7.1 %collective-permute-start.50 = (bf16[48,2176]{1,0:T(8,128)(2,1)S(1)}, bf16[48,2176]{1,0:T(8,128)(2,1)S(1)}, u32[]{:S(2)}, u32[]{:S(2)}) collective-permute-start(bf16[48,2176]{1,0:T(8,128)(2,1)S(1)} %get-tuple-element.80), channel_id=1, source_target_pairs={{0,2},{2,4},{4,6},{6,0},{1,3},{3,5},{5,7},{7,1},{8,10},{10,12},{12... | collective-permute-start | bytes 626696 | tf_op jit(solution)/shard_map/ppermute | solution.py:27
  136.2 8.1 %collective-permute-start.53 = (bf16[48,2176]{1,0:T(8,128)(2,1)S(1)}, bf16[48,2176]{1,0:T(8,128)(2,1)S(1)}, u32[]{:S(2)}, u32[]{:S(2)}) collective-permute-start(bf16[48,2176]{1,0:T(8,128)(2,1)S(1)} %get-tuple-element.84), channel_id=1, source_target_pairs={{0,8},{8,0},{1,9},{9,1},{2,10},{10,2},{3,11},{11,3},{4,12},{12,4},... | collective-permute-start | bytes 626696 | tf_op jit(solution)/shard_map/ppermute | solution.py:31
  137.1 7.4 %collective-permute-start.52 = (bf16[48,2176]{1,0:T(8,128)(2,1)S(1)}, bf16[48,2176]{1,0:T(8,128)(2,1)S(1)}, u32[]{:S(2)}, u32[]{:S(2)}) collective-permute-start(bf16[48,2176]{1,0:T(8,128)(2,1)S(1)} %get-tuple-element.79), channel_id=1, source_target_pairs={{0,2},{2,4},{4,6},{6,0},{1,3},{3,5},{5,7},{7,1},{8,10},{10,12},{12... | collective-permute-start | bytes 626696 | tf_op jit(solution)/shard_map/ppermute | solution.py:27
  144.9 15.2 %collective-permute-start.54 = (bf16[16,2176]{1,0:T(8,128)(2,1)S(1)}, bf16[16,2176]{1,0:T(8,128)(2,1)S(1)}, u32[]{:S(2)}, u32[]{:S(2)}) collective-permute-start(bf16[16,2176]{1,0:T(8,128)(2,1)S(1)} %get-tuple-element.94), channel_id=1, source_target_pairs={{0,24},{8,16},{16,8},{24,0},{32,56},{40,48},{48,40},{56,32},{64,88... | collective-permute-start | bytes 208904 | tf_op jit(solution)/shard_map/ppermute | solution.py:44
  146.0 14.1 %collective-permute-start.55 = (bf16[16,2176]{1,0:T(8,128)(2,1)S(1)}, bf16[16,2176]{1,0:T(8,128)(2,1)S(1)}, u32[]{:S(2)}, u32[]{:S(2)}) collective-permute-start(bf16[16,2176]{1,0:T(8,128)(2,1)S(1)} %get-tuple-element.97), channel_id=1, source_target_pairs={{0,96},{8,104},{16,112},{24,120},{32,0},{40,8},{48,16},{56,24},{64... | collective-permute-start | bytes 208904 | tf_op jit(solution)/shard_map/ppermute | solution.py:44
  150.3 15.4 %collective-permute-start.56 = (bf16[16,2176]{1,0:T(8,128)(2,1)S(1)}, bf16[16,2176]{1,0:T(8,128)(2,1)S(1)}, u32[]{:S(2)}, u32[]{:S(2)}) collective-permute-start(bf16[16,2176]{1,0:T(8,128)(2,1)S(1)} %get-tuple-element.93), channel_id=1, source_target_pairs={{0,120},{8,112},{16,104},{24,96},{32,24},{40,16},{48,8},{56,0},{64... | collective-permute-start | bytes 208904 | tf_op jit(solution)/shard_map/ppermute | solution.py:44
  154.4 11.3 %collective-permute-start.57 = (bf16[16,2176]{1,0:T(8,128)(2,1)S(1)}, bf16[16,2176]{1,0:T(8,128)(2,1)S(1)}, u32[]{:S(2)}, u32[]{:S(2)}) collective-permute-start(bf16[16,2176]{1,0:T(8,128)(2,1)S(1)} %get-tuple-element.96), channel_id=1, source_target_pairs={{0,64},{8,72},{16,80},{24,88},{32,96},{40,104},{48,112},{56,120},{... | collective-permute-start | bytes 208904 | tf_op jit(solution)/shard_map/ppermute | solution.py:44
  154.4 11.3 %collective-permute-start.58 = (bf16[16,2176]{1,0:T(8,128)(2,1)S(1)}, bf16[16,2176]{1,0:T(8,128)(2,1)S(1)}, u32[]{:S(2)}, u32[]{:S(2)}) collective-permute-start(bf16[16,2176]{1,0:T(8,128)(2,1)S(1)} %get-tuple-element.92), channel_id=1, source_target_pairs={{0,88},{8,80},{16,72},{24,64},{32,120},{40,112},{48,104},{56,96},{... | collective-permute-start | bytes 208904 | tf_op jit(solution)/shard_map/ppermute | solution.py:44
  160.1 5.7 %collective-permute-start.59 = (bf16[16,2176]{1,0:T(8,128)(2,1)S(1)}, bf16[16,2176]{1,0:T(8,128)(2,1)S(1)}, u32[]{:S(2)}, u32[]{:S(2)}) collective-permute-start(bf16[16,2176]{1,0:T(8,128)(2,1)S(1)} %get-tuple-element.95), channel_id=1, source_target_pairs={{0,32},{8,40},{16,48},{24,56},{32,64},{40,72},{48,80},{56,88},{64,... | collective-permute-start | bytes 208904 | tf_op jit(solution)/shard_map/ppermute | solution.py:44
  160.1 7.7 %collective-permute-start.60 = (bf16[16,2176]{1,0:T(8,128)(2,1)S(1)}, bf16[16,2176]{1,0:T(8,128)(2,1)S(1)}, u32[]{:S(2)}, u32[]{:S(2)}) collective-permute-start(bf16[16,2176]{1,0:T(8,128)(2,1)S(1)} %get-tuple-element.91), channel_id=1, source_target_pairs={{0,56},{8,48},{16,40},{24,32},{32,88},{40,80},{48,72},{56,64},{64,... | collective-permute-start | bytes 208904 | tf_op jit(solution)/shard_map/ppermute | solution.py:44
  (4 other events, 23.0 us)
